TPU v7x, 32 devices: a whole 2x2x4 slice. The times are simulated.
32 devices in a mesh: rep: 2 (over x), fs: 8 (over z, y), tp: 2 (over core).
Axes of the slice: x: 2, y: 2, z: 4, core: 2. Of those that a mesh axis runs over, the one named last changes fastest.
Arguments:
- x_late: bfloat16 [2048, 2048], P(('rep', 'fs')), parts along dimension 0, may hold values from -6 to 6
- x_early: bfloat16 [2048, 2048], P(('rep', 'fs')), parts along dimension 0, may hold values from -6 to 6
- cotangent: bfloat16 [2048, 2048], P(('rep', 'fs')), parts along dimension 0, may hold values from -6 to 6
- pre_gain: float32 [2048], replicated, may hold values from 0.1 to 1.9
- post_gain: float32 [2048], replicated, may hold values from 0.1 to 1.9
- gate_weight: bfloat16 [2048, 3072], P('fs', 'tp'), may hold values from -0.125 to 0.125
- up_weight: bfloat16 [2048, 3072], P('fs', 'tp'), may hold values from -0.125 to 0.125
- down_weight: bfloat16 [2048, 3072], P('fs', 'tp'), may hold values from -0.109375 to 0.109375
- down_grad_sum: float32 [4096, 3072], P(('rep', 'fs'), 'tp'), parts along dimension 0, may hold values from -6 to 6
Outputs:
- y_late: bfloat16 [2048, 2048], P(('rep', 'fs')), parts along dimension 0
- dx_early: bfloat16 [2048, 2048], P(('rep', 'fs')), parts along dimension 0
- down_grad_out: float32 [4096, 3072], P(('rep', 'fs'), 'tp'), parts along dimension 0
There are 2 independent parts, one for each index of `rep`. A program takes and returns all parts, laid end to end along the dimension named above; an argument that names none is the same for every part. Nothing has to cross between parts.
All inputs are finite; a program needn't handle non-finite values.
Results may differ from a plain program's by a relative error of at most 0.023.
Values may be sent and summed in bfloat16 or wider, within the bound.
No kernel may reach another device: no remote copies, remote signals or barrier semaphores. Data moves between devices by JAX's collectives and lax.ppermute only.
A program may use at most 64 MiB of HBM per device.

v0:
```python
import jax
import jax.numpy as jnp
from jax import lax
from jax.sharding import PartitionSpec as P

eps = 1e-06


def pre_norm(x, pre_gain):
    xf = x.astype(jnp.float32)
    scale = lax.rsqrt(jnp.mean(xf * xf, axis=-1, keepdims=True) + eps)
    return (xf, scale, (xf * scale * pre_gain).astype(jnp.bfloat16))


def right_product(left, right):
    return lax.dot_general(
        left, right, (((1,), (1,)), ((), ())), preferred_element_type=jnp.float32
    )


def body(
    x_late,
    x_early,
    cotangent,
    pre_gain,
    post_gain,
    gate_weight,
    up_weight,
    down_weight,
    down_grad_sum,
):
    rows = x_late.shape[0]
    late_f, late_rs, late_norm = pre_norm(x_late, pre_gain)
    early_f, early_rs, early_norm = pre_norm(x_early, pre_gain)
    normed = jnp.concatenate([late_norm, early_norm], axis=0)
    pieces = (
        lax.all_gather(gate_weight, "fs", axis=0, tiled=True),
        lax.all_gather(up_weight, "fs", axis=0, tiled=True),
    )
    columns = normed
    gate = jnp.dot(columns, pieces[0], preferred_element_type=jnp.float32)
    up = jnp.dot(columns, pieces[1], preferred_element_type=jnp.float32)
    hidden = (jax.nn.silu(gate) * up).astype(jnp.bfloat16)
    partial_value = right_product(hidden, lax.all_gather(down_weight, "fs", axis=0, tiled=True))
    branch = lax.psum(partial_value.astype(jnp.bfloat16), "tp").astype(jnp.float32)
    branch_l = branch[:rows]
    branch_e = branch[rows:]
    late_rz = lax.rsqrt(jnp.mean(branch_l * branch_l, axis=-1, keepdims=True) + eps)
    y_late = (late_f + 0.5 * branch_l * late_rz * post_gain).astype(jnp.bfloat16)
    early_rz = lax.rsqrt(jnp.mean(branch_e * branch_e, axis=-1, keepdims=True) + eps)
    cot_f = cotangent.astype(jnp.float32)
    dpost = 0.5 * cot_f * post_gain
    dbranch = early_rz * (
        dpost - branch_e * early_rz * early_rz * jnp.mean(branch_e * dpost, axis=-1, keepdims=True)
    )
    dbranch = dbranch.astype(jnp.bfloat16)
    columns = dbranch
    dhidden = jnp.dot(
        columns,
        lax.all_gather(down_weight, "fs", axis=0, tiled=True),
        preferred_element_type=jnp.float32,
    )
    gate_e = gate[rows:]
    up_e = up[rows:]
    sig = jax.nn.sigmoid(gate_e)
    dgate = (dhidden * up_e * sig * (1.0 + gate_e * (1.0 - sig))).astype(jnp.bfloat16)
    dup = (dhidden * gate_e * sig).astype(jnp.bfloat16)
    pieces = lax.all_gather((gate_weight, up_weight), "fs", axis=0, tiled=True)
    dpartial = right_product(dgate, pieces[0]) + right_product(dup, pieces[1])
    dnormed = lax.psum(dpartial.astype(jnp.bfloat16), "tp").astype(jnp.float32)
    gained = pre_gain * dnormed
    dx_early = cot_f + early_rs * (
        gained - early_f * early_rs * early_rs * jnp.mean(early_f * gained, axis=-1, keepdims=True)
    )
    dx_early = dx_early.astype(jnp.bfloat16)
    hidden_e = hidden[rows:]
    owned = lax.all_to_all(dbranch, "fs", split_axis=1, concat_axis=0, tiled=True)
    summed = lax.dot_general(
        owned,
        lax.all_gather(hidden_e, "fs", axis=0, tiled=True),
        (((0,), (0,)), ((), ())),
        preferred_element_type=jnp.float32,
    )
    down_grad_out = down_grad_sum + summed
    return (y_late, dx_early, down_grad_out)


def solution(mesh):
    in_specs = (
        P(("rep", "fs"), None),
        P(("rep", "fs"), None),
        P(("rep", "fs"), None),
        P(),
        P(),
        P("fs", "tp"),
        P("fs", "tp"),
        P("fs", "tp"),
        P(("rep", "fs"), "tp"),
    )
    out_specs = (P(("rep", "fs"), None), P(("rep", "fs"), None), P(("rep", "fs"), "tp"))
    return jax.shard_map(body, mesh=mesh, in_specs=in_specs, out_specs=out_specs, check_vma=False)
```

profile of v0, /device:TPU:0, one launch (start us, length us, event | category | flops | bytes accessed | tf_op | source)
XLA Modules:
  0.0 441.1 jit_solution(18082639980764139476)
XLA Ops:
  7.2 0.0 copy-start.2
  7.2 0.0 copy-start.1
  7.2 0.0 copy-start.5
  7.2 0.0 all-gather.5.cloned.1.call-start
  7.2 0.7 all-gather.5.cloned.1.call-update
  7.9 0.0 all-gather.7.cloned.1.call-start
  8.0 0.7 all-gather.7.cloned.1.call-update
  8.7 0.0 all-gather.9.cloned.1.call-start
  8.7 0.7 all-gather.9.cloned.1.call-update
  9.4 0.0 all-reduce.3.cloned.1.call-start
  9.5 0.0 copy-done.2
  9.5 0.2 fusion.13
  9.7 0.0 copy-done.1
  9.7 0.2 fusion.17
  9.9 0.0 copy-done.5
  9.9 0.3 fusion.15
  10.2 101.4 %all-gather.5.cloned.1.call-done = bf16[2048,1536]{1,0:T(8,128)(2,1)} async-done(((bf16[256,1536]{1,0:T(8,128)(2,1)}), bf16[2048,1536]{1,0:T(8,128)(2,1)}) %all-gather.5.cloned.1.call-update) | async-done | bytes 6291472 | tf_op jit(solution)/shard_map/all_gather | solution.py:37
  111.6 5.7 %fusion.23 = f32[256,1536]{1,0:T(8,128)} fusion(bf16[2048,1536]{1,0:T(8,128)(2,1)} %all-gather.5.cloned.1.call-done, bf16[128,2048]{1,0:T(8,128)(2,1)S(1)} %get-tuple-element.9, bf16[128,2048]{1,0:T(8,128)(2,1)S(1)} %get-tuple-element.8), kind=kOutput, calls=%fused_computation.42 | convolution fusion | flops 1612709888 | bytes 8912896 | tf_op jit(solution)/shard_map/dot_general | solution.py:41
  117.4 93.4 %all-gather.7.cloned.1.call-done = bf16[2048,1536]{1,0:T(8,128)(2,1)} async-done(((bf16[256,1536]{1,0:T(8,128)(2,1)}), bf16[2048,1536]{1,0:T(8,128)(2,1)}) %all-gather.7.cloned.1.call-update) | async-done | bytes 6291472 | tf_op jit(solution)/shard_map/all_gather | solution.py:38
  210.7 6.2 %multiply_convert_fusion = (bf16[256,1536]{1,0:T(8,128)(2,1)S(1)}, f32[256,1536]{1,0:T(8,128)}) fusion(f32[256,1536]{1,0:T(8,128)} %fusion.23, bf16[2048,1536]{1,0:T(8,128)(2,1)} %all-gather.7.cloned.1.call-done, bf16[128,2048]{1,0:T(8,128)(2,1)S(1)} %get-tuple-element.9, bf16[128,2048]{1,0:T(8,128)(2,1)S(1)} %get-tuple-element.8), kind=kOutput, calls=%fused_computation.4 | convolution fusion | flops 1615069184 | bytes 11272192 | tf_op jit(solution)/shard_map/dot_general | solution.py:42
  216.9 92.9 %all-gather.9.cloned.1.call-done = bf16[2048,1536]{1,0:T(8,128)(2,1)} async-done(((bf16[256,1536]{1,0:T(8,128)(2,1)}), bf16[2048,1536]{1,0:T(8,128)(2,1)}) %all-gather.9.cloned.1.call-update) | async-done | bytes 6291472 | tf_op jit(solution)/shard_map/all_gather | solution.py:44
  309.8 0.0 copy-start.6
  309.8 5.6 %convolution_convert_fusion = bf16[256,2048]{1,0:T(8,128)(2,1)} fusion(bf16[256,1536]{1,0:T(8,128)(2,1)S(1)} %get-tuple-element.10, bf16[2048,1536]{1,0:T(8,128)(2,1)} %all-gather.9.cloned.1.call-done), kind=kOutput, calls=%fused_computation.1 | convolution fusion | flops 1611137024 | bytes 8126464 | tf_op jit(solution)/shard_map/dot_general | solution.py:16
  315.4 0.0 copy-start.3
  315.4 0.0 all-reduce.3.cloned.1.call-update
  315.5 0.0 all-reduce.5.cloned.1.call-start
  315.5 0.0 copy-done.6
  315.5 17.7 %all-reduce.3.cloned.1.call-done = bf16[256,2048]{1,0:T(8,128)(2,1)} async-done(((bf16[256,2048]{1,0:T(8,128)(2,1)}), bf16[256,2048]{1,0:T(8,128)(2,1)}) %all-reduce.3.cloned.1.call-update) | async-done | bytes 1048592 | tf_op jit(solution)/shard_map/psum | solution.py:45
  333.2 1.5 convert_element_type.51
  334.7 0.0 copy-done.3
  334.7 0.0 copy-start
  334.7 0.4 multiply_reduce_fusion
  335.1 0.0 slice-start
  335.1 0.0 copy-start.7
  335.1 0.0 copy-start.8
  335.1 0.0 slice-start.2
  335.1 1.1 fusion.11
  336.2 1.4 copy-done
  337.7 0.0 slice-start.1
  337.7 0.0 slice-start.3
  337.7 1.0 fusion.32
  338.7 0.3 slice-done
  339.0 0.4 copy-done.7
  339.4 0.4 copy-done.8
  339.8 1.9 slice-done.1
  341.8 2.1 fusion.24
  343.9 0.0 slice-done.2
  343.9 0.0 slice-done.3
  344.0 3.0 fusion
  346.9 0.0 all-reduce.5.cloned.1.call-update
  347.0 0.0 all-gather.11.cloned.1.call-start
  347.0 0.8 slice.24
  347.8 0.0 all-gather.11.cloned.1.call-update
  347.8 0.8 copy.15
  348.6 0.0 copy-start.4
  348.6 5.9 %all-to-all-start = ((bf16[128,8,256]{2,0,1:T(8,128)(2,1)}), bf16[128,8,256]{2,0,1:T(8,128)(2,1)S(1)}, u32[]{:S(2)}, u32[]{:S(2)}) async-start(bf16[128,8,256]{2,0,1:T(8,128)(2,1)} %bitcast.16), calls=%async_computation | async-start | bytes 1048576 | tf_op jit(solution)/shard_map/all_to_all | solution.py:77
  354.6 12.3 %all-reduce.5.cloned.1.call-done = bf16[128,2048]{1,0:T(8,128)(2,1)} async-done(((bf16[128,2048]{1,0:T(8,128)(2,1)}), bf16[128,2048]{1,0:T(8,128)(2,1)}) %all-reduce.5.cloned.1.call-update) | async-done | bytes 524304 | tf_op jit(solution)/shard_map/psum | solution.py:70
  366.9 1.3 fusion.18
  368.2 2.3 fusion.12
  370.5 0.0 all-to-all-done
  370.5 59.7 %all-gather.11.cloned.1.call-done = bf16[1024,1536]{1,0:T(8,128)(2,1)} async-done(((bf16[128,1536]{1,0:T(8,128)(2,1)}), bf16[1024,1536]{1,0:T(8,128)(2,1)}) %all-gather.11.cloned.1.call-update) | async-done | bytes 3145744 | tf_op jit(solution)/shard_map/all_gather | solution.py:80
  430.2 0.0 copy-done.4
  430.2 4.0 convolution_add_fusion
  (8 shorter events, 0.0 us)
Async XLA Ops:
  7.2 2.3 copy-start.2
  7.2 2.5 copy-start.1
  7.2 2.7 copy-start.5
  7.2 104.4 %all-gather.5.cloned.1.call-start = ((), (), s32[]{:S(2)}) async-start(), calls=%async_computation.1 | async-start | bytes 7077888 | tf_op jit(solution)/shard_map/all_gather | solution.py:37
  7.9 202.8 %all-gather.7.cloned.1.call-start = ((), (), s32[]{:S(2)}) async-start(), calls=%async_computation.2 | async-start | bytes 7077888 | tf_op jit(solution)/shard_map/all_gather | solution.py:38
  8.7 301.1 %all-gather.9.cloned.1.call-start = ((), (), s32[]{:S(2)}) async-start(), calls=%async_computation.3 | async-start | bytes 7077888 | tf_op jit(solution)/shard_map/all_gather | solution.py:44
  9.4 323.8 %all-reduce.3.cloned.1.call-start = ((), (), s32[]{:S(2)}) async-start(), calls=%async_computation.4 | async-start | bytes 2097152 | tf_op jit(solution)/shard_map/psum | solution.py:45
  309.8 5.7 %copy-start.6 = (f32[2048]{0:T(1024)S(1)}, f32[2048]{0:T(1024)}, u32[]{:S(2)}) copy-start(f32[2048]{0:T(1024)} %param.13) | copy-start | bytes 24580
  315.4 19.2 %copy-start.3 = (bf16[128,2048]{1,0:T(8,128)(2,1)S(1)}, bf16[128,2048]{1,0:T(8,128)(2,1)}, u32[]{:S(2)}) copy-start(bf16[128,2048]{1,0:T(8,128)(2,1)} %param.11) | copy-start | bytes 1572868
  315.5 51.4 %all-reduce.5.cloned.1.call-start = ((), (), s32[]{:S(2)}) async-start(), calls=%async_computation.5 | async-start | bytes 1048576 | tf_op jit(solution)/shard_map/psum | solution.py:70
  334.7 3.0 copy-start
  335.1 3.9 slice-start
  335.1 4.3 copy-start.7
  335.1 4.7 %copy-start.8 = (f32[256,1536]{1,0:T(8,128)S(1)}, f32[256,1536]{1,0:T(8,128)}, u32[]{:S(2)}) copy-start(f32[256,1536]{1,0:T(8,128)} %get-tuple-element.11) | copy-start | bytes 4718596
  335.1 8.8 %slice-start.2 = ((s8[6291456]{0:T(1024)(128)(4,1)}), s8[4194304]{0:T(1024)(128)(4,1)S(1)}, s32[]{:S(2)}) async-start(s8[6291456]{0:T(1024)(128)(4,1)} %bitcast.21), calls=%async_computation.9 | async-start | bytes 8388608
  337.7 4.1 slice-start.1
  337.7 6.3 %slice-start.3 = ((s8[6291456]{0:T(1024)(128)(4,1)}), s8[2097152]{0:T(1024)(128)(4,1)S(1)}, s32[]{:S(2)}) async-start(s8[6291456]{0:T(1024)(128)(4,1)} %bitcast.21), calls=%async_computation.10 | async-start | bytes 4194304
  347.0 83.2 %all-gather.11.cloned.1.call-start = ((), (), s32[]{:S(2)}) async-start(), calls=%async_computation.6 | async-start | bytes 3538944 | tf_op jit(solution)/shard_map/all_gather | solution.py:80
  348.6 81.6 %copy-start.4 = (f32[256,1536]{1,0:T(8,128)S(1)}, f32[256,1536]{1,0:T(8,128)}, u32[]{:S(2)}) copy-start(f32[256,1536]{1,0:T(8,128)} %param.17) | copy-start | bytes 4718596
  348.6 21.8 %all-to-all-start = ((bf16[128,8,256]{2,0,1:T(8,128)(2,1)}), bf16[128,8,256]{2,0,1:T(8,128)(2,1)S(1)}, u32[]{:S(2)}, u32[]{:S(2)}) async-start(bf16[128,8,256]{2,0,1:T(8,128)(2,1)} %bitcast.16), calls=%async_computation | async-start | bytes 1048576 | tf_op jit(solution)/shard_map/all_to_all | solution.py:77
Sparse Core Ops, SparseCore 0:
  10.2 101.4 all-gather.4
  113.8 96.8 all-gather.6
  212.9 96.8 all-gather.8
  315.6 17.5 all-reduce.2
  347.1 19.7 all-reduce.4
  368.9 61.2 all-gather.10
where the time goes:
time: 442 us; the launch traced here: 441 us
  waiting for transfers between devices  380 us (86%)
  matrix products  27.7 us (6%)
  between operations  14.3 us (3%)
  other arithmetic  7.18 us (2%)
  local copies, waits for them, and re-layouts  6.17 us (1%)
  starting transfers between devices  6.17 us (1%)
    all_gather x1, waiting for transfers between devices, body(): lax.all_gather(gate_weight, 'fs', axis=0, tiled=True)  101 us
    all_gather x1, waiting for transfers between devices, body(): lax.all_gather(up_weight, 'fs', axis=0, tiled=True)  93.4 us
    all_gather x1, waiting for transfers between devices, body(): lax.all_gather(down_weight, 'fs', axis=0, tiled=True)  92.9 us
    all_gather x1, waiting for transfers between devices, body(): lax.all_gather(hidden_e, 'fs', axis=0, tiled=True)  59.7 us
    psum x1, waiting for transfers between devices, body(): lax.psum(partial_value.astype(jnp.bfloat16), 'tp').astype(jnp.float32)  17.7 us
    psum x1, waiting for transfers between devices, body(): dnormed = lax.psum(dpartial.astype(jnp.bfloat16), 'tp').astype(jnp.float32)  12.3 us
    dot_general x3, matrix products, right_product(): lax.dot_general(left, right, (((1,), (1,)), ((), ())), preferred_element_...  10.7 us
  transfers between devices with their start and end apart: 7, of which 6 were waited for; matrix products, arithmetic and copies ran while one was open for 4% of the time, Pallas kernels for 0%

commit v1 on v0

v1 whole, which is shorter than its diff:
```python
import jax
import jax.numpy as jnp
from jax import lax
from jax.sharding import PartitionSpec as P

eps = 1e-06
AXES = ("rep", "fs", "tp")
f32 = jnp.float32
bf16 = jnp.bfloat16


def nt(left, right):
    return lax.dot_general(left, right, (((1,), (1,)), ((), ())), preferred_element_type=f32)


def tn(left, right):
    return lax.dot_general(left, right, (((0,), (0,)), ((), ())), preferred_element_type=f32)


def pick(array, index):
    return lax.dynamic_index_in_dim(array, index, 0, keepdims=False)


def put(array, value, index):
    return lax.dynamic_update_index_in_dim(array, value, index, 0)


def make_body(R, S, T):
    G = 2 if S % 2 == 0 else 1
    Z = S // G
    peers = [(a, b) for a in range(R) for b in range(G)]
    others = peers[1:]

    def send(value, dr=0, dy=0, dz=0, dt=0, lo=0, hi=None, wrap=False):
        hi = Z - 1 if hi is None else hi
        pairs = []
        for r in range(R):
            for z in range(Z):
                for y in range(G):
                    for t in range(T):
                        to = z + dz
                        if wrap:
                            to %= Z
                        if not (lo <= z <= hi and 0 <= to < Z):
                            continue
                        source = (r * S + z * G + y) * T + t
                        target = ((r + dr) % R * S + to * G + (y + dy) % G) * T + (t + dt) % T
                        pairs.append((source, target))
        return lax.ppermute(value, AXES, pairs)

    def line(piece):
        up, down, below, above = piece, piece, [], []
        for s in range(1, Z):
            up = send(up, dz=1, lo=s - 1)
            down = send(down, dz=-1, hi=Z - s)
            below.append(up)
            above.append(down)
        return below, above

    def order(z):
        hops = range(1, Z)
        table = []
        for s in hops:
            if z >= s:
                table.append((0, s))
            if z + s < Z:
                table.append((1, s))
        return table

    def body(x_late, x_early, cotangent, pre_gain, post_gain, gate_weight, up_weight, down_weight, down_grad_sum):
        r, f, t = (lax.axis_index(a) for a in AXES)
        y, z = f % G, f // G
        n, D = x_late.shape
        m = n // T
        K, F = gate_weight.shape
        w = F // (R * G)
        PT = len(peers)

        def columns(weight, dy):
            q = r * G + (y + dy) % G
            return lax.dynamic_slice_in_dim(weight, q * w, w, 1)

        def both(dy):
            return jnp.concatenate([columns(gate_weight, dy), columns(up_weight, dy)], axis=1)

        gu = [both(0)] + [send(both(d), dy=d) for d in range(1, G)]
        dn = [columns(down_weight, 0)] + [send(columns(down_weight, d), dy=d) for d in range(1, G)]

        x = jnp.stack([x_late, x_early]).astype(f32)
        scale = lax.rsqrt(jnp.mean(x * x, axis=-1, keepdims=True) + eps)
        normed = (x * scale * pre_gain).astype(bf16).reshape(2, T, m, D)

        def chunk(array, j):
            return lax.dynamic_index_in_dim(array, (t + j) % T, 1, keepdims=False)

        mine = chunk(normed, 0)
        held = [[chunk(normed, j) for j in range(T)]]
        for dr, dy in others:
            got = send(mine, dr=-dr, dy=-dy)
            held.append([got] + [send(got, dt=-j) for j in range(1, T)])
        tokens = jnp.stack([jnp.stack(h, axis=1) for h in held], axis=1).reshape(2 * PT * n, D)

        full = jnp.zeros((Z, G, K, 2 * w), bf16)

        def place(array, value, zi, yi):
            return lax.dynamic_update_slice(array, value[None, None], (zi, yi, 0, 0))

        lines = [line(piece) for piece in gu]
        for s in range(1, Z):
            for d, (below, above) in enumerate(lines):
                yi = (y - d) % G
                full = place(full, below[s - 1], jnp.where(z >= s, z - s, z), yi)
                full = place(full, above[s - 1], jnp.where(z + s < Z, z + s, z), yi)
        for d, piece in enumerate(gu):
            full = place(full, piece, z, (y - d) % G)
        full = full.reshape(D, 2 * w)

        both_out = jnp.dot(tokens, full, preferred_element_type=f32)
        gate, up = both_out[:, :w], both_out[:, w:]
        hidden = (jax.nn.silu(gate) * up).astype(bf16)

        block = jnp.zeros((G, K, w), bf16)
        for d, piece in enumerate(dn):
            block = put(block, piece, (y - d) % G)
        block = block.reshape(G * K, w)
        below, above = line(block)
        got = (below, above)
        slots, ids = [block], [z]
        tables = [order(i) for i in range(Z)]
        for k in range(Z - 1):
            value, where = None, jnp.int32(0)
            for side, s in sorted({tables[i][k] for i in range(Z)}):
                owners = [i for i in range(Z) if tables[i][k] == (side, s)]
                here = sum((z == i) for i in owners).astype(bool)
                value = got[side][s - 1] if value is None else jnp.where(here, got[side][s - 1], value)
                where = jnp.where(here, z + (s if side else -s), where)
            slots.append(value)
            ids.append(where)

        def reduce_plane(part):
            low = part.astype(bf16)
            chip = part[:, :, 0]
            for j in range(1, T):
                chip = chip + send(low[:, :, j], dt=j).astype(f32)
            low = chip.astype(bf16)
            total = chip[:, 0]
            for p, (dr, dy) in enumerate(peers):
                if p:
                    total = total + send(low[:, p], dr=dr, dy=dy).astype(f32)
            return total

        groups = [[0, 1]] + [[k] for k in range(2, Z)] if Z > 1 else [[0]]
        branch = jnp.zeros((Z, 2, m, G * K), f32)
        for group in groups:
            weight = jnp.concatenate([slots[k] for k in group], axis=0)
            part = nt(hidden, weight).reshape(2, PT, T, m, len(group) * G * K)
            total = reduce_plane(part)
            for i, k in enumerate(group):
                branch = put(branch, total[:, :, i * G * K:(i + 1) * G * K], ids[k])
        branch = branch.transpose(1, 2, 0, 3).reshape(2, m, D)
        branch_l, branch_e = branch[0], branch[1]

        def own_rows(array):
            return lax.dynamic_slice_in_dim(array, t * m, m, 0)

        def all_rows(value):
            out = put(jnp.zeros((T,) + value.shape, value.dtype), value, t)
            for j in range(1, T):
                out = put(out, send(value, dt=-j), (t + j) % T)
            return out.reshape(n, D)

        late_rz = lax.rsqrt(jnp.mean(branch_l * branch_l, axis=-1, keepdims=True) + eps)
        y_late = (own_rows(x_late).astype(f32) + 0.5 * branch_l * late_rz * post_gain).astype(bf16)
        y_late = all_rows(y_late)

        early_rz = lax.rsqrt(jnp.mean(branch_e * branch_e, axis=-1, keepdims=True) + eps)
        cot_f = own_rows(cotangent).astype(f32)
        dpost = 0.5 * cot_f * post_gain
        dbranch = early_rz * (dpost - branch_e * early_rz * early_rz * jnp.mean(branch_e * dpost, axis=-1, keepdims=True))
        dbranch = dbranch.astype(bf16)

        def plane(value):
            out = []
            for p, (dr, dy) in enumerate(peers):
                got = send(value, dr=-dr, dy=-dy) if p else value
                out.append([got] + [send(got, dt=-j) for j in range(1, T)])
            return out

        down_full = jnp.zeros((Z, G * K, w), bf16)
        for slot, where in zip(slots, ids):
            down_full = put(down_full, slot, where)
        down_full = down_full.reshape(D, w)
        spread = plane(dbranch)
        spread = jnp.stack([jnp.stack(h) for h in spread]).reshape(PT * n, D)
        dhidden = jnp.dot(spread, down_full, preferred_element_type=f32)
        gate_e, up_e = gate[PT * n:], up[PT * n:]
        sig = jax.nn.sigmoid(gate_e)
        dgate = (dhidden * up_e * sig * (1.0 + gate_e * (1.0 - sig))).astype(bf16)
        dup = (dhidden * gate_e * sig).astype(bf16)
        dpart = nt(jnp.concatenate([dgate, dup], axis=1), full)
        dnormed = reduce_plane(dpart.reshape(1, PT, T, m, D))[0]
        gained = pre_gain * dnormed
        early_f = own_rows(x_early).astype(f32)
        early_rs = lax.dynamic_slice_in_dim(scale[1], t * m, m, 0)
        dx = cot_f + early_rs * (gained - early_f * early_rs * early_rs * jnp.mean(early_f * gained, axis=-1, keepdims=True))
        dx_early = all_rows(dx.astype(bf16))

        hidden_e = hidden[PT * n:]
        kept = [hidden_e] + [send(hidden_e, dz=k, wrap=True) for k in range(1, Z)]
        parts = dbranch.reshape(m, Z, G * K).transpose(1, 0, 2)
        cols = [pick(parts, z)] + [send(pick(parts, (z + k) % Z), dz=k, wrap=True) for k in range(1, Z)]
        wide = plane(jnp.stack(cols))
        half = G * n
        result = jnp.zeros((R * G, K, w), f32)
        for a in range(R):
            left = jnp.concatenate([wide[a * G + b][j][k] for k in range(Z) for b in range(G) for j in range(T)], axis=0)
            right = jnp.concatenate([h[a * half:(a + 1) * half] for h in kept], axis=0)
            grad = tn(left, right).reshape(G, K, w)
            for b in range(G):
                piece = pick(grad, (y + b) % G)
                if a or b:
                    piece = send(piece.astype(bf16), dr=a, dy=b).astype(f32)
                result = put(result, piece, (r - a) % R * G + (y - b) % G)
        summed = result.transpose(1, 0, 2).reshape(K, F)
        return (y_late, dx_early, down_grad_sum + summed)

    return body


def solution(mesh):
    R, S, T = (mesh.shape[a] for a in AXES)
    in_specs = (
        P(("rep", "fs"), None),
        P(("rep", "fs"), None),
        P(("rep", "fs"), None),
        P(),
        P(),
        P("fs", "tp"),
        P("fs", "tp"),
        P("fs", "tp"),
        P(("rep", "fs"), "tp"),
    )
    out_specs = (P(("rep", "fs"), None), P(("rep", "fs"), None), P(("rep", "fs"), "tp"))
    return jax.shard_map(make_body(R, S, T), mesh=mesh, in_specs=in_specs, out_specs=out_specs, check_vma=False)
```

time: 442 us -> 291 us (0.66)
  waiting for transfers between devices: 380 us -> 107 us
  starting transfers between devices: 6.17 us -> 78.8 us
  local copies, waits for them, and re-layouts: 6.17 us -> 70.8 us
  matrix products: 27.7 us -> 12.4 us
  between operations: 14.3 us -> 2.19 us
  other arithmetic: 7.18 us -> 18.5 us
    all_gather x4 -> x0, waiting for transfers between devices: 347 us -> none  [the longest x1 101 us: body(): lax.all_gather(gate_weight, 'fs', axis=0, tiled=True)]
    ppermute x0 -> x67, waiting for transfers between devices: none -> 107 us  [send(): return lax.ppermute(value, AXES, pairs)]
    ppermute x0 -> x67, starting transfers between devices: none -> 78.8 us  [send(): return lax.ppermute(value, AXES, pairs)]
    dynamic_update_slice x0 -> x26, local copies, waits for them, and re-layouts: none -> 50.1 us  [the longest x13 46.7 us: put(): return lax.dynamic_update_index_in_dim(array, value, index, 0)]
    psum x2 -> x0, waiting for transfers between devices: 30 us -> none  [the longest x1 17.7 us: body(): lax.psum(partial_value.astype(jnp.bfloat16), 'tp').astype(jnp.float32)]
    dot_general x7 -> x8, matrix products: 27.7 us -> 12.4 us  [the longest x4 4.57 us: nt(): lax.dot_general(left, right, (((1,), (1,)), ((), ())), preferred_element_...]
    all_to_all x1 -> x0, starting transfers between devices: 5.93 us -> none  [body(): lax.all_to_all(dbranch, 'fs', split_axis=1, concat_axis=0, tiled=True)]
  transfers between devices with their start and end apart: 7 -> 67, of which waited for: 6 -> 22; matrix products, arithmetic and copies ran while one was open for 4% -> 26% of each run, Pallas kernels for 0% -> 0%
where the time goes in v1:
time: 291 us; the launch traced here: 290 us
  waiting for transfers between devices  107 us (37%)
  starting transfers between devices  78.8 us (27%)
  local copies, waits for them, and re-layouts  70.8 us (24%)
  other arithmetic  18.5 us (6%)
  matrix products  12.4 us (4%)
    ppermute x67, waiting for transfers between devices, send(): return lax.ppermute(value, AXES, pairs)  107 us
    ppermute x67, starting transfers between devices, send(): return lax.ppermute(value, AXES, pairs)  78.8 us
    dynamic_update_slice x13, local copies, waits for them, and re-layouts, put(): return lax.dynamic_update_index_in_dim(array, value, index, 0)  46.7 us
  transfers between devices with their start and end apart: 67, of which 22 were waited for; matrix products, arithmetic and copies ran while one was open for 26% of the time, Pallas kernels for 0%

profile of v1, /device:TPU:0, one launch (start us, length us, event | category | flops | bytes accessed | tf_op | source)
XLA Modules:
  0.0 290.0 jit_solution(13587042563553071405)
XLA Ops:
  0.7 1.4 constant_dynamic-slice_fusion.7
  2.9 5.7 %collective-permute-start.6 = (bf16[256,768]{1,0:T(8,128)(2,1)}, bf16[256,768]{1,0:T(8,128)(2,1)}, u32[]{:S(2)}, u32[]{:S(2)}) collective-permute-start(bf16[256,768]{1,0:T(8,128)(2,1)} %pad_maximum_fusion.2), channel_id=1, source_target_pairs={{0,4},{1,5},{2,6},{3,7},{4,8},{5,9},{6,10},{7,11},{8,12},{9,13},{1... | collective-permute-start | bytes 1179656 | tf_op jit(solution)/shard_map/ppermute | solution.py:49
  8.6 1.3 collective-permute-start.7
  9.9 1.6 constant_dynamic-slice_fusion.6
  11.5 1.5 collective-permute-start.19
  15.1 1.6 collective-permute-start.2
  21.1 1.3 collective-permute-start.20
  22.7 5.2 %collective-permute-start.21 = (bf16[512,384]{1,0:T(8,128)(2,1)S(1)}, bf16[512,384]{1,0:T(8,128)(2,1)S(1)}, u32[]{:S(2)}, u32[]{:S(2)}) collective-permute-start(bf16[512,384]{1,0:T(8,128)(2,1)S(1)} %bitcast.423), channel_id=1, source_target_pairs={{0,4},{1,5},{2,6},{3,7},{4,8},{5,9},{6,10},{7,11},{8,12},{9,13},{1... | collective-permute-start | bytes 1179656 | tf_op jit(solution)/shard_map/ppermute | solution.py:49
  29.1 1.9 collective-permute-start.4
  31.1 3.9 %collective-permute-start.9 = (bf16[256,768]{1,0:T(8,128)(2,1)}, bf16[256,768]{1,0:T(8,128)(2,1)S(1)}, u32[]{:S(2)}, u32[]{:S(2)}) collective-permute-start(bf16[256,768]{1,0:T(8,128)(2,1)} %collective-permute-done.8), channel_id=1, source_target_pairs={{0,4},{1,5},{2,6},{3,7},{4,8},{5,9},{6,10},{7,11},{8,12},{9,13},{1... | collective-permute-start | bytes 1179656 | tf_op jit(solution)/shard_map/ppermute | solution.py:49
  37.1 1.3 collective-permute-start.10
  38.6 4.8 %collective-permute-done.9 = bf16[256,768]{1,0:T(8,128)(2,1)S(1)} collective-permute-done((bf16[256,768]{1,0:T(8,128)(2,1)}, bf16[256,768]{1,0:T(8,128)(2,1)S(1)}, u32[]{:S(2)}, u32[]{:S(2)}) %collective-permute-start.9) | collective-permute-done | bytes 393248 | tf_op jit(solution)/shard_map/ppermute | solution.py:49
  44.1 1.3 collective-permute-start.12
  45.4 2.1 collective-permute-done.10
  47.5 1.3 collective-permute-start.26
  49.6 3.8 %collective-permute-done = bf16[2,64,2048]{2,1,0:T(8,128)(2,1)S(1)} collective-permute-done((bf16[2,64,2048]{2,1,0:T(8,128)(2,1)S(1)}, bf16[2,64,2048]{2,1,0:T(8,128)(2,1)S(1)}, u32[]{:S(2)}, u32[]{:S(2)}) %collective-permute-start) | collective-permute-done | bytes 524320 | tf_op jit(solution)/shard_map/ppermute | solution.py:49
  53.3 7.6 %collective-permute-done.12 = bf16[256,768]{1,0:T(8,128)(2,1)S(1)} collective-permute-done((bf16[256,768]{1,0:T(8,128)(2,1)}, bf16[256,768]{1,0:T(8,128)(2,1)S(1)}, u32[]{:S(2)}, u32[]{:S(2)}) %collective-permute-start.12) | collective-permute-done | bytes 393248 | tf_op jit(solution)/shard_map/ppermute | solution.py:49
  61.0 5.3 %collective-permute-done.26 = bf16[512,384]{1,0:T(8,128)(2,1)S(1)} collective-permute-done((bf16[512,384]{1,0:T(8,128)(2,1)S(1)}, bf16[512,384]{1,0:T(8,128)(2,1)S(1)}, u32[]{:S(2)}, u32[]{:S(2)}) %collective-permute-start.26) | collective-permute-done | bytes 393248 | tf_op jit(solution)/shard_map/ppermute | solution.py:49
  67.0 1.3 collective-permute-start.14
  70.3 1.3 collective-permute-start.16
  71.7 1.3 collective-permute-start.32
  74.3 7.1 %collective-permute-done.14 = bf16[256,768]{1,0:T(8,128)(2,1)S(1)} collective-permute-done((bf16[256,768]{1,0:T(8,128)(2,1)S(1)}, bf16[256,768]{1,0:T(8,128)(2,1)S(1)}, u32[]{:S(2)}, u32[]{:S(2)}) %collective-permute-start.14) | collective-permute-done | bytes 393248 | tf_op jit(solution)/shard_map/ppermute | solution.py:49
  82.1 1.3 collective-permute-start.18
  83.4 6.3 %collective-permute-done.16 = bf16[256,768]{1,0:T(8,128)(2,1)S(1)} collective-permute-done((bf16[256,768]{1,0:T(8,128)(2,1)S(1)}, bf16[256,768]{1,0:T(8,128)(2,1)S(1)}, u32[]{:S(2)}, u32[]{:S(2)}) %collective-permute-start.16) | collective-permute-done | bytes 393248 | tf_op jit(solution)/shard_map/ppermute | solution.py:49
  89.8 8.4 %collective-permute-done.32 = bf16[512,384]{1,0:T(8,128)(2,1)S(1)} collective-permute-done((bf16[512,384]{1,0:T(8,128)(2,1)S(1)}, bf16[512,384]{1,0:T(8,128)(2,1)S(1)}, u32[]{:S(2)}, u32[]{:S(2)}) %collective-permute-start.32) | collective-permute-done | bytes 393248 | tf_op jit(solution)/shard_map/ppermute | solution.py:49
  98.5 4.3 %collective-permute-done.18 = bf16[256,768]{1,0:T(8,128)(2,1)S(1)} collective-permute-done((bf16[256,768]{1,0:T(8,128)(2,1)S(1)}, bf16[256,768]{1,0:T(8,128)(2,1)S(1)}, u32[]{:S(2)}, u32[]{:S(2)}) %collective-permute-start.18) | collective-permute-done | bytes 393248 | tf_op jit(solution)/shard_map/ppermute | solution.py:49
  103.9 3.4 %fusion.84 = f32[1024,768]{1,0:T(8,128)S(1)} fusion(bf16[1024,2048]{1,0:T(8,128)(2,1)S(1)} %bitcast.419, bf16[2048,768]{1,0:T(8,128)(2,1)S(1)} %bitcast.427), kind=kOutput, calls=%fused_computation.247 | convolution fusion | flops 3221225472 | bytes 10485760 | tf_op jit(solution)/shard_map/dot_general | solution.py:118
  109.0 3.8 %collective-permute-start.59 = (bf16[512,384]{1,0:T(8,128)(2,1)S(1)}, bf16[512,384]{1,0:T(8,128)(2,1)S(1)}, u32[]{:S(2)}, u32[]{:S(2)}) collective-permute-start(bf16[512,384]{1,0:T(8,128)(2,1)S(1)} %slice.332), channel_id=1, source_target_pairs={{0,12},{1,13},{2,14},{3,15},{4,0},{5,1},{6,2},{7,3},{8,4},{9,5},{1... | collective-permute-start | bytes 1179656 | tf_op jit(solution)/shard_map/ppermute | solution.py:49
  115.1 1.3 fusion.10
  117.3 5.5 %collective-permute-done.57 = bf16[512,384]{1,0:T(8,128)(2,1)S(1)} collective-permute-done((bf16[512,384]{1,0:T(8,128)(2,1)S(1)}, bf16[512,384]{1,0:T(8,128)(2,1)S(1)}, u32[]{:S(2)}, u32[]{:S(2)}) %collective-permute-start.57) | collective-permute-done | bytes 393248 | tf_op jit(solution)/shard_map/ppermute | solution.py:49
  123.6 11.6 %collective-permute-done.58 = bf16[512,384]{1,0:T(8,128)(2,1)S(1)} collective-permute-done((bf16[512,384]{1,0:T(8,128)(2,1)S(1)}, bf16[512,384]{1,0:T(8,128)(2,1)S(1)}, u32[]{:S(2)}, u32[]{:S(2)}) %collective-permute-start.58) | collective-permute-done | bytes 393248 | tf_op jit(solution)/shard_map/ppermute | solution.py:49
  137.0 1.6 collective-permute-start.35
  139.4 1.2 collective-permute-start.37
  140.9 1.6 collective-permute-start.29
  144.7 1.7 collective-permute-start.31
  148.5 1.8 collective-permute-done.29
  150.3 1.7 collective-permute-start.25
  153.9 4.9 %collective-permute-done.23 = bf16[2,64,1024]{2,1,0:T(8,128)(2,1)S(1)} collective-permute-done((bf16[2,64,1024]{2,1,0:T(8,128)(2,1)S(1)}, bf16[2,64,1024]{2,1,0:T(8,128)(2,1)S(1)}, u32[]{:S(2)}, u32[]{:S(2)}) %collective-permute-start.23) | collective-permute-done | bytes 262176 | tf_op jit(solution)/shard_map/ppermute | solution.py:49
  158.9 2.8 collective-permute-done.25
  162.6 2.5 dynamic_update_slice.117
  165.1 2.5 dynamic_update_slice.118
  167.7 2.5 dynamic_update_slice.119
  170.2 2.5 dynamic_update_slice.120
  175.2 8.1 %collective-permute-start.51 = (bf16[64,512]{1,0:T(8,128)(2,1)S(1)}, bf16[64,512]{1,0:T(8,128)(2,1)S(1)}, u32[]{:S(2)}, u32[]{:S(2)}) collective-permute-start(bf16[64,512]{1,0:T(8,128)(2,1)S(1)} %bitcast.463), channel_id=1, source_target_pairs={{0,4},{1,5},{2,6},{3,7},{4,8},{5,9},{6,10},{7,11},{8,12},{9,13},{1... | collective-permute-start | bytes 196616 | tf_op jit(solution)/shard_map/ppermute | solution.py:49
  183.5 2.6 collective-permute-start.53
  187.8 1.5 collective-permute-start.40
  190.1 1.6 collective-permute-start.44
  192.8 15.7 %collective-permute-done.61 = bf16[4,64,512]{2,1,0:T(8,128)(2,1)S(1)} collective-permute-done((bf16[4,64,512]{2,1,0:T(8,128)(2,1)S(1)}, bf16[4,64,512]{2,1,0:T(8,128)(2,1)S(1)}, u32[]{:S(2)}, u32[]{:S(2)}) %collective-permute-start.61) | collective-permute-done | bytes 262176 | tf_op jit(solution)/shard_map/ppermute | solution.py:49
  209.1 1.7 collective-permute-start.63
  211.5 9.8 %collective-permute-done.55 = bf16[4,64,512]{2,1,0:T(8,128)(2,1)S(1)} collective-permute-done((bf16[4,64,512]{2,1,0:T(8,128)(2,1)S(1)}, bf16[4,64,512]{2,1,0:T(8,128)(2,1)S(1)}, u32[]{:S(2)}, u32[]{:S(2)}) %collective-permute-start.55) | collective-permute-done | bytes 262176 | tf_op jit(solution)/shard_map/ppermute | solution.py:49
  223.6 2.9 %fusion.9 = (bf16[512,384]{1,0:T(8,128)(2,1)S(1)}, bf16[512,384]{1,0:T(8,128)(2,1)S(1)}) fusion(f32[1024,768]{1,0:T(8,128)} %copy-done.4, bf16[512,2048]{1,0:T(8,128)(2,1)S(1)} %bitcast.432, bf16[2048,384]{1,0:T(8,128)(2,1)S(1)} %bitcast.439), kind=kOutput, calls=%fused_computation.27 | convolution fusion | flops 807862272 | bytes 6029312 | tf_op jit(solution)/shard_map/dot_general | solution.py:195
  226.6 1.8 fusion.14
  233.0 1.7 fusion.72
  237.1 2.0 collective-permute-start.49
  241.4 8.6 %dynamic_update_slice.129 = f32[4,256,384]{2,0,1:T(4,128)S(1)} dynamic-update-slice(f32[4,256,384]{2,0,1:T(4,128)S(1)} %broadcast_in_dim.164, f32[1,256,384]{2,0,1:T(1,128)S(1)} %copy.89, s32[]{:T(128)S(6)} %select_n.372, s32[]{:T(128)} %constant.238.clone.1, s32[]{:T(128)} %constant.238.clone.1) | dynamic-update-slice | bytes 786436 | tf_op jit(solution)/shard_map/jit(dynamic_update_index_in_dim)/dynamic_update_slice | solution.py:25
  250.0 1.8 collective-permute-start.66
  252.8 1.5 fusion.44
  254.4 2.2 bitcast_dynamic-update-slice_fusion.19
  256.6 1.7 collective-permute-done.60
  260.5 8.6 %dynamic_update_slice.130 = f32[4,256,384]{2,0,1:T(4,128)S(1)} dynamic-update-slice(f32[4,256,384]{2,0,1:T(4,128)S(1)} %dynamic_update_slice.129, f32[1,256,384]{2,0,1:T(1,128)S(1)} %copy.90, s32[]{:T(128)S(6)} %select_n.374, s32[]{:T(128)} %constant.238.clone.1, s32[]{:T(128)} %constant.238.clone.1) | dynamic-update-slice | bytes 786436 | tf_op jit(solution)/shard_map/jit(dynamic_update_index_in_dim)/dynamic_update_slice | solution.py:25
  269.2 8.6 %dynamic_update_slice.131 = f32[4,256,384]{2,0,1:T(4,128)S(1)} dynamic-update-slice(f32[4,256,384]{2,0,1:T(4,128)S(1)} %dynamic_update_slice.130, f32[1,256,384]{2,0,1:T(1,128)S(1)} %copy.91, s32[]{:T(128)S(6)} %select_n.376, s32[]{:T(128)} %constant.238.clone.1, s32[]{:T(128)} %constant.238.clone.1) | dynamic-update-slice | bytes 786436 | tf_op jit(solution)/shard_map/jit(dynamic_update_index_in_dim)/dynamic_update_slice | solution.py:25
  277.8 8.6 %dynamic_update_slice.132 = f32[4,256,384]{2,0,1:T(4,128)S(1)} dynamic-update-slice(f32[4,256,384]{2,0,1:T(4,128)S(1)} %dynamic_update_slice.131, f32[1,256,384]{2,0,1:T(1,128)S(1)} %copy.92, s32[]{:T(128)S(6)} %select_n.377, s32[]{:T(128)} %constant.238.clone.1, s32[]{:T(128)} %constant.238.clone.1) | dynamic-update-slice | bytes 786436 | tf_op jit(solution)/shard_map/jit(dynamic_update_index_in_dim)/dynamic_update_slice | solution.py:25
  286.5 1.3 copy-done.7
  287.8 1.3 add.439
  (269 shorter events, 57.0 us)
Async XLA Ops:
  2.9 19.8 %collective-permute-start.6 = (bf16[256,768]{1,0:T(8,128)(2,1)}, bf16[256,768]{1,0:T(8,128)(2,1)}, u32[]{:S(2)}, u32[]{:S(2)}) collective-permute-start(bf16[256,768]{1,0:T(8,128)(2,1)} %pad_maximum_fusion.2), channel_id=1, source_target_pairs={{0,4},{1,5},{2,6},{3,7},{4,8},{5,9},{6,10},{7,11},{8,12},{9,13},{1... | collective-permute-start | bytes 1179656 | tf_op jit(solution)/shard_map/ppermute | solution.py:49
  8.6 22.5 %collective-permute-start.7 = (bf16[256,768]{1,0:T(8,128)(2,1)}, bf16[256,768]{1,0:T(8,128)(2,1)}, u32[]{:S(2)}, u32[]{:S(2)}) collective-permute-start(bf16[256,768]{1,0:T(8,128)(2,1)} %pad_maximum_fusion.2), channel_id=1, source_target_pairs={{4,0},{5,1},{6,2},{7,3},{8,4},{9,5},{10,6},{11,7},{12,8},{13,9},{1... | collective-permute-start | bytes 1179656 | tf_op jit(solution)/shard_map/ppermute | solution.py:49
  11.5 8.7 %collective-permute-start.19 = (bf16[256,384]{1,0:T(8,128)(2,1)}, bf16[256,384]{1,0:T(8,128)(2,1)}, u32[]{:S(2)}, u32[]{:S(2)}) collective-permute-start(bf16[256,384]{1,0:T(8,128)(2,1)} %constant_dynamic-slice_fusion.6), channel_id=1, source_target_pairs={{0,2},{1,3},{2,0},{3,1},{4,6},{5,7},{6,4},{7,5},{8,10},{9,11},{10,... | collective-permute-start | bytes 589832 | tf_op jit(solution)/shard_map/ppermute | solution.py:49
  13.8 15.3 %collective-permute-start.8 = (bf16[256,768]{1,0:T(8,128)(2,1)}, bf16[256,768]{1,0:T(8,128)(2,1)}, u32[]{:S(2)}, u32[]{:S(2)}) collective-permute-start(bf16[256,768]{1,0:T(8,128)(2,1)} %pad_maximum_fusion.3), channel_id=1, source_target_pairs={{0,2},{1,3},{2,0},{3,1},{4,6},{5,7},{6,4},{7,5},{8,10},{9,11},{10,... | collective-permute-start | bytes 1179656 | tf_op jit(solution)/shard_map/ppermute | solution.py:49
  15.1 29.0 %collective-permute-start.2 = (bf16[2,64,2048]{2,1,0:T(8,128)(2,1)S(1)}, bf16[2,64,2048]{2,1,0:T(8,128)(2,1)}, u32[]{:S(2)}, u32[]{:S(2)}) collective-permute-start(bf16[2,64,2048]{2,1,0:T(8,128)(2,1)S(1)} %bitcast.436), channel_id=1, source_target_pairs={{0,16},{1,17},{2,18},{3,19},{4,20},{5,21},{6,22},{7,23},{8,24},{9,... | collective-permute-start | bytes 1572872 | tf_op jit(solution)/shard_map/ppermute | solution.py:49
  21.1 14.9 %collective-permute-start.20 = (bf16[512,384]{1,0:T(8,128)(2,1)S(1)}, bf16[512,384]{1,0:T(8,128)(2,1)S(1)}, u32[]{:S(2)}, u32[]{:S(2)}) collective-permute-start(bf16[512,384]{1,0:T(8,128)(2,1)S(1)} %bitcast.421), channel_id=1, source_target_pairs={{4,0},{5,1},{6,2},{7,3},{8,4},{9,5},{10,6},{11,7},{12,8},{13,9},{1... | collective-permute-start | bytes 1179656 | tf_op jit(solution)/shard_map/ppermute | solution.py:49
  22.7 14.5 %collective-permute-start.21 = (bf16[512,384]{1,0:T(8,128)(2,1)S(1)}, bf16[512,384]{1,0:T(8,128)(2,1)S(1)}, u32[]{:S(2)}, u32[]{:S(2)}) collective-permute-start(bf16[512,384]{1,0:T(8,128)(2,1)S(1)} %bitcast.423), channel_id=1, source_target_pairs={{0,4},{1,5},{2,6},{3,7},{4,8},{5,9},{6,10},{7,11},{8,12},{9,13},{1... | collective-permute-start | bytes 1179656 | tf_op jit(solution)/shard_map/ppermute | solution.py:49
  29.1 18.4 %collective-permute-start.4 = (bf16[2,64,2048]{2,1,0:T(8,128)(2,1)S(1)}, bf16[2,64,2048]{2,1,0:T(8,128)(2,1)S(1)}, u32[]{:S(2)}, u32[]{:S(2)}) collective-permute-start(bf16[2,64,2048]{2,1,0:T(8,128)(2,1)S(1)} %bitcast.437), channel_id=1, source_target_pairs={{0,18},{1,19},{2,16},{3,17},{4,22},{5,23},{6,20},{7,21},{8,26},{9,... | collective-permute-start | bytes 1572872 | tf_op jit(solution)/shard_map/ppermute | solution.py:49
  31.1 12.3 %collective-permute-start.9 = (bf16[256,768]{1,0:T(8,128)(2,1)}, bf16[256,768]{1,0:T(8,128)(2,1)S(1)}, u32[]{:S(2)}, u32[]{:S(2)}) collective-permute-start(bf16[256,768]{1,0:T(8,128)(2,1)} %collective-permute-done.8), channel_id=1, source_target_pairs={{0,4},{1,5},{2,6},{3,7},{4,8},{5,9},{6,10},{7,11},{8,12},{9,13},{1... | collective-permute-start | bytes 1179656 | tf_op jit(solution)/shard_map/ppermute | solution.py:49
  36.0 17.3 %collective-permute-start = (bf16[2,64,2048]{2,1,0:T(8,128)(2,1)S(1)}, bf16[2,64,2048]{2,1,0:T(8,128)(2,1)S(1)}, u32[]{:S(2)}, u32[]{:S(2)}) collective-permute-start(bf16[2,64,2048]{2,1,0:T(8,128)(2,1)S(1)} %bitcast.438), channel_id=1, source_target_pairs={{0,2},{1,3},{2,0},{3,1},{4,6},{5,7},{6,4},{7,5},{8,10},{9,11},{10,... | collective-permute-start | bytes 1572872 | tf_op jit(solution)/shard_map/ppermute | solution.py:49
  37.1 10.3 %collective-permute-start.10 = (bf16[256,768]{1,0:T(8,128)(2,1)}, bf16[256,768]{1,0:T(8,128)(2,1)S(1)}, u32[]{:S(2)}, u32[]{:S(2)}) collective-permute-start(bf16[256,768]{1,0:T(8,128)(2,1)} %collective-permute-done.8), channel_id=1, source_target_pairs={{4,0},{5,1},{6,2},{7,3},{8,4},{9,5},{10,6},{11,7},{12,8},{13,9},{1... | collective-permute-start | bytes 1179656 | tf_op jit(solution)/shard_map/ppermute | solution.py:49
  43.3 5.5 %collective-permute-start.11 = (bf16[256,768]{1,0:T(8,128)(2,1)}, bf16[256,768]{1,0:T(8,128)(2,1)S(1)}, u32[]{:S(2)}, u32[]{:S(2)}) collective-permute-start(bf16[256,768]{1,0:T(8,128)(2,1)} %collective-permute-done.6), channel_id=1, source_target_pairs={{4,8},{5,9},{6,10},{7,11},{8,12},{9,13},{10,14},{11,15},{20,24},{2... | collective-permute-start | bytes 1179656 | tf_op jit(solution)/shard_map/ppermute | solution.py:49
  44.1 16.8 %collective-permute-start.12 = (bf16[256,768]{1,0:T(8,128)(2,1)}, bf16[256,768]{1,0:T(8,128)(2,1)S(1)}, u32[]{:S(2)}, u32[]{:S(2)}) collective-permute-start(bf16[256,768]{1,0:T(8,128)(2,1)} %collective-permute-done.7), channel_id=1, source_target_pairs={{4,0},{5,1},{6,2},{7,3},{8,4},{9,5},{10,6},{11,7},{20,16},{21,17},... | collective-permute-start | bytes 1179656 | tf_op jit(solution)/shard_map/ppermute | solution.py:49
  47.5 21.0 %collective-permute-start.3 = (bf16[2,64,2048]{2,1,0:T(8,128)(2,1)}, bf16[2,64,2048]{2,1,0:T(8,128)(2,1)S(1)}, u32[]{:S(2)}, u32[]{:S(2)}) collective-permute-start(bf16[2,64,2048]{2,1,0:T(8,128)(2,1)} %collective-permute-done.2), channel_id=1, source_target_pairs={{0,1},{1,0},{2,3},{3,2},{4,5},{5,4},{6,7},{7,6},{8,9},{9,8},{10,11... | collective-permute-start | bytes 1572872 | tf_op jit(solution)/shard_map/ppermute | solution.py:49
  47.5 18.7 %collective-permute-start.26 = (bf16[512,384]{1,0:T(8,128)(2,1)S(1)}, bf16[512,384]{1,0:T(8,128)(2,1)S(1)}, u32[]{:S(2)}, u32[]{:S(2)}) collective-permute-start(bf16[512,384]{1,0:T(8,128)(2,1)S(1)} %collective-permute-done.20), channel_id=1, source_target_pairs={{4,0},{5,1},{6,2},{7,3},{8,4},{9,5},{10,6},{11,7},{20,16},{21,17},... | collective-permute-start | bytes 1179656 | tf_op jit(solution)/shard_map/ppermute | solution.py:49
  48.8 18.1 %collective-permute-start.27 = (bf16[512,384]{1,0:T(8,128)(2,1)S(1)}, bf16[512,384]{1,0:T(8,128)(2,1)S(1)}, u32[]{:S(2)}, u32[]{:S(2)}) collective-permute-start(bf16[512,384]{1,0:T(8,128)(2,1)S(1)} %collective-permute-done.21), channel_id=1, source_target_pairs={{4,8},{5,9},{6,10},{7,11},{8,12},{9,13},{10,14},{11,15},{20,24},{2... | collective-permute-start | bytes 1179656 | tf_op jit(solution)/shard_map/ppermute | solution.py:49
  53.3 17.0 %collective-permute-start.5 = (bf16[2,64,2048]{2,1,0:T(8,128)(2,1)S(1)}, bf16[2,64,2048]{2,1,0:T(8,128)(2,1)S(1)}, u32[]{:S(2)}, u32[]{:S(2)}) collective-permute-start(bf16[2,64,2048]{2,1,0:T(8,128)(2,1)S(1)} %collective-permute-done.4), channel_id=1, source_target_pairs={{0,1},{1,0},{2,3},{3,2},{4,5},{5,4},{6,7},{7,6},{8,9},{9,8},{10,11... | collective-permute-start | bytes 1572872 | tf_op jit(solution)/shard_map/ppermute | solution.py:49
  60.9 10.8 %collective-permute-start.1 = (bf16[2,64,2048]{2,1,0:T(8,128)(2,1)S(1)}, bf16[2,64,2048]{2,1,0:T(8,128)(2,1)S(1)}, u32[]{:S(2)}, u32[]{:S(2)}) collective-permute-start(bf16[2,64,2048]{2,1,0:T(8,128)(2,1)S(1)} %collective-permute-done), channel_id=1, source_target_pairs={{0,1},{1,0},{2,3},{3,2},{4,5},{5,4},{6,7},{7,6},{8,9},{9,8},{10,11... | collective-permute-start | bytes 1572872 | tf_op jit(solution)/shard_map/ppermute | solution.py:49
  66.3 7.3 %collective-permute-start.13 = (bf16[256,768]{1,0:T(8,128)(2,1)S(1)}, bf16[256,768]{1,0:T(8,128)(2,1)S(1)}, u32[]{:S(2)}, u32[]{:S(2)}) collective-permute-start(bf16[256,768]{1,0:T(8,128)(2,1)S(1)} %collective-permute-done.9), channel_id=1, source_target_pairs={{4,8},{5,9},{6,10},{7,11},{8,12},{9,13},{10,14},{11,15},{20,24},{2... | collective-permute-start | bytes 1179656 | tf_op jit(solution)/shard_map/ppermute | solution.py:49
  67.0 14.4 %collective-permute-start.14 = (bf16[256,768]{1,0:T(8,128)(2,1)S(1)}, bf16[256,768]{1,0:T(8,128)(2,1)S(1)}, u32[]{:S(2)}, u32[]{:S(2)}) collective-permute-start(bf16[256,768]{1,0:T(8,128)(2,1)S(1)} %collective-permute-done.10), channel_id=1, source_target_pairs={{4,0},{5,1},{6,2},{7,3},{8,4},{9,5},{10,6},{11,7},{20,16},{21,17},... | collective-permute-start | bytes 1179656 | tf_op jit(solution)/shard_map/ppermute | solution.py:49
  68.5 13.6 %collective-permute-start.15 = (bf16[256,768]{1,0:T(8,128)(2,1)S(1)}, bf16[256,768]{1,0:T(8,128)(2,1)S(1)}, u32[]{:S(2)}, u32[]{:S(2)}) collective-permute-start(bf16[256,768]{1,0:T(8,128)(2,1)S(1)} %collective-permute-done.11), channel_id=1, source_target_pairs={{8,12},{9,13},{10,14},{11,15},{24,28},{25,29},{26,30},{27,31}} | collective-permute-start | bytes 1179656 | tf_op jit(solution)/shard_map/ppermute | solution.py:49
  70.3 19.4 %collective-permute-start.16 = (bf16[256,768]{1,0:T(8,128)(2,1)S(1)}, bf16[256,768]{1,0:T(8,128)(2,1)S(1)}, u32[]{:S(2)}, u32[]{:S(2)}) collective-permute-start(bf16[256,768]{1,0:T(8,128)(2,1)S(1)} %collective-permute-done.12), channel_id=1, source_target_pairs={{4,0},{5,1},{6,2},{7,3},{20,16},{21,17},{22,18},{23,19}} | collective-permute-start | bytes 1179656 | tf_op jit(solution)/shard_map/ppermute | solution.py:49
  71.7 26.5 %collective-permute-start.32 = (bf16[512,384]{1,0:T(8,128)(2,1)S(1)}, bf16[512,384]{1,0:T(8,128)(2,1)S(1)}, u32[]{:S(2)}, u32[]{:S(2)}) collective-permute-start(bf16[512,384]{1,0:T(8,128)(2,1)S(1)} %collective-permute-done.26), channel_id=1, source_target_pairs={{4,0},{5,1},{6,2},{7,3},{20,16},{21,17},{22,18},{23,19}} | collective-permute-start | bytes 1179656 | tf_op jit(solution)/shard_map/ppermute | solution.py:49
  73.5 24.7 %collective-permute-start.33 = (bf16[512,384]{1,0:T(8,128)(2,1)S(1)}, bf16[512,384]{1,0:T(8,128)(2,1)S(1)}, u32[]{:S(2)}, u32[]{:S(2)}) collective-permute-start(bf16[512,384]{1,0:T(8,128)(2,1)S(1)} %collective-permute-done.27), channel_id=1, source_target_pairs={{8,12},{9,13},{10,14},{11,15},{24,28},{25,29},{26,30},{27,31}} | collective-permute-start | bytes 1179656 | tf_op jit(solution)/shard_map/ppermute | solution.py:49
  81.3 17.1 %collective-permute-start.17 = (bf16[256,768]{1,0:T(8,128)(2,1)S(1)}, bf16[256,768]{1,0:T(8,128)(2,1)S(1)}, u32[]{:S(2)}, u32[]{:S(2)}) collective-permute-start(bf16[256,768]{1,0:T(8,128)(2,1)S(1)} %collective-permute-done.13), channel_id=1, source_target_pairs={{8,12},{9,13},{10,14},{11,15},{24,28},{25,29},{26,30},{27,31}} | collective-permute-start | bytes 1179656 | tf_op jit(solution)/shard_map/ppermute | solution.py:49
  82.1 20.7 %collective-permute-start.18 = (bf16[256,768]{1,0:T(8,128)(2,1)S(1)}, bf16[256,768]{1,0:T(8,128)(2,1)S(1)}, u32[]{:S(2)}, u32[]{:S(2)}) collective-permute-start(bf16[256,768]{1,0:T(8,128)(2,1)S(1)} %collective-permute-done.14), channel_id=1, source_target_pairs={{4,0},{5,1},{6,2},{7,3},{20,16},{21,17},{22,18},{23,19}} | collective-permute-start | bytes 1179656 | tf_op jit(solution)/shard_map/ppermute | solution.py:49
  109.0 13.8 %collective-permute-start.57 = (bf16[512,384]{1,0:T(8,128)(2,1)S(1)}, bf16[512,384]{1,0:T(8,128)(2,1)S(1)}, u32[]{:S(2)}, u32[]{:S(2)}) collective-permute-start(bf16[512,384]{1,0:T(8,128)(2,1)S(1)} %slice.332), channel_id=1, source_target_pairs={{0,4},{1,5},{2,6},{3,7},{4,8},{5,9},{6,10},{7,11},{8,12},{9,13},{1... | collective-permute-start | bytes 1179656 | tf_op jit(solution)/shard_map/ppermute | solution.py:49
  109.0 26.1 %collective-permute-start.58 = (bf16[512,384]{1,0:T(8,128)(2,1)S(1)}, bf16[512,384]{1,0:T(8,128)(2,1)S(1)}, u32[]{:S(2)}, u32[]{:S(2)}) collective-permute-start(bf16[512,384]{1,0:T(8,128)(2,1)S(1)} %slice.332), channel_id=1, source_target_pairs={{0,8},{1,9},{2,10},{3,11},{4,12},{5,13},{6,14},{7,15},{8,0},{9,1},... | collective-permute-start | bytes 1179656 | tf_op jit(solution)/shard_map/ppermute | solution.py:49
  109.0 26.9 %collective-permute-start.59 = (bf16[512,384]{1,0:T(8,128)(2,1)S(1)}, bf16[512,384]{1,0:T(8,128)(2,1)S(1)}, u32[]{:S(2)}, u32[]{:S(2)}) collective-permute-start(bf16[512,384]{1,0:T(8,128)(2,1)S(1)} %slice.332), channel_id=1, source_target_pairs={{0,12},{1,13},{2,14},{3,15},{4,0},{5,1},{6,2},{7,3},{8,4},{9,5},{1... | collective-permute-start | bytes 1179656 | tf_op jit(solution)/shard_map/ppermute | solution.py:49
  113.7 23.1 %collective-permute-start.34 = (bf16[2,4,64,512]{3,2,1,0:T(8,128)(2,1)S(1)}, bf16[2,4,64,512]{3,2,1,0:T(8,128)(2,1)S(1)}, u32[]{:S(2)}, u32[]{:S(2)}) collective-permute-start(bf16[2,4,64,512]{3,2,1,0:T(8,128)(2,1)S(1)} %fusion.46), channel_id=1, source_target_pairs={{0,1},{1,0},{2,3},{3,2},{4,5},{5,4},{6,7},{7,6},{8,9},{9,8},{10,11... | collective-permute-start | bytes 1572872 | tf_op jit(solution)/shard_map/ppermute | solution.py:49
  114.6 26.0 %collective-permute-start.28 = (bf16[2,4,64,512]{3,2,1,0:T(8,128)(2,1)S(1)}, bf16[2,4,64,512]{3,2,1,0:T(8,128)(2,1)S(1)}, u32[]{:S(2)}, u32[]{:S(2)}) collective-permute-start(bf16[2,4,64,512]{3,2,1,0:T(8,128)(2,1)S(1)} %fusion.45), channel_id=1, source_target_pairs={{0,1},{1,0},{2,3},{3,2},{4,5},{5,4},{6,7},{7,6},{8,9},{9,8},{10,11... | collective-permute-start | bytes 1572872 | tf_op jit(solution)/shard_map/ppermute | solution.py:49
  122.8 19.6 %collective-permute-start.22 = (bf16[2,4,64,1024]{3,2,1,0:T(8,128)(2,1)S(1)}, bf16[2,4,64,1024]{3,2,1,0:T(8,128)(2,1)S(1)}, u32[]{:S(2)}, u32[]{:S(2)}) collective-permute-start(bf16[2,4,64,1024]{3,2,1,0:T(8,128)(2,1)S(1)} %fusion.3), channel_id=1, source_target_pairs={{0,1},{1,0},{2,3},{3,2},{4,5},{5,4},{6,7},{7,6},{8,9},{9,8},{10,11... | collective-permute-start | bytes 3145736 | tf_op jit(solution)/shard_map/ppermute | solution.py:49
  137.0 7.6 %collective-permute-start.35 = (bf16[2,64,512]{2,1,0:T(8,128)(2,1)S(1)}, bf16[2,64,512]{2,1,0:T(8,128)(2,1)S(1)}, u32[]{:S(2)}, u32[]{:S(2)}) collective-permute-start(bf16[2,64,512]{2,1,0:T(8,128)(2,1)S(1)} %get-tuple-element.41), channel_id=1, source_target_pairs={{0,2},{1,3},{2,0},{3,1},{4,6},{5,7},{6,4},{7,5},{8,10},{9,11},{10,... | collective-permute-start | bytes 393224 | tf_op jit(solution)/shard_map/ppermute | solution.py:49
  138.6 7.7 %collective-permute-start.36 = (bf16[2,64,512]{2,1,0:T(8,128)(2,1)S(1)}, bf16[2,64,512]{2,1,0:T(8,128)(2,1)S(1)}, u32[]{:S(2)}, u32[]{:S(2)}) collective-permute-start(bf16[2,64,512]{2,1,0:T(8,128)(2,1)S(1)} %get-tuple-element.43), channel_id=1, source_target_pairs={{0,16},{1,17},{2,18},{3,19},{4,20},{5,21},{6,22},{7,23},{8,24},{9,... | collective-permute-start | bytes 393224 | tf_op jit(solution)/shard_map/ppermute | solution.py:49
  139.4 8.4 %collective-permute-start.37 = (bf16[2,64,512]{2,1,0:T(8,128)(2,1)S(1)}, bf16[2,64,512]{2,1,0:T(8,128)(2,1)S(1)}, u32[]{:S(2)}, u32[]{:S(2)}) collective-permute-start(bf16[2,64,512]{2,1,0:T(8,128)(2,1)S(1)} %get-tuple-element.42), channel_id=1, source_target_pairs={{0,18},{1,19},{2,16},{3,17},{4,22},{5,23},{6,20},{7,21},{8,26},{9,... | collective-permute-start | bytes 393224 | tf_op jit(solution)/shard_map/ppermute | solution.py:49
  140.9 9.4 %collective-permute-start.29 = (bf16[2,64,512]{2,1,0:T(8,128)(2,1)S(1)}, bf16[2,64,512]{2,1,0:T(8,128)(2,1)S(1)}, u32[]{:S(2)}, u32[]{:S(2)}) collective-permute-start(bf16[2,64,512]{2,1,0:T(8,128)(2,1)S(1)} %get-tuple-element.44), channel_id=1, source_target_pairs={{0,2},{1,3},{2,0},{3,1},{4,6},{5,7},{6,4},{7,5},{8,10},{9,11},{10,... | collective-permute-start | bytes 393224 | tf_op jit(solution)/shard_map/ppermute | solution.py:49
  142.4 9.9 %collective-permute-start.30 = (bf16[2,64,512]{2,1,0:T(8,128)(2,1)S(1)}, bf16[2,64,512]{2,1,0:T(8,128)(2,1)S(1)}, u32[]{:S(2)}, u32[]{:S(2)}) collective-permute-start(bf16[2,64,512]{2,1,0:T(8,128)(2,1)S(1)} %get-tuple-element.46), channel_id=1, source_target_pairs={{0,16},{1,17},{2,18},{3,19},{4,20},{5,21},{6,22},{7,23},{8,24},{9,... | collective-permute-start | bytes 393224 | tf_op jit(solution)/shard_map/ppermute | solution.py:49
  144.7 8.8 %collective-permute-start.31 = (bf16[2,64,512]{2,1,0:T(8,128)(2,1)S(1)}, bf16[2,64,512]{2,1,0:T(8,128)(2,1)S(1)}, u32[]{:S(2)}, u32[]{:S(2)}) collective-permute-start(bf16[2,64,512]{2,1,0:T(8,128)(2,1)S(1)} %get-tuple-element.45), channel_id=1, source_target_pairs={{0,18},{1,19},{2,16},{3,17},{4,22},{5,23},{6,20},{7,21},{8,26},{9,... | collective-permute-start | bytes 393224 | tf_op jit(solution)/shard_map/ppermute | solution.py:49
  146.4 12.4 %collective-permute-start.23 = (bf16[2,64,1024]{2,1,0:T(8,128)(2,1)S(1)}, bf16[2,64,1024]{2,1,0:T(8,128)(2,1)S(1)}, u32[]{:S(2)}, u32[]{:S(2)}) collective-permute-start(bf16[2,64,1024]{2,1,0:T(8,128)(2,1)S(1)} %get-tuple-element.30), channel_id=1, source_target_pairs={{0,2},{1,3},{2,0},{3,1},{4,6},{5,7},{6,4},{7,5},{8,10},{9,11},{10,... | collective-permute-start | bytes 786440 | tf_op jit(solution)/shard_map/ppermute | solution.py:49
  147.8 11.1 %collective-permute-start.24 = (bf16[2,64,1024]{2,1,0:T(8,128)(2,1)S(1)}, bf16[2,64,1024]{2,1,0:T(8,128)(2,1)S(1)}, u32[]{:S(2)}, u32[]{:S(2)}) collective-permute-start(bf16[2,64,1024]{2,1,0:T(8,128)(2,1)S(1)} %get-tuple-element.32), channel_id=1, source_target_pairs={{0,16},{1,17},{2,18},{3,19},{4,20},{5,21},{6,22},{7,23},{8,24},{9,... | collective-permute-start | bytes 786440 | tf_op jit(solution)/shard_map/ppermute | solution.py:49
  150.3 11.4 %collective-permute-start.25 = (bf16[2,64,1024]{2,1,0:T(8,128)(2,1)S(1)}, bf16[2,64,1024]{2,1,0:T(8,128)(2,1)S(1)}, u32[]{:S(2)}, u32[]{:S(2)}) collective-permute-start(bf16[2,64,1024]{2,1,0:T(8,128)(2,1)S(1)} %get-tuple-element.31), channel_id=1, source_target_pairs={{0,18},{1,19},{2,16},{3,17},{4,22},{5,23},{6,20},{7,21},{8,26},{9,... | collective-permute-start | bytes 786440 | tf_op jit(solution)/shard_map/ppermute | solution.py:49
  175.2 12.6 %collective-permute-start.51 = (bf16[64,512]{1,0:T(8,128)(2,1)S(1)}, bf16[64,512]{1,0:T(8,128)(2,1)S(1)}, u32[]{:S(2)}, u32[]{:S(2)}) collective-permute-start(bf16[64,512]{1,0:T(8,128)(2,1)S(1)} %bitcast.463), channel_id=1, source_target_pairs={{0,4},{1,5},{2,6},{3,7},{4,8},{5,9},{6,10},{7,11},{8,12},{9,13},{1... | collective-permute-start | bytes 196616 | tf_op jit(solution)/shard_map/ppermute | solution.py:49
  183.4 5.9 %collective-permute-start.52 = (bf16[64,512]{1,0:T(8,128)(2,1)S(1)}, bf16[64,512]{1,0:T(8,128)(2,1)S(1)}, u32[]{:S(2)}, u32[]{:S(2)}) collective-permute-start(bf16[64,512]{1,0:T(8,128)(2,1)S(1)} %bitcast.462), channel_id=1, source_target_pairs={{0,8},{1,9},{2,10},{3,11},{4,12},{5,13},{6,14},{7,15},{8,0},{9,1},... | collective-permute-start | bytes 196616 | tf_op jit(solution)/shard_map/ppermute | solution.py:49
  183.5 6.6 %collective-permute-start.53 = (bf16[64,512]{1,0:T(8,128)(2,1)S(1)}, bf16[64,512]{1,0:T(8,128)(2,1)S(1)}, u32[]{:S(2)}, u32[]{:S(2)}) collective-permute-start(bf16[64,512]{1,0:T(8,128)(2,1)S(1)} %bitcast.461), channel_id=1, source_target_pairs={{0,12},{1,13},{2,14},{3,15},{4,0},{5,1},{6,2},{7,3},{8,4},{9,5},{1... | collective-permute-start | bytes 196616 | tf_op jit(solution)/shard_map/ppermute | solution.py:49
  187.8 21.3 %collective-permute-start.40 = (bf16[64,2048]{1,0:T(8,128)(2,1)S(1)}, bf16[64,2048]{1,0:T(8,128)(2,1)S(1)}, u32[]{:S(2)}, u32[]{:S(2)}) collective-permute-start(bf16[64,2048]{1,0:T(8,128)(2,1)S(1)} %fusion.38), channel_id=1, source_target_pairs={{0,2},{1,3},{2,0},{3,1},{4,6},{5,7},{6,4},{7,5},{8,10},{9,11},{10,... | collective-permute-start | bytes 786440 | tf_op jit(solution)/shard_map/ppermute | solution.py:49
  189.3 21.6 %collective-permute-start.42 = (bf16[64,2048]{1,0:T(8,128)(2,1)S(1)}, bf16[64,2048]{1,0:T(8,128)(2,1)S(1)}, u32[]{:S(2)}, u32[]{:S(2)}) collective-permute-start(bf16[64,2048]{1,0:T(8,128)(2,1)S(1)} %fusion.38), channel_id=1, source_target_pairs={{0,16},{1,17},{2,18},{3,19},{4,20},{5,21},{6,22},{7,23},{8,24},{9,... | collective-permute-start | bytes 786440 | tf_op jit(solution)/shard_map/ppermute | solution.py:49
  190.1 20.8 %collective-permute-start.44 = (bf16[64,2048]{1,0:T(8,128)(2,1)S(1)}, bf16[64,2048]{1,0:T(8,128)(2,1)S(1)}, u32[]{:S(2)}, u32[]{:S(2)}) collective-permute-start(bf16[64,2048]{1,0:T(8,128)(2,1)S(1)} %fusion.38), channel_id=1, source_target_pairs={{0,18},{1,19},{2,16},{3,17},{4,22},{5,23},{6,20},{7,21},{8,26},{9,... | collective-permute-start | bytes 786440 | tf_op jit(solution)/shard_map/ppermute | solution.py:49
  191.7 16.8 %collective-permute-start.61 = (bf16[4,64,512]{2,1,0:T(8,128)(2,1)S(1)}, bf16[4,64,512]{2,1,0:T(8,128)(2,1)S(1)}, u32[]{:S(2)}, u32[]{:S(2)}) collective-permute-start(bf16[4,64,512]{2,1,0:T(8,128)(2,1)S(1)} %pad_maximum_fusion.4), channel_id=1, source_target_pairs={{0,16},{1,17},{2,18},{3,19},{4,20},{5,21},{6,22},{7,23},{8,24},{9,... | collective-permute-start | bytes 786440 | tf_op jit(solution)/shard_map/ppermute | solution.py:49
  192.7 18.7 %collective-permute-start.54 = (bf16[4,64,512]{2,1,0:T(8,128)(2,1)S(1)}, bf16[4,64,512]{2,1,0:T(8,128)(2,1)S(1)}, u32[]{:S(2)}, u32[]{:S(2)}) collective-permute-start(bf16[4,64,512]{2,1,0:T(8,128)(2,1)S(1)} %pad_maximum_fusion.4), channel_id=1, source_target_pairs={{0,1},{1,0},{2,3},{3,2},{4,5},{5,4},{6,7},{7,6},{8,9},{9,8},{10,11... | collective-permute-start | bytes 786440 | tf_op jit(solution)/shard_map/ppermute | solution.py:49
  208.5 12.8 %collective-permute-start.55 = (bf16[4,64,512]{2,1,0:T(8,128)(2,1)S(1)}, bf16[4,64,512]{2,1,0:T(8,128)(2,1)S(1)}, u32[]{:S(2)}, u32[]{:S(2)}) collective-permute-start(bf16[4,64,512]{2,1,0:T(8,128)(2,1)S(1)} %pad_maximum_fusion.4), channel_id=1, source_target_pairs={{0,2},{1,3},{2,0},{3,1},{4,6},{5,7},{6,4},{7,5},{8,10},{9,11},{10,... | collective-permute-start | bytes 786440 | tf_op jit(solution)/shard_map/ppermute | solution.py:49
  209.1 12.2 %collective-permute-start.63 = (bf16[4,64,512]{2,1,0:T(8,128)(2,1)S(1)}, bf16[4,64,512]{2,1,0:T(8,128)(2,1)S(1)}, u32[]{:S(2)}, u32[]{:S(2)}) collective-permute-start(bf16[4,64,512]{2,1,0:T(8,128)(2,1)S(1)} %pad_maximum_fusion.4), channel_id=1, source_target_pairs={{0,18},{1,19},{2,16},{3,17},{4,22},{5,23},{6,20},{7,21},{8,26},{9,... | collective-permute-start | bytes 786440 | tf_op jit(solution)/shard_map/ppermute | solution.py:49
  210.9 11.0 %collective-permute-start.41 = (bf16[64,2048]{1,0:T(8,128)(2,1)S(1)}, bf16[64,2048]{1,0:T(8,128)(2,1)S(1)}, u32[]{:S(2)}, u32[]{:S(2)}) collective-permute-start(bf16[64,2048]{1,0:T(8,128)(2,1)S(1)} %collective-permute-done.40), channel_id=1, source_target_pairs={{0,1},{1,0},{2,3},{3,2},{4,5},{5,4},{6,7},{7,6},{8,9},{9,8},{10,11... | collective-permute-start | bytes 786440 | tf_op jit(solution)/shard_map/ppermute | solution.py:49
  210.9 11.2 %collective-permute-start.43 = (bf16[64,2048]{1,0:T(8,128)(2,1)S(1)}, bf16[64,2048]{1,0:T(8,128)(2,1)S(1)}, u32[]{:S(2)}, u32[]{:S(2)}) collective-permute-start(bf16[64,2048]{1,0:T(8,128)(2,1)S(1)} %collective-permute-done.42), channel_id=1, source_target_pairs={{0,1},{1,0},{2,3},{3,2},{4,5},{5,4},{6,7},{7,6},{8,9},{9,8},{10,11... | collective-permute-start | bytes 786440 | tf_op jit(solution)/shard_map/ppermute | solution.py:49
  211.4 10.7 %collective-permute-start.45 = (bf16[64,2048]{1,0:T(8,128)(2,1)S(1)}, bf16[64,2048]{1,0:T(8,128)(2,1)S(1)}, u32[]{:S(2)}, u32[]{:S(2)}) collective-permute-start(bf16[64,2048]{1,0:T(8,128)(2,1)S(1)} %collective-permute-done.44), channel_id=1, source_target_pairs={{0,1},{1,0},{2,3},{3,2},{4,5},{5,4},{6,7},{7,6},{8,9},{9,8},{10,11... | collective-permute-start | bytes 786440 | tf_op jit(solution)/shard_map/ppermute | solution.py:49
  221.3 7.8 %collective-permute-start.62 = (bf16[4,64,512]{2,1,0:T(8,128)(2,1)S(1)}, bf16[4,64,512]{2,1,0:T(8,128)(2,1)S(1)}, u32[]{:S(2)}, u32[]{:S(2)}) collective-permute-start(bf16[4,64,512]{2,1,0:T(8,128)(2,1)S(1)} %collective-permute-done.61), channel_id=1, source_target_pairs={{0,1},{1,0},{2,3},{3,2},{4,5},{5,4},{6,7},{7,6},{8,9},{9,8},{10,11... | collective-permute-start | bytes 786440 | tf_op jit(solution)/shard_map/ppermute | solution.py:49
  221.3 10.7 %collective-permute-start.56 = (bf16[4,64,512]{2,1,0:T(8,128)(2,1)S(1)}, bf16[4,64,512]{2,1,0:T(8,128)(2,1)S(1)}, u32[]{:S(2)}, u32[]{:S(2)}) collective-permute-start(bf16[4,64,512]{2,1,0:T(8,128)(2,1)S(1)} %collective-permute-done.55), channel_id=1, source_target_pairs={{0,1},{1,0},{2,3},{3,2},{4,5},{5,4},{6,7},{7,6},{8,9},{9,8},{10,11... | collective-permute-start | bytes 786440 | tf_op jit(solution)/shard_map/ppermute | solution.py:49
  221.9 7.2 %collective-permute-start.64 = (bf16[4,64,512]{2,1,0:T(8,128)(2,1)S(1)}, bf16[4,64,512]{2,1,0:T(8,128)(2,1)S(1)}, u32[]{:S(2)}, u32[]{:S(2)}) collective-permute-start(bf16[4,64,512]{2,1,0:T(8,128)(2,1)S(1)} %collective-permute-done.63), channel_id=1, source_target_pairs={{0,1},{1,0},{2,3},{3,2},{4,5},{5,4},{6,7},{7,6},{8,9},{9,8},{10,11... | collective-permute-start | bytes 786440 | tf_op jit(solution)/shard_map/ppermute | solution.py:49
  231.2 18.8 %collective-permute-start.65 = (bf16[256,384]{1,0:T(8,128)(2,1)}, bf16[256,384]{1,0:T(8,128)(2,1)}, u32[]{:S(2)}, u32[]{:S(2)}) collective-permute-start(bf16[256,384]{1,0:T(8,128)(2,1)} %get-tuple-element.50), channel_id=1, source_target_pairs={{0,16},{1,17},{2,18},{3,19},{4,20},{5,21},{6,22},{7,23},{8,24},{9,... | collective-permute-start | bytes 589832 | tf_op jit(solution)/shard_map/ppermute | solution.py:49
  235.6 17.2 %collective-permute-start.47 = (bf16[1,64,2048]{2,1,0:T(8,128)(2,1)}, bf16[1,64,2048]{2,1,0:T(8,128)(2,1)S(1)}, u32[]{:S(2)}, u32[]{:S(2)}) collective-permute-start(bf16[1,64,2048]{2,1,0:T(8,128)(2,1)} %get-tuple-element.25), channel_id=1, source_target_pairs={{0,2},{1,3},{2,0},{3,1},{4,6},{5,7},{6,4},{7,5},{8,10},{9,11},{10,... | collective-permute-start | bytes 786440 | tf_op jit(solution)/shard_map/ppermute | solution.py:49
  236.5 16.2 %collective-permute-start.48 = (bf16[1,64,2048]{2,1,0:T(8,128)(2,1)}, bf16[1,64,2048]{2,1,0:T(8,128)(2,1)}, u32[]{:S(2)}, u32[]{:S(2)}) collective-permute-start(bf16[1,64,2048]{2,1,0:T(8,128)(2,1)} %get-tuple-element.27), channel_id=1, source_target_pairs={{0,16},{1,17},{2,18},{3,19},{4,20},{5,21},{6,22},{7,23},{8,24},{9,... | collective-permute-start | bytes 786440 | tf_op jit(solution)/shard_map/ppermute | solution.py:49
  237.1 15.7 %collective-permute-start.49 = (bf16[1,64,2048]{2,1,0:T(8,128)(2,1)}, bf16[1,64,2048]{2,1,0:T(8,128)(2,1)}, u32[]{:S(2)}, u32[]{:S(2)}) collective-permute-start(bf16[1,64,2048]{2,1,0:T(8,128)(2,1)} %get-tuple-element.26), channel_id=1, source_target_pairs={{0,18},{1,19},{2,16},{3,17},{4,22},{5,23},{6,20},{7,21},{8,26},{9,... | collective-permute-start | bytes 786440 | tf_op jit(solution)/shard_map/ppermute | solution.py:49
  239.8 18.5 %collective-permute-start.60 = (bf16[256,384]{1,0:T(8,128)(2,1)}, bf16[256,384]{1,0:T(8,128)(2,1)}, u32[]{:S(2)}, u32[]{:S(2)}) collective-permute-start(bf16[256,384]{1,0:T(8,128)(2,1)} %fusion.63), channel_id=1, source_target_pairs={{0,2},{1,3},{2,0},{3,1},{4,6},{5,7},{6,4},{7,5},{8,10},{9,11},{10,... | collective-permute-start | bytes 589832 | tf_op jit(solution)/shard_map/ppermute | solution.py:49
  250.0 10.0 %collective-permute-start.66 = (bf16[256,384]{1,0:T(8,128)(2,1)}, bf16[256,384]{1,0:T(8,128)(2,1)S(1)}, u32[]{:S(2)}, u32[]{:S(2)}) collective-permute-start(bf16[256,384]{1,0:T(8,128)(2,1)} %get-tuple-element.49), channel_id=1, source_target_pairs={{0,18},{1,19},{2,16},{3,17},{4,22},{5,23},{6,20},{7,21},{8,26},{9,... | collective-permute-start | bytes 589832 | tf_op jit(solution)/shard_map/ppermute | solution.py:49
  256.6 32.6 %collective-permute-start.50 = (bf16[64,2048]{1,0:T(8,128)(2,1)}, bf16[64,2048]{1,0:T(8,128)(2,1)S(1)}, u32[]{:S(2)}, u32[]{:S(2)}) collective-permute-start(bf16[64,2048]{1,0:T(8,128)(2,1)} %get-tuple-element.6), channel_id=1, source_target_pairs={{0,1},{1,0},{2,3},{3,2},{4,5},{5,4},{6,7},{7,6},{8,9},{9,8},{10,11... | collective-permute-start | bytes 786440 | tf_op jit(solution)/shard_map/ppermute | solution.py:49
  (25 other events, 146.0 us)

commit v2 on v1

v2 whole, which is shorter than its diff:
```python
import jax
import jax.numpy as jnp
from jax import lax
from jax.experimental import pallas as pl
from jax.experimental.pallas import tpu as pltpu
from jax.sharding import PartitionSpec as P


eps = 1e-06
AXES = ("rep", "fs", "tp")
f32 = jnp.float32
bf16 = jnp.bfloat16


def nt(left, right):
    return lax.dot_general(left, right, (((1,), (1,)), ((), ())), preferred_element_type=f32)


def tn(left, right):
    return lax.dot_general(left, right, (((0,), (0,)), ((), ())), preferred_element_type=f32)


def pick(array, index):
    return lax.dynamic_index_in_dim(array, index, 0, keepdims=False)


def put(array, value, index):
    return lax.dynamic_update_index_in_dim(array, value, index, 0)


def arrange(values, ids, count, axis=-1):
    out = []
    for i in range(count):
        value = values[0]
        for k in range(1, len(values)):
            value = jnp.where(ids[k] == i, values[k], value)
        out.append(value)
    return jnp.concatenate(out, axis=axis)


def after(value, *others):
    return lax.optimization_barrier((value,) + others)[0]


def whole(n, scalar=0):
    vmem = [pl.BlockSpec(memory_space=pltpu.VMEM)] * n
    return [pl.BlockSpec(memory_space=pltpu.SMEM)] * scalar + vmem


def here(z, owners):
    hit = z == owners[0]
    for i in owners[1:]:
        hit = hit | (z == i)
    return hit


def by_slot(zref, slots, refs, count, emit):
    at = 0
    for k, slot in enumerate(slots):
        for owners in slot:
            ref = refs[at]
            at += 1
            if len(owners) == count:
                emit(k, ref)
            else:
                pl.when(here(zref[0], owners))(lambda k=k, ref=ref: emit(k, ref))


def sent_product(z, left, slots, count):
    rows, (columns, w) = left.shape[0], slots[0][0][0].shape
    owners = [[o for _, o in slot] for slot in slots]
    values = [v for slot in slots for v, _ in slot]

    def kernel(zref, left_ref, *refs):
        out = refs[-1]

        def emit(k, ref):
            out[:, k * columns:(k + 1) * columns] = nt(left_ref[...], ref[...]).astype(bf16)

        by_slot(zref, owners, refs, count, emit)

    return pl.pallas_call(
        kernel,
        out_shape=jax.ShapeDtypeStruct((rows, len(slots) * columns), bf16),
        in_specs=whole(1 + len(values), 1),
        out_specs=whole(1)[0],
        cost_estimate=pl.CostEstimate(flops=2 * rows * w * columns * len(slots), bytes_accessed=4 * rows * columns, transcendentals=0),
    )(z, left, *values)


def chip_product(z, left, got, slots, count, lead, parts):
    rows, (columns, w) = left.shape[0], slots[0][0][0].shape
    m = rows // (lead * parts)
    owners = [[o for _, o in slot] for slot in slots]
    values = [v for slot in slots for v, _ in slot]

    def kernel(zref, left_ref, *refs):
        received, refs, outs = refs[:len(got)], refs[len(got):-parts], refs[-parts:]

        def emit(k, ref):
            span = slice(k * columns, (k + 1) * columns)
            chip = nt(left_ref[...], ref[...])
            for other in received:
                chip = chip + other[:, span].astype(f32)
            chip = chip.astype(bf16)
            for a in range(lead):
                for p, out in enumerate(outs):
                    out[a * m:(a + 1) * m, span] = chip[(a * parts + p) * m:(a * parts + p + 1) * m]

        by_slot(zref, owners, refs, count, emit)

    return pl.pallas_call(
        kernel,
        out_shape=[jax.ShapeDtypeStruct((lead * m, len(slots) * columns), bf16)] * parts,
        in_specs=whole(1 + len(got) + len(values), 1),
        out_specs=whole(parts),
        cost_estimate=pl.CostEstimate(flops=2 * rows * w * columns * len(slots), bytes_accessed=8 * rows * columns, transcendentals=0),
    )(z, left, *got, *values)


def plan(R, S):
    G = 2 if S % 2 == 0 else 1
    Z = S // G
    peers = [(a, b) for a in range(R) for b in range(G)]
    ways = sorted(range(1, len(peers)), key=lambda p: (peers[p][0] == 0, peers[p][1] != 0))
    return G, Z, peers, ways


def edges(Z, s):
    out = []
    for kind in (0, 1):
        pairs = []
        for i in range(kind, Z - 1, 2):
            if i - (s - 1) >= 0:
                pairs.append((i, i + 1))
            if i + s < Z:
                pairs.append((i + 1, i))
        if pairs:
            out.append((kind, pairs))
    return out


def make_body(R, S, T):
    G, Z, peers, ways = plan(R, S)

    def send(value, dr=0, dy=0, dz=0, dt=0, moves=None):
        moves = [(z, (z + dz) % Z) for z in range(Z)] if moves is None else moves
        pairs = []
        for r in range(R):
            for z, to in moves:
                for y in range(G):
                    for t in range(T):
                        source = (r * S + z * G + y) * T + t
                        target = ((r + dr) % R * S + to * G + (y + dy) % G) * T + (t + dt) % T
                        pairs.append((source, target))
        return lax.ppermute(value, AXES, pairs)

    def line(piece):
        got = [(piece, piece)]
        for s in range(1, Z):
            step = [None, None]
            for kind, moves in edges(Z, s):
                step[kind] = send(got[s - 1][1 - kind], moves=moves)
            got.append(tuple(step))
        return got

    def source(z, kind, s):
        for a, b in dict(edges(Z, s)).get(kind, []):
            if b == z:
                return z - s if a < b else z + s
        return None

    def body(x_late, x_early, cotangent, pre_gain, post_gain, gate_weight, up_weight, down_weight, down_grad_sum):
        r, f, t = (lax.axis_index(a) for a in AXES)
        y, z = f % G, f // G
        n, D = x_late.shape
        m = n // T
        K, F = gate_weight.shape
        w = F // (R * G)
        PT = len(peers)

        def columns(weight, dy):
            q = r * G + (y + dy) % G
            return lax.dynamic_slice_in_dim(weight, q * w, w, 1)

        def both(dy):
            return jnp.concatenate([columns(gate_weight, dy), columns(up_weight, dy)], axis=1)

        gu = [both(0)] + [send(both(d), dy=d) for d in range(1, G)]
        dn = [columns(down_weight, 0)] + [send(columns(down_weight, d), dy=d) for d in range(1, G)]

        x = after(jnp.stack([x_late, x_early]), gu[0]).astype(f32)
        scale = lax.rsqrt(jnp.mean(x * x, axis=-1, keepdims=True) + eps)
        normed = (x * scale * pre_gain).astype(bf16).reshape(2, T, m, D)

        def chunk(array, j):
            return lax.dynamic_index_in_dim(array, (t + j) % T, 1, keepdims=False)

        def plane(value):
            out = []
            for p, (dr, dy) in enumerate(peers):
                got = send(value, dr=-dr, dy=-dy) if p else value
                out.append(got)
            return out

        def cores(got):
            return [got] + [send(got, dt=-j) for j in range(1, T)]

        held = [[chunk(normed, j) for j in range(T)]]
        held += [cores(got) for p, got in enumerate(plane(chunk(normed, 0))) if p]
        tokens = jnp.stack([jnp.stack([h[j] for h in held], axis=1) for j in range(T)], axis=1)
        tokens = tokens.reshape(2 * PT * n, D)

        full = jnp.zeros((Z, G, K, 2 * w), bf16)

        def place(array, value, zi, yi):
            return lax.dynamic_update_slice(array, value[None, None], (zi, yi, 0, 0))

        lines = [line(piece) for piece in gu]

        def target(kind, s):
            where = z
            for i in range(Z):
                j = source(i, kind, s)
                if j is not None:
                    where = jnp.where(z == i, j, where)
            return where

        for s in range(1, Z):
            for d, got in enumerate(lines):
                for kind, _ in edges(Z, s):
                    full = place(full, got[s][kind], target(kind, s), (y - d) % G)
        for d, piece in enumerate(gu):
            full = place(full, piece, z, (y - d) % G)
        full = full.reshape(D, 2 * w)

        both_out = jnp.dot(tokens, full, preferred_element_type=f32)
        gate, up = both_out[:, :w], both_out[:, w:]
        hidden = (jax.nn.silu(gate) * up).astype(bf16)

        block = jnp.zeros((G, K, w), bf16)
        for d, piece in enumerate(dn):
            block = put(block, piece, (y - d) % G)
        block = block.reshape(G * K, w)
        if Z > 1:
            block = after(block, *[v for v in lines[-1][Z - 2] if v is not None])
        got = arrived = line(block)
        tables = [[(s, k) for s in range(1, Z) for k in (0, 1) if source(i, k, s) is not None] for i in range(Z)]
        slots, ids = [[(block, list(range(Z)))]], [z]
        for k in range(Z - 1):
            slot, where = [], z
            for s, kind in sorted({tables[i][k] for i in range(Z)}):
                owners = [i for i in range(Z) if tables[i][k] == (s, kind)]
                slot.append((got[s][kind], owners))
                for i in owners:
                    where = jnp.where(z == i, source(i, kind, s), where)
            slots.append(slot)
            ids.append(where)
        z_ref = z.reshape(1)

        def plane_sum(low):
            total = low[0].astype(f32)
            for p, (dr, dy) in enumerate(peers):
                if p:
                    total = total + send(low[p], dr=dr, dy=dy).astype(f32)
            return total

        def reduce_plane(left, weight):
            got = []
            for j in range(1, T):
                value = nt(left[j], weight).astype(bf16)
                got.append(send(value, dt=j))
            chip = nt(left[0], weight)
            for value in got:
                chip = chip + value.astype(f32)
            low = chip.astype(bf16)
            low = low.reshape(PT, m, -1)
            return plane_sum([low[p] for p in range(PT)]), low

        by_core = hidden.reshape(2, T, PT * m, w)
        by_core = [by_core[:, j].reshape(2 * PT * m, w) for j in range(T)]
        groups = [[0, 1]] + [[k] for k in range(2, Z)] if Z > 1 else [[0]]
        totals, total_ids = [], []
        for group in groups:
            some = [slots[k] for k in group]
            got = []
            for j in range(1, T):
                value = sent_product(z_ref, by_core[j], some, Z)
                got.append(send(value, dt=j))
            low = chip_product(z_ref, by_core[0], got, some, Z, 2, PT)
            total = plane_sum(low)
            for i, k in enumerate(group):
                totals.append(total[:, i * G * K:(i + 1) * G * K])
                total_ids.append(ids[k])
        branch = arrange(totals, total_ids, Z)
        branch_l, branch_e = branch[:m], branch[m:]

        def own_rows(array):
            return lax.dynamic_slice_in_dim(array, t * m, m, 0)

        def all_rows(value):
            rows = [value] + [send(value, dt=-j) for j in range(1, T)]
            return arrange(rows, [(t + j) % T for j in range(T)], T, axis=0)

        early_rz = lax.rsqrt(jnp.mean(branch_e * branch_e, axis=-1, keepdims=True) + eps)
        cot_f = own_rows(cotangent).astype(f32)
        dpost = 0.5 * cot_f * post_gain
        dbranch = early_rz * (dpost - branch_e * early_rz * early_rz * jnp.mean(branch_e * dpost, axis=-1, keepdims=True))
        dbranch = dbranch.astype(bf16)

        late_rz = lax.rsqrt(jnp.mean(branch_l * branch_l, axis=-1, keepdims=True) + eps)
        y_late = (own_rows(x_late).astype(f32) + 0.5 * branch_l * late_rz * post_gain).astype(bf16)
        y_late = all_rows(y_late)

        down_full = jnp.zeros((Z, G * K, w), bf16)
        pieces, _ = lax.optimization_barrier(([[v for v, _ in slot] for slot in slots], dbranch))
        for slot, values, where in zip(slots, pieces, ids):
            value = values[0]
            for other, (_, owners) in zip(values[1:], slot[1:]):
                value = jnp.where(here(z, owners), other, value)
            down_full = put(down_full, value, where)
        down_full = down_full.reshape(D, w)
        raw = plane(dbranch)
        spread = [cores(h) for h in raw]
        spread = jnp.stack([jnp.stack([h[j] for h in spread]) for j in range(T)]).reshape(PT * n, D)
        dhidden = jnp.dot(spread, down_full, preferred_element_type=f32)
        gate_e, up_e = gate[PT * n:], up[PT * n:]
        sig = jax.nn.sigmoid(gate_e)
        dgate = (dhidden * up_e * sig * (1.0 + gate_e * (1.0 - sig))).astype(bf16)
        dup = (dhidden * gate_e * sig).astype(bf16)
        dgu = jnp.concatenate([dgate, dup], axis=1).reshape(T, PT * m, 2 * w)
        dnormed, dlow = reduce_plane([dgu[j] for j in range(T)], full)
        early_f = own_rows(x_early).astype(f32)
        early_rs = lax.dynamic_slice_in_dim(scale[1], t * m, m, 0)
        gained = pre_gain * dnormed
        dx = cot_f + early_rs * (gained - early_f * early_rs * early_rs * jnp.mean(early_f * gained, axis=-1, keepdims=True))
        dx = dx.astype(bf16)
        dx_early = all_rows(dx)

        hidden_e = hidden[PT * n:]
        if Z > 2:
            hidden_e = after(hidden_e, *[v for v in arrived[Z - 2] if v is not None])
        kept = [hidden_e] + [send(hidden_e, dz=k) for k in range(1, Z)]
        parts = after(dbranch, raw[ways[0]] if ways else dbranch).reshape(m, Z, G * K).transpose(1, 0, 2)
        cols = [pick(parts, z)] + [send(pick(parts, (z + k) % Z), dz=k) for k in range(1, Z)]
        wide = plane(after(jnp.stack(cols), *raw[1:]))
        wide = [cores(h) for h in wide]
        wide = [[wide[p][j] for p in range(PT)] for j in range(T)]
        wide, kept, _ = lax.optimization_barrier((wide, kept, dlow))
        wide = jnp.stack([jnp.stack(row) for row in wide])
        kept = jnp.stack([h.reshape(T, PT, m, w) for h in kept], axis=2)
        pieces, sources = [], []
        for a in range(R):
            grad = 0.0
            for j in range(T):
                left = wide[j, a * G:(a + 1) * G].reshape(G * Z * m, G * K)
                right = kept[j, a * G:(a + 1) * G].reshape(G * Z * m, w)
                grad = grad + tn(left, right)
            grad = grad.reshape(G, K, w)
            for b in range(G):
                piece = pick(grad, (y + b) % G)
                if a or b:
                    piece = send(piece.astype(bf16), dr=a, dy=b).astype(f32)
                pieces.append(piece)
                sources.append((r - a) % R * G + (y - b) % G)
        summed = arrange(pieces, sources, R * G)
        return (y_late, dx_early, down_grad_sum + summed)

    return body


def solution(mesh):
    R, S, T = (mesh.shape[a] for a in AXES)
    in_specs = (
        P(("rep", "fs"), None),
        P(("rep", "fs"), None),
        P(("rep", "fs"), None),
        P(),
        P(),
        P("fs", "tp"),
        P("fs", "tp"),
        P("fs", "tp"),
        P(("rep", "fs"), "tp"),
    )
    out_specs = (P(("rep", "fs"), None), P(("rep", "fs"), None), P(("rep", "fs"), "tp"))
    step = jax.shard_map(make_body(R, S, T), mesh=mesh, in_specs=in_specs, out_specs=out_specs, check_vma=False)
    if S // plan(R, S)[0] > 4:
        return step
    return step
```

time: 291 us -> 250 us (0.86)
  the two profiles are of different devices: /device:TPU:0 before, /device:TPU:25 now
where the time goes in v2:
time: 250 us; the launch traced here: 249 us
  waiting for transfers between devices  115 us (46%)
  starting transfers between devices  67.6 us (27%)
  local copies, waits for them, and re-layouts  19.8 us (8%)
  other arithmetic  18.4 us (7%)
  Pallas kernels  16.5 us (7%)
  matrix products  10.2 us (4%)
    ppermute x64, waiting for transfers between devices, send(): return lax.ppermute(value, AXES, pairs)  115 us
    ppermute x64, starting transfers between devices, send(): return lax.ppermute(value, AXES, pairs)  67.6 us
    pallas_call x3, Pallas kernels, chip_product(): pl.pallas_call(kernel, out_shape=[jax.ShapeDtypeStruct((lead * m, len(slo...  8.53 us
    pallas_call x3, Pallas kernels, sent_product(): pl.pallas_call(kernel, out_shape=jax.ShapeDtypeStruct((rows, len(slots) *...  7.93 us
  transfers between devices with their start and end apart: 64, of which 19 were waited for; matrix products, arithmetic and copies ran while one was open for 15% of the time, Pallas kernels for 7%

profile of v2, /device:TPU:25, one launch (start us, length us, event | category | flops | bytes accessed | tf_op | source)
XLA Modules:
  0.0 249.2 jit_solution(1373920216710292921)
XLA Ops:
  0.7 1.4 constant_dynamic-slice_fusion.6
  3.1 1.4 collective-permute-start.7
  5.3 1.2 collective-permute-start.8
  6.6 1.6 constant_dynamic-slice_fusion.5
  10.3 1.2 collective-permute-start
  12.5 6.9 %collective-permute-done.17 = bf16[256,384]{1,0:T(8,128)(2,1)S(1)} collective-permute-done((bf16[256,384]{1,0:T(8,128)(2,1)}, bf16[256,384]{1,0:T(8,128)(2,1)S(1)}, u32[]{:S(2)}, u32[]{:S(2)}) %collective-permute-start.17) | collective-permute-done | bytes 196640 | tf_op jit(solution)/shard_map/ppermute | solution.py:156
  19.5 1.2 collective-permute-start.1
  20.7 1.2 collective-permute-start.2
  22.0 1.9 collective-permute-start.9
  26.6 4.2 %collective-permute-done = bf16[2,64,2048]{2,1,0:T(8,128)(2,1)} collective-permute-done((bf16[2,64,2048]{2,1,0:T(8,128)(2,1)}, bf16[2,64,2048]{2,1,0:T(8,128)(2,1)}, u32[]{:S(2)}, u32[]{:S(2)}) %collective-permute-start) | collective-permute-done | bytes 524320 | tf_op jit(solution)/shard_map/ppermute | solution.py:156
  30.8 1.3 collective-permute-start.11
  32.8 9.3 %collective-permute-done.2 = bf16[2,64,2048]{2,1,0:T(8,128)(2,1)S(1)} collective-permute-done((bf16[2,64,2048]{2,1,0:T(8,128)(2,1)}, bf16[2,64,2048]{2,1,0:T(8,128)(2,1)S(1)}, u32[]{:S(2)}, u32[]{:S(2)}) %collective-permute-start.2) | collective-permute-done | bytes 524320 | tf_op jit(solution)/shard_map/ppermute | solution.py:156
  42.1 4.1 %collective-permute-start.3 = (bf16[2,64,2048]{2,1,0:T(8,128)(2,1)}, bf16[2,64,2048]{2,1,0:T(8,128)(2,1)S(1)}, u32[]{:S(2)}, u32[]{:S(2)}) collective-permute-start(bf16[2,64,2048]{2,1,0:T(8,128)(2,1)} %collective-permute-done), channel_id=1, source_target_pairs={{0,1},{1,0},{2,3},{3,2},{4,5},{5,4},{6,7},{7,6},{8,9},{9,8},{10,11... | collective-permute-start | bytes 1572872 | tf_op jit(solution)/shard_map/ppermute | solution.py:156
  46.2 1.5 maximum_bitcast_fusion
  48.4 1.3 collective-permute-start.13
  50.5 1.3 collective-permute-start.15
  53.1 7.8 %collective-permute-done.13 = bf16[256,768]{1,0:T(8,128)(2,1)S(1)} collective-permute-done((bf16[256,768]{1,0:T(8,128)(2,1)S(1)}, bf16[256,768]{1,0:T(8,128)(2,1)S(1)}, u32[]{:S(2)}, u32[]{:S(2)}) %collective-permute-start.13) | collective-permute-done | bytes 393248 | tf_op jit(solution)/shard_map/ppermute | solution.py:156
  61.0 3.2 %collective-permute-start.18 = (bf16[512,384]{1,0:T(8,128)(2,1)S(1)}, bf16[512,384]{1,0:T(8,128)(2,1)S(1)}, u32[]{:S(2)}, u32[]{:S(2)}) collective-permute-start(bf16[512,384]{1,0:T(8,128)(2,1)S(1)} %bitcast.192), channel_id=1, source_target_pairs={{0,4},{1,5},{2,6},{3,7},{4,0},{5,1},{6,2},{7,3},{8,12},{9,13},{10,... | collective-permute-start | bytes 1179656 | tf_op jit(solution)/shard_map/ppermute | solution.py:156
  64.2 1.5 collective-permute-start.25
  65.6 1.3 collective-permute-start.16
  67.0 2.4 collective-permute-done.15
  69.4 16.8 %collective-permute-done.16 = bf16[256,768]{1,0:T(8,128)(2,1)S(1)} collective-permute-done((bf16[256,768]{1,0:T(8,128)(2,1)S(1)}, bf16[256,768]{1,0:T(8,128)(2,1)S(1)}, u32[]{:S(2)}, u32[]{:S(2)}) %collective-permute-start.16) | collective-permute-done | bytes 393248 | tf_op jit(solution)/shard_map/ppermute | solution.py:156
  87.4 3.4 %fusion.32 = f32[1024,768]{1,0:T(8,128)S(1)} fusion(bf16[1024,2048]{1,0:T(8,128)(2,1)S(1)} %bitcast.204, bf16[2048,768]{1,0:T(8,128)(2,1)S(1)} %bitcast.189), kind=kOutput, calls=%fused_computation.145 | convolution fusion | flops 3221225472 | bytes 10485760 | tf_op jit(solution)/shard_map/dot_general | solution.py:237
  91.3 1.3 fusion.31
  93.8 2.9 %shard_map.116 = bf16[512,1024]{1,0:T(8,128)(2,1)} custom-call(s32[1]{0:T(128)} %bitcast.zref, bf16[512,384]{1,0:T(8,128)(2,1)} %bitcast.200, bf16[512,384]{1,0:T(8,128)(2,1)} %bitcast.194, bf16[512,384]{1,0:T(8,128)(2,1)} %copy-done.3), custom_call_target="tpu_custom_call" | custom-call | flops 402653184 | bytes 1048576 | tf_op jit(solution)/shard_map/pallas_call | solution.py:82
  97.6 1.5 collective-permute-start.19
  99.0 1.3 collective-permute-start.26
  100.3 1.3 collective-permute-start.20
  101.6 10.2 %collective-permute-done.26.refs_1_.refs_2_ = bf16[512,384]{1,0:T(8,128)(2,1)S(1)} collective-permute-done((bf16[512,384]{1,0:T(8,128)(2,1)}, bf16[512,384]{1,0:T(8,128)(2,1)S(1)}, u32[]{:S(2)}, u32[]{:S(2)}) %collective-permute-start.26) | collective-permute-done | bytes 393248 | tf_op jit(solution)/shard_map/ppermute | solution.py:156
  112.5 2.5 shard_map.114
  115.9 4.0 %collective-permute-done.20.refs_1_.refs_2_ = bf16[512,384]{1,0:T(8,128)(2,1)} collective-permute-done((bf16[512,384]{1,0:T(8,128)(2,1)}, bf16[512,384]{1,0:T(8,128)(2,1)}, u32[]{:S(2)}, u32[]{:S(2)}) %collective-permute-start.20) | collective-permute-done | bytes 393248 | tf_op jit(solution)/shard_map/ppermute | solution.py:156
  119.9 2.5 %shard_map.112 = bf16[512,512]{1,0:T(8,128)(2,1)} custom-call(s32[1]{0:T(128)} %bitcast.zref, bf16[512,384]{1,0:T(8,128)(2,1)} %bitcast.202, bf16[512,384]{1,0:T(8,128)(2,1)} %collective-permute-done.19.refs_0_.refs_1_, bf16[512,384]{1,0:T(8,128)(2,1)} %collective-permute-done.20.refs_1_.refs_2_), custom_call_target="tpu_custom_call" | custom-call | flops 201326592 | bytes 1048576 | tf_op jit(solution)/shard_map/pallas_call | solution.py:82
  122.4 1.4 collective-permute-start.21
  123.9 3.2 %shard_map.117 = (bf16[128,1024]{1,0:T(8,128)(2,1)}, bf16[128,1024]{1,0:T(8,128)(2,1)}, bf16[128,1024]{1,0:T(8,128)(2,1)}, bf16[128,1024]{1,0:T(8,128)(2,1)}) custom-call(s32[1]{0:T(128)} %bitcast.zref, bf16[512,384]{1,0:T(8,128)(2,1)} %bitcast.197, bf16[512,1024]{1,0:T(8,128)(2,1)} %collective-permute-done.31.refs_0_, bf16[512,384]{1,0:T(8,128)(2,1)} %bitcast.195, ...), custom_call_target="tpu_custom_call" | custom-call | flops 402653184 | bytes 2097152 | tf_op jit(solution)/shard_map/pallas_call | solution.py:112
  127.3 1.2 collective-permute-start.33
  128.5 1.2 collective-permute-start.34
  130.2 2.7 %shard_map.115 = (bf16[128,512]{1,0:T(8,128)(2,1)}, bf16[128,512]{1,0:T(8,128)(2,1)}, bf16[128,512]{1,0:T(8,128)(2,1)}, bf16[128,512]{1,0:T(8,128)(2,1)}) custom-call(s32[1]{0:T(128)} %bitcast.zref, bf16[512,384]{1,0:T(8,128)(2,1)} %bitcast.198, bf16[512,512]{1,0:T(8,128)(2,1)} %collective-permute-done.27.refs_0_, ...), custom_call_target="tpu_custom_call" | custom-call | flops 201326592 | bytes 2097152 | tf_op jit(solution)/shard_map/pallas_call | solution.py:112
  134.3 1.8 slice.129
  136.1 1.2 collective-permute-start.29
  137.3 2.6 %shard_map.113 = (bf16[128,512]{1,0:T(8,128)(2,1)}, bf16[128,512]{1,0:T(8,128)(2,1)}, bf16[128,512]{1,0:T(8,128)(2,1)}, bf16[128,512]{1,0:T(8,128)(2,1)}) custom-call(s32[1]{0:T(128)} %bitcast.zref, bf16[512,384]{1,0:T(8,128)(2,1)} %bitcast.199, bf16[512,512]{1,0:T(8,128)(2,1)} %collective-permute-done.21.refs_0_, ...), custom_call_target="tpu_custom_call" | custom-call | flops 201326592 | bytes 2097152 | tf_op jit(solution)/shard_map/pallas_call | solution.py:112
  139.9 3.7 %collective-permute-done.28 = bf16[128,512]{1,0:T(8,128)(2,1)} collective-permute-done((bf16[128,512]{1,0:T(8,128)(2,1)}, bf16[128,512]{1,0:T(8,128)(2,1)}, u32[]{:S(2)}, u32[]{:S(2)}) %collective-permute-start.28) | collective-permute-done | bytes 131104 | tf_op jit(solution)/shard_map/ppermute | solution.py:156
  144.8 1.2 collective-permute-start.22
  147.4 1.3 convert_add_fusion.1
  148.7 4.8 %collective-permute-done.22 = bf16[128,512]{1,0:T(8,128)(2,1)S(1)} collective-permute-done((bf16[128,512]{1,0:T(8,128)(2,1)}, bf16[128,512]{1,0:T(8,128)(2,1)S(1)}, u32[]{:S(2)}, u32[]{:S(2)}) %collective-permute-start.22) | collective-permute-done | bytes 131104 | tf_op jit(solution)/shard_map/ppermute | solution.py:156
  154.0 1.2 select_select_fusion.3
  157.7 1.2 collective-permute-start.37
  160.3 3.1 %collective-permute-start.39 = (bf16[64,2048]{1,0:T(8,128)(2,1)}, bf16[64,2048]{1,0:T(8,128)(2,1)}, u32[]{:S(2)}, u32[]{:S(2)}) collective-permute-start(bf16[64,2048]{1,0:T(8,128)(2,1)} %get-tuple-element.58), channel_id=1, source_target_pairs={{0,1},{1,0},{2,3},{3,2},{4,5},{5,4},{6,7},{7,6},{8,9},{9,8},{10,11... | collective-permute-start | bytes 786440 | tf_op jit(solution)/shard_map/ppermute | solution.py:156
  167.9 1.9 collective-permute-start.48
  171.9 3.3 %collective-permute-start.40 = (bf16[64,2048]{1,0:T(8,128)(2,1)}, bf16[64,2048]{1,0:T(8,128)(2,1)S(1)}, u32[]{:S(2)}, u32[]{:S(2)}) collective-permute-start(bf16[64,2048]{1,0:T(8,128)(2,1)} %collective-permute-done.36), channel_id=1, source_target_pairs={{0,1},{1,0},{2,3},{3,2},{4,5},{5,4},{6,7},{7,6},{8,9},{9,8},{10,11... | collective-permute-start | bytes 786440 | tf_op jit(solution)/shard_map/ppermute | solution.py:156
  175.1 1.3 maximum_bitcast_fusion.2
  176.5 2.1 collective-permute-start.42
  179.5 1.6 collective-permute-start.58
  184.7 4.9 %collective-permute-done.58 = bf16[512,384]{1,0:T(8,128)(2,1)S(1)} collective-permute-done((bf16[512,384]{1,0:T(8,128)(2,1)S(1)}, bf16[512,384]{1,0:T(8,128)(2,1)S(1)}, u32[]{:S(2)}, u32[]{:S(2)}) %collective-permute-start.58) | collective-permute-done | bytes 393248 | tf_op jit(solution)/shard_map/ppermute | solution.py:156
  189.7 1.2 collective-permute-start.53
  190.9 2.8 %fusion.9 = (bf16[512,384]{1,0:T(8,128)(2,1)S(1)}, bf16[512,384]{1,0:T(8,128)(2,1)S(1)}) fusion(f32[1024,768]{1,0:T(8,128)} %copy-done.7, bf16[512,2048]{1,0:T(8,128)(2,1)S(1)} %bitcast.206, bf16[2048,384]{1,0:T(8,128)(2,1)S(1)} %bitcast.208), kind=kOutput, calls=%fused_computation.31 | convolution fusion | flops 807862272 | bytes 6029312 | tf_op jit(solution)/shard_map/dot_general | solution.py:326
  193.7 22.5 %collective-permute-done.59 = bf16[512,384]{1,0:T(8,128)(2,1)S(1)} collective-permute-done((bf16[512,384]{1,0:T(8,128)(2,1)S(1)}, bf16[512,384]{1,0:T(8,128)(2,1)S(1)}, u32[]{:S(2)}, u32[]{:S(2)}) %collective-permute-start.59) | collective-permute-done | bytes 393248 | tf_op jit(solution)/shard_map/ppermute | solution.py:156
  222.4 2.1 collective-permute-start.61
  227.4 3.7 %collective-permute-done.63 = bf16[256,384]{1,0:T(8,128)(2,1)S(1)} collective-permute-done((bf16[256,384]{1,0:T(8,128)(2,1)S(1)}, bf16[256,384]{1,0:T(8,128)(2,1)S(1)}, u32[]{:S(2)}, u32[]{:S(2)}) %collective-permute-start.63) | collective-permute-done | bytes 196640 | tf_op jit(solution)/shard_map/ppermute | solution.py:156
  231.6 1.8 collective-permute-done.62
  233.6 3.3 %collective-permute-done.44 = bf16[64,2048]{1,0:T(8,128)(2,1)S(1)} collective-permute-done((bf16[64,2048]{1,0:T(8,128)(2,1)S(1)}, bf16[64,2048]{1,0:T(8,128)(2,1)S(1)}, u32[]{:S(2)}, u32[]{:S(2)}) %collective-permute-start.44) | collective-permute-done | bytes 262176 | tf_op jit(solution)/shard_map/ppermute | solution.py:156
  236.9 2.1 collective-permute-done.45
  239.0 5.7 %collective-permute-done.46 = bf16[64,2048]{1,0:T(8,128)(2,1)S(1)} collective-permute-done((bf16[64,2048]{1,0:T(8,128)(2,1)S(1)}, bf16[64,2048]{1,0:T(8,128)(2,1)S(1)}, u32[]{:S(2)}, u32[]{:S(2)}) %collective-permute-start.46) | collective-permute-done | bytes 262176 | tf_op jit(solution)/shard_map/ppermute | solution.py:156
  245.4 1.5 collective-permute-start.47
  246.9 1.4 maximum_add_fusion
  (218 shorter events, 47.5 us)
Async XLA Ops:
  3.0 17.7 %collective-permute-start.6 = (bf16[256,768]{1,0:T(8,128)(2,1)}, bf16[256,768]{1,0:T(8,128)(2,1)S(1)}, u32[]{:S(2)}, u32[]{:S(2)}) collective-permute-start(bf16[256,768]{1,0:T(8,128)(2,1)} %pad_maximum_fusion.9), channel_id=1, source_target_pairs={{0,4},{1,5},{2,6},{3,7},{4,0},{5,1},{6,2},{7,3},{8,12},{9,13},{10,... | collective-permute-start | bytes 1179656 | tf_op jit(solution)/shard_map/ppermute | solution.py:156
  3.1 21.8 %collective-permute-start.7 = (bf16[256,768]{1,0:T(8,128)(2,1)}, bf16[256,768]{1,0:T(8,128)(2,1)}, u32[]{:S(2)}, u32[]{:S(2)}) collective-permute-start(bf16[256,768]{1,0:T(8,128)(2,1)} %pad_maximum_fusion.9), channel_id=1, source_target_pairs={{4,8},{5,9},{6,10},{7,11},{8,4},{9,5},{10,6},{11,7},{20,24},{21,25... | collective-permute-start | bytes 1179656 | tf_op jit(solution)/shard_map/ppermute | solution.py:156
  5.3 16.6 %collective-permute-start.8 = (bf16[256,768]{1,0:T(8,128)(2,1)}, bf16[256,768]{1,0:T(8,128)(2,1)}, u32[]{:S(2)}, u32[]{:S(2)}) collective-permute-start(bf16[256,768]{1,0:T(8,128)(2,1)} %pad_maximum_fusion.10), channel_id=1, source_target_pairs={{0,2},{1,3},{2,0},{3,1},{4,6},{5,7},{6,4},{7,5},{8,10},{9,11},{10,... | collective-permute-start | bytes 1179656 | tf_op jit(solution)/shard_map/ppermute | solution.py:156
  8.2 11.3 %collective-permute-start.17 = (bf16[256,384]{1,0:T(8,128)(2,1)}, bf16[256,384]{1,0:T(8,128)(2,1)S(1)}, u32[]{:S(2)}, u32[]{:S(2)}) collective-permute-start(bf16[256,384]{1,0:T(8,128)(2,1)} %constant_dynamic-slice_fusion.5), channel_id=1, source_target_pairs={{0,2},{1,3},{2,0},{3,1},{4,6},{5,7},{6,4},{7,5},{8,10},{9,11},{10,... | collective-permute-start | bytes 589832 | tf_op jit(solution)/shard_map/ppermute | solution.py:156
  10.3 20.5 %collective-permute-start = (bf16[2,64,2048]{2,1,0:T(8,128)(2,1)}, bf16[2,64,2048]{2,1,0:T(8,128)(2,1)}, u32[]{:S(2)}, u32[]{:S(2)}) collective-permute-start(bf16[2,64,2048]{2,1,0:T(8,128)(2,1)} %bitcast.4), channel_id=1, source_target_pairs={{0,2},{1,3},{2,0},{3,1},{4,6},{5,7},{6,4},{7,5},{8,10},{9,11},{10,... | collective-permute-start | bytes 1572872 | tf_op jit(solution)/shard_map/ppermute | solution.py:156
  19.5 12.6 %collective-permute-start.1 = (bf16[2,64,2048]{2,1,0:T(8,128)(2,1)}, bf16[2,64,2048]{2,1,0:T(8,128)(2,1)S(1)}, u32[]{:S(2)}, u32[]{:S(2)}) collective-permute-start(bf16[2,64,2048]{2,1,0:T(8,128)(2,1)} %bitcast.4), channel_id=1, source_target_pairs={{0,16},{1,17},{2,18},{3,19},{4,20},{5,21},{6,22},{7,23},{8,24},{9,... | collective-permute-start | bytes 1572872 | tf_op jit(solution)/shard_map/ppermute | solution.py:156
  20.7 21.4 %collective-permute-start.2 = (bf16[2,64,2048]{2,1,0:T(8,128)(2,1)}, bf16[2,64,2048]{2,1,0:T(8,128)(2,1)S(1)}, u32[]{:S(2)}, u32[]{:S(2)}) collective-permute-start(bf16[2,64,2048]{2,1,0:T(8,128)(2,1)} %bitcast.4), channel_id=1, source_target_pairs={{0,18},{1,19},{2,16},{3,17},{4,22},{5,23},{6,20},{7,21},{8,26},{9,... | collective-permute-start | bytes 1572872 | tf_op jit(solution)/shard_map/ppermute | solution.py:156
  22.0 25.7 %collective-permute-start.9 = (bf16[256,768]{1,0:T(8,128)(2,1)}, bf16[256,768]{1,0:T(8,128)(2,1)S(1)}, u32[]{:S(2)}, u32[]{:S(2)}) collective-permute-start(bf16[256,768]{1,0:T(8,128)(2,1)} %collective-permute-done.8), channel_id=1, source_target_pairs={{0,4},{1,5},{2,6},{3,7},{4,0},{5,1},{6,2},{7,3},{8,12},{9,13},{10,... | collective-permute-start | bytes 1179656 | tf_op jit(solution)/shard_map/ppermute | solution.py:156
  24.9 22.9 %collective-permute-start.10 = (bf16[256,768]{1,0:T(8,128)(2,1)}, bf16[256,768]{1,0:T(8,128)(2,1)S(1)}, u32[]{:S(2)}, u32[]{:S(2)}) collective-permute-start(bf16[256,768]{1,0:T(8,128)(2,1)} %collective-permute-done.8), channel_id=1, source_target_pairs={{4,8},{5,9},{6,10},{7,11},{8,4},{9,5},{10,6},{11,7},{20,24},{21,25... | collective-permute-start | bytes 1179656 | tf_op jit(solution)/shard_map/ppermute | solution.py:156
  30.8 17.6 %collective-permute-start.11 = (bf16[256,768]{1,0:T(8,128)(2,1)}, bf16[256,768]{1,0:T(8,128)(2,1)S(1)}, u32[]{:S(2)}, u32[]{:S(2)}) collective-permute-start(bf16[256,768]{1,0:T(8,128)(2,1)} %collective-permute-done.7), channel_id=1, source_target_pairs={{4,0},{5,1},{6,2},{7,3},{8,12},{9,13},{10,14},{11,15},{20,16},{21,... | collective-permute-start | bytes 1179656 | tf_op jit(solution)/shard_map/ppermute | solution.py:156
  32.1 17.7 %collective-permute-start.12 = (bf16[256,768]{1,0:T(8,128)(2,1)S(1)}, bf16[256,768]{1,0:T(8,128)(2,1)S(1)}, u32[]{:S(2)}, u32[]{:S(2)}) collective-permute-start(bf16[256,768]{1,0:T(8,128)(2,1)S(1)} %copy-done.24), channel_id=1, source_target_pairs={{4,8},{5,9},{6,10},{7,11},{8,4},{9,5},{10,6},{11,7},{20,24},{21,25... | collective-permute-start | bytes 1179656 | tf_op jit(solution)/shard_map/ppermute | solution.py:156
  42.1 8.4 %collective-permute-start.3 = (bf16[2,64,2048]{2,1,0:T(8,128)(2,1)}, bf16[2,64,2048]{2,1,0:T(8,128)(2,1)S(1)}, u32[]{:S(2)}, u32[]{:S(2)}) collective-permute-start(bf16[2,64,2048]{2,1,0:T(8,128)(2,1)} %collective-permute-done), channel_id=1, source_target_pairs={{0,1},{1,0},{2,3},{3,2},{4,5},{5,4},{6,7},{7,6},{8,9},{9,8},{10,11... | collective-permute-start | bytes 1572872 | tf_op jit(solution)/shard_map/ppermute | solution.py:156
  47.7 4.1 %collective-permute-start.4 = (bf16[2,64,2048]{2,1,0:T(8,128)(2,1)S(1)}, bf16[2,64,2048]{2,1,0:T(8,128)(2,1)S(1)}, u32[]{:S(2)}, u32[]{:S(2)}) collective-permute-start(bf16[2,64,2048]{2,1,0:T(8,128)(2,1)S(1)} %collective-permute-done.1), channel_id=1, source_target_pairs={{0,1},{1,0},{2,3},{3,2},{4,5},{5,4},{6,7},{7,6},{8,9},{9,8},{10,11... | collective-permute-start | bytes 1572872 | tf_op jit(solution)/shard_map/ppermute | solution.py:156
  47.8 4.0 %collective-permute-start.5 = (bf16[2,64,2048]{2,1,0:T(8,128)(2,1)S(1)}, bf16[2,64,2048]{2,1,0:T(8,128)(2,1)S(1)}, u32[]{:S(2)}, u32[]{:S(2)}) collective-permute-start(bf16[2,64,2048]{2,1,0:T(8,128)(2,1)S(1)} %collective-permute-done.2), channel_id=1, source_target_pairs={{0,1},{1,0},{2,3},{3,2},{4,5},{5,4},{6,7},{7,6},{8,9},{9,8},{10,11... | collective-permute-start | bytes 1572872 | tf_op jit(solution)/shard_map/ppermute | solution.py:156
  48.4 12.5 %collective-permute-start.13 = (bf16[256,768]{1,0:T(8,128)(2,1)S(1)}, bf16[256,768]{1,0:T(8,128)(2,1)S(1)}, u32[]{:S(2)}, u32[]{:S(2)}) collective-permute-start(bf16[256,768]{1,0:T(8,128)(2,1)S(1)} %collective-permute-done.10), channel_id=1, source_target_pairs={{4,0},{5,1},{6,2},{7,3},{8,12},{9,13},{10,14},{11,15},{20,16},{21,... | collective-permute-start | bytes 1179656 | tf_op jit(solution)/shard_map/ppermute | solution.py:156
  49.8 11.2 %collective-permute-start.14 = (bf16[256,768]{1,0:T(8,128)(2,1)S(1)}, bf16[256,768]{1,0:T(8,128)(2,1)S(1)}, u32[]{:S(2)}, u32[]{:S(2)}) collective-permute-start(bf16[256,768]{1,0:T(8,128)(2,1)S(1)} %collective-permute-done.9), channel_id=1, source_target_pairs={{4,8},{5,9},{6,10},{7,11},{8,4},{9,5},{10,6},{11,7},{20,24},{21,25... | collective-permute-start | bytes 1179656 | tf_op jit(solution)/shard_map/ppermute | solution.py:156
  50.5 18.9 %collective-permute-start.15 = (bf16[256,768]{1,0:T(8,128)(2,1)S(1)}, bf16[256,768]{1,0:T(8,128)(2,1)S(1)}, u32[]{:S(2)}, u32[]{:S(2)}) collective-permute-start(bf16[256,768]{1,0:T(8,128)(2,1)S(1)} %collective-permute-done.12), channel_id=1, source_target_pairs={{4,0},{5,1},{6,2},{7,3},{8,12},{9,13},{10,14},{11,15},{20,16},{21,... | collective-permute-start | bytes 1179656 | tf_op jit(solution)/shard_map/ppermute | solution.py:156
  61.0 31.7 %collective-permute-start.18 = (bf16[512,384]{1,0:T(8,128)(2,1)S(1)}, bf16[512,384]{1,0:T(8,128)(2,1)S(1)}, u32[]{:S(2)}, u32[]{:S(2)}) collective-permute-start(bf16[512,384]{1,0:T(8,128)(2,1)S(1)} %bitcast.192), channel_id=1, source_target_pairs={{0,4},{1,5},{2,6},{3,7},{4,0},{5,1},{6,2},{7,3},{8,12},{9,13},{10,... | collective-permute-start | bytes 1179656 | tf_op jit(solution)/shard_map/ppermute | solution.py:156
  64.2 34.9 %collective-permute-start.25 = (bf16[512,384]{1,0:T(8,128)(2,1)S(1)}, bf16[512,384]{1,0:T(8,128)(2,1)}, u32[]{:S(2)}, u32[]{:S(2)}) collective-permute-start(bf16[512,384]{1,0:T(8,128)(2,1)S(1)} %bitcast.193), channel_id=1, source_target_pairs={{4,8},{5,9},{6,10},{7,11},{8,4},{9,5},{10,6},{11,7},{20,24},{21,25... | collective-permute-start | bytes 1179656 | tf_op jit(solution)/shard_map/ppermute | solution.py:156
  65.6 20.6 %collective-permute-start.16 = (bf16[256,768]{1,0:T(8,128)(2,1)S(1)}, bf16[256,768]{1,0:T(8,128)(2,1)S(1)}, u32[]{:S(2)}, u32[]{:S(2)}) collective-permute-start(bf16[256,768]{1,0:T(8,128)(2,1)S(1)} %collective-permute-done.14), channel_id=1, source_target_pairs={{4,0},{5,1},{6,2},{7,3},{8,12},{9,13},{10,14},{11,15},{20,16},{21,... | collective-permute-start | bytes 1179656 | tf_op jit(solution)/shard_map/ppermute | solution.py:156
  96.7 27.2 %collective-permute-start.31 = (bf16[512,1024]{1,0:T(8,128)(2,1)}, bf16[512,1024]{1,0:T(8,128)(2,1)}, u32[]{:S(2)}, u32[]{:S(2)}) collective-permute-start(bf16[512,1024]{1,0:T(8,128)(2,1)} %shard_map.116), channel_id=1, source_target_pairs={{0,1},{1,0},{2,3},{3,2},{4,5},{5,4},{6,7},{7,6},{8,9},{9,8},{10,11... | collective-permute-start | bytes 3145736 | tf_op jit(solution)/shard_map/ppermute | solution.py:156
  97.6 2.7 %collective-permute-start.19 = (bf16[512,384]{1,0:T(8,128)(2,1)}, bf16[512,384]{1,0:T(8,128)(2,1)}, u32[]{:S(2)}, u32[]{:S(2)}) collective-permute-start(bf16[512,384]{1,0:T(8,128)(2,1)} %copy-done.3), channel_id=1, source_target_pairs={{4,8},{5,9},{6,10},{7,11},{8,4},{9,5},{10,6},{11,7},{20,24},{21,25... | collective-permute-start | bytes 1179656 | tf_op jit(solution)/shard_map/ppermute | solution.py:156
  99.0 12.8 %collective-permute-start.26 = (bf16[512,384]{1,0:T(8,128)(2,1)}, bf16[512,384]{1,0:T(8,128)(2,1)S(1)}, u32[]{:S(2)}, u32[]{:S(2)}) collective-permute-start(bf16[512,384]{1,0:T(8,128)(2,1)} %collective-permute-done.25.refs_0_.refs_1_), channel_id=1, source_target_pairs={{4,0},{5,1},{6,2},{7,3},{8,12},{9,13},{10,14},{11,15},{20,16},{21,... | collective-permute-start | bytes 1179656 | tf_op jit(solution)/shard_map/ppermute | solution.py:156
  100.3 19.6 %collective-permute-start.20 = (bf16[512,384]{1,0:T(8,128)(2,1)}, bf16[512,384]{1,0:T(8,128)(2,1)}, u32[]{:S(2)}, u32[]{:S(2)}) collective-permute-start(bf16[512,384]{1,0:T(8,128)(2,1)} %collective-permute-done.19.refs_0_.refs_1_), channel_id=1, source_target_pairs={{4,0},{5,1},{6,2},{7,3},{8,12},{9,13},{10,14},{11,15},{20,16},{21,... | collective-permute-start | bytes 1179656 | tf_op jit(solution)/shard_map/ppermute | solution.py:156
  115.0 15.2 %collective-permute-start.27 = (bf16[512,512]{1,0:T(8,128)(2,1)}, bf16[512,512]{1,0:T(8,128)(2,1)}, u32[]{:S(2)}, u32[]{:S(2)}) collective-permute-start(bf16[512,512]{1,0:T(8,128)(2,1)} %shard_map.114), channel_id=1, source_target_pairs={{0,1},{1,0},{2,3},{3,2},{4,5},{5,4},{6,7},{7,6},{8,9},{9,8},{10,11... | collective-permute-start | bytes 1572872 | tf_op jit(solution)/shard_map/ppermute | solution.py:156
  122.4 13.6 %collective-permute-start.21 = (bf16[512,512]{1,0:T(8,128)(2,1)}, bf16[512,512]{1,0:T(8,128)(2,1)}, u32[]{:S(2)}, u32[]{:S(2)}) collective-permute-start(bf16[512,512]{1,0:T(8,128)(2,1)} %shard_map.112), channel_id=1, source_target_pairs={{0,1},{1,0},{2,3},{3,2},{4,5},{5,4},{6,7},{7,6},{8,9},{9,8},{10,11... | collective-permute-start | bytes 1572872 | tf_op jit(solution)/shard_map/ppermute | solution.py:156
  127.1 17.7 %collective-permute-start.32 = (bf16[128,1024]{1,0:T(8,128)(2,1)}, bf16[128,1024]{1,0:T(8,128)(2,1)}, u32[]{:S(2)}, u32[]{:S(2)}) collective-permute-start(bf16[128,1024]{1,0:T(8,128)(2,1)} %get-tuple-element.49), channel_id=1, source_target_pairs={{0,2},{1,3},{2,0},{3,1},{4,6},{5,7},{6,4},{7,5},{8,10},{9,11},{10,... | collective-permute-start | bytes 786440 | tf_op jit(solution)/shard_map/ppermute | solution.py:156
  127.3 18.7 %collective-permute-start.33 = (bf16[128,1024]{1,0:T(8,128)(2,1)}, bf16[128,1024]{1,0:T(8,128)(2,1)}, u32[]{:S(2)}, u32[]{:S(2)}) collective-permute-start(bf16[128,1024]{1,0:T(8,128)(2,1)} %get-tuple-element.50), channel_id=1, source_target_pairs={{0,16},{1,17},{2,18},{3,19},{4,20},{5,21},{6,22},{7,23},{8,24},{9,... | collective-permute-start | bytes 786440 | tf_op jit(solution)/shard_map/ppermute | solution.py:156
  128.5 17.7 %collective-permute-start.34 = (bf16[128,1024]{1,0:T(8,128)(2,1)}, bf16[128,1024]{1,0:T(8,128)(2,1)}, u32[]{:S(2)}, u32[]{:S(2)}) collective-permute-start(bf16[128,1024]{1,0:T(8,128)(2,1)} %get-tuple-element.51), channel_id=1, source_target_pairs={{0,18},{1,19},{2,16},{3,17},{4,22},{5,23},{6,20},{7,21},{8,26},{9,... | collective-permute-start | bytes 786440 | tf_op jit(solution)/shard_map/ppermute | solution.py:156
  132.9 10.7 %collective-permute-start.28 = (bf16[128,512]{1,0:T(8,128)(2,1)}, bf16[128,512]{1,0:T(8,128)(2,1)}, u32[]{:S(2)}, u32[]{:S(2)}) collective-permute-start(bf16[128,512]{1,0:T(8,128)(2,1)} %get-tuple-element.45), channel_id=1, source_target_pairs={{0,2},{1,3},{2,0},{3,1},{4,6},{5,7},{6,4},{7,5},{8,10},{9,11},{10,... | collective-permute-start | bytes 393224 | tf_op jit(solution)/shard_map/ppermute | solution.py:156
  136.1 12.6 %collective-permute-start.29 = (bf16[128,512]{1,0:T(8,128)(2,1)}, bf16[128,512]{1,0:T(8,128)(2,1)}, u32[]{:S(2)}, u32[]{:S(2)}) collective-permute-start(bf16[128,512]{1,0:T(8,128)(2,1)} %get-tuple-element.46), channel_id=1, source_target_pairs={{0,16},{1,17},{2,18},{3,19},{4,20},{5,21},{6,22},{7,23},{8,24},{9,... | collective-permute-start | bytes 393224 | tf_op jit(solution)/shard_map/ppermute | solution.py:156
  143.6 5.1 %collective-permute-start.30 = (bf16[128,512]{1,0:T(8,128)(2,1)}, bf16[128,512]{1,0:T(8,128)(2,1)S(1)}, u32[]{:S(2)}, u32[]{:S(2)}) collective-permute-start(bf16[128,512]{1,0:T(8,128)(2,1)} %get-tuple-element.47), channel_id=1, source_target_pairs={{0,18},{1,19},{2,16},{3,17},{4,22},{5,23},{6,20},{7,21},{8,26},{9,... | collective-permute-start | bytes 393224 | tf_op jit(solution)/shard_map/ppermute | solution.py:156
  144.8 8.8 %collective-permute-start.22 = (bf16[128,512]{1,0:T(8,128)(2,1)}, bf16[128,512]{1,0:T(8,128)(2,1)S(1)}, u32[]{:S(2)}, u32[]{:S(2)}) collective-permute-start(bf16[128,512]{1,0:T(8,128)(2,1)} %get-tuple-element.41), channel_id=1, source_target_pairs={{0,2},{1,3},{2,0},{3,1},{4,6},{5,7},{6,4},{7,5},{8,10},{9,11},{10,... | collective-permute-start | bytes 393224 | tf_op jit(solution)/shard_map/ppermute | solution.py:156
  146.0 7.6 %collective-permute-start.23 = (bf16[128,512]{1,0:T(8,128)(2,1)}, bf16[128,512]{1,0:T(8,128)(2,1)S(1)}, u32[]{:S(2)}, u32[]{:S(2)}) collective-permute-start(bf16[128,512]{1,0:T(8,128)(2,1)} %get-tuple-element.42), channel_id=1, source_target_pairs={{0,16},{1,17},{2,18},{3,19},{4,20},{5,21},{6,22},{7,23},{8,24},{9,... | collective-permute-start | bytes 393224 | tf_op jit(solution)/shard_map/ppermute | solution.py:156
  146.3 7.8 %collective-permute-start.24 = (bf16[128,512]{1,0:T(8,128)(2,1)}, bf16[128,512]{1,0:T(8,128)(2,1)S(1)}, u32[]{:S(2)}, u32[]{:S(2)}) collective-permute-start(bf16[128,512]{1,0:T(8,128)(2,1)} %get-tuple-element.43), channel_id=1, source_target_pairs={{0,18},{1,19},{2,16},{3,17},{4,22},{5,23},{6,20},{7,21},{8,26},{9,... | collective-permute-start | bytes 393224 | tf_op jit(solution)/shard_map/ppermute | solution.py:156
  157.7 8.5 %collective-permute-start.37 = (bf16[64,2048]{1,0:T(8,128)(2,1)}, bf16[64,2048]{1,0:T(8,128)(2,1)}, u32[]{:S(2)}, u32[]{:S(2)}) collective-permute-start(bf16[64,2048]{1,0:T(8,128)(2,1)} %get-tuple-element.58), channel_id=1, source_target_pairs={{0,16},{1,17},{2,18},{3,19},{4,20},{5,21},{6,22},{7,23},{8,24},{9,... | collective-permute-start | bytes 786440 | tf_op jit(solution)/shard_map/ppermute | solution.py:156
  158.9 12.1 %collective-permute-start.36 = (bf16[64,2048]{1,0:T(8,128)(2,1)}, bf16[64,2048]{1,0:T(8,128)(2,1)}, u32[]{:S(2)}, u32[]{:S(2)}) collective-permute-start(bf16[64,2048]{1,0:T(8,128)(2,1)} %get-tuple-element.58), channel_id=1, source_target_pairs={{0,2},{1,3},{2,0},{3,1},{4,6},{5,7},{6,4},{7,5},{8,10},{9,11},{10,... | collective-permute-start | bytes 786440 | tf_op jit(solution)/shard_map/ppermute | solution.py:156
  159.2 12.7 %collective-permute-start.38 = (bf16[64,2048]{1,0:T(8,128)(2,1)}, bf16[64,2048]{1,0:T(8,128)(2,1)}, u32[]{:S(2)}, u32[]{:S(2)}) collective-permute-start(bf16[64,2048]{1,0:T(8,128)(2,1)} %get-tuple-element.58), channel_id=1, source_target_pairs={{0,18},{1,19},{2,16},{3,17},{4,22},{5,23},{6,20},{7,21},{8,26},{9,... | collective-permute-start | bytes 786440 | tf_op jit(solution)/shard_map/ppermute | solution.py:156
  160.3 20.8 %collective-permute-start.39 = (bf16[64,2048]{1,0:T(8,128)(2,1)}, bf16[64,2048]{1,0:T(8,128)(2,1)}, u32[]{:S(2)}, u32[]{:S(2)}) collective-permute-start(bf16[64,2048]{1,0:T(8,128)(2,1)} %get-tuple-element.58), channel_id=1, source_target_pairs={{0,1},{1,0},{2,3},{3,2},{4,5},{5,4},{6,7},{7,6},{8,9},{9,8},{10,11... | collective-permute-start | bytes 786440 | tf_op jit(solution)/shard_map/ppermute | solution.py:156
  163.4 6.4 %collective-permute-start.35 = (bf16[64,2048]{1,0:T(8,128)(2,1)}, bf16[64,2048]{1,0:T(8,128)(2,1)}, u32[]{:S(2)}, u32[]{:S(2)}) collective-permute-start(bf16[64,2048]{1,0:T(8,128)(2,1)} %get-tuple-element.89), channel_id=1, source_target_pairs={{0,1},{1,0},{2,3},{3,2},{4,5},{5,4},{6,7},{7,6},{8,9},{9,8},{10,11... | collective-permute-start | bytes 786440 | tf_op jit(solution)/shard_map/ppermute | solution.py:156
  167.9 8.5 %collective-permute-start.48 = (bf16[64,512]{1,0:T(8,128)(2,1)S(1)}, bf16[64,512]{1,0:T(8,128)(2,1)S(1)}, u32[]{:S(2)}, u32[]{:S(2)}) collective-permute-start(bf16[64,512]{1,0:T(8,128)(2,1)S(1)} %bitcast.236), channel_id=1, source_target_pairs={{0,4},{1,5},{2,6},{3,7},{4,8},{5,9},{6,10},{7,11},{8,12},{9,13},{1... | collective-permute-start | bytes 196616 | tf_op jit(solution)/shard_map/ppermute | solution.py:156
  169.8 6.7 %collective-permute-start.49 = (bf16[64,512]{1,0:T(8,128)(2,1)S(1)}, bf16[64,512]{1,0:T(8,128)(2,1)S(1)}, u32[]{:S(2)}, u32[]{:S(2)}) collective-permute-start(bf16[64,512]{1,0:T(8,128)(2,1)S(1)} %bitcast.235), channel_id=1, source_target_pairs={{0,8},{1,9},{2,10},{3,11},{4,12},{5,13},{6,14},{7,15},{8,0},{9,1},... | collective-permute-start | bytes 196616 | tf_op jit(solution)/shard_map/ppermute | solution.py:156
  171.0 8.5 %collective-permute-start.50 = (bf16[64,512]{1,0:T(8,128)(2,1)S(1)}, bf16[64,512]{1,0:T(8,128)(2,1)S(1)}, u32[]{:S(2)}, u32[]{:S(2)}) collective-permute-start(bf16[64,512]{1,0:T(8,128)(2,1)S(1)} %bitcast.234), channel_id=1, source_target_pairs={{0,12},{1,13},{2,14},{3,15},{4,0},{5,1},{6,2},{7,3},{8,4},{9,5},{1... | collective-permute-start | bytes 196616 | tf_op jit(solution)/shard_map/ppermute | solution.py:156
  171.9 10.0 %collective-permute-start.40 = (bf16[64,2048]{1,0:T(8,128)(2,1)}, bf16[64,2048]{1,0:T(8,128)(2,1)S(1)}, u32[]{:S(2)}, u32[]{:S(2)}) collective-permute-start(bf16[64,2048]{1,0:T(8,128)(2,1)} %collective-permute-done.36), channel_id=1, source_target_pairs={{0,1},{1,0},{2,3},{3,2},{4,5},{5,4},{6,7},{7,6},{8,9},{9,8},{10,11... | collective-permute-start | bytes 786440 | tf_op jit(solution)/shard_map/ppermute | solution.py:156
  176.4 5.4 %collective-permute-start.41 = (bf16[64,2048]{1,0:T(8,128)(2,1)}, bf16[64,2048]{1,0:T(8,128)(2,1)S(1)}, u32[]{:S(2)}, u32[]{:S(2)}) collective-permute-start(bf16[64,2048]{1,0:T(8,128)(2,1)} %collective-permute-done.37), channel_id=1, source_target_pairs={{0,1},{1,0},{2,3},{3,2},{4,5},{5,4},{6,7},{7,6},{8,9},{9,8},{10,11... | collective-permute-start | bytes 786440 | tf_op jit(solution)/shard_map/ppermute | solution.py:156
  176.5 5.8 %collective-permute-start.42 = (bf16[64,2048]{1,0:T(8,128)(2,1)}, bf16[64,2048]{1,0:T(8,128)(2,1)S(1)}, u32[]{:S(2)}, u32[]{:S(2)}) collective-permute-start(bf16[64,2048]{1,0:T(8,128)(2,1)} %collective-permute-done.38), channel_id=1, source_target_pairs={{0,1},{1,0},{2,3},{3,2},{4,5},{5,4},{6,7},{7,6},{8,9},{9,8},{10,11... | collective-permute-start | bytes 786440 | tf_op jit(solution)/shard_map/ppermute | solution.py:156
  179.5 10.2 %collective-permute-start.58 = (bf16[512,384]{1,0:T(8,128)(2,1)S(1)}, bf16[512,384]{1,0:T(8,128)(2,1)S(1)}, u32[]{:S(2)}, u32[]{:S(2)}) collective-permute-start(bf16[512,384]{1,0:T(8,128)(2,1)S(1)} %copy-done.17), channel_id=1, source_target_pairs={{0,4},{1,5},{2,6},{3,7},{4,8},{5,9},{6,10},{7,11},{8,12},{9,13},{1... | collective-permute-start | bytes 1179656 | tf_op jit(solution)/shard_map/ppermute | solution.py:156
  181.2 35.0 %collective-permute-start.59 = (bf16[512,384]{1,0:T(8,128)(2,1)S(1)}, bf16[512,384]{1,0:T(8,128)(2,1)S(1)}, u32[]{:S(2)}, u32[]{:S(2)}) collective-permute-start(bf16[512,384]{1,0:T(8,128)(2,1)S(1)} %copy-done.17), channel_id=1, source_target_pairs={{0,8},{1,9},{2,10},{3,11},{4,12},{5,13},{6,14},{7,15},{8,0},{9,1},... | collective-permute-start | bytes 1179656 | tf_op jit(solution)/shard_map/ppermute | solution.py:156
  181.9 36.9 %collective-permute-start.60 = (bf16[512,384]{1,0:T(8,128)(2,1)S(1)}, bf16[512,384]{1,0:T(8,128)(2,1)S(1)}, u32[]{:S(2)}, u32[]{:S(2)}) collective-permute-start(bf16[512,384]{1,0:T(8,128)(2,1)S(1)} %copy-done.17), channel_id=1, source_target_pairs={{0,12},{1,13},{2,14},{3,15},{4,0},{5,1},{6,2},{7,3},{8,4},{9,5},{1... | collective-permute-start | bytes 1179656 | tf_op jit(solution)/shard_map/ppermute | solution.py:156
  181.9 35.2 %collective-permute-start.51 = (bf16[4,64,512]{2,1,0:T(8,128)(2,1)S(1)}, bf16[4,64,512]{2,1,0:T(8,128)(2,1)S(1)}, u32[]{:S(2)}, u32[]{:S(2)}) collective-permute-start(bf16[4,64,512]{2,1,0:T(8,128)(2,1)S(1)} %pad_maximum_fusion.11), channel_id=1, source_target_pairs={{0,2},{1,3},{2,0},{3,1},{4,6},{5,7},{6,4},{7,5},{8,10},{9,11},{10,... | collective-permute-start | bytes 786440 | tf_op jit(solution)/shard_map/ppermute | solution.py:156
  182.4 34.7 %collective-permute-start.52 = (bf16[4,64,512]{2,1,0:T(8,128)(2,1)S(1)}, bf16[4,64,512]{2,1,0:T(8,128)(2,1)S(1)}, u32[]{:S(2)}, u32[]{:S(2)}) collective-permute-start(bf16[4,64,512]{2,1,0:T(8,128)(2,1)S(1)} %pad_maximum_fusion.11), channel_id=1, source_target_pairs={{0,16},{1,17},{2,18},{3,19},{4,20},{5,21},{6,22},{7,23},{8,24},{9,... | collective-permute-start | bytes 786440 | tf_op jit(solution)/shard_map/ppermute | solution.py:156
  189.7 28.0 %collective-permute-start.53 = (bf16[4,64,512]{2,1,0:T(8,128)(2,1)S(1)}, bf16[4,64,512]{2,1,0:T(8,128)(2,1)S(1)}, u32[]{:S(2)}, u32[]{:S(2)}) collective-permute-start(bf16[4,64,512]{2,1,0:T(8,128)(2,1)S(1)} %pad_maximum_fusion.11), channel_id=1, source_target_pairs={{0,18},{1,19},{2,16},{3,17},{4,22},{5,23},{6,20},{7,21},{8,26},{9,... | collective-permute-start | bytes 786440 | tf_op jit(solution)/shard_map/ppermute | solution.py:156
  216.2 3.1 %collective-permute-start.54 = (bf16[4,64,512]{2,1,0:T(8,128)(2,1)S(1)}, bf16[4,64,512]{2,1,0:T(8,128)(2,1)S(1)}, u32[]{:S(2)}, u32[]{:S(2)}) collective-permute-start(bf16[4,64,512]{2,1,0:T(8,128)(2,1)S(1)} %pad_maximum_fusion.11), channel_id=1, source_target_pairs={{0,1},{1,0},{2,3},{3,2},{4,5},{5,4},{6,7},{7,6},{8,9},{9,8},{10,11... | collective-permute-start | bytes 786440 | tf_op jit(solution)/shard_map/ppermute | solution.py:156
  217.1 2.2 collective-permute-start.55
  217.1 2.1 collective-permute-start.56
  217.6 1.8 collective-permute-start.57
  218.7 6.0 %collective-permute-start.43 = (bf16[256,2048]{1,0:T(8,128)(2,1)S(1)}, bf16[256,2048]{1,0:T(8,128)(2,1)S(1)}, u32[]{:S(2)}, u32[]{:S(2)}) collective-permute-start(bf16[256,2048]{1,0:T(8,128)(2,1)S(1)} %convolution_convert_fusion), channel_id=1, source_target_pairs={{0,1},{1,0},{2,3},{3,2},{4,5},{5,4},{6,7},{7,6},{8,9},{9,8},{10,11... | collective-permute-start | bytes 3145736 | tf_op jit(solution)/shard_map/ppermute | solution.py:156
  220.9 10.2 %collective-permute-start.63 = (bf16[256,384]{1,0:T(8,128)(2,1)S(1)}, bf16[256,384]{1,0:T(8,128)(2,1)S(1)}, u32[]{:S(2)}, u32[]{:S(2)}) collective-permute-start(bf16[256,384]{1,0:T(8,128)(2,1)S(1)} %fusion.26), channel_id=1, source_target_pairs={{0,2},{1,3},{2,0},{3,1},{4,6},{5,7},{6,4},{7,5},{8,10},{9,11},{10,... | collective-permute-start | bytes 589832 | tf_op jit(solution)/shard_map/ppermute | solution.py:156
  222.4 9.2 %collective-permute-start.61 = (bf16[256,384]{1,0:T(8,128)(2,1)S(1)}, bf16[256,384]{1,0:T(8,128)(2,1)S(1)}, u32[]{:S(2)}, u32[]{:S(2)}) collective-permute-start(bf16[256,384]{1,0:T(8,128)(2,1)S(1)} %get-tuple-element.106), channel_id=1, source_target_pairs={{0,18},{1,19},{2,16},{3,17},{4,22},{5,23},{6,20},{7,21},{8,26},{9,... | collective-permute-start | bytes 589832 | tf_op jit(solution)/shard_map/ppermute | solution.py:156
  224.5 8.9 %collective-permute-start.62 = (bf16[256,384]{1,0:T(8,128)(2,1)S(1)}, bf16[256,384]{1,0:T(8,128)(2,1)S(1)}, u32[]{:S(2)}, u32[]{:S(2)}) collective-permute-start(bf16[256,384]{1,0:T(8,128)(2,1)S(1)} %get-tuple-element.105), channel_id=1, source_target_pairs={{0,16},{1,17},{2,18},{3,19},{4,20},{5,21},{6,22},{7,23},{8,24},{9,... | collective-permute-start | bytes 589832 | tf_op jit(solution)/shard_map/ppermute | solution.py:156
  225.9 11.0 %collective-permute-start.44 = (bf16[64,2048]{1,0:T(8,128)(2,1)S(1)}, bf16[64,2048]{1,0:T(8,128)(2,1)S(1)}, u32[]{:S(2)}, u32[]{:S(2)}) collective-permute-start(bf16[64,2048]{1,0:T(8,128)(2,1)S(1)} %get-tuple-element.85), channel_id=1, source_target_pairs={{0,2},{1,3},{2,0},{3,1},{4,6},{5,7},{6,4},{7,5},{8,10},{9,11},{10,... | collective-permute-start | bytes 786440 | tf_op jit(solution)/shard_map/ppermute | solution.py:156
  226.4 12.6 %collective-permute-start.45 = (bf16[64,2048]{1,0:T(8,128)(2,1)S(1)}, bf16[64,2048]{1,0:T(8,128)(2,1)S(1)}, u32[]{:S(2)}, u32[]{:S(2)}) collective-permute-start(bf16[64,2048]{1,0:T(8,128)(2,1)S(1)} %get-tuple-element.87), channel_id=1, source_target_pairs={{0,16},{1,17},{2,18},{3,19},{4,20},{5,21},{6,22},{7,23},{8,24},{9,... | collective-permute-start | bytes 786440 | tf_op jit(solution)/shard_map/ppermute | solution.py:156
  231.1 13.6 %collective-permute-start.46 = (bf16[64,2048]{1,0:T(8,128)(2,1)S(1)}, bf16[64,2048]{1,0:T(8,128)(2,1)S(1)}, u32[]{:S(2)}, u32[]{:S(2)}) collective-permute-start(bf16[64,2048]{1,0:T(8,128)(2,1)S(1)} %get-tuple-element.86), channel_id=1, source_target_pairs={{0,18},{1,19},{2,16},{3,17},{4,22},{5,23},{6,20},{7,21},{8,26},{9,... | collective-permute-start | bytes 786440 | tf_op jit(solution)/shard_map/ppermute | solution.py:156
  245.4 2.9 %collective-permute-start.47 = (bf16[64,2048]{1,0:T(8,128)(2,1)S(1)}, bf16[64,2048]{1,0:T(8,128)(2,1)S(1)}, u32[]{:S(2)}, u32[]{:S(2)}) collective-permute-start(bf16[64,2048]{1,0:T(8,128)(2,1)S(1)} %fusion.15), channel_id=1, source_target_pairs={{0,1},{1,0},{2,3},{3,2},{4,5},{5,4},{6,7},{7,6},{8,9},{9,8},{10,11... | collective-permute-start | bytes 786440 | tf_op jit(solution)/shard_map/ppermute | solution.py:156
  (33 other events, 334.0 us)

commit v3 on v2

--- a/solution.py
+++ b/solution.py
@@ -8,6 +8,7 @@
 
 eps = 1e-06
 AXES = ("rep", "fs", "tp")
+VMEM = 67_043_328
 f32 = jnp.float32
 bf16 = jnp.bfloat16
 
@@ -18,10 +19,6 @@
 
 def tn(left, right):
     return lax.dot_general(left, right, (((0,), (0,)), ((), ())), preferred_element_type=f32)
-
-
-def pick(array, index):
-    return lax.dynamic_index_in_dim(array, index, 0, keepdims=False)
 
 
 def put(array, value, index):
@@ -52,6 +49,45 @@
     for i in owners[1:]:
         hit = hit | (z == i)
     return hit
+
+
+def params(*arrays):
+    held = sum(a.size * a.dtype.itemsize for a in arrays)
+    return pltpu.CompilerParams(vmem_limit_bytes=max(2 * held, 1 << 20) + (2 << 20))
+
+
+def cut(places, sources, shapes, jobs, room=None):
+    lane = 128
+    if any(job[2] % lane for job in jobs):
+        outs = [jnp.zeros(shape, bf16) for shape in shapes]
+        for src, place, width, out, row, col in jobs:
+            block = lax.dynamic_slice_in_dim(sources[src], places[place] * width, width, 1)
+            outs[out] = lax.dynamic_update_slice(outs[out], block, (row, col))
+        return outs
+
+    def kernel(place_ref, *refs):
+        srcs, outs, sems = refs[:len(sources)], refs[len(sources):-1], refs[-1]
+        copies = []
+        for i, (src, place, width, out, row, col) in enumerate(jobs):
+            start = pl.multiple_of(place_ref[place] * width, lane)
+            rows = sources[src].shape[0]
+            copies.append(pltpu.make_async_copy(
+                srcs[src].at[:, pl.ds(start, width)], outs[out].at[row:row + rows, col:col + width], sems.at[i]))
+        for copy in copies:
+            copy.start()
+        for copy in copies:
+            copy.wait()
+
+    outs = [jax.ShapeDtypeStruct(shape, bf16) for shape in shapes]
+    return list(pl.pallas_call(
+        kernel,
+        out_shape=outs,
+        in_specs=[pl.BlockSpec(memory_space=pltpu.SMEM)] + [pl.BlockSpec(memory_space=pl.ANY)] * len(sources),
+        out_specs=whole(len(shapes)),
+        scratch_shapes=[pltpu.SemaphoreType.DMA((len(jobs),))],
+        compiler_params=params(*outs) if room is None else pltpu.CompilerParams(vmem_limit_bytes=VMEM - room),
+        cost_estimate=pl.CostEstimate(flops=2_000_000, bytes_accessed=1 << 20, transcendentals=0),
+    )(jnp.stack(places).astype(jnp.int32), *sources))
 
 
 def by_slot(zref, slots, refs, count, emit):
@@ -84,6 +120,7 @@
         out_shape=jax.ShapeDtypeStruct((rows, len(slots) * columns), bf16),
         in_specs=whole(1 + len(values), 1),
         out_specs=whole(1)[0],
+        compiler_params=params(left, *values, left, left),
         cost_estimate=pl.CostEstimate(flops=2 * rows * w * columns * len(slots), bytes_accessed=4 * rows * columns, transcendentals=0),
     )(z, left, *values)
 
@@ -114,15 +151,50 @@
         out_shape=[jax.ShapeDtypeStruct((lead * m, len(slots) * columns), bf16)] * parts,
         in_specs=whole(1 + len(got) + len(values), 1),
         out_specs=whole(parts),
+        compiler_params=params(left, *values, *got, *got),
         cost_estimate=pl.CostEstimate(flops=2 * rows * w * columns * len(slots), bytes_accessed=8 * rows * columns, transcendentals=0),
     )(z, left, *got, *values)
+
+
+def weight_gradient(places, left, right, cases, T, G):
+    Z, (rows, high), wide = len(cases), left[0].shape, right[0].shape[1]
+    K = high // G
+
+    def kernel(place_ref, *refs):
+        lefts, rights, outs, total = refs[:len(left)], refs[len(left):len(left) + len(right)], refs[-1 - G:-1], refs[-1]
+
+        def case(i):
+            value = None
+            for index, k in cases[i]:
+                a = jnp.concatenate([lefts[k * T + j][...] for j in range(T)], axis=0)
+                term = tn(a, rights[index][...])
+                value = term if value is None else value + term
+            total[...] = value
+
+        for i in range(Z):
+            pl.when(place_ref[0] == i)(lambda i=i: case(i))
+        for b, out in enumerate(outs):
+            start = pl.multiple_of(lax.rem(place_ref[1] + b, G) * K, K)
+            out[...] = total[pl.ds(start, K), :].astype(out.dtype)
+
+    shapes = [jax.ShapeDtypeStruct((K, wide), bf16 if b else f32) for b in range(G)]
+    scratch = jax.ShapeDtypeStruct((high, wide), f32)
+    return pl.pallas_call(
+        kernel,
+        out_shape=shapes,
+        in_specs=whole(len(left) + len(right), 1),
+        out_specs=whole(G),
+        scratch_shapes=[pltpu.VMEM((high, wide), f32)],
+        compiler_params=params(*left, *right, *shapes, scratch, scratch),
+        cost_estimate=pl.CostEstimate(flops=2 * Z * T * rows * high * wide, bytes_accessed=1 << 22, transcendentals=0),
+    )(places.astype(jnp.int32), *left, *right)
 
 
 def plan(R, S):
     G = 2 if S % 2 == 0 else 1
     Z = S // G
     peers = [(a, b) for a in range(R) for b in range(G)]
-    ways = sorted(range(1, len(peers)), key=lambda p: (peers[p][0] == 0, peers[p][1] != 0))
+    ways = sorted(range(1, len(peers)), key=lambda p: (peers[p][0] != 0, peers[p][1] != 0))
     return G, Z, peers, ways
 
 
@@ -141,7 +213,7 @@
 
 
 def make_body(R, S, T):
-    G, Z, peers, ways = plan(R, S)
+    G, Z, peers, _ = plan(R, S)
 
     def send(value, dr=0, dy=0, dz=0, dt=0, moves=None):
         moves = [(z, (z + dz) % Z) for z in range(Z)] if moves is None else moves
@@ -164,6 +236,9 @@
             got.append(tuple(step))
         return got
 
+    def partner(z, k):
+        return z ^ k if Z & (Z - 1) == 0 else (z + k) % Z
+
     def source(z, kind, s):
         for a, b in dict(edges(Z, s)).get(kind, []):
             if b == z:
@@ -179,15 +254,15 @@
         w = F // (R * G)
         PT = len(peers)
 
-        def columns(weight, dy):
-            q = r * G + (y + dy) % G
-            return lax.dynamic_slice_in_dim(weight, q * w, w, 1)
-
-        def both(dy):
-            return jnp.concatenate([columns(gate_weight, dy), columns(up_weight, dy)], axis=1)
-
-        gu = [both(0)] + [send(both(d), dy=d) for d in range(1, G)]
-        dn = [columns(down_weight, 0)] + [send(columns(down_weight, d), dy=d) for d in range(1, G)]
+        def block(d):
+            return r * G + (y + d) % G
+
+        spots = [block(d) for d in range(G)]
+        pairs = [(i, d, w, d, 0, i * w) for d in range(G) for i in range(2)]
+        wide = cut(spots, [gate_weight, up_weight], [(K, 2 * w)] * G, pairs)
+        thin = cut(spots, [down_weight], [(K, w)] * G, [(0, d, w, d, 0, 0) for d in range(G)])
+        gu = wide[:1] + [send(wide[d], dy=d) for d in range(1, G)]
+        dn = thin[:1] + [send(thin[d], dy=d) for d in range(1, G)]
 
         x = after(jnp.stack([x_late, x_early]), gu[0]).astype(f32)
         scale = lax.rsqrt(jnp.mean(x * x, axis=-1, keepdims=True) + eps)
@@ -234,14 +309,14 @@
             full = place(full, piece, z, (y - d) % G)
         full = full.reshape(D, 2 * w)
 
-        both_out = jnp.dot(tokens, full, preferred_element_type=f32)
-        gate, up = both_out[:, :w], both_out[:, w:]
-        hidden = (jax.nn.silu(gate) * up).astype(bf16)
-
-        block = jnp.zeros((G, K, w), bf16)
-        for d, piece in enumerate(dn):
-            block = put(block, piece, (y - d) % G)
-        block = block.reshape(G * K, w)
+        halves = []
+        for i in range(2):
+            value = jnp.dot(tokens[i * PT * n:(i + 1) * PT * n], full, preferred_element_type=f32)
+            gate, up = value[:, :w], value[:, w:]
+            halves.append((jax.nn.silu(gate) * up).astype(bf16).reshape(T, PT * m, w))
+        gate_e, up_e = gate, up
+
+        block = arrange(dn, [(y - d) % G for d in range(G)], G, axis=0)
         if Z > 1:
             block = after(block, *[v for v in lines[-1][Z - 2] if v is not None])
         got = arrived = line(block)
@@ -277,8 +352,7 @@
             low = low.reshape(PT, m, -1)
             return plane_sum([low[p] for p in range(PT)]), low
 
-        by_core = hidden.reshape(2, T, PT * m, w)
-        by_core = [by_core[:, j].reshape(2 * PT * m, w) for j in range(T)]
+        by_core = [jnp.concatenate([half[j] for half in halves]) for j in range(T)]
         groups = [[0, 1]] + [[k] for k in range(2, Z)] if Z > 1 else [[0]]
         totals, total_ids = [], []
         for group in groups:
@@ -321,10 +395,9 @@
             down_full = put(down_full, value, where)
         down_full = down_full.reshape(D, w)
         raw = plane(dbranch)
-        spread = [cores(h) for h in raw]
+        spread = spread_c = [cores(h) for h in raw]
         spread = jnp.stack([jnp.stack([h[j] for h in spread]) for j in range(T)]).reshape(PT * n, D)
         dhidden = jnp.dot(spread, down_full, preferred_element_type=f32)
-        gate_e, up_e = gate[PT * n:], up[PT * n:]
         sig = jax.nn.sigmoid(gate_e)
         dgate = (dhidden * up_e * sig * (1.0 + gate_e * (1.0 - sig))).astype(bf16)
         dup = (dhidden * gate_e * sig).astype(bf16)
@@ -337,31 +410,38 @@
         dx = dx.astype(bf16)
         dx_early = all_rows(dx)
 
-        hidden_e = hidden[PT * n:]
-        if Z > 2:
-            hidden_e = after(hidden_e, *[v for v in arrived[Z - 2] if v is not None])
-        kept = [hidden_e] + [send(hidden_e, dz=k) for k in range(1, Z)]
-        parts = after(dbranch, raw[ways[0]] if ways else dbranch).reshape(m, Z, G * K).transpose(1, 0, 2)
-        cols = [pick(parts, z)] + [send(pick(parts, (z + k) % Z), dz=k) for k in range(1, Z)]
-        wide = plane(after(jnp.stack(cols), *raw[1:]))
-        wide = [cores(h) for h in wide]
-        wide = [[wide[p][j] for p in range(PT)] for j in range(T)]
-        wide, kept, _ = lax.optimization_barrier((wide, kept, dlow))
-        wide = jnp.stack([jnp.stack(row) for row in wide])
-        kept = jnp.stack([h.reshape(T, PT, m, w) for h in kept], axis=2)
+        hidden_e = halves[1].reshape(T, R, G * m, w)
+        units = [hidden_e[:, 0]] + [send(hidden_e[:, a], dr=a) for a in range(1, R)]
+        units = jnp.concatenate([u.reshape(G * n, w) for u in units], axis=1)
+        passed = line(units)
+        own = [raw[b] for b in range(G)]
+        cols = cut(
+            [partner(z, k) for k in range(Z)], own, [(G * m, G * K)] * Z, [(b, k, G * K, k, b * m, 0) for k in range(Z) for b in range(G)])
+        cols = [value if k == 0 else send(value, moves=[(i, partner(i, k)) for i in range(Z)]) for k, value in enumerate(cols)]
+        mates = [[spread_c[b][j] for b in range(G)] for j in range(T)]
+        left = []
+        for k, value in enumerate(cols):
+            left.append(value)
+            for j in range(1, T):
+                if k:
+                    left.append(send(value, dt=-j))
+                else:
+                    left.extend(cut([z], mates[j], [(G * m, G * K)], [(b, 0, G * K, 0, b * m, 0) for b in range(G)]))
+        right, cases = [units], [[(0, 0)] for _ in range(Z)]
+        for s in range(1, Z):
+            for kind, _ in edges(Z, s):
+                for i in range(Z):
+                    j = source(i, kind, s)
+                    if j is not None:
+                        cases[i].append((len(right), next(k for k in range(Z) if partner(j, k) == i)))
+                right.append(passed[s][kind])
+        left, right, _ = lax.optimization_barrier((left, right, dlow))
+        grads = weight_gradient(jnp.stack([z, y]), left, right, cases, T, G)
         pieces, sources = [], []
-        for a in range(R):
-            grad = 0.0
-            for j in range(T):
-                left = wide[j, a * G:(a + 1) * G].reshape(G * Z * m, G * K)
-                right = kept[j, a * G:(a + 1) * G].reshape(G * Z * m, w)
-                grad = grad + tn(left, right)
-            grad = grad.reshape(G, K, w)
-            for b in range(G):
-                piece = pick(grad, (y + b) % G)
-                if a or b:
-                    piece = send(piece.astype(bf16), dr=a, dy=b).astype(f32)
-                pieces.append(piece)
+        for b in range(G):
+            piece = send(grads[b], dy=b).astype(f32) if b else grads[0]
+            for a in range(R):
+                pieces.append(piece[:, a * w:(a + 1) * w])
                 sources.append((r - a) % R * G + (y - b) % G)
         summed = arrange(pieces, sources, R * G)
         return (y_late, dx_early, down_grad_sum + summed)

time: 250 us -> 232 us (0.928)
  the two profiles are of different devices: /device:TPU:25 before, /device:TPU:0 now
where the time goes in v3:
time: 232 us; the launch traced here: 231 us
  waiting for transfers between devices  125 us (54%)
  starting transfers between devices  61.6 us (27%)
  Pallas kernels  12.9 us (6%)
  other arithmetic  12.8 us (6%)
  local copies, waits for them, and re-layouts  10.2 us (4%)
  matrix products  7.09 us (3%)
    ppermute x61, waiting for transfers between devices, send(): return lax.ppermute(value, AXES, pairs)  125 us
    ppermute x61, starting transfers between devices, send(): return lax.ppermute(value, AXES, pairs)  61.6 us
    unnamed x36, local copies, waits for them, and re-layouts  4.79 us
  transfers between devices with their start and end apart: 61, of which 24 were waited for; matrix products, arithmetic and copies ran while one was open for 10% of the time, Pallas kernels for 5%

profile of v3, /device:TPU:0, one launch (start us, length us, event | category | flops | bytes accessed | tf_op | source)
XLA Modules:
  0.0 230.7 jit_solution(471801159842190282)
XLA Ops:
  3.7 3.1 %collective-permute-start.6 = (bf16[256,768]{1,0:T(8,128)(2,1)S(1)}, bf16[256,768]{1,0:T(8,128)(2,1)}, u32[]{:S(2)}, u32[]{:S(2)}) collective-permute-start(bf16[256,768]{1,0:T(8,128)(2,1)S(1)} %get-tuple-element.47), channel_id=1, source_target_pairs={{0,4},{1,5},{2,6},{3,7},{4,0},{5,1},{6,2},{7,3},{8,12},{9,13},{10,... | collective-permute-start | bytes 1179656 | tf_op jit(solution)/shard_map/ppermute | solution.py:228
  6.8 1.4 collective-permute-start.7
  8.2 1.5 collective-permute-start.8
  12.6 1.5 collective-permute-start
  14.1 10.3 %collective-permute-done.17 = bf16[256,384]{1,0:T(8,128)(2,1)S(1)} collective-permute-done((bf16[256,384]{1,0:T(8,128)(2,1)S(1)}, bf16[256,384]{1,0:T(8,128)(2,1)S(1)}, u32[]{:S(2)}, u32[]{:S(2)}) %collective-permute-start.17) | collective-permute-done | bytes 196640 | tf_op jit(solution)/shard_map/ppermute | solution.py:228
  24.4 1.5 collective-permute-start.1
  26.9 1.7 collective-permute-start.2
  28.7 3.8 %collective-permute-start.9 = (bf16[256,768]{1,0:T(8,128)(2,1)S(1)}, bf16[256,768]{1,0:T(8,128)(2,1)S(1)}, u32[]{:S(2)}, u32[]{:S(2)}) collective-permute-start(bf16[256,768]{1,0:T(8,128)(2,1)S(1)} %collective-permute-done.8), channel_id=1, source_target_pairs={{0,4},{1,5},{2,6},{3,7},{4,0},{5,1},{6,2},{7,3},{8,12},{9,13},{10,... | collective-permute-start | bytes 1179656 | tf_op jit(solution)/shard_map/ppermute | solution.py:228
  35.5 1.3 collective-permute-start.11
  36.8 2.7 %collective-permute-done.1 = bf16[2,64,2048]{2,1,0:T(8,128)(2,1)S(1)} collective-permute-done((bf16[2,64,2048]{2,1,0:T(8,128)(2,1)}, bf16[2,64,2048]{2,1,0:T(8,128)(2,1)S(1)}, u32[]{:S(2)}, u32[]{:S(2)}) %collective-permute-start.1) | collective-permute-done | bytes 524320 | tf_op jit(solution)/shard_map/ppermute | solution.py:228
  40.1 7.8 %collective-permute-done.2 = bf16[2,64,2048]{2,1,0:T(8,128)(2,1)S(1)} collective-permute-done((bf16[2,64,2048]{2,1,0:T(8,128)(2,1)}, bf16[2,64,2048]{2,1,0:T(8,128)(2,1)S(1)}, u32[]{:S(2)}, u32[]{:S(2)}) %collective-permute-start.2) | collective-permute-done | bytes 524320 | tf_op jit(solution)/shard_map/ppermute | solution.py:228
  48.0 1.3 maximum_bitcast_fusion
  50.0 1.3 collective-permute-start.13
  52.1 1.3 collective-permute-start.15
  54.1 10.3 %collective-permute-done.13 = bf16[256,768]{1,0:T(8,128)(2,1)S(1)} collective-permute-done((bf16[256,768]{1,0:T(8,128)(2,1)S(1)}, bf16[256,768]{1,0:T(8,128)(2,1)S(1)}, u32[]{:S(2)}, u32[]{:S(2)}) %collective-permute-start.13) | collective-permute-done | bytes 393248 | tf_op jit(solution)/shard_map/ppermute | solution.py:228
  64.4 3.5 %collective-permute-start.18 = (bf16[512,384]{1,0:T(8,128)(2,1)S(1)}, bf16[512,384]{1,0:T(8,128)(2,1)S(1)}, u32[]{:S(2)}, u32[]{:S(2)}) collective-permute-start(bf16[512,384]{1,0:T(8,128)(2,1)S(1)} %pad_maximum_fusion.10.refs_0_.refs_1_), channel_id=1, source_target_pairs={{0,4},{1,5},{2,6},{3,7},{4,0},{5,1},{6,2},{7,3},{8,12},{9,13},{10,... | collective-permute-start | bytes 1179656 | tf_op jit(solution)/shard_map/ppermute | solution.py:228
  68.6 1.3 collective-permute-start.16
  70.0 2.8 %collective-permute-done.15 = bf16[256,768]{1,0:T(8,128)(2,1)S(1)} collective-permute-done((bf16[256,768]{1,0:T(8,128)(2,1)S(1)}, bf16[256,768]{1,0:T(8,128)(2,1)S(1)}, u32[]{:S(2)}, u32[]{:S(2)}) %collective-permute-start.15) | collective-permute-done | bytes 393248 | tf_op jit(solution)/shard_map/ppermute | solution.py:228
  72.9 16.6 %collective-permute-done.16 = bf16[256,768]{1,0:T(8,128)(2,1)S(1)} collective-permute-done((bf16[256,768]{1,0:T(8,128)(2,1)S(1)}, bf16[256,768]{1,0:T(8,128)(2,1)S(1)}, u32[]{:S(2)}, u32[]{:S(2)}) %collective-permute-start.16) | collective-permute-done | bytes 393248 | tf_op jit(solution)/shard_map/ppermute | solution.py:228
  89.6 1.8 fusion.28
  91.5 1.8 fusion.27
  95.3 1.7 shard_map.118
  97.0 1.3 collective-permute-start.26
  98.3 1.3 collective-permute-start.20
  100.4 1.5 collective-permute-start.54
  101.9 9.0 %collective-permute-done.26.refs_1_.refs_2_ = bf16[512,384]{1,0:T(8,128)(2,1)S(1)} collective-permute-done((bf16[512,384]{1,0:T(8,128)(2,1)S(1)}, bf16[512,384]{1,0:T(8,128)(2,1)S(1)}, u32[]{:S(2)}, u32[]{:S(2)}) %collective-permute-start.26) | collective-permute-done | bytes 393248 | tf_op jit(solution)/shard_map/ppermute | solution.py:228
  110.9 1.3 shard_map.116
  112.1 6.7 %collective-permute-done.20.refs_1_.refs_2_ = bf16[512,384]{1,0:T(8,128)(2,1)S(1)} collective-permute-done((bf16[512,384]{1,0:T(8,128)(2,1)S(1)}, bf16[512,384]{1,0:T(8,128)(2,1)S(1)}, u32[]{:S(2)}, u32[]{:S(2)}) %collective-permute-start.20) | collective-permute-done | bytes 393248 | tf_op jit(solution)/shard_map/ppermute | solution.py:228
  118.8 1.3 shard_map.114
  122.3 2.0 shard_map.119
  124.9 1.5 collective-permute-start.33
  126.4 1.5 collective-permute-start.34
  127.9 1.5 shard_map.117
  130.6 2.3 %collective-permute-done.55.refs_9_ = bf16[256,768]{1,0:T(8,128)(2,1)} collective-permute-done((bf16[256,768]{1,0:T(8,128)(2,1)S(1)}, bf16[256,768]{1,0:T(8,128)(2,1)}, u32[]{:S(2)}, u32[]{:S(2)}) %collective-permute-start.55) | collective-permute-done | bytes 393248 | tf_op jit(solution)/shard_map/ppermute | solution.py:228
  132.9 1.5 collective-permute-start.29
  134.4 7.0 %collective-permute-done.28 = bf16[128,512]{1,0:T(8,128)(2,1)S(1)} collective-permute-done((bf16[128,512]{1,0:T(8,128)(2,1)S(1)}, bf16[128,512]{1,0:T(8,128)(2,1)S(1)}, u32[]{:S(2)}, u32[]{:S(2)}) %collective-permute-start.28) | collective-permute-done | bytes 131104 | tf_op jit(solution)/shard_map/ppermute | solution.py:228
  141.4 1.4 collective-permute-start.30
  142.9 1.5 collective-permute-start.22
  144.9 1.4 collective-permute-start.24
  146.6 1.4 collective-permute-start.56
  148.7 1.4 collective-permute-start.58
  150.1 1.4 collective-permute-done.22
  151.5 1.4 collective-permute-done.24
  156.0 1.3 collective-permute-start.57
  157.3 1.3 collective-permute-start.59
  158.7 1.6 collective-permute-start.37
  160.5 1.9 collective-permute-done.36.refs_1_
  162.3 1.5 collective-permute-start.38
  164.6 7.4 %collective-permute-done.57.refs_11_ = bf16[256,768]{1,0:T(8,128)(2,1)S(1)} collective-permute-done((bf16[256,768]{1,0:T(8,128)(2,1)}, bf16[256,768]{1,0:T(8,128)(2,1)S(1)}, u32[]{:S(2)}, u32[]{:S(2)}) %collective-permute-start.57) | collective-permute-done | bytes 393248 | tf_op jit(solution)/shard_map/ppermute | solution.py:228
  172.0 1.2 collective-permute-start.48
  173.2 6.1 %collective-permute-done.59.refs_13_ = bf16[256,768]{1,0:T(8,128)(2,1)S(1)} collective-permute-done((bf16[256,768]{1,0:T(8,128)(2,1)}, bf16[256,768]{1,0:T(8,128)(2,1)S(1)}, u32[]{:S(2)}, u32[]{:S(2)}) %collective-permute-start.59) | collective-permute-done | bytes 393248 | tf_op jit(solution)/shard_map/ppermute | solution.py:228
  179.6 2.0 collective-permute-start.52
  182.2 8.9 %collective-permute-done.50.refs_4_ = bf16[128,512]{1,0:T(8,128)(2,1)S(1)} collective-permute-done((bf16[128,512]{1,0:T(8,128)(2,1)S(1)}, bf16[128,512]{1,0:T(8,128)(2,1)S(1)}, u32[]{:S(2)}, u32[]{:S(2)}) %collective-permute-start.50) | collective-permute-done | bytes 131104 | tf_op jit(solution)/shard_map/ppermute | solution.py:228
  193.3 1.2 copy-done.9
  194.5 1.4 multiply_convert_fusion.1
  197.7 2.6 %shard_map.122 = (f32[256,768]{1,0:T(8,128)S(1)}, bf16[256,768]{1,0:T(8,128)(2,1)S(1)}) custom-call(s32[2]{0:T(128)S(1)} %pad_add_fusion.1.place_ref, bf16[128,512]{1,0:T(8,128)(2,1)S(1)} %get-tuple-element.75.refs_0_, bf16[128,512]{1,0:T(8,128)(2,1)S(1)} %shard_map.121.refs_1_, bf16[128,512]{1,0:T(8,128)(2,1)S(1)} %collective-permute-done.48.refs_2_, ...), custom_call_target="tpu_custom_call" | custom-call | flops 805306368 | bytes 4194304 | tf_op jit(solution)/shard_map/pallas_call | solution.py:182
  200.3 1.6 collective-permute-start.60
  202.8 8.9 %collective-permute-done.60 = bf16[256,768]{1,0:T(8,128)(2,1)S(1)} collective-permute-done((bf16[256,768]{1,0:T(8,128)(2,1)S(1)}, bf16[256,768]{1,0:T(8,128)(2,1)S(1)}, u32[]{:S(2)}, u32[]{:S(2)}) %collective-permute-start.60) | collective-permute-done | bytes 393248 | tf_op jit(solution)/shard_map/ppermute | solution.py:228
  213.0 1.6 collective-permute-start.44
  215.1 1.4 collective-permute-start.46
  216.7 4.7 %collective-permute-done.44 = bf16[64,2048]{1,0:T(8,128)(2,1)S(1)} collective-permute-done((bf16[64,2048]{1,0:T(8,128)(2,1)S(1)}, bf16[64,2048]{1,0:T(8,128)(2,1)S(1)}, u32[]{:S(2)}, u32[]{:S(2)}) %collective-permute-start.44) | collective-permute-done | bytes 262176 | tf_op jit(solution)/shard_map/ppermute | solution.py:228
  221.4 2.4 %collective-permute-done.45 = bf16[64,2048]{1,0:T(8,128)(2,1)S(1)} collective-permute-done((bf16[64,2048]{1,0:T(8,128)(2,1)S(1)}, bf16[64,2048]{1,0:T(8,128)(2,1)S(1)}, u32[]{:S(2)}, u32[]{:S(2)}) %collective-permute-start.45) | collective-permute-done | bytes 262176 | tf_op jit(solution)/shard_map/ppermute | solution.py:228
  223.8 3.8 %collective-permute-done.46 = bf16[64,2048]{1,0:T(8,128)(2,1)S(1)} collective-permute-done((bf16[64,2048]{1,0:T(8,128)(2,1)S(1)}, bf16[64,2048]{1,0:T(8,128)(2,1)S(1)}, u32[]{:S(2)}, u32[]{:S(2)}) %collective-permute-start.46) | collective-permute-done | bytes 262176 | tf_op jit(solution)/shard_map/ppermute | solution.py:228
  228.3 1.3 maximum_add_fusion
  (175 shorter events, 34.8 us)
Async XLA Ops:
  3.7 23.2 %collective-permute-start.6 = (bf16[256,768]{1,0:T(8,128)(2,1)S(1)}, bf16[256,768]{1,0:T(8,128)(2,1)}, u32[]{:S(2)}, u32[]{:S(2)}) collective-permute-start(bf16[256,768]{1,0:T(8,128)(2,1)S(1)} %get-tuple-element.47), channel_id=1, source_target_pairs={{0,4},{1,5},{2,6},{3,7},{4,0},{5,1},{6,2},{7,3},{8,12},{9,13},{10,... | collective-permute-start | bytes 1179656 | tf_op jit(solution)/shard_map/ppermute | solution.py:228
  6.8 26.9 %collective-permute-start.7 = (bf16[256,768]{1,0:T(8,128)(2,1)S(1)}, bf16[256,768]{1,0:T(8,128)(2,1)}, u32[]{:S(2)}, u32[]{:S(2)}) collective-permute-start(bf16[256,768]{1,0:T(8,128)(2,1)S(1)} %get-tuple-element.47), channel_id=1, source_target_pairs={{4,8},{5,9},{6,10},{7,11},{8,4},{9,5},{10,6},{11,7},{20,24},{21,25... | collective-permute-start | bytes 1179656 | tf_op jit(solution)/shard_map/ppermute | solution.py:228
  8.2 20.4 %collective-permute-start.8 = (bf16[256,768]{1,0:T(8,128)(2,1)S(1)}, bf16[256,768]{1,0:T(8,128)(2,1)S(1)}, u32[]{:S(2)}, u32[]{:S(2)}) collective-permute-start(bf16[256,768]{1,0:T(8,128)(2,1)S(1)} %get-tuple-element.49), channel_id=1, source_target_pairs={{0,2},{1,3},{2,0},{3,1},{4,6},{5,7},{6,4},{7,5},{8,10},{9,11},{10,... | collective-permute-start | bytes 1179656 | tf_op jit(solution)/shard_map/ppermute | solution.py:228
  10.4 14.1 %collective-permute-start.17 = (bf16[256,384]{1,0:T(8,128)(2,1)S(1)}, bf16[256,384]{1,0:T(8,128)(2,1)S(1)}, u32[]{:S(2)}, u32[]{:S(2)}) collective-permute-start(bf16[256,384]{1,0:T(8,128)(2,1)S(1)} %get-tuple-element.50), channel_id=1, source_target_pairs={{0,2},{1,3},{2,0},{3,1},{4,6},{5,7},{6,4},{7,5},{8,10},{9,11},{10,... | collective-permute-start | bytes 589832 | tf_op jit(solution)/shard_map/ppermute | solution.py:228
  12.6 22.9 %collective-permute-start = (bf16[2,64,2048]{2,1,0:T(8,128)(2,1)}, bf16[2,64,2048]{2,1,0:T(8,128)(2,1)S(1)}, u32[]{:S(2)}, u32[]{:S(2)}) collective-permute-start(bf16[2,64,2048]{2,1,0:T(8,128)(2,1)} %bitcast.6), channel_id=1, source_target_pairs={{0,2},{1,3},{2,0},{3,1},{4,6},{5,7},{6,4},{7,5},{8,10},{9,11},{10,... | collective-permute-start | bytes 1572872 | tf_op jit(solution)/shard_map/ppermute | solution.py:228
  24.4 15.0 %collective-permute-start.1 = (bf16[2,64,2048]{2,1,0:T(8,128)(2,1)}, bf16[2,64,2048]{2,1,0:T(8,128)(2,1)S(1)}, u32[]{:S(2)}, u32[]{:S(2)}) collective-permute-start(bf16[2,64,2048]{2,1,0:T(8,128)(2,1)} %bitcast.6), channel_id=1, source_target_pairs={{0,16},{1,17},{2,18},{3,19},{4,20},{5,21},{6,22},{7,23},{8,24},{9,... | collective-permute-start | bytes 1572872 | tf_op jit(solution)/shard_map/ppermute | solution.py:228
  26.9 21.0 %collective-permute-start.2 = (bf16[2,64,2048]{2,1,0:T(8,128)(2,1)}, bf16[2,64,2048]{2,1,0:T(8,128)(2,1)S(1)}, u32[]{:S(2)}, u32[]{:S(2)}) collective-permute-start(bf16[2,64,2048]{2,1,0:T(8,128)(2,1)} %bitcast.6), channel_id=1, source_target_pairs={{0,18},{1,19},{2,16},{3,17},{4,22},{5,23},{6,20},{7,21},{8,26},{9,... | collective-permute-start | bytes 1572872 | tf_op jit(solution)/shard_map/ppermute | solution.py:228
  28.7 20.6 %collective-permute-start.9 = (bf16[256,768]{1,0:T(8,128)(2,1)S(1)}, bf16[256,768]{1,0:T(8,128)(2,1)S(1)}, u32[]{:S(2)}, u32[]{:S(2)}) collective-permute-start(bf16[256,768]{1,0:T(8,128)(2,1)S(1)} %collective-permute-done.8), channel_id=1, source_target_pairs={{0,4},{1,5},{2,6},{3,7},{4,0},{5,1},{6,2},{7,3},{8,12},{9,13},{10,... | collective-permute-start | bytes 1179656 | tf_op jit(solution)/shard_map/ppermute | solution.py:228
  33.7 16.2 %collective-permute-start.10 = (bf16[256,768]{1,0:T(8,128)(2,1)S(1)}, bf16[256,768]{1,0:T(8,128)(2,1)S(1)}, u32[]{:S(2)}, u32[]{:S(2)}) collective-permute-start(bf16[256,768]{1,0:T(8,128)(2,1)S(1)} %collective-permute-done.8), channel_id=1, source_target_pairs={{4,8},{5,9},{6,10},{7,11},{8,4},{9,5},{10,6},{11,7},{20,24},{21,25... | collective-permute-start | bytes 1179656 | tf_op jit(solution)/shard_map/ppermute | solution.py:228
  35.5 14.5 %collective-permute-start.11 = (bf16[256,768]{1,0:T(8,128)(2,1)}, bf16[256,768]{1,0:T(8,128)(2,1)S(1)}, u32[]{:S(2)}, u32[]{:S(2)}) collective-permute-start(bf16[256,768]{1,0:T(8,128)(2,1)} %collective-permute-done.7), channel_id=1, source_target_pairs={{4,0},{5,1},{6,2},{7,3},{8,12},{9,13},{10,14},{11,15},{20,16},{21,... | collective-permute-start | bytes 1179656 | tf_op jit(solution)/shard_map/ppermute | solution.py:228
  39.4 11.9 %collective-permute-start.12 = (bf16[256,768]{1,0:T(8,128)(2,1)}, bf16[256,768]{1,0:T(8,128)(2,1)S(1)}, u32[]{:S(2)}, u32[]{:S(2)}) collective-permute-start(bf16[256,768]{1,0:T(8,128)(2,1)} %collective-permute-done.6), channel_id=1, source_target_pairs={{4,8},{5,9},{6,10},{7,11},{8,4},{9,5},{10,6},{11,7},{20,24},{21,25... | collective-permute-start | bytes 1179656 | tf_op jit(solution)/shard_map/ppermute | solution.py:228
  48.0 4.2 %collective-permute-start.3 = (bf16[2,64,2048]{2,1,0:T(8,128)(2,1)S(1)}, bf16[2,64,2048]{2,1,0:T(8,128)(2,1)S(1)}, u32[]{:S(2)}, u32[]{:S(2)}) collective-permute-start(bf16[2,64,2048]{2,1,0:T(8,128)(2,1)S(1)} %collective-permute-done), channel_id=1, source_target_pairs={{0,1},{1,0},{2,3},{3,2},{4,5},{5,4},{6,7},{7,6},{8,9},{9,8},{10,11... | collective-permute-start | bytes 1572872 | tf_op jit(solution)/shard_map/ppermute | solution.py:228
  49.3 4.2 %collective-permute-start.4 = (bf16[2,64,2048]{2,1,0:T(8,128)(2,1)S(1)}, bf16[2,64,2048]{2,1,0:T(8,128)(2,1)S(1)}, u32[]{:S(2)}, u32[]{:S(2)}) collective-permute-start(bf16[2,64,2048]{2,1,0:T(8,128)(2,1)S(1)} %collective-permute-done.1), channel_id=1, source_target_pairs={{0,1},{1,0},{2,3},{3,2},{4,5},{5,4},{6,7},{7,6},{8,9},{9,8},{10,11... | collective-permute-start | bytes 1572872 | tf_op jit(solution)/shard_map/ppermute | solution.py:228
  49.9 3.5 %collective-permute-start.5 = (bf16[2,64,2048]{2,1,0:T(8,128)(2,1)S(1)}, bf16[2,64,2048]{2,1,0:T(8,128)(2,1)S(1)}, u32[]{:S(2)}, u32[]{:S(2)}) collective-permute-start(bf16[2,64,2048]{2,1,0:T(8,128)(2,1)S(1)} %collective-permute-done.2), channel_id=1, source_target_pairs={{0,1},{1,0},{2,3},{3,2},{4,5},{5,4},{6,7},{7,6},{8,9},{9,8},{10,11... | collective-permute-start | bytes 1572872 | tf_op jit(solution)/shard_map/ppermute | solution.py:228
  50.0 14.4 %collective-permute-start.13 = (bf16[256,768]{1,0:T(8,128)(2,1)S(1)}, bf16[256,768]{1,0:T(8,128)(2,1)S(1)}, u32[]{:S(2)}, u32[]{:S(2)}) collective-permute-start(bf16[256,768]{1,0:T(8,128)(2,1)S(1)} %collective-permute-done.10), channel_id=1, source_target_pairs={{4,0},{5,1},{6,2},{7,3},{8,12},{9,13},{10,14},{11,15},{20,16},{21,... | collective-permute-start | bytes 1179656 | tf_op jit(solution)/shard_map/ppermute | solution.py:228
  51.4 13.0 %collective-permute-start.14 = (bf16[256,768]{1,0:T(8,128)(2,1)S(1)}, bf16[256,768]{1,0:T(8,128)(2,1)S(1)}, u32[]{:S(2)}, u32[]{:S(2)}) collective-permute-start(bf16[256,768]{1,0:T(8,128)(2,1)S(1)} %collective-permute-done.9), channel_id=1, source_target_pairs={{4,8},{5,9},{6,10},{7,11},{8,4},{9,5},{10,6},{11,7},{20,24},{21,25... | collective-permute-start | bytes 1179656 | tf_op jit(solution)/shard_map/ppermute | solution.py:228
  52.1 20.7 %collective-permute-start.15 = (bf16[256,768]{1,0:T(8,128)(2,1)S(1)}, bf16[256,768]{1,0:T(8,128)(2,1)S(1)}, u32[]{:S(2)}, u32[]{:S(2)}) collective-permute-start(bf16[256,768]{1,0:T(8,128)(2,1)S(1)} %collective-permute-done.12), channel_id=1, source_target_pairs={{4,0},{5,1},{6,2},{7,3},{8,12},{9,13},{10,14},{11,15},{20,16},{21,... | collective-permute-start | bytes 1179656 | tf_op jit(solution)/shard_map/ppermute | solution.py:228
  64.4 29.3 %collective-permute-start.18 = (bf16[512,384]{1,0:T(8,128)(2,1)S(1)}, bf16[512,384]{1,0:T(8,128)(2,1)S(1)}, u32[]{:S(2)}, u32[]{:S(2)}) collective-permute-start(bf16[512,384]{1,0:T(8,128)(2,1)S(1)} %pad_maximum_fusion.10.refs_0_.refs_1_), channel_id=1, source_target_pairs={{0,4},{1,5},{2,6},{3,7},{4,0},{5,1},{6,2},{7,3},{8,12},{9,13},{10,... | collective-permute-start | bytes 1179656 | tf_op jit(solution)/shard_map/ppermute | solution.py:228
  68.0 29.1 %collective-permute-start.25 = (bf16[512,384]{1,0:T(8,128)(2,1)S(1)}, bf16[512,384]{1,0:T(8,128)(2,1)S(1)}, u32[]{:S(2)}, u32[]{:S(2)}) collective-permute-start(bf16[512,384]{1,0:T(8,128)(2,1)S(1)} %pad_maximum_fusion.10.refs_0_.refs_1_), channel_id=1, source_target_pairs={{4,8},{5,9},{6,10},{7,11},{8,4},{9,5},{10,6},{11,7},{20,24},{21,25... | collective-permute-start | bytes 1179656 | tf_op jit(solution)/shard_map/ppermute | solution.py:228
  68.6 20.9 %collective-permute-start.16 = (bf16[256,768]{1,0:T(8,128)(2,1)S(1)}, bf16[256,768]{1,0:T(8,128)(2,1)S(1)}, u32[]{:S(2)}, u32[]{:S(2)}) collective-permute-start(bf16[256,768]{1,0:T(8,128)(2,1)S(1)} %collective-permute-done.14), channel_id=1, source_target_pairs={{4,0},{5,1},{6,2},{7,3},{8,12},{9,13},{10,14},{11,15},{20,16},{21,... | collective-permute-start | bytes 1179656 | tf_op jit(solution)/shard_map/ppermute | solution.py:228
  93.8 4.5 %collective-permute-start.19 = (bf16[512,384]{1,0:T(8,128)(2,1)S(1)}, bf16[512,384]{1,0:T(8,128)(2,1)S(1)}, u32[]{:S(2)}, u32[]{:S(2)}) collective-permute-start(bf16[512,384]{1,0:T(8,128)(2,1)S(1)} %collective-permute-done.18.refs_1_.refs_2_), channel_id=1, source_target_pairs={{4,8},{5,9},{6,10},{7,11},{8,4},{9,5},{10,6},{11,7},{20,24},{21,25... | collective-permute-start | bytes 1179656 | tf_op jit(solution)/shard_map/ppermute | solution.py:228
  97.0 25.3 %collective-permute-start.31 = (bf16[512,1024]{1,0:T(8,128)(2,1)}, bf16[512,1024]{1,0:T(8,128)(2,1)}, u32[]{:S(2)}, u32[]{:S(2)}) collective-permute-start(bf16[512,1024]{1,0:T(8,128)(2,1)} %shard_map.118), channel_id=1, source_target_pairs={{0,1},{1,0},{2,3},{3,2},{4,5},{5,4},{6,7},{7,6},{8,9},{9,8},{10,11... | collective-permute-start | bytes 3145736 | tf_op jit(solution)/shard_map/ppermute | solution.py:228
  97.0 13.9 %collective-permute-start.26 = (bf16[512,384]{1,0:T(8,128)(2,1)S(1)}, bf16[512,384]{1,0:T(8,128)(2,1)S(1)}, u32[]{:S(2)}, u32[]{:S(2)}) collective-permute-start(bf16[512,384]{1,0:T(8,128)(2,1)S(1)} %collective-permute-done.25.refs_0_.refs_1_), channel_id=1, source_target_pairs={{4,0},{5,1},{6,2},{7,3},{8,12},{9,13},{10,14},{11,15},{20,16},{21,... | collective-permute-start | bytes 1179656 | tf_op jit(solution)/shard_map/ppermute | solution.py:228
  98.3 20.5 %collective-permute-start.20 = (bf16[512,384]{1,0:T(8,128)(2,1)S(1)}, bf16[512,384]{1,0:T(8,128)(2,1)S(1)}, u32[]{:S(2)}, u32[]{:S(2)}) collective-permute-start(bf16[512,384]{1,0:T(8,128)(2,1)S(1)} %collective-permute-done.19.refs_0_.refs_1_), channel_id=1, source_target_pairs={{4,0},{5,1},{6,2},{7,3},{8,12},{9,13},{10,14},{11,15},{20,16},{21,... | collective-permute-start | bytes 1179656 | tf_op jit(solution)/shard_map/ppermute | solution.py:228
  99.6 20.5 %copy-start.17 = (f32[2048]{0:T(1024)S(1)}, f32[2048]{0:T(1024)}, u32[]{:S(2)}) copy-start(f32[2048]{0:T(1024)} %param.13) | copy-start | bytes 24580
  100.4 19.8 %collective-permute-start.54 = (bf16[2,128,384]{2,1,0:T(8,128)(2,1)}, bf16[2,128,384]{2,1,0:T(8,128)(2,1)}, u32[]{:S(2)}, u32[]{:S(2)}) collective-permute-start(bf16[2,128,384]{2,1,0:T(8,128)(2,1)} %get-tuple-element.120), channel_id=1, source_target_pairs={{0,16},{1,17},{2,18},{3,19},{4,20},{5,21},{6,22},{7,23},{8,24},{9,... | collective-permute-start | bytes 589832 | tf_op jit(solution)/shard_map/ppermute | solution.py:228
  112.1 14.2 %collective-permute-start.27 = (bf16[512,512]{1,0:T(8,128)(2,1)}, bf16[512,512]{1,0:T(8,128)(2,1)}, u32[]{:S(2)}, u32[]{:S(2)}) collective-permute-start(bf16[512,512]{1,0:T(8,128)(2,1)} %shard_map.116), channel_id=1, source_target_pairs={{0,1},{1,0},{2,3},{3,2},{4,5},{5,4},{6,7},{7,6},{8,9},{9,8},{10,11... | collective-permute-start | bytes 1572872 | tf_op jit(solution)/shard_map/ppermute | solution.py:228
  120.1 9.3 %collective-permute-start.21 = (bf16[512,512]{1,0:T(8,128)(2,1)}, bf16[512,512]{1,0:T(8,128)(2,1)S(1)}, u32[]{:S(2)}, u32[]{:S(2)}) collective-permute-start(bf16[512,512]{1,0:T(8,128)(2,1)} %shard_map.114), channel_id=1, source_target_pairs={{0,1},{1,0},{2,3},{3,2},{4,5},{5,4},{6,7},{7,6},{8,9},{9,8},{10,11... | collective-permute-start | bytes 1572872 | tf_op jit(solution)/shard_map/ppermute | solution.py:228
  121.3 11.6 %collective-permute-start.55 = (bf16[256,768]{1,0:T(8,128)(2,1)S(1)}, bf16[256,768]{1,0:T(8,128)(2,1)}, u32[]{:S(2)}, u32[]{:S(2)}) collective-permute-start(bf16[256,768]{1,0:T(8,128)(2,1)S(1)} %pad_maximum_fusion.11.refs_8_), channel_id=1, source_target_pairs={{0,4},{1,5},{2,6},{3,7},{4,0},{5,1},{6,2},{7,3},{8,12},{9,13},{10,... | collective-permute-start | bytes 1179656 | tf_op jit(solution)/shard_map/ppermute | solution.py:228
  124.3 18.6 %collective-permute-start.32 = (bf16[128,1024]{1,0:T(8,128)(2,1)S(1)}, bf16[128,1024]{1,0:T(8,128)(2,1)S(1)}, u32[]{:S(2)}, u32[]{:S(2)}) collective-permute-start(bf16[128,1024]{1,0:T(8,128)(2,1)S(1)} %get-tuple-element.62), channel_id=1, source_target_pairs={{0,2},{1,3},{2,0},{3,1},{4,6},{5,7},{6,4},{7,5},{8,10},{9,11},{10,... | collective-permute-start | bytes 786440 | tf_op jit(solution)/shard_map/ppermute | solution.py:228
  124.9 19.6 %collective-permute-start.33 = (bf16[128,1024]{1,0:T(8,128)(2,1)S(1)}, bf16[128,1024]{1,0:T(8,128)(2,1)S(1)}, u32[]{:S(2)}, u32[]{:S(2)}) collective-permute-start(bf16[128,1024]{1,0:T(8,128)(2,1)S(1)} %get-tuple-element.63), channel_id=1, source_target_pairs={{0,16},{1,17},{2,18},{3,19},{4,20},{5,21},{6,22},{7,23},{8,24},{9,... | collective-permute-start | bytes 786440 | tf_op jit(solution)/shard_map/ppermute | solution.py:228
  126.4 18.6 %collective-permute-start.34 = (bf16[128,1024]{1,0:T(8,128)(2,1)S(1)}, bf16[128,1024]{1,0:T(8,128)(2,1)S(1)}, u32[]{:S(2)}, u32[]{:S(2)}) collective-permute-start(bf16[128,1024]{1,0:T(8,128)(2,1)S(1)} %get-tuple-element.64), channel_id=1, source_target_pairs={{0,18},{1,19},{2,16},{3,17},{4,22},{5,23},{6,20},{7,21},{8,26},{9,... | collective-permute-start | bytes 786440 | tf_op jit(solution)/shard_map/ppermute | solution.py:228
  129.4 12.0 %collective-permute-start.28 = (bf16[128,512]{1,0:T(8,128)(2,1)S(1)}, bf16[128,512]{1,0:T(8,128)(2,1)S(1)}, u32[]{:S(2)}, u32[]{:S(2)}) collective-permute-start(bf16[128,512]{1,0:T(8,128)(2,1)S(1)} %get-tuple-element.58), channel_id=1, source_target_pairs={{0,2},{1,3},{2,0},{3,1},{4,6},{5,7},{6,4},{7,5},{8,10},{9,11},{10,... | collective-permute-start | bytes 393224 | tf_op jit(solution)/shard_map/ppermute | solution.py:228
  132.9 13.6 %collective-permute-start.29 = (bf16[128,512]{1,0:T(8,128)(2,1)S(1)}, bf16[128,512]{1,0:T(8,128)(2,1)S(1)}, u32[]{:S(2)}, u32[]{:S(2)}) collective-permute-start(bf16[128,512]{1,0:T(8,128)(2,1)S(1)} %get-tuple-element.59), channel_id=1, source_target_pairs={{0,16},{1,17},{2,18},{3,19},{4,20},{5,21},{6,22},{7,23},{8,24},{9,... | collective-permute-start | bytes 393224 | tf_op jit(solution)/shard_map/ppermute | solution.py:228
  141.4 7.2 %collective-permute-start.30 = (bf16[128,512]{1,0:T(8,128)(2,1)S(1)}, bf16[128,512]{1,0:T(8,128)(2,1)S(1)}, u32[]{:S(2)}, u32[]{:S(2)}) collective-permute-start(bf16[128,512]{1,0:T(8,128)(2,1)S(1)} %get-tuple-element.60), channel_id=1, source_target_pairs={{0,18},{1,19},{2,16},{3,17},{4,22},{5,23},{6,20},{7,21},{8,26},{9,... | collective-permute-start | bytes 393224 | tf_op jit(solution)/shard_map/ppermute | solution.py:228
  142.9 8.6 %collective-permute-start.22 = (bf16[128,512]{1,0:T(8,128)(2,1)S(1)}, bf16[128,512]{1,0:T(8,128)(2,1)S(1)}, u32[]{:S(2)}, u32[]{:S(2)}) collective-permute-start(bf16[128,512]{1,0:T(8,128)(2,1)S(1)} %get-tuple-element.54), channel_id=1, source_target_pairs={{0,2},{1,3},{2,0},{3,1},{4,6},{5,7},{6,4},{7,5},{8,10},{9,11},{10,... | collective-permute-start | bytes 393224 | tf_op jit(solution)/shard_map/ppermute | solution.py:228
  144.4 7.1 %collective-permute-start.23 = (bf16[128,512]{1,0:T(8,128)(2,1)S(1)}, bf16[128,512]{1,0:T(8,128)(2,1)S(1)}, u32[]{:S(2)}, u32[]{:S(2)}) collective-permute-start(bf16[128,512]{1,0:T(8,128)(2,1)S(1)} %get-tuple-element.55), channel_id=1, source_target_pairs={{0,16},{1,17},{2,18},{3,19},{4,20},{5,21},{6,22},{7,23},{8,24},{9,... | collective-permute-start | bytes 393224 | tf_op jit(solution)/shard_map/ppermute | solution.py:228
  144.9 8.0 %collective-permute-start.24 = (bf16[128,512]{1,0:T(8,128)(2,1)S(1)}, bf16[128,512]{1,0:T(8,128)(2,1)S(1)}, u32[]{:S(2)}, u32[]{:S(2)}) collective-permute-start(bf16[128,512]{1,0:T(8,128)(2,1)S(1)} %get-tuple-element.56), channel_id=1, source_target_pairs={{0,18},{1,19},{2,16},{3,17},{4,22},{5,23},{6,20},{7,21},{8,26},{9,... | collective-permute-start | bytes 393224 | tf_op jit(solution)/shard_map/ppermute | solution.py:228
  146.6 9.4 %collective-permute-start.56 = (bf16[256,768]{1,0:T(8,128)(2,1)S(1)}, bf16[256,768]{1,0:T(8,128)(2,1)}, u32[]{:S(2)}, u32[]{:S(2)}) collective-permute-start(bf16[256,768]{1,0:T(8,128)(2,1)S(1)} %pad_maximum_fusion.11.refs_8_), channel_id=1, source_target_pairs={{4,8},{5,9},{6,10},{7,11},{8,4},{9,5},{10,6},{11,7},{20,24},{21,25... | collective-permute-start | bytes 1179656 | tf_op jit(solution)/shard_map/ppermute | solution.py:228
  148.7 8.6 %collective-permute-start.58 = (bf16[256,768]{1,0:T(8,128)(2,1)}, bf16[256,768]{1,0:T(8,128)(2,1)}, u32[]{:S(2)}, u32[]{:S(2)}) collective-permute-start(bf16[256,768]{1,0:T(8,128)(2,1)} %collective-permute-done.55.refs_9_), channel_id=1, source_target_pairs={{4,8},{5,9},{6,10},{7,11},{8,4},{9,5},{10,6},{11,7},{20,24},{21,25... | collective-permute-start | bytes 1179656 | tf_op jit(solution)/shard_map/ppermute | solution.py:228
  155.4 7.0 %collective-permute-start.36 = (bf16[64,2048]{1,0:T(8,128)(2,1)S(1)}, bf16[64,2048]{1,0:T(8,128)(2,1)S(1)}, u32[]{:S(2)}, u32[]{:S(2)}) collective-permute-start(bf16[64,2048]{1,0:T(8,128)(2,1)S(1)} %get-tuple-element.108.refs_0_), channel_id=1, source_target_pairs={{0,2},{1,3},{2,0},{3,1},{4,6},{5,7},{6,4},{7,5},{8,10},{9,11},{10,... | collective-permute-start | bytes 786440 | tf_op jit(solution)/shard_map/ppermute | solution.py:228
  156.0 16.0 %collective-permute-start.57 = (bf16[256,768]{1,0:T(8,128)(2,1)}, bf16[256,768]{1,0:T(8,128)(2,1)S(1)}, u32[]{:S(2)}, u32[]{:S(2)}) collective-permute-start(bf16[256,768]{1,0:T(8,128)(2,1)} %collective-permute-done.56.refs_10_), channel_id=1, source_target_pairs={{4,0},{5,1},{6,2},{7,3},{8,12},{9,13},{10,14},{11,15},{20,16},{21,... | collective-permute-start | bytes 1179656 | tf_op jit(solution)/shard_map/ppermute | solution.py:228
  157.3 22.0 %collective-permute-start.59 = (bf16[256,768]{1,0:T(8,128)(2,1)}, bf16[256,768]{1,0:T(8,128)(2,1)S(1)}, u32[]{:S(2)}, u32[]{:S(2)}) collective-permute-start(bf16[256,768]{1,0:T(8,128)(2,1)} %collective-permute-done.58.refs_12_), channel_id=1, source_target_pairs={{4,0},{5,1},{6,2},{7,3},{8,12},{9,13},{10,14},{11,15},{20,16},{21,... | collective-permute-start | bytes 1179656 | tf_op jit(solution)/shard_map/ppermute | solution.py:228
  158.6 20.9 %collective-permute-start.39 = (bf16[64,2048]{1,0:T(8,128)(2,1)S(1)}, bf16[64,2048]{1,0:T(8,128)(2,1)S(1)}, u32[]{:S(2)}, u32[]{:S(2)}) collective-permute-start(bf16[64,2048]{1,0:T(8,128)(2,1)S(1)} %get-tuple-element.108.refs_0_), channel_id=1, source_target_pairs={{0,1},{1,0},{2,3},{3,2},{4,5},{5,4},{6,7},{7,6},{8,9},{9,8},{10,11... | collective-permute-start | bytes 786440 | tf_op jit(solution)/shard_map/ppermute | solution.py:228
  158.7 20.9 %collective-permute-start.37 = (bf16[64,2048]{1,0:T(8,128)(2,1)S(1)}, bf16[64,2048]{1,0:T(8,128)(2,1)S(1)}, u32[]{:S(2)}, u32[]{:S(2)}) collective-permute-start(bf16[64,2048]{1,0:T(8,128)(2,1)S(1)} %get-tuple-element.108.refs_0_), channel_id=1, source_target_pairs={{0,16},{1,17},{2,18},{3,19},{4,20},{5,21},{6,22},{7,23},{8,24},{9,... | collective-permute-start | bytes 786440 | tf_op jit(solution)/shard_map/ppermute | solution.py:228
  162.3 19.2 %collective-permute-start.38 = (bf16[64,2048]{1,0:T(8,128)(2,1)S(1)}, bf16[64,2048]{1,0:T(8,128)(2,1)S(1)}, u32[]{:S(2)}, u32[]{:S(2)}) collective-permute-start(bf16[64,2048]{1,0:T(8,128)(2,1)S(1)} %get-tuple-element.108.refs_0_), channel_id=1, source_target_pairs={{0,18},{1,19},{2,16},{3,17},{4,22},{5,23},{6,20},{7,21},{8,26},{9,... | collective-permute-start | bytes 786440 | tf_op jit(solution)/shard_map/ppermute | solution.py:228
  172.0 9.6 %collective-permute-start.48 = (bf16[128,512]{1,0:T(8,128)(2,1)S(1)}, bf16[128,512]{1,0:T(8,128)(2,1)S(1)}, u32[]{:S(2)}, u32[]{:S(2)}) collective-permute-start(bf16[128,512]{1,0:T(8,128)(2,1)S(1)} %get-tuple-element.72), channel_id=1, source_target_pairs={{0,4},{1,5},{2,6},{3,7},{4,0},{5,1},{6,2},{7,3},{8,12},{9,13},{10,... | collective-permute-start | bytes 393224 | tf_op jit(solution)/shard_map/ppermute | solution.py:228
  179.3 12.3 %collective-permute-start.40 = (bf16[64,2048]{1,0:T(8,128)(2,1)S(1)}, bf16[64,2048]{1,0:T(8,128)(2,1)S(1)}, u32[]{:S(2)}, u32[]{:S(2)}) collective-permute-start(bf16[64,2048]{1,0:T(8,128)(2,1)S(1)} %collective-permute-done.36.refs_1_), channel_id=1, source_target_pairs={{0,1},{1,0},{2,3},{3,2},{4,5},{5,4},{6,7},{7,6},{8,9},{9,8},{10,11... | collective-permute-start | bytes 786440 | tf_op jit(solution)/shard_map/ppermute | solution.py:228
  179.5 11.6 %collective-permute-start.50 = (bf16[128,512]{1,0:T(8,128)(2,1)S(1)}, bf16[128,512]{1,0:T(8,128)(2,1)S(1)}, u32[]{:S(2)}, u32[]{:S(2)}) collective-permute-start(bf16[128,512]{1,0:T(8,128)(2,1)S(1)} %get-tuple-element.73), channel_id=1, source_target_pairs={{0,8},{1,9},{2,10},{3,11},{4,12},{5,13},{6,14},{7,15},{8,0},{9,1},... | collective-permute-start | bytes 393224 | tf_op jit(solution)/shard_map/ppermute | solution.py:228
  179.6 11.6 %collective-permute-start.52 = (bf16[128,512]{1,0:T(8,128)(2,1)S(1)}, bf16[128,512]{1,0:T(8,128)(2,1)S(1)}, u32[]{:S(2)}, u32[]{:S(2)}) collective-permute-start(bf16[128,512]{1,0:T(8,128)(2,1)S(1)} %get-tuple-element.74), channel_id=1, source_target_pairs={{0,12},{1,13},{2,14},{3,15},{4,8},{5,9},{6,10},{7,11},{8,4},{9,5},... | collective-permute-start | bytes 393224 | tf_op jit(solution)/shard_map/ppermute | solution.py:228
  181.6 11.4 %collective-permute-start.41 = (bf16[64,2048]{1,0:T(8,128)(2,1)S(1)}, bf16[64,2048]{1,0:T(8,128)(2,1)S(1)}, u32[]{:S(2)}, u32[]{:S(2)}) collective-permute-start(bf16[64,2048]{1,0:T(8,128)(2,1)S(1)} %collective-permute-done.37), channel_id=1, source_target_pairs={{0,1},{1,0},{2,3},{3,2},{4,5},{5,4},{6,7},{7,6},{8,9},{9,8},{10,11... | collective-permute-start | bytes 786440 | tf_op jit(solution)/shard_map/ppermute | solution.py:228
  181.6 11.4 %collective-permute-start.42 = (bf16[64,2048]{1,0:T(8,128)(2,1)S(1)}, bf16[64,2048]{1,0:T(8,128)(2,1)S(1)}, u32[]{:S(2)}, u32[]{:S(2)}) collective-permute-start(bf16[64,2048]{1,0:T(8,128)(2,1)S(1)} %collective-permute-done.38), channel_id=1, source_target_pairs={{0,1},{1,0},{2,3},{3,2},{4,5},{5,4},{6,7},{7,6},{8,9},{9,8},{10,11... | collective-permute-start | bytes 786440 | tf_op jit(solution)/shard_map/ppermute | solution.py:228
  191.1 1.3 collective-permute-start.49
  191.2 1.5 collective-permute-start.51
  191.6 1.3 collective-permute-start.53
  192.5 9.5 %collective-permute-start.35 = (bf16[64,2048]{1,0:T(8,128)(2,1)S(1)}, bf16[64,2048]{1,0:T(8,128)(2,1)S(1)}, u32[]{:S(2)}, u32[]{:S(2)}) collective-permute-start(bf16[64,2048]{1,0:T(8,128)(2,1)S(1)} %copy-done.14), channel_id=1, source_target_pairs={{0,1},{1,0},{2,3},{3,2},{4,5},{5,4},{6,7},{7,6},{8,9},{9,8},{10,11... | collective-permute-start | bytes 786440 | tf_op jit(solution)/shard_map/ppermute | solution.py:228
  197.4 14.4 %collective-permute-start.43 = (bf16[256,2048]{1,0:T(8,128)(2,1)S(1)}, bf16[256,2048]{1,0:T(8,128)(2,1)S(1)}, u32[]{:S(2)}, u32[]{:S(2)}) collective-permute-start(bf16[256,2048]{1,0:T(8,128)(2,1)S(1)} %convolution_convert_fusion), channel_id=1, source_target_pairs={{0,1},{1,0},{2,3},{3,2},{4,5},{5,4},{6,7},{7,6},{8,9},{9,8},{10,11... | collective-permute-start | bytes 3145736 | tf_op jit(solution)/shard_map/ppermute | solution.py:228
  200.3 11.4 %collective-permute-start.60 = (bf16[256,768]{1,0:T(8,128)(2,1)S(1)}, bf16[256,768]{1,0:T(8,128)(2,1)S(1)}, u32[]{:S(2)}, u32[]{:S(2)}) collective-permute-start(bf16[256,768]{1,0:T(8,128)(2,1)S(1)} %get-tuple-element.89), channel_id=1, source_target_pairs={{0,2},{1,3},{2,0},{3,1},{4,6},{5,7},{6,4},{7,5},{8,10},{9,11},{10,... | collective-permute-start | bytes 1179656 | tf_op jit(solution)/shard_map/ppermute | solution.py:228
  212.9 14.6 %copy-start.6 = (bf16[128,2048]{1,0:T(8,128)(2,1)S(1)}, bf16[128,2048]{1,0:T(8,128)(2,1)}, u32[]{:S(2)}) copy-start(bf16[128,2048]{1,0:T(8,128)(2,1)} %param.10) | copy-start | bytes 1572868
  213.0 14.9 %copy-start.13 = (bf16[128,2048]{1,0:T(8,128)(2,1)S(1)}, bf16[128,2048]{1,0:T(8,128)(2,1)}, u32[]{:S(2)}) copy-start(bf16[128,2048]{1,0:T(8,128)(2,1)} %param.11) | copy-start | bytes 1572868
  213.0 8.3 %collective-permute-start.44 = (bf16[64,2048]{1,0:T(8,128)(2,1)S(1)}, bf16[64,2048]{1,0:T(8,128)(2,1)S(1)}, u32[]{:S(2)}, u32[]{:S(2)}) collective-permute-start(bf16[64,2048]{1,0:T(8,128)(2,1)S(1)} %get-tuple-element.105), channel_id=1, source_target_pairs={{0,2},{1,3},{2,0},{3,1},{4,6},{5,7},{6,4},{7,5},{8,10},{9,11},{10,... | collective-permute-start | bytes 786440 | tf_op jit(solution)/shard_map/ppermute | solution.py:228
  214.6 9.2 %collective-permute-start.45 = (bf16[64,2048]{1,0:T(8,128)(2,1)S(1)}, bf16[64,2048]{1,0:T(8,128)(2,1)S(1)}, u32[]{:S(2)}, u32[]{:S(2)}) collective-permute-start(bf16[64,2048]{1,0:T(8,128)(2,1)S(1)} %get-tuple-element.107), channel_id=1, source_target_pairs={{0,16},{1,17},{2,18},{3,19},{4,20},{5,21},{6,22},{7,23},{8,24},{9,... | collective-permute-start | bytes 786440 | tf_op jit(solution)/shard_map/ppermute | solution.py:228
  215.1 12.4 %collective-permute-start.46 = (bf16[64,2048]{1,0:T(8,128)(2,1)S(1)}, bf16[64,2048]{1,0:T(8,128)(2,1)S(1)}, u32[]{:S(2)}, u32[]{:S(2)}) collective-permute-start(bf16[64,2048]{1,0:T(8,128)(2,1)S(1)} %get-tuple-element.106), channel_id=1, source_target_pairs={{0,18},{1,19},{2,16},{3,17},{4,22},{5,23},{6,20},{7,21},{8,26},{9,... | collective-permute-start | bytes 786440 | tf_op jit(solution)/shard_map/ppermute | solution.py:228
  228.2 1.6 collective-permute-start.47
  (15 other events, 67.9 us)

commit v4 on v3

--- a/solution.py
+++ b/solution.py
@@ -19,10 +19,6 @@
 
 def tn(left, right):
     return lax.dot_general(left, right, (((0,), (0,)), ((), ())), preferred_element_type=f32)
-
-
-def put(array, value, index):
-    return lax.dynamic_update_index_in_dim(array, value, index, 0)
 
 
 def arrange(values, ids, count, axis=-1):
@@ -87,7 +83,31 @@
         scratch_shapes=[pltpu.SemaphoreType.DMA((len(jobs),))],
         compiler_params=params(*outs) if room is None else pltpu.CompilerParams(vmem_limit_bytes=VMEM - room),
         cost_estimate=pl.CostEstimate(flops=2_000_000, bytes_accessed=1 << 20, transcendentals=0),
-    )(jnp.stack(places).astype(jnp.int32), *sources))
+    )(places, *sources))
+
+
+def in_arrival(table, t, cotangent, gain, m, Z):
+    D = gain.shape[1]
+    B = D // Z
+
+    def kernel(table_ref, core_ref, cot_ref, gain_ref, out_ref, post_ref):
+        rows = pl.ds(pl.multiple_of(core_ref[0] * m, m), m)
+        for k in range(Z):
+            here_ = pl.ds(pl.multiple_of(table_ref[k] * B, B), B)
+            there_ = slice(k * B, (k + 1) * B)
+            scale = gain_ref[:, here_]
+            post_ref[:, there_] = scale
+            out_ref[:, there_] = 0.5 * cot_ref[rows, here_].astype(f32) * scale
+
+    shapes = [jax.ShapeDtypeStruct((m, D), f32), jax.ShapeDtypeStruct((1, D), f32)]
+    return pl.pallas_call(
+        kernel,
+        out_shape=shapes,
+        in_specs=whole(2, 2),
+        out_specs=whole(2),
+        compiler_params=params(cotangent, gain, *shapes),
+        cost_estimate=pl.CostEstimate(flops=4 * m * D, bytes_accessed=8 * m * D, transcendentals=0),
+    )(table, t.reshape(1).astype(jnp.int32), cotangent, gain)
 
 
 def by_slot(zref, slots, refs, count, emit):
@@ -257,7 +277,7 @@
         def block(d):
             return r * G + (y + d) % G
 
-        spots = [block(d) for d in range(G)]
+        spots = jnp.stack([block(d) for d in range(G)]).astype(jnp.int32)
         pairs = [(i, d, w, d, 0, i * w) for d in range(G) for i in range(2)]
         wide = cut(spots, [gate_weight, up_weight], [(K, 2 * w)] * G, pairs)
         thin = cut(spots, [down_weight], [(K, w)] * G, [(0, d, w, d, 0, 0) for d in range(G)])
@@ -285,6 +305,13 @@
         held += [cores(got) for p, got in enumerate(plane(chunk(normed, 0))) if p]
         tokens = jnp.stack([jnp.stack([h[j] for h in held], axis=1) for j in range(T)], axis=1)
         tokens = tokens.reshape(2 * PT * n, D)
+
+        turn = [[i] + [source(i, k, s) for s in range(1, Z) for k in (0, 1) if source(i, k, s) is not None] for i in range(Z)]
+        rows = [t_ + [t_.index(partner(i, k)) for k in range(Z)] + [0] for i, t_ in enumerate(turn)]
+        table = lax.dynamic_slice_in_dim(jnp.asarray(rows, jnp.int32), z, 1, 0).reshape(-1)
+
+        def own_rows(array):
+            return lax.dynamic_slice_in_dim(array, t * m, m, 0)
 
         full = jnp.zeros((Z, G, K, 2 * w), bf16)
 
@@ -301,20 +328,49 @@
                     where = jnp.where(z == i, j, where)
             return where
 
+        final = []
         for s in range(1, Z):
             for d, got in enumerate(lines):
                 for kind, _ in edges(Z, s):
+                    if (s, d) == (Z - 1, G - 1):
+                        final.append((kind, got[s][kind]))
+                        continue
                     full = place(full, got[s][kind], target(kind, s), (y - d) % G)
         for d, piece in enumerate(gu):
             full = place(full, piece, z, (y - d) % G)
-        full = full.reshape(D, 2 * w)
+        most, full_last = full.reshape(D, 2 * w), full
+        ready = [v for v in lines[-1][max(Z - 2, 0)] if v is not None]
+        cot_late, gain_late = lax.optimization_barrier((cotangent, post_gain, ready))[:2]
+        dpost, post = in_arrival(table, t, cot_late, gain_late.reshape(1, D), m, Z)
+        most, dpost, post = lax.optimization_barrier((most, dpost, post))
+        y_last = (y - (G - 1)) % G
+        lasts = []
+        for kind, piece in final:
+            at = (target(kind, Z - 1) * G + y_last) * K
+            lasts.append((piece, lax.dynamic_slice_in_dim(tokens, at, K, 1)))
+
+        def complete(*ready):
+            out = full_last
+            for kind, piece in final:
+                piece, out = lax.optimization_barrier((piece, out) + ready)[:2]
+                spot = target(kind, Z - 1)
+                zs, ys = lax.broadcasted_iota(jnp.int32, (Z, G, 1, 1), 0), lax.broadcasted_iota(jnp.int32, (Z, G, 1, 1), 1)
+                out = jnp.where((zs == spot) & (ys == y_last) & (spot != z), piece[None, None], out)
+            return out.reshape(D, 2 * w)
 
         halves = []
         for i in range(2):
-            value = jnp.dot(tokens[i * PT * n:(i + 1) * PT * n], full, preferred_element_type=f32)
+            rows = slice(i * PT * n, (i + 1) * PT * n)
+            value = jnp.dot(tokens[rows], most, preferred_element_type=f32)
+            value = after(value, *[p for line_ in lines[:-1] for p in line_[Z - 1] if p is not None])
+            for piece, left in lasts:
+                value = value + jnp.dot(left[rows], piece, preferred_element_type=f32)
             gate, up = value[:, :w], value[:, w:]
-            halves.append((jax.nn.silu(gate) * up).astype(bf16).reshape(T, PT * m, w))
-        gate_e, up_e = gate, up
+            sig = jax.nn.sigmoid(gate)
+            halves.append((gate * sig * up).astype(bf16).reshape(T, PT * m, w))
+        for_gate = (up * sig * (1.0 + gate * (1.0 - sig))).astype(bf16)
+        for_up = (gate * sig).astype(bf16)
+        for_gate, for_up = lax.optimization_barrier((for_gate, for_up))
 
         block = arrange(dn, [(y - d) % G for d in range(G)], G, axis=0)
         if Z > 1:
@@ -362,15 +418,10 @@
                 value = sent_product(z_ref, by_core[j], some, Z)
                 got.append(send(value, dt=j))
             low = chip_product(z_ref, by_core[0], got, some, Z, 2, PT)
-            total = plane_sum(low)
-            for i, k in enumerate(group):
-                totals.append(total[:, i * G * K:(i + 1) * G * K])
-                total_ids.append(ids[k])
-        branch = arrange(totals, total_ids, Z)
+            totals.append(plane_sum(low))
+            total_ids += [ids[k] for k in group]
+        branch = jnp.concatenate(totals, axis=-1)
         branch_l, branch_e = branch[:m], branch[m:]
-
-        def own_rows(array):
-            return lax.dynamic_slice_in_dim(array, t * m, m, 0)
 
         def all_rows(value):
             rows = [value] + [send(value, dt=-j) for j in range(1, T)]
@@ -378,30 +429,31 @@
 
         early_rz = lax.rsqrt(jnp.mean(branch_e * branch_e, axis=-1, keepdims=True) + eps)
         cot_f = own_rows(cotangent).astype(f32)
-        dpost = 0.5 * cot_f * post_gain
         dbranch = early_rz * (dpost - branch_e * early_rz * early_rz * jnp.mean(branch_e * dpost, axis=-1, keepdims=True))
         dbranch = dbranch.astype(bf16)
 
         late_rz = lax.rsqrt(jnp.mean(branch_l * branch_l, axis=-1, keepdims=True) + eps)
-        y_late = (own_rows(x_late).astype(f32) + 0.5 * branch_l * late_rz * post_gain).astype(bf16)
+        added = 0.5 * branch_l * late_rz * post
+        added = arrange([added[:, k * G * K:(k + 1) * G * K] for k in range(Z)], total_ids, Z)
+        y_late = (own_rows(x_late).astype(f32) + added).astype(bf16)
         y_late = all_rows(y_late)
 
-        down_full = jnp.zeros((Z, G * K, w), bf16)
         pieces, _ = lax.optimization_barrier(([[v for v, _ in slot] for slot in slots], dbranch))
-        for slot, values, where in zip(slots, pieces, ids):
+        down_full = []
+        for slot, values in zip(slots, pieces):
             value = values[0]
             for other, (_, owners) in zip(values[1:], slot[1:]):
                 value = jnp.where(here(z, owners), other, value)
-            down_full = put(down_full, value, where)
-        down_full = down_full.reshape(D, w)
+            down_full.append(value)
+        down_full = jnp.concatenate(down_full, axis=0)
         raw = plane(dbranch)
         spread = spread_c = [cores(h) for h in raw]
         spread = jnp.stack([jnp.stack([h[j] for h in spread]) for j in range(T)]).reshape(PT * n, D)
         dhidden = jnp.dot(spread, down_full, preferred_element_type=f32)
-        sig = jax.nn.sigmoid(gate_e)
-        dgate = (dhidden * up_e * sig * (1.0 + gate_e * (1.0 - sig))).astype(bf16)
-        dup = (dhidden * gate_e * sig).astype(bf16)
+        dgate = (dhidden * for_gate.astype(f32)).astype(bf16)
+        dup = (dhidden * for_up.astype(f32)).astype(bf16)
         dgu = jnp.concatenate([dgate, dup], axis=1).reshape(T, PT * m, 2 * w)
+        full = complete(dbranch)
         dnormed, dlow = reduce_plane([dgu[j] for j in range(T)], full)
         early_f = own_rows(x_early).astype(f32)
         early_rs = lax.dynamic_slice_in_dim(scale[1], t * m, m, 0)
@@ -416,7 +468,7 @@
         passed = line(units)
         own = [raw[b] for b in range(G)]
         cols = cut(
-            [partner(z, k) for k in range(Z)], own, [(G * m, G * K)] * Z, [(b, k, G * K, k, b * m, 0) for k in range(Z) for b in range(G)])
+            table, own, [(G * m, G * K)] * Z, [(b, Z + k, G * K, k, b * m, 0) for k in range(Z) for b in range(G)])
         cols = [value if k == 0 else send(value, moves=[(i, partner(i, k)) for i in range(Z)]) for k, value in enumerate(cols)]
         mates = [[spread_c[b][j] for b in range(G)] for j in range(T)]
         left = []
@@ -426,7 +478,7 @@
                 if k:
                     left.append(send(value, dt=-j))
                 else:
-                    left.extend(cut([z], mates[j], [(G * m, G * K)], [(b, 0, G * K, 0, b * m, 0) for b in range(G)]))
+                    left.extend(cut(table, mates[j], [(G * m, G * K)], [(b, Z, G * K, 0, b * m, 0) for b in range(G)]))
         right, cases = [units], [[(0, 0)] for _ in range(Z)]
         for s in range(1, Z):
             for kind, _ in edges(Z, s):
@@ -439,12 +491,17 @@
         grads = weight_gradient(jnp.stack([z, y]), left, right, cases, T, G)
         pieces, sources = [], []
         for b in range(G):
-            piece = send(grads[b], dy=b).astype(f32) if b else grads[0]
+            piece = send(grads[b], dy=b) if b else grads[0]
             for a in range(R):
                 pieces.append(piece[:, a * w:(a + 1) * w])
                 sources.append((r - a) % R * G + (y - b) % G)
-        summed = arrange(pieces, sources, R * G)
-        return (y_late, dx_early, down_grad_sum + summed)
+        mine, theirs = pieces[:R], pieces[R:]
+        blank = [jnp.zeros((K, w), f32)] * (len(pieces) - R)
+        partly = down_grad_sum + arrange(mine + blank, sources, R * G)
+        if theirs:
+            partly, theirs = lax.optimization_barrier((partly, theirs))
+        total = partly + arrange([jnp.zeros((K, w), bf16)] * R + theirs, sources, R * G).astype(f32)
+        return (y_late, dx_early, total)
 
     return body
 

time: 232 us -> 229 us (0.987)
  waiting for transfers between devices: 125 us -> 119 us
  starting transfers between devices: 61.6 us -> 66 us
    ppermute x61, waiting for transfers between devices: 125 us -> 119 us  [send(): return lax.ppermute(value, AXES, pairs)]
    ppermute x61, starting transfers between devices: 61.6 us -> 66 us  [send(): return lax.ppermute(value, AXES, pairs)]
    unnamed x36 -> x38, local copies, waits for them, and re-layouts: 4.79 us -> 3.95 us
  transfers between devices with their start and end apart: 61 -> 61, of which waited for: 24 -> 25; matrix products, arithmetic and copies ran while one was open for 10% -> 10% of each run, Pallas kernels for 5% -> 6%
where the time goes in v4:
time: 229 us; the launch traced here: 228 us
  waiting for transfers between devices  119 us (52%)
  starting transfers between devices  66 us (29%)
  Pallas kernels  13.2 us (6%)
  other arithmetic  11.8 us (5%)
  local copies, waits for them, and re-layouts  8.68 us (4%)
  matrix products  7.69 us (3%)
    ppermute x61, waiting for transfers between devices, send(): return lax.ppermute(value, AXES, pairs)  119 us
    ppermute x61, starting transfers between devices, send(): return lax.ppermute(value, AXES, pairs)  66 us
  transfers between devices with their start and end apart: 61, of which 25 were waited for; matrix products, arithmetic and copies ran while one was open for 10% of the time, Pallas kernels for 6%

profile of v4, /device:TPU:0, one launch (start us, length us, event | category | flops | bytes accessed | tf_op | source)
XLA Modules:
  0.0 228.2 jit_solution(1447687813975341381)
XLA Ops:
  0.8 1.1 copy-done.2
  1.9 1.1 copy-done.3
  3.7 3.1 %collective-permute-start.6 = (bf16[256,768]{1,0:T(8,128)(2,1)S(1)}, bf16[256,768]{1,0:T(8,128)(2,1)S(1)}, u32[]{:S(2)}, u32[]{:S(2)}) collective-permute-start(bf16[256,768]{1,0:T(8,128)(2,1)S(1)} %get-tuple-element.63), channel_id=1, source_target_pairs={{0,4},{1,5},{2,6},{3,7},{4,0},{5,1},{6,2},{7,3},{8,12},{9,13},{10,... | collective-permute-start | bytes 1179656 | tf_op jit(solution)/shard_map/ppermute | solution.py:248
  7.5 1.6 collective-permute-start.17
  11.2 1.5 collective-permute-start.1
  12.7 1.5 collective-permute-start.8
  16.0 2.6 %collective-permute-start.2 = (bf16[2,64,2048]{2,1,0:T(8,128)(2,1)S(1)}, bf16[2,64,2048]{2,1,0:T(8,128)(2,1)S(1)}, u32[]{:S(2)}, u32[]{:S(2)}) collective-permute-start(bf16[2,64,2048]{2,1,0:T(8,128)(2,1)S(1)} %bitcast.113), channel_id=1, source_target_pairs={{0,18},{1,19},{2,16},{3,17},{4,22},{5,23},{6,20},{7,21},{8,26},{9,... | collective-permute-start | bytes 1572872 | tf_op jit(solution)/shard_map/ppermute | solution.py:248
  18.6 26.3 %collective-permute-done.8 = bf16[256,768]{1,0:T(8,128)(2,1)} collective-permute-done((bf16[256,768]{1,0:T(8,128)(2,1)S(1)}, bf16[256,768]{1,0:T(8,128)(2,1)}, u32[]{:S(2)}, u32[]{:S(2)}) %collective-permute-start.8) | collective-permute-done | bytes 393248 | tf_op jit(solution)/shard_map/ppermute | solution.py:248
  46.5 1.3 collective-permute-start.11
  48.9 8.2 %collective-permute-done.9 = bf16[256,768]{1,0:T(8,128)(2,1)S(1)} collective-permute-done((bf16[256,768]{1,0:T(8,128)(2,1)}, bf16[256,768]{1,0:T(8,128)(2,1)S(1)}, u32[]{:S(2)}, u32[]{:S(2)}) %collective-permute-start.9) | collective-permute-done | bytes 393248 | tf_op jit(solution)/shard_map/ppermute | solution.py:248
  57.7 5.6 %collective-permute-done.11 = bf16[256,768]{1,0:T(8,128)(2,1)S(1)} collective-permute-done((bf16[256,768]{1,0:T(8,128)(2,1)S(1)}, bf16[256,768]{1,0:T(8,128)(2,1)S(1)}, u32[]{:S(2)}, u32[]{:S(2)}) %collective-permute-start.11) | collective-permute-done | bytes 393248 | tf_op jit(solution)/shard_map/ppermute | solution.py:248
  63.3 1.3 collective-permute-start.13
  65.4 1.3 collective-permute-start.15
  68.4 8.8 %collective-permute-done.13 = bf16[256,768]{1,0:T(8,128)(2,1)S(1)} collective-permute-done((bf16[256,768]{1,0:T(8,128)(2,1)S(1)}, bf16[256,768]{1,0:T(8,128)(2,1)S(1)}, u32[]{:S(2)}, u32[]{:S(2)}) %collective-permute-start.13) | collective-permute-done | bytes 393248 | tf_op jit(solution)/shard_map/ppermute | solution.py:248
  78.9 6.7 %collective-permute-done.15 = bf16[256,768]{1,0:T(8,128)(2,1)S(1)} collective-permute-done((bf16[256,768]{1,0:T(8,128)(2,1)S(1)}, bf16[256,768]{1,0:T(8,128)(2,1)S(1)}, u32[]{:S(2)}, u32[]{:S(2)}) %collective-permute-start.15) | collective-permute-done | bytes 393248 | tf_op jit(solution)/shard_map/ppermute | solution.py:248
  87.4 1.8 fusion.44
  89.2 1.3 collective-permute-start.16
  90.5 1.8 fusion.43
  92.3 7.1 %collective-permute-done.16 = bf16[256,768]{1,0:T(8,128)(2,1)S(1)} collective-permute-done((bf16[256,768]{1,0:T(8,128)(2,1)S(1)}, bf16[256,768]{1,0:T(8,128)(2,1)S(1)}, u32[]{:S(2)}, u32[]{:S(2)}) %collective-permute-start.16) | collective-permute-done | bytes 393248 | tf_op jit(solution)/shard_map/ppermute | solution.py:248
  99.8 1.3 fusion.31
  102.5 1.7 shard_map.124
  104.9 1.3 collective-permute-start.24
  106.3 1.6 collective-permute-start.54
  107.8 10.7 %collective-permute-done.24.refs_1_.refs_2_ = bf16[512,384]{1,0:T(8,128)(2,1)S(1)} collective-permute-done((bf16[512,384]{1,0:T(8,128)(2,1)S(1)}, bf16[512,384]{1,0:T(8,128)(2,1)S(1)}, u32[]{:S(2)}, u32[]{:S(2)}) %collective-permute-start.24) | collective-permute-done | bytes 393248 | tf_op jit(solution)/shard_map/ppermute | solution.py:248
  118.5 1.3 shard_map.126
  119.8 1.3 collective-permute-start.30
  121.9 2.7 %collective-permute-start.55 = (bf16[256,768]{1,0:T(8,128)(2,1)}, bf16[256,768]{1,0:T(8,128)(2,1)}, u32[]{:S(2)}, u32[]{:S(2)}) collective-permute-start(bf16[256,768]{1,0:T(8,128)(2,1)} %pad_maximum_fusion.11.refs_8_), channel_id=1, source_target_pairs={{0,4},{1,5},{2,6},{3,7},{4,0},{5,1},{6,2},{7,3},{8,12},{9,13},{10,... | collective-permute-start | bytes 1179656 | tf_op jit(solution)/shard_map/ppermute | solution.py:248
  124.5 1.4 collective-permute-start.56
  126.1 7.6 %collective-permute-done.30.refs_1_.refs_2_ = bf16[512,384]{1,0:T(8,128)(2,1)S(1)} collective-permute-done((bf16[512,384]{1,0:T(8,128)(2,1)S(1)}, bf16[512,384]{1,0:T(8,128)(2,1)S(1)}, u32[]{:S(2)}, u32[]{:S(2)}) %collective-permute-start.30) | collective-permute-done | bytes 393248 | tf_op jit(solution)/shard_map/ppermute | solution.py:248
  135.2 6.5 %collective-permute-done.55.refs_9_ = bf16[256,768]{1,0:T(8,128)(2,1)} collective-permute-done((bf16[256,768]{1,0:T(8,128)(2,1)}, bf16[256,768]{1,0:T(8,128)(2,1)}, u32[]{:S(2)}, u32[]{:S(2)}) %collective-permute-start.55) | collective-permute-done | bytes 393248 | tf_op jit(solution)/shard_map/ppermute | solution.py:248
  142.4 1.5 shard_map.127
  143.9 1.6 collective-permute-start.26
  145.5 1.5 collective-permute-start.27
  147.6 2.0 shard_map.125
  149.5 1.6 collective-permute-start.20
  151.7 1.5 collective-permute-start.21
  153.2 1.1 collective-permute-done.28
  154.3 2.0 collective-permute-start.22
  156.4 1.3 collective-permute-start.57
  157.7 1.3 collective-permute-start.59
  160.2 1.3 collective-permute-start.32
  161.5 1.5 collective-permute-start.33
  163.0 2.9 %collective-permute-done.22 = bf16[128,1024]{1,0:T(8,128)(2,1)S(1)} collective-permute-done((bf16[128,1024]{1,0:T(8,128)(2,1)S(1)}, bf16[128,1024]{1,0:T(8,128)(2,1)S(1)}, u32[]{:S(2)}, u32[]{:S(2)}) %collective-permute-start.22) | collective-permute-done | bytes 262176 | tf_op jit(solution)/shard_map/ppermute | solution.py:248
  165.9 2.2 collective-permute-start.34
  168.5 3.3 %collective-permute-done.34 = bf16[128,512]{1,0:T(8,128)(2,1)S(1)} collective-permute-done((bf16[128,512]{1,0:T(8,128)(2,1)S(1)}, bf16[128,512]{1,0:T(8,128)(2,1)S(1)}, u32[]{:S(2)}, u32[]{:S(2)}) %collective-permute-start.34) | collective-permute-done | bytes 131104 | tf_op jit(solution)/shard_map/ppermute | solution.py:248
  172.4 1.4 collective-permute-start.36
  175.1 1.6 collective-permute-start.37
  176.7 2.2 collective-permute-done.36.refs_1_
  178.9 2.2 collective-permute-start.38
  181.9 2.5 %collective-permute-start.48 = (bf16[128,512]{1,0:T(8,128)(2,1)S(1)}, bf16[128,512]{1,0:T(8,128)(2,1)S(1)}, u32[]{:S(2)}, u32[]{:S(2)}) collective-permute-start(bf16[128,512]{1,0:T(8,128)(2,1)S(1)} %get-tuple-element.101), channel_id=1, source_target_pairs={{0,4},{1,5},{2,6},{3,7},{4,0},{5,1},{6,2},{7,3},{8,12},{9,13},{10,... | collective-permute-start | bytes 393224 | tf_op jit(solution)/shard_map/ppermute | solution.py:248
  184.4 2.1 collective-permute-start.50
  186.5 2.7 %collective-permute-done.38 = bf16[64,2048]{1,0:T(8,128)(2,1)S(1)} collective-permute-done((bf16[64,2048]{1,0:T(8,128)(2,1)S(1)}, bf16[64,2048]{1,0:T(8,128)(2,1)S(1)}, u32[]{:S(2)}, u32[]{:S(2)}) %collective-permute-start.38) | collective-permute-done | bytes 262176 | tf_op jit(solution)/shard_map/ppermute | solution.py:248
  189.2 2.8 %collective-permute-start.52 = (bf16[128,512]{1,0:T(8,128)(2,1)S(1)}, bf16[128,512]{1,0:T(8,128)(2,1)S(1)}, u32[]{:S(2)}, u32[]{:S(2)}) collective-permute-start(bf16[128,512]{1,0:T(8,128)(2,1)S(1)} %get-tuple-element.103), channel_id=1, source_target_pairs={{0,12},{1,13},{2,14},{3,15},{4,8},{5,9},{6,10},{7,11},{8,4},{9,5},... | collective-permute-start | bytes 393224 | tf_op jit(solution)/shard_map/ppermute | solution.py:248
  192.7 4.6 %collective-permute-done.50.refs_4_ = bf16[128,512]{1,0:T(8,128)(2,1)S(1)} collective-permute-done((bf16[128,512]{1,0:T(8,128)(2,1)S(1)}, bf16[128,512]{1,0:T(8,128)(2,1)S(1)}, u32[]{:S(2)}, u32[]{:S(2)}) %collective-permute-start.50) | collective-permute-done | bytes 131104 | tf_op jit(solution)/shard_map/ppermute | solution.py:248
  199.3 2.6 %shard_map.132 = (f32[256,768]{1,0:T(8,128)S(1)}, bf16[256,768]{1,0:T(8,128)(2,1)S(1)}) custom-call(s32[2]{0:T(128)S(1)} %pad_add_fusion.1.place_ref, bf16[128,512]{1,0:T(8,128)(2,1)S(1)} %get-tuple-element.104.refs_0_, bf16[128,512]{1,0:T(8,128)(2,1)S(1)} %shard_map.131.refs_1_, bf16[128,512]{1,0:T(8,128)(2,1)S(1)} %collective-permute-done.48.refs_2_, ...), custom_call_target="tpu_custom_call" | custom-call | flops 805306368 | bytes 4194304 | tf_op jit(solution)/shard_map/pallas_call | solution.py:202
  203.3 1.3 multiply_convert_fusion.1
  207.2 1.2 collective-permute-done.43
  208.4 1.0 add_convert_fusion
  209.6 2.0 collective-permute-start.44
  211.9 1.2 collective-permute-start.46
  214.1 5.4 %collective-permute-done.44 = bf16[64,2048]{1,0:T(8,128)(2,1)S(1)} collective-permute-done((bf16[64,2048]{1,0:T(8,128)(2,1)S(1)}, bf16[64,2048]{1,0:T(8,128)(2,1)S(1)}, u32[]{:S(2)}, u32[]{:S(2)}) %collective-permute-start.44) | collective-permute-done | bytes 262176 | tf_op jit(solution)/shard_map/ppermute | solution.py:248
  219.5 1.2 collective-permute-done.45
  220.8 4.3 %collective-permute-done.46 = bf16[64,2048]{1,0:T(8,128)(2,1)S(1)} collective-permute-done((bf16[64,2048]{1,0:T(8,128)(2,1)S(1)}, bf16[64,2048]{1,0:T(8,128)(2,1)S(1)}, u32[]{:S(2)}, u32[]{:S(2)}) %collective-permute-start.46) | collective-permute-done | bytes 262176 | tf_op jit(solution)/shard_map/ppermute | solution.py:248
  225.8 1.4 convert_add_fusion
  (186 shorter events, 35.3 us)
Async XLA Ops:
  3.7 12.2 %collective-permute-start.6 = (bf16[256,768]{1,0:T(8,128)(2,1)S(1)}, bf16[256,768]{1,0:T(8,128)(2,1)S(1)}, u32[]{:S(2)}, u32[]{:S(2)}) collective-permute-start(bf16[256,768]{1,0:T(8,128)(2,1)S(1)} %get-tuple-element.63), channel_id=1, source_target_pairs={{0,4},{1,5},{2,6},{3,7},{4,0},{5,1},{6,2},{7,3},{8,12},{9,13},{10,... | collective-permute-start | bytes 1179656 | tf_op jit(solution)/shard_map/ppermute | solution.py:248
  7.5 7.8 %collective-permute-start.17 = (bf16[256,384]{1,0:T(8,128)(2,1)S(1)}, bf16[256,384]{1,0:T(8,128)(2,1)S(1)}, u32[]{:S(2)}, u32[]{:S(2)}) collective-permute-start(bf16[256,384]{1,0:T(8,128)(2,1)S(1)} %get-tuple-element.73), channel_id=1, source_target_pairs={{0,2},{1,3},{2,0},{3,1},{4,6},{5,7},{6,4},{7,5},{8,10},{9,11},{10,... | collective-permute-start | bytes 589832 | tf_op jit(solution)/shard_map/ppermute | solution.py:248
  10.7 35.9 %collective-permute-start = (bf16[2,64,2048]{2,1,0:T(8,128)(2,1)S(1)}, bf16[2,64,2048]{2,1,0:T(8,128)(2,1)S(1)}, u32[]{:S(2)}, u32[]{:S(2)}) collective-permute-start(bf16[2,64,2048]{2,1,0:T(8,128)(2,1)S(1)} %bitcast.111), channel_id=1, source_target_pairs={{0,2},{1,3},{2,0},{3,1},{4,6},{5,7},{6,4},{7,5},{8,10},{9,11},{10,... | collective-permute-start | bytes 1572872 | tf_op jit(solution)/shard_map/ppermute | solution.py:248
  11.2 36.7 %collective-permute-start.1 = (bf16[2,64,2048]{2,1,0:T(8,128)(2,1)S(1)}, bf16[2,64,2048]{2,1,0:T(8,128)(2,1)S(1)}, u32[]{:S(2)}, u32[]{:S(2)}) collective-permute-start(bf16[2,64,2048]{2,1,0:T(8,128)(2,1)S(1)} %bitcast.112), channel_id=1, source_target_pairs={{0,16},{1,17},{2,18},{3,19},{4,20},{5,21},{6,22},{7,23},{8,24},{9,... | collective-permute-start | bytes 1572872 | tf_op jit(solution)/shard_map/ppermute | solution.py:248
  12.7 32.2 %collective-permute-start.8 = (bf16[256,768]{1,0:T(8,128)(2,1)S(1)}, bf16[256,768]{1,0:T(8,128)(2,1)}, u32[]{:S(2)}, u32[]{:S(2)}) collective-permute-start(bf16[256,768]{1,0:T(8,128)(2,1)S(1)} %get-tuple-element.65), channel_id=1, source_target_pairs={{0,2},{1,3},{2,0},{3,1},{4,6},{5,7},{6,4},{7,5},{8,10},{9,11},{10,... | collective-permute-start | bytes 1179656 | tf_op jit(solution)/shard_map/ppermute | solution.py:248
  15.2 30.6 %collective-permute-start.7 = (bf16[256,768]{1,0:T(8,128)(2,1)S(1)}, bf16[256,768]{1,0:T(8,128)(2,1)S(1)}, u32[]{:S(2)}, u32[]{:S(2)}) collective-permute-start(bf16[256,768]{1,0:T(8,128)(2,1)S(1)} %get-tuple-element.63), channel_id=1, source_target_pairs={{4,8},{5,9},{6,10},{7,11},{8,4},{9,5},{10,6},{11,7},{20,24},{21,25... | collective-permute-start | bytes 1179656 | tf_op jit(solution)/shard_map/ppermute | solution.py:248
  16.0 32.6 %collective-permute-start.2 = (bf16[2,64,2048]{2,1,0:T(8,128)(2,1)S(1)}, bf16[2,64,2048]{2,1,0:T(8,128)(2,1)S(1)}, u32[]{:S(2)}, u32[]{:S(2)}) collective-permute-start(bf16[2,64,2048]{2,1,0:T(8,128)(2,1)S(1)} %bitcast.113), channel_id=1, source_target_pairs={{0,18},{1,19},{2,16},{3,17},{4,22},{5,23},{6,20},{7,21},{8,26},{9,... | collective-permute-start | bytes 1572872 | tf_op jit(solution)/shard_map/ppermute | solution.py:248
  44.9 12.2 %collective-permute-start.9 = (bf16[256,768]{1,0:T(8,128)(2,1)}, bf16[256,768]{1,0:T(8,128)(2,1)S(1)}, u32[]{:S(2)}, u32[]{:S(2)}) collective-permute-start(bf16[256,768]{1,0:T(8,128)(2,1)} %collective-permute-done.8), channel_id=1, source_target_pairs={{0,4},{1,5},{2,6},{3,7},{4,0},{5,1},{6,2},{7,3},{8,12},{9,13},{10,... | collective-permute-start | bytes 1179656 | tf_op jit(solution)/shard_map/ppermute | solution.py:248
  45.8 11.3 %collective-permute-start.10 = (bf16[256,768]{1,0:T(8,128)(2,1)}, bf16[256,768]{1,0:T(8,128)(2,1)S(1)}, u32[]{:S(2)}, u32[]{:S(2)}) collective-permute-start(bf16[256,768]{1,0:T(8,128)(2,1)} %collective-permute-done.8), channel_id=1, source_target_pairs={{4,8},{5,9},{6,10},{7,11},{8,4},{9,5},{10,6},{11,7},{20,24},{21,25... | collective-permute-start | bytes 1179656 | tf_op jit(solution)/shard_map/ppermute | solution.py:248
  46.5 16.8 %collective-permute-start.11 = (bf16[256,768]{1,0:T(8,128)(2,1)S(1)}, bf16[256,768]{1,0:T(8,128)(2,1)S(1)}, u32[]{:S(2)}, u32[]{:S(2)}) collective-permute-start(bf16[256,768]{1,0:T(8,128)(2,1)S(1)} %collective-permute-done.7), channel_id=1, source_target_pairs={{4,0},{5,1},{6,2},{7,3},{8,12},{9,13},{10,14},{11,15},{20,16},{21,... | collective-permute-start | bytes 1179656 | tf_op jit(solution)/shard_map/ppermute | solution.py:248
  47.9 16.8 %collective-permute-start.12 = (bf16[256,768]{1,0:T(8,128)(2,1)S(1)}, bf16[256,768]{1,0:T(8,128)(2,1)S(1)}, u32[]{:S(2)}, u32[]{:S(2)}) collective-permute-start(bf16[256,768]{1,0:T(8,128)(2,1)S(1)} %collective-permute-done.6), channel_id=1, source_target_pairs={{4,8},{5,9},{6,10},{7,11},{8,4},{9,5},{10,6},{11,7},{20,24},{21,25... | collective-permute-start | bytes 1179656 | tf_op jit(solution)/shard_map/ppermute | solution.py:248
  48.6 16.8 %collective-permute-start.3 = (bf16[2,64,2048]{2,1,0:T(8,128)(2,1)S(1)}, bf16[2,64,2048]{2,1,0:T(8,128)(2,1)S(1)}, u32[]{:S(2)}, u32[]{:S(2)}) collective-permute-start(bf16[2,64,2048]{2,1,0:T(8,128)(2,1)S(1)} %collective-permute-done), channel_id=1, source_target_pairs={{0,1},{1,0},{2,3},{3,2},{4,5},{5,4},{6,7},{7,6},{8,9},{9,8},{10,11... | collective-permute-start | bytes 1572872 | tf_op jit(solution)/shard_map/ppermute | solution.py:248
  48.9 17.8 %copy-start.12 = (bf16[2,1,64,2048]{3,2,1,0:T(8,128)(2,1)S(1)}, bf16[2,1,64,2048]{3,2,1,0:T(8,128)(2,1)}, u32[]{:S(2)}) copy-start(bf16[2,1,64,2048]{3,2,1,0:T(8,128)(2,1)} %get-tuple-element.136) | copy-start | bytes 1572868
  57.1 9.6 %collective-permute-start.4 = (bf16[2,64,2048]{2,1,0:T(8,128)(2,1)S(1)}, bf16[2,64,2048]{2,1,0:T(8,128)(2,1)S(1)}, u32[]{:S(2)}, u32[]{:S(2)}) collective-permute-start(bf16[2,64,2048]{2,1,0:T(8,128)(2,1)S(1)} %collective-permute-done.1), channel_id=1, source_target_pairs={{0,1},{1,0},{2,3},{3,2},{4,5},{5,4},{6,7},{7,6},{8,9},{9,8},{10,11... | collective-permute-start | bytes 1572872 | tf_op jit(solution)/shard_map/ppermute | solution.py:248
  57.1 9.6 %collective-permute-start.5 = (bf16[2,64,2048]{2,1,0:T(8,128)(2,1)S(1)}, bf16[2,64,2048]{2,1,0:T(8,128)(2,1)S(1)}, u32[]{:S(2)}, u32[]{:S(2)}) collective-permute-start(bf16[2,64,2048]{2,1,0:T(8,128)(2,1)S(1)} %collective-permute-done.2), channel_id=1, source_target_pairs={{0,1},{1,0},{2,3},{3,2},{4,5},{5,4},{6,7},{7,6},{8,9},{9,8},{10,11... | collective-permute-start | bytes 1572872 | tf_op jit(solution)/shard_map/ppermute | solution.py:248
  63.3 13.9 %collective-permute-start.13 = (bf16[256,768]{1,0:T(8,128)(2,1)S(1)}, bf16[256,768]{1,0:T(8,128)(2,1)S(1)}, u32[]{:S(2)}, u32[]{:S(2)}) collective-permute-start(bf16[256,768]{1,0:T(8,128)(2,1)S(1)} %collective-permute-done.10), channel_id=1, source_target_pairs={{4,0},{5,1},{6,2},{7,3},{8,12},{9,13},{10,14},{11,15},{20,16},{21,... | collective-permute-start | bytes 1179656 | tf_op jit(solution)/shard_map/ppermute | solution.py:248
  64.7 12.5 %collective-permute-start.14 = (bf16[256,768]{1,0:T(8,128)(2,1)S(1)}, bf16[256,768]{1,0:T(8,128)(2,1)S(1)}, u32[]{:S(2)}, u32[]{:S(2)}) collective-permute-start(bf16[256,768]{1,0:T(8,128)(2,1)S(1)} %collective-permute-done.9), channel_id=1, source_target_pairs={{4,8},{5,9},{6,10},{7,11},{8,4},{9,5},{10,6},{11,7},{20,24},{21,25... | collective-permute-start | bytes 1179656 | tf_op jit(solution)/shard_map/ppermute | solution.py:248
  65.4 20.2 %collective-permute-start.15 = (bf16[256,768]{1,0:T(8,128)(2,1)S(1)}, bf16[256,768]{1,0:T(8,128)(2,1)S(1)}, u32[]{:S(2)}, u32[]{:S(2)}) collective-permute-start(bf16[256,768]{1,0:T(8,128)(2,1)S(1)} %collective-permute-done.12), channel_id=1, source_target_pairs={{4,0},{5,1},{6,2},{7,3},{8,12},{9,13},{10,14},{11,15},{20,16},{21,... | collective-permute-start | bytes 1179656 | tf_op jit(solution)/shard_map/ppermute | solution.py:248
  68.4 17.3 %copy-start = (bf16[128,2048]{1,0:T(8,128)(2,1)S(1)}, bf16[128,2048]{1,0:T(8,128)(2,1)}, u32[]{:S(2)}) copy-start(bf16[128,2048]{1,0:T(8,128)(2,1)} %cot_ref) | copy-start | bytes 1572868
  68.4 17.3 %copy-start.5 = (f32[2048]{0:T(1024)S(1)}, f32[2048]{0:T(1024)}, u32[]{:S(2)}) copy-start(f32[2048]{0:T(1024)} %param.14) | copy-start | bytes 24580
  77.2 25.3 %collective-permute-start.18 = (bf16[512,384]{1,0:T(8,128)(2,1)S(1)}, bf16[512,384]{1,0:T(8,128)(2,1)S(1)}, u32[]{:S(2)}, u32[]{:S(2)}) collective-permute-start(bf16[512,384]{1,0:T(8,128)(2,1)S(1)} %pad_maximum_fusion.10.refs_0_.refs_1_), channel_id=1, source_target_pairs={{0,4},{1,5},{2,6},{3,7},{4,0},{5,1},{6,2},{7,3},{8,12},{9,13},{10,... | collective-permute-start | bytes 1179656 | tf_op jit(solution)/shard_map/ppermute | solution.py:248
  78.1 26.8 %collective-permute-start.23 = (bf16[512,384]{1,0:T(8,128)(2,1)S(1)}, bf16[512,384]{1,0:T(8,128)(2,1)S(1)}, u32[]{:S(2)}, u32[]{:S(2)}) collective-permute-start(bf16[512,384]{1,0:T(8,128)(2,1)S(1)} %pad_maximum_fusion.10.refs_0_.refs_1_), channel_id=1, source_target_pairs={{4,8},{5,9},{6,10},{7,11},{8,4},{9,5},{10,6},{11,7},{20,24},{21,25... | collective-permute-start | bytes 1179656 | tf_op jit(solution)/shard_map/ppermute | solution.py:248
  89.2 10.2 %collective-permute-start.16 = (bf16[256,768]{1,0:T(8,128)(2,1)S(1)}, bf16[256,768]{1,0:T(8,128)(2,1)S(1)}, u32[]{:S(2)}, u32[]{:S(2)}) collective-permute-start(bf16[256,768]{1,0:T(8,128)(2,1)S(1)} %collective-permute-done.14), channel_id=1, source_target_pairs={{4,0},{5,1},{6,2},{7,3},{8,12},{9,13},{10,14},{11,15},{20,16},{21,... | collective-permute-start | bytes 1179656 | tf_op jit(solution)/shard_map/ppermute | solution.py:248
  104.2 42.8 %collective-permute-start.19 = (bf16[512,1024]{1,0:T(8,128)(2,1)}, bf16[512,1024]{1,0:T(8,128)(2,1)}, u32[]{:S(2)}, u32[]{:S(2)}) collective-permute-start(bf16[512,1024]{1,0:T(8,128)(2,1)} %shard_map.124), channel_id=1, source_target_pairs={{0,1},{1,0},{2,3},{3,2},{4,5},{5,4},{6,7},{7,6},{8,9},{9,8},{10,11... | collective-permute-start | bytes 3145736 | tf_op jit(solution)/shard_map/ppermute | solution.py:248
  104.2 15.5 %collective-permute-start.29 = (bf16[512,384]{1,0:T(8,128)(2,1)S(1)}, bf16[512,384]{1,0:T(8,128)(2,1)S(1)}, u32[]{:S(2)}, u32[]{:S(2)}) collective-permute-start(bf16[512,384]{1,0:T(8,128)(2,1)S(1)} %collective-permute-done.18.refs_1_.refs_2_), channel_id=1, source_target_pairs={{4,8},{5,9},{6,10},{7,11},{8,4},{9,5},{10,6},{11,7},{20,24},{21,25... | collective-permute-start | bytes 1179656 | tf_op jit(solution)/shard_map/ppermute | solution.py:248
  104.9 13.6 %collective-permute-start.24 = (bf16[512,384]{1,0:T(8,128)(2,1)S(1)}, bf16[512,384]{1,0:T(8,128)(2,1)S(1)}, u32[]{:S(2)}, u32[]{:S(2)}) collective-permute-start(bf16[512,384]{1,0:T(8,128)(2,1)S(1)} %collective-permute-done.23.refs_0_.refs_1_), channel_id=1, source_target_pairs={{4,0},{5,1},{6,2},{7,3},{8,12},{9,13},{10,14},{11,15},{20,16},{21,... | collective-permute-start | bytes 1179656 | tf_op jit(solution)/shard_map/ppermute | solution.py:248
  106.3 14.8 %collective-permute-start.54 = (bf16[2,128,384]{2,1,0:T(8,128)(2,1)S(1)}, bf16[2,128,384]{2,1,0:T(8,128)(2,1)S(1)}, u32[]{:S(2)}, u32[]{:S(2)}) collective-permute-start(bf16[2,128,384]{2,1,0:T(8,128)(2,1)S(1)} %get-tuple-element.158), channel_id=1, source_target_pairs={{0,16},{1,17},{2,18},{3,19},{4,20},{5,21},{6,22},{7,23},{8,24},{9,... | collective-permute-start | bytes 589832 | tf_op jit(solution)/shard_map/ppermute | solution.py:248
  119.8 22.6 %collective-permute-start.25 = (bf16[512,512]{1,0:T(8,128)(2,1)}, bf16[512,512]{1,0:T(8,128)(2,1)}, u32[]{:S(2)}, u32[]{:S(2)}) collective-permute-start(bf16[512,512]{1,0:T(8,128)(2,1)} %shard_map.126), channel_id=1, source_target_pairs={{0,1},{1,0},{2,3},{3,2},{4,5},{5,4},{6,7},{7,6},{8,9},{9,8},{10,11... | collective-permute-start | bytes 1572872 | tf_op jit(solution)/shard_map/ppermute | solution.py:248
  119.8 13.9 %collective-permute-start.30 = (bf16[512,384]{1,0:T(8,128)(2,1)S(1)}, bf16[512,384]{1,0:T(8,128)(2,1)S(1)}, u32[]{:S(2)}, u32[]{:S(2)}) collective-permute-start(bf16[512,384]{1,0:T(8,128)(2,1)S(1)} %collective-permute-done.29.refs_0_.refs_1_), channel_id=1, source_target_pairs={{4,0},{5,1},{6,2},{7,3},{8,12},{9,13},{10,14},{11,15},{20,16},{21,... | collective-permute-start | bytes 1179656 | tf_op jit(solution)/shard_map/ppermute | solution.py:248
  121.9 19.9 %collective-permute-start.55 = (bf16[256,768]{1,0:T(8,128)(2,1)}, bf16[256,768]{1,0:T(8,128)(2,1)}, u32[]{:S(2)}, u32[]{:S(2)}) collective-permute-start(bf16[256,768]{1,0:T(8,128)(2,1)} %pad_maximum_fusion.11.refs_8_), channel_id=1, source_target_pairs={{0,4},{1,5},{2,6},{3,7},{4,0},{5,1},{6,2},{7,3},{8,12},{9,13},{10,... | collective-permute-start | bytes 1179656 | tf_op jit(solution)/shard_map/ppermute | solution.py:248
  124.5 21.0 %collective-permute-start.56 = (bf16[256,768]{1,0:T(8,128)(2,1)}, bf16[256,768]{1,0:T(8,128)(2,1)}, u32[]{:S(2)}, u32[]{:S(2)}) collective-permute-start(bf16[256,768]{1,0:T(8,128)(2,1)} %pad_maximum_fusion.11.refs_8_), channel_id=1, source_target_pairs={{4,8},{5,9},{6,10},{7,11},{8,4},{9,5},{10,6},{11,7},{20,24},{21,25... | collective-permute-start | bytes 1179656 | tf_op jit(solution)/shard_map/ppermute | solution.py:248
  134.1 23.6 %collective-permute-start.31 = (bf16[512,512]{1,0:T(8,128)(2,1)S(1)}, bf16[512,512]{1,0:T(8,128)(2,1)S(1)}, u32[]{:S(2)}, u32[]{:S(2)}) collective-permute-start(bf16[512,512]{1,0:T(8,128)(2,1)S(1)} %shard_map.128), channel_id=1, source_target_pairs={{0,1},{1,0},{2,3},{3,2},{4,5},{5,4},{6,7},{7,6},{8,9},{9,8},{10,11... | collective-permute-start | bytes 1572872 | tf_op jit(solution)/shard_map/ppermute | solution.py:248
  141.7 14.7 %collective-permute-start.58 = (bf16[256,768]{1,0:T(8,128)(2,1)}, bf16[256,768]{1,0:T(8,128)(2,1)S(1)}, u32[]{:S(2)}, u32[]{:S(2)}) collective-permute-start(bf16[256,768]{1,0:T(8,128)(2,1)} %collective-permute-done.55.refs_9_), channel_id=1, source_target_pairs={{4,8},{5,9},{6,10},{7,11},{8,4},{9,5},{10,6},{11,7},{20,24},{21,25... | collective-permute-start | bytes 1179656 | tf_op jit(solution)/shard_map/ppermute | solution.py:248
  143.9 5.6 %collective-permute-start.26 = (bf16[128,512]{1,0:T(8,128)(2,1)S(1)}, bf16[128,512]{1,0:T(8,128)(2,1)S(1)}, u32[]{:S(2)}, u32[]{:S(2)}) collective-permute-start(bf16[128,512]{1,0:T(8,128)(2,1)S(1)} %get-tuple-element.81), channel_id=1, source_target_pairs={{0,2},{1,3},{2,0},{3,1},{4,6},{5,7},{6,4},{7,5},{8,10},{9,11},{10,... | collective-permute-start | bytes 393224 | tf_op jit(solution)/shard_map/ppermute | solution.py:248
  145.5 6.2 %collective-permute-start.27 = (bf16[128,512]{1,0:T(8,128)(2,1)S(1)}, bf16[128,512]{1,0:T(8,128)(2,1)S(1)}, u32[]{:S(2)}, u32[]{:S(2)}) collective-permute-start(bf16[128,512]{1,0:T(8,128)(2,1)S(1)} %get-tuple-element.82), channel_id=1, source_target_pairs={{0,16},{1,17},{2,18},{3,19},{4,20},{5,21},{6,22},{7,23},{8,24},{9,... | collective-permute-start | bytes 393224 | tf_op jit(solution)/shard_map/ppermute | solution.py:248
  147.0 7.3 %collective-permute-start.28 = (bf16[128,512]{1,0:T(8,128)(2,1)S(1)}, bf16[128,512]{1,0:T(8,128)(2,1)S(1)}, u32[]{:S(2)}, u32[]{:S(2)}) collective-permute-start(bf16[128,512]{1,0:T(8,128)(2,1)S(1)} %get-tuple-element.83), channel_id=1, source_target_pairs={{0,18},{1,19},{2,16},{3,17},{4,22},{5,23},{6,20},{7,21},{8,26},{9,... | collective-permute-start | bytes 393224 | tf_op jit(solution)/shard_map/ppermute | solution.py:248
  149.5 10.6 %collective-permute-start.20 = (bf16[128,1024]{1,0:T(8,128)(2,1)S(1)}, bf16[128,1024]{1,0:T(8,128)(2,1)S(1)}, u32[]{:S(2)}, u32[]{:S(2)}) collective-permute-start(bf16[128,1024]{1,0:T(8,128)(2,1)S(1)} %get-tuple-element.77), channel_id=1, source_target_pairs={{0,2},{1,3},{2,0},{3,1},{4,6},{5,7},{6,4},{7,5},{8,10},{9,11},{10,... | collective-permute-start | bytes 786440 | tf_op jit(solution)/shard_map/ppermute | solution.py:248
  151.7 9.8 %collective-permute-start.21 = (bf16[128,1024]{1,0:T(8,128)(2,1)S(1)}, bf16[128,1024]{1,0:T(8,128)(2,1)S(1)}, u32[]{:S(2)}, u32[]{:S(2)}) collective-permute-start(bf16[128,1024]{1,0:T(8,128)(2,1)S(1)} %get-tuple-element.78), channel_id=1, source_target_pairs={{0,16},{1,17},{2,18},{3,19},{4,20},{5,21},{6,22},{7,23},{8,24},{9,... | collective-permute-start | bytes 786440 | tf_op jit(solution)/shard_map/ppermute | solution.py:248
  154.3 11.6 %collective-permute-start.22 = (bf16[128,1024]{1,0:T(8,128)(2,1)S(1)}, bf16[128,1024]{1,0:T(8,128)(2,1)S(1)}, u32[]{:S(2)}, u32[]{:S(2)}) collective-permute-start(bf16[128,1024]{1,0:T(8,128)(2,1)S(1)} %get-tuple-element.79), channel_id=1, source_target_pairs={{0,18},{1,19},{2,16},{3,17},{4,22},{5,23},{6,20},{7,21},{8,26},{9,... | collective-permute-start | bytes 786440 | tf_op jit(solution)/shard_map/ppermute | solution.py:248
  156.4 18.7 %collective-permute-start.57 = (bf16[256,768]{1,0:T(8,128)(2,1)}, bf16[256,768]{1,0:T(8,128)(2,1)S(1)}, u32[]{:S(2)}, u32[]{:S(2)}) collective-permute-start(bf16[256,768]{1,0:T(8,128)(2,1)} %collective-permute-done.56.refs_10_), channel_id=1, source_target_pairs={{4,0},{5,1},{6,2},{7,3},{8,12},{9,13},{10,14},{11,15},{20,16},{21,... | collective-permute-start | bytes 1179656 | tf_op jit(solution)/shard_map/ppermute | solution.py:248
  157.7 24.2 %collective-permute-start.59 = (bf16[256,768]{1,0:T(8,128)(2,1)S(1)}, bf16[256,768]{1,0:T(8,128)(2,1)S(1)}, u32[]{:S(2)}, u32[]{:S(2)}) collective-permute-start(bf16[256,768]{1,0:T(8,128)(2,1)S(1)} %collective-permute-done.58.refs_12_), channel_id=1, source_target_pairs={{4,0},{5,1},{6,2},{7,3},{8,12},{9,13},{10,14},{11,15},{20,16},{21,... | collective-permute-start | bytes 1179656 | tf_op jit(solution)/shard_map/ppermute | solution.py:248
  160.2 8.1 %collective-permute-start.32 = (bf16[128,512]{1,0:T(8,128)(2,1)S(1)}, bf16[128,512]{1,0:T(8,128)(2,1)S(1)}, u32[]{:S(2)}, u32[]{:S(2)}) collective-permute-start(bf16[128,512]{1,0:T(8,128)(2,1)S(1)} %get-tuple-element.85), channel_id=1, source_target_pairs={{0,2},{1,3},{2,0},{3,1},{4,6},{5,7},{6,4},{7,5},{8,10},{9,11},{10,... | collective-permute-start | bytes 393224 | tf_op jit(solution)/shard_map/ppermute | solution.py:248
  161.5 7.0 %collective-permute-start.33 = (bf16[128,512]{1,0:T(8,128)(2,1)S(1)}, bf16[128,512]{1,0:T(8,128)(2,1)S(1)}, u32[]{:S(2)}, u32[]{:S(2)}) collective-permute-start(bf16[128,512]{1,0:T(8,128)(2,1)S(1)} %get-tuple-element.86), channel_id=1, source_target_pairs={{0,16},{1,17},{2,18},{3,19},{4,20},{5,21},{6,22},{7,23},{8,24},{9,... | collective-permute-start | bytes 393224 | tf_op jit(solution)/shard_map/ppermute | solution.py:248
  165.9 5.9 %collective-permute-start.34 = (bf16[128,512]{1,0:T(8,128)(2,1)S(1)}, bf16[128,512]{1,0:T(8,128)(2,1)S(1)}, u32[]{:S(2)}, u32[]{:S(2)}) collective-permute-start(bf16[128,512]{1,0:T(8,128)(2,1)S(1)} %get-tuple-element.87), channel_id=1, source_target_pairs={{0,18},{1,19},{2,16},{3,17},{4,22},{5,23},{6,20},{7,21},{8,26},{9,... | collective-permute-start | bytes 393224 | tf_op jit(solution)/shard_map/ppermute | solution.py:248
  172.4 6.4 %collective-permute-start.36 = (bf16[64,2048]{1,0:T(8,128)(2,1)S(1)}, bf16[64,2048]{1,0:T(8,128)(2,1)S(1)}, u32[]{:S(2)}, u32[]{:S(2)}) collective-permute-start(bf16[64,2048]{1,0:T(8,128)(2,1)S(1)} %get-tuple-element.134.refs_0_), channel_id=1, source_target_pairs={{0,2},{1,3},{2,0},{3,1},{4,6},{5,7},{6,4},{7,5},{8,10},{9,11},{10,... | collective-permute-start | bytes 786440 | tf_op jit(solution)/shard_map/ppermute | solution.py:248
  173.8 18.3 %collective-permute-start.39 = (bf16[64,2048]{1,0:T(8,128)(2,1)S(1)}, bf16[64,2048]{1,0:T(8,128)(2,1)S(1)}, u32[]{:S(2)}, u32[]{:S(2)}) collective-permute-start(bf16[64,2048]{1,0:T(8,128)(2,1)S(1)} %get-tuple-element.134.refs_0_), channel_id=1, source_target_pairs={{0,1},{1,0},{2,3},{3,2},{4,5},{5,4},{6,7},{7,6},{8,9},{9,8},{10,11... | collective-permute-start | bytes 786440 | tf_op jit(solution)/shard_map/ppermute | solution.py:248
  174.0 7.1 %collective-permute-start.35 = (bf16[64,2048]{1,0:T(8,128)(2,1)S(1)}, bf16[64,2048]{1,0:T(8,128)(2,1)S(1)}, u32[]{:S(2)}, u32[]{:S(2)}) collective-permute-start(bf16[64,2048]{1,0:T(8,128)(2,1)S(1)} %fusion.22), channel_id=1, source_target_pairs={{0,1},{1,0},{2,3},{3,2},{4,5},{5,4},{6,7},{7,6},{8,9},{9,8},{10,11... | collective-permute-start | bytes 786440 | tf_op jit(solution)/shard_map/ppermute | solution.py:248
  175.1 9.3 %collective-permute-start.37 = (bf16[64,2048]{1,0:T(8,128)(2,1)S(1)}, bf16[64,2048]{1,0:T(8,128)(2,1)S(1)}, u32[]{:S(2)}, u32[]{:S(2)}) collective-permute-start(bf16[64,2048]{1,0:T(8,128)(2,1)S(1)} %get-tuple-element.134.refs_0_), channel_id=1, source_target_pairs={{0,16},{1,17},{2,18},{3,19},{4,20},{5,21},{6,22},{7,23},{8,24},{9,... | collective-permute-start | bytes 786440 | tf_op jit(solution)/shard_map/ppermute | solution.py:248
  178.9 10.3 %collective-permute-start.38 = (bf16[64,2048]{1,0:T(8,128)(2,1)S(1)}, bf16[64,2048]{1,0:T(8,128)(2,1)S(1)}, u32[]{:S(2)}, u32[]{:S(2)}) collective-permute-start(bf16[64,2048]{1,0:T(8,128)(2,1)S(1)} %get-tuple-element.134.refs_0_), channel_id=1, source_target_pairs={{0,18},{1,19},{2,16},{3,17},{4,22},{5,23},{6,20},{7,21},{8,26},{9,... | collective-permute-start | bytes 786440 | tf_op jit(solution)/shard_map/ppermute | solution.py:248
  181.1 16.7 %collective-permute-start.40 = (bf16[64,2048]{1,0:T(8,128)(2,1)S(1)}, bf16[64,2048]{1,0:T(8,128)(2,1)S(1)}, u32[]{:S(2)}, u32[]{:S(2)}) collective-permute-start(bf16[64,2048]{1,0:T(8,128)(2,1)S(1)} %collective-permute-done.36.refs_1_), channel_id=1, source_target_pairs={{0,1},{1,0},{2,3},{3,2},{4,5},{5,4},{6,7},{7,6},{8,9},{9,8},{10,11... | collective-permute-start | bytes 786440 | tf_op jit(solution)/shard_map/ppermute | solution.py:248
  181.9 10.3 %collective-permute-start.48 = (bf16[128,512]{1,0:T(8,128)(2,1)S(1)}, bf16[128,512]{1,0:T(8,128)(2,1)S(1)}, u32[]{:S(2)}, u32[]{:S(2)}) collective-permute-start(bf16[128,512]{1,0:T(8,128)(2,1)S(1)} %get-tuple-element.101), channel_id=1, source_target_pairs={{0,4},{1,5},{2,6},{3,7},{4,0},{5,1},{6,2},{7,3},{8,12},{9,13},{10,... | collective-permute-start | bytes 393224 | tf_op jit(solution)/shard_map/ppermute | solution.py:248
  184.4 12.9 %collective-permute-start.50 = (bf16[128,512]{1,0:T(8,128)(2,1)S(1)}, bf16[128,512]{1,0:T(8,128)(2,1)S(1)}, u32[]{:S(2)}, u32[]{:S(2)}) collective-permute-start(bf16[128,512]{1,0:T(8,128)(2,1)S(1)} %get-tuple-element.102), channel_id=1, source_target_pairs={{0,8},{1,9},{2,10},{3,11},{4,12},{5,13},{6,14},{7,15},{8,0},{9,1},... | collective-permute-start | bytes 393224 | tf_op jit(solution)/shard_map/ppermute | solution.py:248
  189.2 8.1 %collective-permute-start.52 = (bf16[128,512]{1,0:T(8,128)(2,1)S(1)}, bf16[128,512]{1,0:T(8,128)(2,1)S(1)}, u32[]{:S(2)}, u32[]{:S(2)}) collective-permute-start(bf16[128,512]{1,0:T(8,128)(2,1)S(1)} %get-tuple-element.103), channel_id=1, source_target_pairs={{0,12},{1,13},{2,14},{3,15},{4,8},{5,9},{6,10},{7,11},{8,4},{9,5},... | collective-permute-start | bytes 393224 | tf_op jit(solution)/shard_map/ppermute | solution.py:248
  192.1 9.9 %collective-permute-start.41 = (bf16[64,2048]{1,0:T(8,128)(2,1)S(1)}, bf16[64,2048]{1,0:T(8,128)(2,1)S(1)}, u32[]{:S(2)}, u32[]{:S(2)}) collective-permute-start(bf16[64,2048]{1,0:T(8,128)(2,1)S(1)} %collective-permute-done.37), channel_id=1, source_target_pairs={{0,1},{1,0},{2,3},{3,2},{4,5},{5,4},{6,7},{7,6},{8,9},{9,8},{10,11... | collective-permute-start | bytes 786440 | tf_op jit(solution)/shard_map/ppermute | solution.py:248
  192.2 9.8 %collective-permute-start.42 = (bf16[64,2048]{1,0:T(8,128)(2,1)S(1)}, bf16[64,2048]{1,0:T(8,128)(2,1)S(1)}, u32[]{:S(2)}, u32[]{:S(2)}) collective-permute-start(bf16[64,2048]{1,0:T(8,128)(2,1)S(1)} %collective-permute-done.38), channel_id=1, source_target_pairs={{0,1},{1,0},{2,3},{3,2},{4,5},{5,4},{6,7},{7,6},{8,9},{9,8},{10,11... | collective-permute-start | bytes 786440 | tf_op jit(solution)/shard_map/ppermute | solution.py:248
  197.3 2.0 collective-permute-start.49
  197.3 2.0 collective-permute-start.51
  197.8 1.5 collective-permute-start.53
  201.9 12.1 %collective-permute-start.60 = (bf16[256,768]{1,0:T(8,128)(2,1)S(1)}, bf16[256,768]{1,0:T(8,128)(2,1)S(1)}, u32[]{:S(2)}, u32[]{:S(2)}) collective-permute-start(bf16[256,768]{1,0:T(8,128)(2,1)S(1)} %get-tuple-element.119), channel_id=1, source_target_pairs={{0,2},{1,3},{2,0},{3,1},{4,6},{5,7},{6,4},{7,5},{8,10},{9,11},{10,... | collective-permute-start | bytes 1179656 | tf_op jit(solution)/shard_map/ppermute | solution.py:248
  205.6 2.8 %collective-permute-start.43 = (bf16[256,2048]{1,0:T(8,128)(2,1)S(1)}, bf16[256,2048]{1,0:T(8,128)(2,1)S(1)}, u32[]{:S(2)}, u32[]{:S(2)}) collective-permute-start(bf16[256,2048]{1,0:T(8,128)(2,1)S(1)} %convolution_convert_fusion), channel_id=1, source_target_pairs={{0,1},{1,0},{2,3},{3,2},{4,5},{5,4},{6,7},{7,6},{8,9},{9,8},{10,11... | collective-permute-start | bytes 3145736 | tf_op jit(solution)/shard_map/ppermute | solution.py:248
  209.6 10.0 %collective-permute-start.44 = (bf16[64,2048]{1,0:T(8,128)(2,1)S(1)}, bf16[64,2048]{1,0:T(8,128)(2,1)S(1)}, u32[]{:S(2)}, u32[]{:S(2)}) collective-permute-start(bf16[64,2048]{1,0:T(8,128)(2,1)S(1)} %get-tuple-element.131), channel_id=1, source_target_pairs={{0,2},{1,3},{2,0},{3,1},{4,6},{5,7},{6,4},{7,5},{8,10},{9,11},{10,... | collective-permute-start | bytes 786440 | tf_op jit(solution)/shard_map/ppermute | solution.py:248
  211.6 9.2 %collective-permute-start.45 = (bf16[64,2048]{1,0:T(8,128)(2,1)S(1)}, bf16[64,2048]{1,0:T(8,128)(2,1)S(1)}, u32[]{:S(2)}, u32[]{:S(2)}) collective-permute-start(bf16[64,2048]{1,0:T(8,128)(2,1)S(1)} %get-tuple-element.133), channel_id=1, source_target_pairs={{0,16},{1,17},{2,18},{3,19},{4,20},{5,21},{6,22},{7,23},{8,24},{9,... | collective-permute-start | bytes 786440 | tf_op jit(solution)/shard_map/ppermute | solution.py:248
  211.9 13.1 %collective-permute-start.46 = (bf16[64,2048]{1,0:T(8,128)(2,1)S(1)}, bf16[64,2048]{1,0:T(8,128)(2,1)S(1)}, u32[]{:S(2)}, u32[]{:S(2)}) collective-permute-start(bf16[64,2048]{1,0:T(8,128)(2,1)S(1)} %get-tuple-element.132), channel_id=1, source_target_pairs={{0,18},{1,19},{2,16},{3,17},{4,22},{5,23},{6,20},{7,21},{8,26},{9,... | collective-permute-start | bytes 786440 | tf_op jit(solution)/shard_map/ppermute | solution.py:248
  225.7 1.6 collective-permute-start.47
  (16 other events, 70.1 us)

commit v5 on v4

--- a/solution.py
+++ b/solution.py
@@ -177,7 +177,8 @@
 
 
 def weight_gradient(places, left, right, cases, T, G):
-    Z, (rows, high), wide = len(cases), left[0].shape, right[0].shape[1]
+    Z, rows, high = left[0].shape
+    wide, rows = right[0].shape[1], rows * G
     K = high // G
 
     def kernel(place_ref, *refs):
@@ -186,7 +187,7 @@
         def case(i):
             value = None
             for index, k in cases[i]:
-                a = jnp.concatenate([lefts[k * T + j][...] for j in range(T)], axis=0)
+                a = jnp.concatenate([ref[k] for ref in lefts], axis=0)
                 term = tn(a, rights[index][...])
                 value = term if value is None else value + term
             total[...] = value
@@ -466,19 +467,12 @@
         units = [hidden_e[:, 0]] + [send(hidden_e[:, a], dr=a) for a in range(1, R)]
         units = jnp.concatenate([u.reshape(G * n, w) for u in units], axis=1)
         passed = line(units)
-        own = [raw[b] for b in range(G)]
-        cols = cut(
-            table, own, [(G * m, G * K)] * Z, [(b, Z + k, G * K, k, b * m, 0) for k in range(Z) for b in range(G)])
-        cols = [value if k == 0 else send(value, moves=[(i, partner(i, k)) for i in range(Z)]) for k, value in enumerate(cols)]
-        mates = [[spread_c[b][j] for b in range(G)] for j in range(T)]
-        left = []
-        for k, value in enumerate(cols):
-            left.append(value)
-            for j in range(1, T):
-                if k:
-                    left.append(send(value, dt=-j))
-                else:
-                    left.extend(cut(table, mates[j], [(G * m, G * K)], [(b, Z, G * K, 0, b * m, 0) for b in range(G)]))
+        cols = cut(table, [dbranch], [(m, G * K)] * Z, [(0, Z + k, G * K, k, 0, 0) for k in range(Z)])
+        cols = [v if k == 0 else send(v, moves=[(i, partner(i, k)) for i in range(Z)]) for k, v in enumerate(cols)]
+        cols = jnp.stack(cols)
+        cols = [send(cols, dy=-b) if b else cols for b in range(G)]
+        mates = [[send(v, dt=-j) for v in cols] for j in range(1, T)]
+        left = cols + [v for row in mates for v in row]
         right, cases = [units], [[(0, 0)] for _ in range(Z)]
         for s in range(1, Z):
             for kind, _ in edges(Z, s):

time: 229 us -> 236 us (1.031)
  waiting for transfers between devices: 119 us -> 125 us
  other arithmetic: 11.8 us -> 14.3 us
    ppermute x61, waiting for transfers between devices: 119 us -> 125 us  [send(): return lax.ppermute(value, AXES, pairs)]
  transfers between devices with their start and end apart: 61 -> 61, of which waited for: 25 -> 23; matrix products, arithmetic and copies ran while one was open for 10% -> 11% of each run, Pallas kernels for 6% -> 5%
where the time goes in v5:
time: 236 us; the launch traced here: 235 us
  waiting for transfers between devices  125 us (53%)
  starting transfers between devices  64.5 us (27%)
  other arithmetic  14.3 us (6%)
  Pallas kernels  11.9 us (5%)
  local copies, waits for them, and re-layouts  9.38 us (4%)
  matrix products  7.65 us (3%)
    ppermute x61, waiting for transfers between devices, send(): return lax.ppermute(value, AXES, pairs)  125 us
    ppermute x61, starting transfers between devices, send(): return lax.ppermute(value, AXES, pairs)  64.5 us
  transfers between devices with their start and end apart: 61, of which 23 were waited for; matrix products, arithmetic and copies ran while one was open for 11% of the time, Pallas kernels for 5%

profile of v5, /device:TPU:0, one launch (start us, length us, event | category | flops | bytes accessed | tf_op | source)
XLA Modules:
  0.0 234.7 jit_solution(13119609823955024940)
XLA Ops:
  0.8 1.4 pad_maximum_fusion.2
  3.6 1.0 constant_dynamic-slice_fusion.2
  4.7 3.0 %collective-permute-start = (bf16[2,64,2048]{2,1,0:T(8,128)(2,1)}, bf16[2,64,2048]{2,1,0:T(8,128)(2,1)S(1)}, u32[]{:S(2)}, u32[]{:S(2)}) collective-permute-start(bf16[2,64,2048]{2,1,0:T(8,128)(2,1)} %bitcast.6), channel_id=1, source_target_pairs={{0,2},{1,3},{2,0},{3,1},{4,6},{5,7},{6,4},{7,5},{8,10},{9,11},{10,... | collective-permute-start | bytes 1572872 | tf_op jit(solution)/shard_map/ppermute | solution.py:249
  7.7 1.5 collective-permute-start.1
  9.2 1.6 collective-permute-start.6
  11.9 1.6 collective-permute-start.17
  14.2 18.3 %collective-permute-done.17 = bf16[256,384]{1,0:T(8,128)(2,1)S(1)} collective-permute-done((bf16[256,384]{1,0:T(8,128)(2,1)S(1)}, bf16[256,384]{1,0:T(8,128)(2,1)S(1)}, u32[]{:S(2)}, u32[]{:S(2)}) %collective-permute-start.17) | collective-permute-done | bytes 196640 | tf_op jit(solution)/shard_map/ppermute | solution.py:249
  33.2 2.7 %collective-permute-start.2 = (bf16[2,64,2048]{2,1,0:T(8,128)(2,1)}, bf16[2,64,2048]{2,1,0:T(8,128)(2,1)S(1)}, u32[]{:S(2)}, u32[]{:S(2)}) collective-permute-start(bf16[2,64,2048]{2,1,0:T(8,128)(2,1)} %bitcast.6), channel_id=1, source_target_pairs={{0,18},{1,19},{2,16},{3,17},{4,22},{5,23},{6,20},{7,21},{8,26},{9,... | collective-permute-start | bytes 1572872 | tf_op jit(solution)/shard_map/ppermute | solution.py:249
  36.0 4.4 %collective-permute-start.9 = (bf16[256,768]{1,0:T(8,128)(2,1)}, bf16[256,768]{1,0:T(8,128)(2,1)S(1)}, u32[]{:S(2)}, u32[]{:S(2)}) collective-permute-start(bf16[256,768]{1,0:T(8,128)(2,1)} %collective-permute-done.8), channel_id=1, source_target_pairs={{0,4},{1,5},{2,6},{3,7},{4,0},{5,1},{6,2},{7,3},{8,12},{9,13},{10,... | collective-permute-start | bytes 1179656 | tf_op jit(solution)/shard_map/ppermute | solution.py:249
  42.4 1.3 collective-permute-start.11
  44.4 3.0 %collective-permute-done.2 = bf16[2,64,2048]{2,1,0:T(8,128)(2,1)S(1)} collective-permute-done((bf16[2,64,2048]{2,1,0:T(8,128)(2,1)}, bf16[2,64,2048]{2,1,0:T(8,128)(2,1)S(1)}, u32[]{:S(2)}, u32[]{:S(2)}) %collective-permute-start.2) | collective-permute-done | bytes 524320 | tf_op jit(solution)/shard_map/ppermute | solution.py:249
  47.5 1.3 maximum_bitcast_fusion
  49.5 8.5 %collective-permute-done.11 = bf16[256,768]{1,0:T(8,128)(2,1)S(1)} collective-permute-done((bf16[256,768]{1,0:T(8,128)(2,1)S(1)}, bf16[256,768]{1,0:T(8,128)(2,1)S(1)}, u32[]{:S(2)}, u32[]{:S(2)}) %collective-permute-start.11) | collective-permute-done | bytes 393248 | tf_op jit(solution)/shard_map/ppermute | solution.py:249
  58.1 1.3 collective-permute-start.13
  60.2 1.3 collective-permute-start.15
  63.2 8.8 %collective-permute-done.13 = bf16[256,768]{1,0:T(8,128)(2,1)S(1)} collective-permute-done((bf16[256,768]{1,0:T(8,128)(2,1)S(1)}, bf16[256,768]{1,0:T(8,128)(2,1)S(1)}, u32[]{:S(2)}, u32[]{:S(2)}) %collective-permute-start.13) | collective-permute-done | bytes 393248 | tf_op jit(solution)/shard_map/ppermute | solution.py:249
  71.9 4.0 %collective-permute-start.18 = (bf16[512,384]{1,0:T(8,128)(2,1)S(1)}, bf16[512,384]{1,0:T(8,128)(2,1)S(1)}, u32[]{:S(2)}, u32[]{:S(2)}) collective-permute-start(bf16[512,384]{1,0:T(8,128)(2,1)S(1)} %pad_maximum_fusion.10.refs_0_.refs_1_), channel_id=1, source_target_pairs={{0,4},{1,5},{2,6},{3,7},{4,0},{5,1},{6,2},{7,3},{8,12},{9,13},{10,... | collective-permute-start | bytes 1179656 | tf_op jit(solution)/shard_map/ppermute | solution.py:249
  76.7 3.8 %collective-permute-done.15 = bf16[256,768]{1,0:T(8,128)(2,1)S(1)} collective-permute-done((bf16[256,768]{1,0:T(8,128)(2,1)S(1)}, bf16[256,768]{1,0:T(8,128)(2,1)S(1)}, u32[]{:S(2)}, u32[]{:S(2)}) %collective-permute-start.15) | collective-permute-done | bytes 393248 | tf_op jit(solution)/shard_map/ppermute | solution.py:249
  82.3 1.8 fusion.44
  84.1 1.3 collective-permute-start.16
  85.4 1.8 fusion.43
  87.2 9.4 %collective-permute-done.16 = bf16[256,768]{1,0:T(8,128)(2,1)S(1)} collective-permute-done((bf16[256,768]{1,0:T(8,128)(2,1)S(1)}, bf16[256,768]{1,0:T(8,128)(2,1)S(1)}, u32[]{:S(2)}, u32[]{:S(2)}) %collective-permute-start.16) | collective-permute-done | bytes 393248 | tf_op jit(solution)/shard_map/ppermute | solution.py:249
  97.0 1.3 fusion.31
  98.6 1.3 collective-permute-start.24
  101.7 1.7 shard_map.124
  103.5 6.8 %collective-permute-done.24.refs_1_.refs_2_ = bf16[512,384]{1,0:T(8,128)(2,1)S(1)} collective-permute-done((bf16[512,384]{1,0:T(8,128)(2,1)S(1)}, bf16[512,384]{1,0:T(8,128)(2,1)S(1)}, u32[]{:S(2)}, u32[]{:S(2)}) %collective-permute-start.24) | collective-permute-done | bytes 393248 | tf_op jit(solution)/shard_map/ppermute | solution.py:249
  110.3 1.3 shard_map.126
  111.5 1.3 collective-permute-start.30
  112.9 1.8 fusion.40
  114.7 1.5 collective-permute-start.54
  116.3 8.7 %collective-permute-done.30.refs_1_.refs_2_ = bf16[512,384]{1,0:T(8,128)(2,1)S(1)} collective-permute-done((bf16[512,384]{1,0:T(8,128)(2,1)S(1)}, bf16[512,384]{1,0:T(8,128)(2,1)S(1)}, u32[]{:S(2)}, u32[]{:S(2)}) %collective-permute-start.30) | collective-permute-done | bytes 393248 | tf_op jit(solution)/shard_map/ppermute | solution.py:249
  126.5 1.5 shard_map.127
  128.0 1.6 collective-permute-start.26
  129.6 1.5 collective-permute-start.27
  132.6 2.0 shard_map.125
  134.6 1.6 collective-permute-start.20
  136.2 1.5 collective-permute-start.21
  138.1 2.5 %collective-permute-start.22 = (bf16[128,1024]{1,0:T(8,128)(2,1)S(1)}, bf16[128,1024]{1,0:T(8,128)(2,1)S(1)}, u32[]{:S(2)}, u32[]{:S(2)}) collective-permute-start(bf16[128,1024]{1,0:T(8,128)(2,1)S(1)} %get-tuple-element.75), channel_id=1, source_target_pairs={{0,18},{1,19},{2,16},{3,17},{4,22},{5,23},{6,20},{7,21},{8,26},{9,... | collective-permute-start | bytes 786440 | tf_op jit(solution)/shard_map/ppermute | solution.py:249
  141.6 6.7 %collective-permute-done.20 = bf16[128,1024]{1,0:T(8,128)(2,1)S(1)} collective-permute-done((bf16[128,1024]{1,0:T(8,128)(2,1)S(1)}, bf16[128,1024]{1,0:T(8,128)(2,1)S(1)}, u32[]{:S(2)}, u32[]{:S(2)}) %collective-permute-start.20) | collective-permute-done | bytes 262176 | tf_op jit(solution)/shard_map/ppermute | solution.py:249
  148.3 1.5 collective-permute-start.33
  149.8 1.2 collective-permute-start.34
  151.1 2.3 collective-permute-done.32
  153.7 2.0 collective-permute-done.34
  157.0 1.4 collective-permute-start.48
  158.3 2.4 %collective-permute-start.49 = (bf16[64,512]{1,0:T(8,128)(2,1)S(1)}, bf16[64,512]{1,0:T(8,128)(2,1)S(1)}, u32[]{:S(2)}, u32[]{:S(2)}) collective-permute-start(bf16[64,512]{1,0:T(8,128)(2,1)S(1)} %get-tuple-element.98), channel_id=1, source_target_pairs={{0,8},{1,9},{2,10},{3,11},{4,12},{5,13},{6,14},{7,15},{8,0},{9,1},... | collective-permute-start | bytes 196616 | tf_op jit(solution)/shard_map/ppermute | solution.py:249
  163.7 1.6 collective-permute-start.36
  165.3 1.5 collective-permute-done.50
  166.8 1.1 collective-permute-start.37
  168.0 1.6 collective-permute-start.38
  170.6 4.6 %collective-permute-done.36 = bf16[64,2048]{1,0:T(8,128)(2,1)S(1)} collective-permute-done((bf16[64,2048]{1,0:T(8,128)(2,1)S(1)}, bf16[64,2048]{1,0:T(8,128)(2,1)S(1)}, u32[]{:S(2)}, u32[]{:S(2)}) %collective-permute-start.36) | collective-permute-done | bytes 262176 | tf_op jit(solution)/shard_map/ppermute | solution.py:249
  175.9 3.3 %collective-permute-done.38 = bf16[64,2048]{1,0:T(8,128)(2,1)S(1)} collective-permute-done((bf16[64,2048]{1,0:T(8,128)(2,1)S(1)}, bf16[64,2048]{1,0:T(8,128)(2,1)S(1)}, u32[]{:S(2)}, u32[]{:S(2)}) %collective-permute-start.38) | collective-permute-done | bytes 262176 | tf_op jit(solution)/shard_map/ppermute | solution.py:249
  180.3 1.3 collective-permute-start.57
  181.6 2.1 collective-permute-done.51.refs_1_
  183.7 1.3 collective-permute-start.59
  186.8 1.3 multiply_convert_fusion.1
  189.3 10.0 %collective-permute-done.57.refs_7_ = bf16[256,768]{1,0:T(8,128)(2,1)S(1)} collective-permute-done((bf16[256,768]{1,0:T(8,128)(2,1)S(1)}, bf16[256,768]{1,0:T(8,128)(2,1)S(1)}, u32[]{:S(2)}, u32[]{:S(2)}) %collective-permute-start.57) | collective-permute-done | bytes 393248 | tf_op jit(solution)/shard_map/ppermute | solution.py:249
  199.3 8.2 %collective-permute-done.59.refs_9_ = bf16[256,768]{1,0:T(8,128)(2,1)S(1)} collective-permute-done((bf16[256,768]{1,0:T(8,128)(2,1)S(1)}, bf16[256,768]{1,0:T(8,128)(2,1)S(1)}, u32[]{:S(2)}, u32[]{:S(2)}) %collective-permute-start.59) | collective-permute-done | bytes 393248 | tf_op jit(solution)/shard_map/ppermute | solution.py:249
  207.5 1.9 shard_map.131
  211.0 1.0 add_convert_fusion
  213.1 1.3 collective-permute-start.45
  214.4 1.3 collective-permute-start.46
  215.7 7.1 %collective-permute-done.60 = bf16[256,768]{1,0:T(8,128)(2,1)S(1)} collective-permute-done((bf16[256,768]{1,0:T(8,128)(2,1)S(1)}, bf16[256,768]{1,0:T(8,128)(2,1)S(1)}, u32[]{:S(2)}, u32[]{:S(2)}) %collective-permute-start.60) | collective-permute-done | bytes 393248 | tf_op jit(solution)/shard_map/ppermute | solution.py:249
  223.0 8.6 %collective-permute-done.44 = bf16[64,2048]{1,0:T(8,128)(2,1)S(1)} collective-permute-done((bf16[64,2048]{1,0:T(8,128)(2,1)S(1)}, bf16[64,2048]{1,0:T(8,128)(2,1)S(1)}, u32[]{:S(2)}, u32[]{:S(2)}) %collective-permute-start.44) | collective-permute-done | bytes 262176 | tf_op jit(solution)/shard_map/ppermute | solution.py:249
  232.3 1.4 convert_add_fusion
  (186 shorter events, 34.4 us)
Async XLA Ops:
  4.7 37.7 %collective-permute-start = (bf16[2,64,2048]{2,1,0:T(8,128)(2,1)}, bf16[2,64,2048]{2,1,0:T(8,128)(2,1)S(1)}, u32[]{:S(2)}, u32[]{:S(2)}) collective-permute-start(bf16[2,64,2048]{2,1,0:T(8,128)(2,1)} %bitcast.6), channel_id=1, source_target_pairs={{0,2},{1,3},{2,0},{3,1},{4,6},{5,7},{6,4},{7,5},{8,10},{9,11},{10,... | collective-permute-start | bytes 1572872 | tf_op jit(solution)/shard_map/ppermute | solution.py:249
  7.7 36.1 %collective-permute-start.1 = (bf16[2,64,2048]{2,1,0:T(8,128)(2,1)}, bf16[2,64,2048]{2,1,0:T(8,128)(2,1)S(1)}, u32[]{:S(2)}, u32[]{:S(2)}) collective-permute-start(bf16[2,64,2048]{2,1,0:T(8,128)(2,1)} %bitcast.6), channel_id=1, source_target_pairs={{0,16},{1,17},{2,18},{3,19},{4,20},{5,21},{6,22},{7,23},{8,24},{9,... | collective-permute-start | bytes 1572872 | tf_op jit(solution)/shard_map/ppermute | solution.py:249
  9.2 24.0 %collective-permute-start.6 = (bf16[256,768]{1,0:T(8,128)(2,1)S(1)}, bf16[256,768]{1,0:T(8,128)(2,1)}, u32[]{:S(2)}, u32[]{:S(2)}) collective-permute-start(bf16[256,768]{1,0:T(8,128)(2,1)S(1)} %get-tuple-element.59), channel_id=1, source_target_pairs={{0,4},{1,5},{2,6},{3,7},{4,0},{5,1},{6,2},{7,3},{8,12},{9,13},{10,... | collective-permute-start | bytes 1179656 | tf_op jit(solution)/shard_map/ppermute | solution.py:249
  10.7 25.2 %collective-permute-start.8 = (bf16[256,768]{1,0:T(8,128)(2,1)S(1)}, bf16[256,768]{1,0:T(8,128)(2,1)}, u32[]{:S(2)}, u32[]{:S(2)}) collective-permute-start(bf16[256,768]{1,0:T(8,128)(2,1)S(1)} %get-tuple-element.61), channel_id=1, source_target_pairs={{0,2},{1,3},{2,0},{3,1},{4,6},{5,7},{6,4},{7,5},{8,10},{9,11},{10,... | collective-permute-start | bytes 1179656 | tf_op jit(solution)/shard_map/ppermute | solution.py:249
  11.9 20.6 %collective-permute-start.17 = (bf16[256,384]{1,0:T(8,128)(2,1)S(1)}, bf16[256,384]{1,0:T(8,128)(2,1)S(1)}, u32[]{:S(2)}, u32[]{:S(2)}) collective-permute-start(bf16[256,384]{1,0:T(8,128)(2,1)S(1)} %get-tuple-element.69), channel_id=1, source_target_pairs={{0,2},{1,3},{2,0},{3,1},{4,6},{5,7},{6,4},{7,5},{8,10},{9,11},{10,... | collective-permute-start | bytes 589832 | tf_op jit(solution)/shard_map/ppermute | solution.py:249
  32.5 9.2 %collective-permute-start.7 = (bf16[256,768]{1,0:T(8,128)(2,1)S(1)}, bf16[256,768]{1,0:T(8,128)(2,1)S(1)}, u32[]{:S(2)}, u32[]{:S(2)}) collective-permute-start(bf16[256,768]{1,0:T(8,128)(2,1)S(1)} %get-tuple-element.59), channel_id=1, source_target_pairs={{4,8},{5,9},{6,10},{7,11},{8,4},{9,5},{10,6},{11,7},{20,24},{21,25... | collective-permute-start | bytes 1179656 | tf_op jit(solution)/shard_map/ppermute | solution.py:249
  33.2 14.3 %collective-permute-start.2 = (bf16[2,64,2048]{2,1,0:T(8,128)(2,1)}, bf16[2,64,2048]{2,1,0:T(8,128)(2,1)S(1)}, u32[]{:S(2)}, u32[]{:S(2)}) collective-permute-start(bf16[2,64,2048]{2,1,0:T(8,128)(2,1)} %bitcast.6), channel_id=1, source_target_pairs={{0,18},{1,19},{2,16},{3,17},{4,22},{5,23},{6,20},{7,21},{8,26},{9,... | collective-permute-start | bytes 1572872 | tf_op jit(solution)/shard_map/ppermute | solution.py:249
  36.0 12.8 %collective-permute-start.9 = (bf16[256,768]{1,0:T(8,128)(2,1)}, bf16[256,768]{1,0:T(8,128)(2,1)S(1)}, u32[]{:S(2)}, u32[]{:S(2)}) collective-permute-start(bf16[256,768]{1,0:T(8,128)(2,1)} %collective-permute-done.8), channel_id=1, source_target_pairs={{0,4},{1,5},{2,6},{3,7},{4,0},{5,1},{6,2},{7,3},{8,12},{9,13},{10,... | collective-permute-start | bytes 1179656 | tf_op jit(solution)/shard_map/ppermute | solution.py:249
  41.7 7.7 %collective-permute-start.10 = (bf16[256,768]{1,0:T(8,128)(2,1)}, bf16[256,768]{1,0:T(8,128)(2,1)S(1)}, u32[]{:S(2)}, u32[]{:S(2)}) collective-permute-start(bf16[256,768]{1,0:T(8,128)(2,1)} %collective-permute-done.8), channel_id=1, source_target_pairs={{4,8},{5,9},{6,10},{7,11},{8,4},{9,5},{10,6},{11,7},{20,24},{21,25... | collective-permute-start | bytes 1179656 | tf_op jit(solution)/shard_map/ppermute | solution.py:249
  42.4 15.6 %collective-permute-start.11 = (bf16[256,768]{1,0:T(8,128)(2,1)S(1)}, bf16[256,768]{1,0:T(8,128)(2,1)S(1)}, u32[]{:S(2)}, u32[]{:S(2)}) collective-permute-start(bf16[256,768]{1,0:T(8,128)(2,1)S(1)} %collective-permute-done.7), channel_id=1, source_target_pairs={{4,0},{5,1},{6,2},{7,3},{8,12},{9,13},{10,14},{11,15},{20,16},{21,... | collective-permute-start | bytes 1179656 | tf_op jit(solution)/shard_map/ppermute | solution.py:249
  43.7 15.7 %collective-permute-start.12 = (bf16[256,768]{1,0:T(8,128)(2,1)}, bf16[256,768]{1,0:T(8,128)(2,1)S(1)}, u32[]{:S(2)}, u32[]{:S(2)}) collective-permute-start(bf16[256,768]{1,0:T(8,128)(2,1)} %collective-permute-done.6), channel_id=1, source_target_pairs={{4,8},{5,9},{6,10},{7,11},{8,4},{9,5},{10,6},{11,7},{20,24},{21,25... | collective-permute-start | bytes 1179656 | tf_op jit(solution)/shard_map/ppermute | solution.py:249
  47.5 12.7 %collective-permute-start.3 = (bf16[2,64,2048]{2,1,0:T(8,128)(2,1)S(1)}, bf16[2,64,2048]{2,1,0:T(8,128)(2,1)S(1)}, u32[]{:S(2)}, u32[]{:S(2)}) collective-permute-start(bf16[2,64,2048]{2,1,0:T(8,128)(2,1)S(1)} %collective-permute-done), channel_id=1, source_target_pairs={{0,1},{1,0},{2,3},{3,2},{4,5},{5,4},{6,7},{7,6},{8,9},{9,8},{10,11... | collective-permute-start | bytes 1572872 | tf_op jit(solution)/shard_map/ppermute | solution.py:249
  48.8 12.7 %collective-permute-start.4 = (bf16[2,64,2048]{2,1,0:T(8,128)(2,1)S(1)}, bf16[2,64,2048]{2,1,0:T(8,128)(2,1)S(1)}, u32[]{:S(2)}, u32[]{:S(2)}) collective-permute-start(bf16[2,64,2048]{2,1,0:T(8,128)(2,1)S(1)} %collective-permute-done.1), channel_id=1, source_target_pairs={{0,1},{1,0},{2,3},{3,2},{4,5},{5,4},{6,7},{7,6},{8,9},{9,8},{10,11... | collective-permute-start | bytes 1572872 | tf_op jit(solution)/shard_map/ppermute | solution.py:249
  49.4 12.1 %collective-permute-start.5 = (bf16[2,64,2048]{2,1,0:T(8,128)(2,1)S(1)}, bf16[2,64,2048]{2,1,0:T(8,128)(2,1)S(1)}, u32[]{:S(2)}, u32[]{:S(2)}) collective-permute-start(bf16[2,64,2048]{2,1,0:T(8,128)(2,1)S(1)} %collective-permute-done.2), channel_id=1, source_target_pairs={{0,1},{1,0},{2,3},{3,2},{4,5},{5,4},{6,7},{7,6},{8,9},{9,8},{10,11... | collective-permute-start | bytes 1572872 | tf_op jit(solution)/shard_map/ppermute | solution.py:249
  58.1 13.9 %collective-permute-start.13 = (bf16[256,768]{1,0:T(8,128)(2,1)S(1)}, bf16[256,768]{1,0:T(8,128)(2,1)S(1)}, u32[]{:S(2)}, u32[]{:S(2)}) collective-permute-start(bf16[256,768]{1,0:T(8,128)(2,1)S(1)} %collective-permute-done.10), channel_id=1, source_target_pairs={{4,0},{5,1},{6,2},{7,3},{8,12},{9,13},{10,14},{11,15},{20,16},{21,... | collective-permute-start | bytes 1179656 | tf_op jit(solution)/shard_map/ppermute | solution.py:249
  59.4 12.5 %collective-permute-start.14 = (bf16[256,768]{1,0:T(8,128)(2,1)S(1)}, bf16[256,768]{1,0:T(8,128)(2,1)S(1)}, u32[]{:S(2)}, u32[]{:S(2)}) collective-permute-start(bf16[256,768]{1,0:T(8,128)(2,1)S(1)} %collective-permute-done.9), channel_id=1, source_target_pairs={{4,8},{5,9},{6,10},{7,11},{8,4},{9,5},{10,6},{11,7},{20,24},{21,25... | collective-permute-start | bytes 1179656 | tf_op jit(solution)/shard_map/ppermute | solution.py:249
  60.2 20.4 %collective-permute-start.15 = (bf16[256,768]{1,0:T(8,128)(2,1)S(1)}, bf16[256,768]{1,0:T(8,128)(2,1)S(1)}, u32[]{:S(2)}, u32[]{:S(2)}) collective-permute-start(bf16[256,768]{1,0:T(8,128)(2,1)S(1)} %collective-permute-done.12), channel_id=1, source_target_pairs={{4,0},{5,1},{6,2},{7,3},{8,12},{9,13},{10,14},{11,15},{20,16},{21,... | collective-permute-start | bytes 1179656 | tf_op jit(solution)/shard_map/ppermute | solution.py:249
  63.2 17.5 %copy-start = (bf16[128,2048]{1,0:T(8,128)(2,1)S(1)}, bf16[128,2048]{1,0:T(8,128)(2,1)}, u32[]{:S(2)}) copy-start(bf16[128,2048]{1,0:T(8,128)(2,1)} %cot_ref) | copy-start | bytes 1572868
  71.9 29.0 %collective-permute-start.18 = (bf16[512,384]{1,0:T(8,128)(2,1)S(1)}, bf16[512,384]{1,0:T(8,128)(2,1)S(1)}, u32[]{:S(2)}, u32[]{:S(2)}) collective-permute-start(bf16[512,384]{1,0:T(8,128)(2,1)S(1)} %pad_maximum_fusion.10.refs_0_.refs_1_), channel_id=1, source_target_pairs={{0,4},{1,5},{2,6},{3,7},{4,0},{5,1},{6,2},{7,3},{8,12},{9,13},{10,... | collective-permute-start | bytes 1179656 | tf_op jit(solution)/shard_map/ppermute | solution.py:249
  76.0 22.7 %collective-permute-start.23 = (bf16[512,384]{1,0:T(8,128)(2,1)S(1)}, bf16[512,384]{1,0:T(8,128)(2,1)S(1)}, u32[]{:S(2)}, u32[]{:S(2)}) collective-permute-start(bf16[512,384]{1,0:T(8,128)(2,1)S(1)} %pad_maximum_fusion.10.refs_0_.refs_1_), channel_id=1, source_target_pairs={{4,8},{5,9},{6,10},{7,11},{8,4},{9,5},{10,6},{11,7},{20,24},{21,25... | collective-permute-start | bytes 1179656 | tf_op jit(solution)/shard_map/ppermute | solution.py:249
  84.1 12.5 %collective-permute-start.16 = (bf16[256,768]{1,0:T(8,128)(2,1)S(1)}, bf16[256,768]{1,0:T(8,128)(2,1)S(1)}, u32[]{:S(2)}, u32[]{:S(2)}) collective-permute-start(bf16[256,768]{1,0:T(8,128)(2,1)S(1)} %collective-permute-done.14), channel_id=1, source_target_pairs={{4,0},{5,1},{6,2},{7,3},{8,12},{9,13},{10,14},{11,15},{20,16},{21,... | collective-permute-start | bytes 1179656 | tf_op jit(solution)/shard_map/ppermute | solution.py:249
  98.6 11.6 %collective-permute-start.24 = (bf16[512,384]{1,0:T(8,128)(2,1)S(1)}, bf16[512,384]{1,0:T(8,128)(2,1)S(1)}, u32[]{:S(2)}, u32[]{:S(2)}) collective-permute-start(bf16[512,384]{1,0:T(8,128)(2,1)S(1)} %collective-permute-done.23.refs_0_.refs_1_), channel_id=1, source_target_pairs={{4,0},{5,1},{6,2},{7,3},{8,12},{9,13},{10,14},{11,15},{20,16},{21,... | collective-permute-start | bytes 1179656 | tf_op jit(solution)/shard_map/ppermute | solution.py:249
  101.0 10.6 %collective-permute-start.29 = (bf16[512,384]{1,0:T(8,128)(2,1)S(1)}, bf16[512,384]{1,0:T(8,128)(2,1)S(1)}, u32[]{:S(2)}, u32[]{:S(2)}) collective-permute-start(bf16[512,384]{1,0:T(8,128)(2,1)S(1)} %collective-permute-done.18.refs_1_.refs_2_), channel_id=1, source_target_pairs={{4,8},{5,9},{6,10},{7,11},{8,4},{9,5},{10,6},{11,7},{20,24},{21,25... | collective-permute-start | bytes 1179656 | tf_op jit(solution)/shard_map/ppermute | solution.py:249
  103.4 29.1 %collective-permute-start.19 = (bf16[512,1024]{1,0:T(8,128)(2,1)}, bf16[512,1024]{1,0:T(8,128)(2,1)}, u32[]{:S(2)}, u32[]{:S(2)}) collective-permute-start(bf16[512,1024]{1,0:T(8,128)(2,1)} %shard_map.124), channel_id=1, source_target_pairs={{0,1},{1,0},{2,3},{3,2},{4,5},{5,4},{6,7},{7,6},{8,9},{9,8},{10,11... | collective-permute-start | bytes 3145736 | tf_op jit(solution)/shard_map/ppermute | solution.py:249
  111.5 14.9 %collective-permute-start.25 = (bf16[512,512]{1,0:T(8,128)(2,1)}, bf16[512,512]{1,0:T(8,128)(2,1)}, u32[]{:S(2)}, u32[]{:S(2)}) collective-permute-start(bf16[512,512]{1,0:T(8,128)(2,1)} %shard_map.126), channel_id=1, source_target_pairs={{0,1},{1,0},{2,3},{3,2},{4,5},{5,4},{6,7},{7,6},{8,9},{9,8},{10,11... | collective-permute-start | bytes 1572872 | tf_op jit(solution)/shard_map/ppermute | solution.py:249
  111.5 13.4 %collective-permute-start.30 = (bf16[512,384]{1,0:T(8,128)(2,1)S(1)}, bf16[512,384]{1,0:T(8,128)(2,1)S(1)}, u32[]{:S(2)}, u32[]{:S(2)}) collective-permute-start(bf16[512,384]{1,0:T(8,128)(2,1)S(1)} %collective-permute-done.29.refs_0_.refs_1_), channel_id=1, source_target_pairs={{4,0},{5,1},{6,2},{7,3},{8,12},{9,13},{10,14},{11,15},{20,16},{21,... | collective-permute-start | bytes 1179656 | tf_op jit(solution)/shard_map/ppermute | solution.py:249
  114.7 16.4 %collective-permute-start.54 = (bf16[2,128,384]{2,1,0:T(8,128)(2,1)}, bf16[2,128,384]{2,1,0:T(8,128)(2,1)}, u32[]{:S(2)}, u32[]{:S(2)}) collective-permute-start(bf16[2,128,384]{2,1,0:T(8,128)(2,1)} %get-tuple-element.150), channel_id=1, source_target_pairs={{0,16},{1,17},{2,18},{3,19},{4,20},{5,21},{6,22},{7,23},{8,24},{9,... | collective-permute-start | bytes 589832 | tf_op jit(solution)/shard_map/ppermute | solution.py:249
  125.4 15.2 %collective-permute-start.31 = (bf16[512,512]{1,0:T(8,128)(2,1)S(1)}, bf16[512,512]{1,0:T(8,128)(2,1)S(1)}, u32[]{:S(2)}, u32[]{:S(2)}) collective-permute-start(bf16[512,512]{1,0:T(8,128)(2,1)S(1)} %shard_map.128), channel_id=1, source_target_pairs={{0,1},{1,0},{2,3},{3,2},{4,5},{5,4},{6,7},{7,6},{8,9},{9,8},{10,11... | collective-permute-start | bytes 1572872 | tf_op jit(solution)/shard_map/ppermute | solution.py:249
  128.0 6.6 %collective-permute-start.26 = (bf16[128,512]{1,0:T(8,128)(2,1)S(1)}, bf16[128,512]{1,0:T(8,128)(2,1)S(1)}, u32[]{:S(2)}, u32[]{:S(2)}) collective-permute-start(bf16[128,512]{1,0:T(8,128)(2,1)S(1)} %get-tuple-element.77), channel_id=1, source_target_pairs={{0,2},{1,3},{2,0},{3,1},{4,6},{5,7},{6,4},{7,5},{8,10},{9,11},{10,... | collective-permute-start | bytes 393224 | tf_op jit(solution)/shard_map/ppermute | solution.py:249
  129.6 6.6 %collective-permute-start.27 = (bf16[128,512]{1,0:T(8,128)(2,1)S(1)}, bf16[128,512]{1,0:T(8,128)(2,1)S(1)}, u32[]{:S(2)}, u32[]{:S(2)}) collective-permute-start(bf16[128,512]{1,0:T(8,128)(2,1)S(1)} %get-tuple-element.78), channel_id=1, source_target_pairs={{0,16},{1,17},{2,18},{3,19},{4,20},{5,21},{6,22},{7,23},{8,24},{9,... | collective-permute-start | bytes 393224 | tf_op jit(solution)/shard_map/ppermute | solution.py:249
  131.1 7.0 %collective-permute-start.28 = (bf16[128,512]{1,0:T(8,128)(2,1)S(1)}, bf16[128,512]{1,0:T(8,128)(2,1)S(1)}, u32[]{:S(2)}, u32[]{:S(2)}) collective-permute-start(bf16[128,512]{1,0:T(8,128)(2,1)S(1)} %get-tuple-element.79), channel_id=1, source_target_pairs={{0,18},{1,19},{2,16},{3,17},{4,22},{5,23},{6,20},{7,21},{8,26},{9,... | collective-permute-start | bytes 393224 | tf_op jit(solution)/shard_map/ppermute | solution.py:249
  132.5 29.8 %collective-permute-start.55 = (bf16[256,768]{1,0:T(8,128)(2,1)S(1)}, bf16[256,768]{1,0:T(8,128)(2,1)S(1)}, u32[]{:S(2)}, u32[]{:S(2)}) collective-permute-start(bf16[256,768]{1,0:T(8,128)(2,1)S(1)} %pad_maximum_fusion.11.refs_4_), channel_id=1, source_target_pairs={{0,4},{1,5},{2,6},{3,7},{4,0},{5,1},{6,2},{7,3},{8,12},{9,13},{10,... | collective-permute-start | bytes 1179656 | tf_op jit(solution)/shard_map/ppermute | solution.py:249
  134.6 13.7 %collective-permute-start.20 = (bf16[128,1024]{1,0:T(8,128)(2,1)S(1)}, bf16[128,1024]{1,0:T(8,128)(2,1)S(1)}, u32[]{:S(2)}, u32[]{:S(2)}) collective-permute-start(bf16[128,1024]{1,0:T(8,128)(2,1)S(1)} %get-tuple-element.73), channel_id=1, source_target_pairs={{0,2},{1,3},{2,0},{3,1},{4,6},{5,7},{6,4},{7,5},{8,10},{9,11},{10,... | collective-permute-start | bytes 786440 | tf_op jit(solution)/shard_map/ppermute | solution.py:249
  136.2 13.6 %collective-permute-start.21 = (bf16[128,1024]{1,0:T(8,128)(2,1)S(1)}, bf16[128,1024]{1,0:T(8,128)(2,1)S(1)}, u32[]{:S(2)}, u32[]{:S(2)}) collective-permute-start(bf16[128,1024]{1,0:T(8,128)(2,1)S(1)} %get-tuple-element.74), channel_id=1, source_target_pairs={{0,16},{1,17},{2,18},{3,19},{4,20},{5,21},{6,22},{7,23},{8,24},{9,... | collective-permute-start | bytes 786440 | tf_op jit(solution)/shard_map/ppermute | solution.py:249
  138.1 12.9 %collective-permute-start.22 = (bf16[128,1024]{1,0:T(8,128)(2,1)S(1)}, bf16[128,1024]{1,0:T(8,128)(2,1)S(1)}, u32[]{:S(2)}, u32[]{:S(2)}) collective-permute-start(bf16[128,1024]{1,0:T(8,128)(2,1)S(1)} %get-tuple-element.75), channel_id=1, source_target_pairs={{0,18},{1,19},{2,16},{3,17},{4,22},{5,23},{6,20},{7,21},{8,26},{9,... | collective-permute-start | bytes 786440 | tf_op jit(solution)/shard_map/ppermute | solution.py:249
  141.1 12.3 %collective-permute-start.32 = (bf16[128,512]{1,0:T(8,128)(2,1)S(1)}, bf16[128,512]{1,0:T(8,128)(2,1)S(1)}, u32[]{:S(2)}, u32[]{:S(2)}) collective-permute-start(bf16[128,512]{1,0:T(8,128)(2,1)S(1)} %get-tuple-element.81), channel_id=1, source_target_pairs={{0,2},{1,3},{2,0},{3,1},{4,6},{5,7},{6,4},{7,5},{8,10},{9,11},{10,... | collective-permute-start | bytes 393224 | tf_op jit(solution)/shard_map/ppermute | solution.py:249
  148.3 5.4 %collective-permute-start.33 = (bf16[128,512]{1,0:T(8,128)(2,1)S(1)}, bf16[128,512]{1,0:T(8,128)(2,1)S(1)}, u32[]{:S(2)}, u32[]{:S(2)}) collective-permute-start(bf16[128,512]{1,0:T(8,128)(2,1)S(1)} %get-tuple-element.82), channel_id=1, source_target_pairs={{0,16},{1,17},{2,18},{3,19},{4,20},{5,21},{6,22},{7,23},{8,24},{9,... | collective-permute-start | bytes 393224 | tf_op jit(solution)/shard_map/ppermute | solution.py:249
  149.8 5.9 %collective-permute-start.34 = (bf16[128,512]{1,0:T(8,128)(2,1)S(1)}, bf16[128,512]{1,0:T(8,128)(2,1)S(1)}, u32[]{:S(2)}, u32[]{:S(2)}) collective-permute-start(bf16[128,512]{1,0:T(8,128)(2,1)S(1)} %get-tuple-element.83), channel_id=1, source_target_pairs={{0,18},{1,19},{2,16},{3,17},{4,22},{5,23},{6,20},{7,21},{8,26},{9,... | collective-permute-start | bytes 393224 | tf_op jit(solution)/shard_map/ppermute | solution.py:249
  157.0 6.0 %collective-permute-start.48 = (bf16[64,512]{1,0:T(8,128)(2,1)S(1)}, bf16[64,512]{1,0:T(8,128)(2,1)S(1)}, u32[]{:S(2)}, u32[]{:S(2)}) collective-permute-start(bf16[64,512]{1,0:T(8,128)(2,1)S(1)} %get-tuple-element.97), channel_id=1, source_target_pairs={{0,4},{1,5},{2,6},{3,7},{4,0},{5,1},{6,2},{7,3},{8,12},{9,13},{10,... | collective-permute-start | bytes 196616 | tf_op jit(solution)/shard_map/ppermute | solution.py:249
  158.3 5.4 %collective-permute-start.49 = (bf16[64,512]{1,0:T(8,128)(2,1)S(1)}, bf16[64,512]{1,0:T(8,128)(2,1)S(1)}, u32[]{:S(2)}, u32[]{:S(2)}) collective-permute-start(bf16[64,512]{1,0:T(8,128)(2,1)S(1)} %get-tuple-element.98), channel_id=1, source_target_pairs={{0,8},{1,9},{2,10},{3,11},{4,12},{5,13},{6,14},{7,15},{8,0},{9,1},... | collective-permute-start | bytes 196616 | tf_op jit(solution)/shard_map/ppermute | solution.py:249
  160.7 6.1 %collective-permute-start.50 = (bf16[64,512]{1,0:T(8,128)(2,1)S(1)}, bf16[64,512]{1,0:T(8,128)(2,1)S(1)}, u32[]{:S(2)}, u32[]{:S(2)}) collective-permute-start(bf16[64,512]{1,0:T(8,128)(2,1)S(1)} %get-tuple-element.99), channel_id=1, source_target_pairs={{0,12},{1,13},{2,14},{3,15},{4,8},{5,9},{6,10},{7,11},{8,4},{9,5},... | collective-permute-start | bytes 196616 | tf_op jit(solution)/shard_map/ppermute | solution.py:249
  161.6 6.3 %collective-permute-start.35 = (bf16[64,2048]{1,0:T(8,128)(2,1)S(1)}, bf16[64,2048]{1,0:T(8,128)(2,1)S(1)}, u32[]{:S(2)}, u32[]{:S(2)}) collective-permute-start(bf16[64,2048]{1,0:T(8,128)(2,1)S(1)} %fusion.22), channel_id=1, source_target_pairs={{0,1},{1,0},{2,3},{3,2},{4,5},{5,4},{6,7},{7,6},{8,9},{9,8},{10,11... | collective-permute-start | bytes 786440 | tf_op jit(solution)/shard_map/ppermute | solution.py:249
  162.3 7.3 %collective-permute-start.56 = (bf16[256,768]{1,0:T(8,128)(2,1)S(1)}, bf16[256,768]{1,0:T(8,128)(2,1)S(1)}, u32[]{:S(2)}, u32[]{:S(2)}) collective-permute-start(bf16[256,768]{1,0:T(8,128)(2,1)S(1)} %pad_maximum_fusion.11.refs_4_), channel_id=1, source_target_pairs={{4,8},{5,9},{6,10},{7,11},{8,4},{9,5},{10,6},{11,7},{20,24},{21,25... | collective-permute-start | bytes 1179656 | tf_op jit(solution)/shard_map/ppermute | solution.py:249
  163.0 6.7 %collective-permute-start.58 = (bf16[256,768]{1,0:T(8,128)(2,1)S(1)}, bf16[256,768]{1,0:T(8,128)(2,1)S(1)}, u32[]{:S(2)}, u32[]{:S(2)}) collective-permute-start(bf16[256,768]{1,0:T(8,128)(2,1)S(1)} %collective-permute-done.55.refs_5_), channel_id=1, source_target_pairs={{4,8},{5,9},{6,10},{7,11},{8,4},{9,5},{10,6},{11,7},{20,24},{21,25... | collective-permute-start | bytes 1179656 | tf_op jit(solution)/shard_map/ppermute | solution.py:249
  163.7 11.5 %collective-permute-start.36 = (bf16[64,2048]{1,0:T(8,128)(2,1)S(1)}, bf16[64,2048]{1,0:T(8,128)(2,1)S(1)}, u32[]{:S(2)}, u32[]{:S(2)}) collective-permute-start(bf16[64,2048]{1,0:T(8,128)(2,1)S(1)} %get-tuple-element.126.refs_0_), channel_id=1, source_target_pairs={{0,2},{1,3},{2,0},{3,1},{4,6},{5,7},{6,4},{7,5},{8,10},{9,11},{10,... | collective-permute-start | bytes 786440 | tf_op jit(solution)/shard_map/ppermute | solution.py:249
  166.8 9.2 %collective-permute-start.37 = (bf16[64,2048]{1,0:T(8,128)(2,1)S(1)}, bf16[64,2048]{1,0:T(8,128)(2,1)S(1)}, u32[]{:S(2)}, u32[]{:S(2)}) collective-permute-start(bf16[64,2048]{1,0:T(8,128)(2,1)S(1)} %get-tuple-element.126.refs_0_), channel_id=1, source_target_pairs={{0,16},{1,17},{2,18},{3,19},{4,20},{5,21},{6,22},{7,23},{8,24},{9,... | collective-permute-start | bytes 786440 | tf_op jit(solution)/shard_map/ppermute | solution.py:249
  168.0 11.3 %collective-permute-start.38 = (bf16[64,2048]{1,0:T(8,128)(2,1)S(1)}, bf16[64,2048]{1,0:T(8,128)(2,1)S(1)}, u32[]{:S(2)}, u32[]{:S(2)}) collective-permute-start(bf16[64,2048]{1,0:T(8,128)(2,1)S(1)} %get-tuple-element.126.refs_0_), channel_id=1, source_target_pairs={{0,18},{1,19},{2,16},{3,17},{4,22},{5,23},{6,20},{7,21},{8,26},{9,... | collective-permute-start | bytes 786440 | tf_op jit(solution)/shard_map/ppermute | solution.py:249
  169.6 10.6 %collective-permute-start.39 = (bf16[64,2048]{1,0:T(8,128)(2,1)S(1)}, bf16[64,2048]{1,0:T(8,128)(2,1)S(1)}, u32[]{:S(2)}, u32[]{:S(2)}) collective-permute-start(bf16[64,2048]{1,0:T(8,128)(2,1)S(1)} %get-tuple-element.126.refs_0_), channel_id=1, source_target_pairs={{0,1},{1,0},{2,3},{3,2},{4,5},{5,4},{6,7},{7,6},{8,9},{9,8},{10,11... | collective-permute-start | bytes 786440 | tf_op jit(solution)/shard_map/ppermute | solution.py:249
  169.7 14.0 %collective-permute-start.51 = (bf16[4,64,512]{2,1,0:T(8,128)(2,1)S(1)}, bf16[4,64,512]{2,1,0:T(8,128)(2,1)S(1)}, u32[]{:S(2)}, u32[]{:S(2)}) collective-permute-start(bf16[4,64,512]{2,1,0:T(8,128)(2,1)S(1)} %pad_maximum_fusion.12.refs_0_), channel_id=1, source_target_pairs={{0,2},{1,3},{2,0},{3,1},{4,6},{5,7},{6,4},{7,5},{8,10},{9,11},{10,... | collective-permute-start | bytes 786440 | tf_op jit(solution)/shard_map/ppermute | solution.py:249
  175.2 9.8 %collective-permute-start.40 = (bf16[64,2048]{1,0:T(8,128)(2,1)S(1)}, bf16[64,2048]{1,0:T(8,128)(2,1)S(1)}, u32[]{:S(2)}, u32[]{:S(2)}) collective-permute-start(bf16[64,2048]{1,0:T(8,128)(2,1)S(1)} %collective-permute-done.36), channel_id=1, source_target_pairs={{0,1},{1,0},{2,3},{3,2},{4,5},{5,4},{6,7},{7,6},{8,9},{9,8},{10,11... | collective-permute-start | bytes 786440 | tf_op jit(solution)/shard_map/ppermute | solution.py:249
  175.9 9.1 %collective-permute-start.41 = (bf16[64,2048]{1,0:T(8,128)(2,1)S(1)}, bf16[64,2048]{1,0:T(8,128)(2,1)S(1)}, u32[]{:S(2)}, u32[]{:S(2)}) collective-permute-start(bf16[64,2048]{1,0:T(8,128)(2,1)S(1)} %collective-permute-done.37), channel_id=1, source_target_pairs={{0,1},{1,0},{2,3},{3,2},{4,5},{5,4},{6,7},{7,6},{8,9},{9,8},{10,11... | collective-permute-start | bytes 786440 | tf_op jit(solution)/shard_map/ppermute | solution.py:249
  179.3 6.3 %collective-permute-start.42 = (bf16[64,2048]{1,0:T(8,128)(2,1)S(1)}, bf16[64,2048]{1,0:T(8,128)(2,1)S(1)}, u32[]{:S(2)}, u32[]{:S(2)}) collective-permute-start(bf16[64,2048]{1,0:T(8,128)(2,1)S(1)} %collective-permute-done.38), channel_id=1, source_target_pairs={{0,1},{1,0},{2,3},{3,2},{4,5},{5,4},{6,7},{7,6},{8,9},{9,8},{10,11... | collective-permute-start | bytes 786440 | tf_op jit(solution)/shard_map/ppermute | solution.py:249
  180.3 19.0 %collective-permute-start.57 = (bf16[256,768]{1,0:T(8,128)(2,1)S(1)}, bf16[256,768]{1,0:T(8,128)(2,1)S(1)}, u32[]{:S(2)}, u32[]{:S(2)}) collective-permute-start(bf16[256,768]{1,0:T(8,128)(2,1)S(1)} %collective-permute-done.56.refs_6_), channel_id=1, source_target_pairs={{4,0},{5,1},{6,2},{7,3},{8,12},{9,13},{10,14},{11,15},{20,16},{21,... | collective-permute-start | bytes 1179656 | tf_op jit(solution)/shard_map/ppermute | solution.py:249
  183.7 23.8 %collective-permute-start.59 = (bf16[256,768]{1,0:T(8,128)(2,1)S(1)}, bf16[256,768]{1,0:T(8,128)(2,1)S(1)}, u32[]{:S(2)}, u32[]{:S(2)}) collective-permute-start(bf16[256,768]{1,0:T(8,128)(2,1)S(1)} %collective-permute-done.58.refs_8_), channel_id=1, source_target_pairs={{4,0},{5,1},{6,2},{7,3},{8,12},{9,13},{10,14},{11,15},{20,16},{21,... | collective-permute-start | bytes 1179656 | tf_op jit(solution)/shard_map/ppermute | solution.py:249
  185.0 22.5 %collective-permute-start.52 = (bf16[4,64,512]{2,1,0:T(8,128)(2,1)S(1)}, bf16[4,64,512]{2,1,0:T(8,128)(2,1)S(1)}, u32[]{:S(2)}, u32[]{:S(2)}) collective-permute-start(bf16[4,64,512]{2,1,0:T(8,128)(2,1)S(1)} %pad_maximum_fusion.12.refs_0_), channel_id=1, source_target_pairs={{0,1},{1,0},{2,3},{3,2},{4,5},{5,4},{6,7},{7,6},{8,9},{9,8},{10,11... | collective-permute-start | bytes 786440 | tf_op jit(solution)/shard_map/ppermute | solution.py:249
  185.1 22.4 %collective-permute-start.53 = (bf16[4,64,512]{2,1,0:T(8,128)(2,1)S(1)}, bf16[4,64,512]{2,1,0:T(8,128)(2,1)S(1)}, u32[]{:S(2)}, u32[]{:S(2)}) collective-permute-start(bf16[4,64,512]{2,1,0:T(8,128)(2,1)S(1)} %collective-permute-done.51.refs_1_), channel_id=1, source_target_pairs={{0,1},{1,0},{2,3},{3,2},{4,5},{5,4},{6,7},{7,6},{8,9},{9,8},{10,11... | collective-permute-start | bytes 786440 | tf_op jit(solution)/shard_map/ppermute | solution.py:249
  189.1 21.9 %collective-permute-start.43 = (bf16[256,2048]{1,0:T(8,128)(2,1)S(1)}, bf16[256,2048]{1,0:T(8,128)(2,1)S(1)}, u32[]{:S(2)}, u32[]{:S(2)}) collective-permute-start(bf16[256,2048]{1,0:T(8,128)(2,1)S(1)} %convolution_convert_fusion), channel_id=1, source_target_pairs={{0,1},{1,0},{2,3},{3,2},{4,5},{5,4},{6,7},{7,6},{8,9},{9,8},{10,11... | collective-permute-start | bytes 3145736 | tf_op jit(solution)/shard_map/ppermute | solution.py:249
  209.4 13.4 %collective-permute-start.60 = (bf16[256,768]{1,0:T(8,128)(2,1)S(1)}, bf16[256,768]{1,0:T(8,128)(2,1)S(1)}, u32[]{:S(2)}, u32[]{:S(2)}) collective-permute-start(bf16[256,768]{1,0:T(8,128)(2,1)S(1)} %get-tuple-element.111), channel_id=1, source_target_pairs={{0,2},{1,3},{2,0},{3,1},{4,6},{5,7},{6,4},{7,5},{8,10},{9,11},{10,... | collective-permute-start | bytes 1179656 | tf_op jit(solution)/shard_map/ppermute | solution.py:249
  212.1 19.6 %copy-start.11 = (bf16[128,2048]{1,0:T(8,128)(2,1)S(1)}, bf16[128,2048]{1,0:T(8,128)(2,1)}, u32[]{:S(2)}) copy-start(bf16[128,2048]{1,0:T(8,128)(2,1)} %param.11) | copy-start | bytes 1572868
  212.1 19.9 %copy-start.1 = (bf16[128,2048]{1,0:T(8,128)(2,1)S(1)}, bf16[128,2048]{1,0:T(8,128)(2,1)}, u32[]{:S(2)}) copy-start(bf16[128,2048]{1,0:T(8,128)(2,1)} %cot_ref) | copy-start | bytes 1572868
  212.2 19.4 %collective-permute-start.44 = (bf16[64,2048]{1,0:T(8,128)(2,1)S(1)}, bf16[64,2048]{1,0:T(8,128)(2,1)S(1)}, u32[]{:S(2)}, u32[]{:S(2)}) collective-permute-start(bf16[64,2048]{1,0:T(8,128)(2,1)S(1)} %get-tuple-element.123), channel_id=1, source_target_pairs={{0,2},{1,3},{2,0},{3,1},{4,6},{5,7},{6,4},{7,5},{8,10},{9,11},{10,... | collective-permute-start | bytes 786440 | tf_op jit(solution)/shard_map/ppermute | solution.py:249
  213.1 18.5 %collective-permute-start.45 = (bf16[64,2048]{1,0:T(8,128)(2,1)S(1)}, bf16[64,2048]{1,0:T(8,128)(2,1)S(1)}, u32[]{:S(2)}, u32[]{:S(2)}) collective-permute-start(bf16[64,2048]{1,0:T(8,128)(2,1)S(1)} %get-tuple-element.125), channel_id=1, source_target_pairs={{0,16},{1,17},{2,18},{3,19},{4,20},{5,21},{6,22},{7,23},{8,24},{9,... | collective-permute-start | bytes 786440 | tf_op jit(solution)/shard_map/ppermute | solution.py:249
  214.4 17.2 %collective-permute-start.46 = (bf16[64,2048]{1,0:T(8,128)(2,1)S(1)}, bf16[64,2048]{1,0:T(8,128)(2,1)S(1)}, u32[]{:S(2)}, u32[]{:S(2)}) collective-permute-start(bf16[64,2048]{1,0:T(8,128)(2,1)S(1)} %get-tuple-element.124), channel_id=1, source_target_pairs={{0,18},{1,19},{2,16},{3,17},{4,22},{5,23},{6,20},{7,21},{8,26},{9,... | collective-permute-start | bytes 786440 | tf_op jit(solution)/shard_map/ppermute | solution.py:249
  232.2 1.6 collective-permute-start.47
  (16 other events, 86.2 us)

commit v6 on v5

--- a/solution.py
+++ b/solution.py
@@ -371,7 +371,8 @@
             halves.append((gate * sig * up).astype(bf16).reshape(T, PT * m, w))
         for_gate = (up * sig * (1.0 + gate * (1.0 - sig))).astype(bf16)
         for_up = (gate * sig).astype(bf16)
-        for_gate, for_up = lax.optimization_barrier((for_gate, for_up))
+        by_rep = [[v.reshape(T, R, G * m, w)[:, a].reshape(G * n, w) for v in (for_gate, for_up)] for a in range(R)]
+        by_rep = lax.optimization_barrier(by_rep)
 
         block = arrange(dn, [(y - d) % G for d in range(G)], G, axis=0)
         if Z > 1:
@@ -397,18 +398,6 @@
                     total = total + send(low[p], dr=dr, dy=dy).astype(f32)
             return total
 
-        def reduce_plane(left, weight):
-            got = []
-            for j in range(1, T):
-                value = nt(left[j], weight).astype(bf16)
-                got.append(send(value, dt=j))
-            chip = nt(left[0], weight)
-            for value in got:
-                chip = chip + value.astype(f32)
-            low = chip.astype(bf16)
-            low = low.reshape(PT, m, -1)
-            return plane_sum([low[p] for p in range(PT)]), low
-
         by_core = [jnp.concatenate([half[j] for half in halves]) for j in range(T)]
         groups = [[0, 1]] + [[k] for k in range(2, Z)] if Z > 1 else [[0]]
         totals, total_ids = [], []
@@ -448,14 +437,27 @@
             down_full.append(value)
         down_full = jnp.concatenate(down_full, axis=0)
         raw = plane(dbranch)
-        spread = spread_c = [cores(h) for h in raw]
-        spread = jnp.stack([jnp.stack([h[j] for h in spread]) for j in range(T)]).reshape(PT * n, D)
-        dhidden = jnp.dot(spread, down_full, preferred_element_type=f32)
-        dgate = (dhidden * for_gate.astype(f32)).astype(bf16)
-        dup = (dhidden * for_up.astype(f32)).astype(bf16)
-        dgu = jnp.concatenate([dgate, dup], axis=1).reshape(T, PT * m, 2 * w)
+        spread = [cores(h) for h in raw]
         full = complete(dbranch)
-        dnormed, dlow = reduce_plane([dgu[j] for j in range(T)], full)
+        dnormed = None
+        for a in range(R):
+            some = range(a * G, (a + 1) * G)
+            rows = jnp.stack([jnp.stack([spread[p][j] for p in some]) for j in range(T)]).reshape(G * n, D)
+            dhidden = jnp.dot(rows, down_full, preferred_element_type=f32)
+            dgu = jnp.concatenate([(dhidden * v.astype(f32)).astype(bf16) for v in by_rep[a]], axis=1)
+            dgu = dgu.reshape(T, G * m, 2 * w)
+            got = []
+            for j in range(1, T):
+                value = nt(dgu[j], full).astype(bf16)
+                got.append(send(value, dt=j))
+            chip = nt(dgu[0], full)
+            for value in got:
+                chip = chip + value.astype(f32)
+            dlow = chip.astype(bf16).reshape(G, m, D)
+            for b in range(G):
+                p = a * G + b
+                term = (send(dlow[b], dr=a, dy=b) if p else dlow[b]).astype(f32)
+                dnormed = term if dnormed is None else dnormed + term
         early_f = own_rows(x_early).astype(f32)
         early_rs = lax.dynamic_slice_in_dim(scale[1], t * m, m, 0)
         gained = pre_gain * dnormed

time: 236 us -> 223 us (0.945)
  waiting for transfers between devices: 125 us -> 115 us
  matrix products: 7.65 us -> 10.4 us
  local copies, waits for them, and re-layouts: 9.38 us -> 6.94 us
    ppermute x61 -> x62, waiting for transfers between devices: 125 us -> 115 us  [send(): return lax.ppermute(value, AXES, pairs)]
    dot_general x2 -> x4, matrix products: 2.05 us -> 4.64 us  [nt(): lax.dot_general(left, right, (((1,), (1,)), ((), ())), preferred_element_...]
    ppermute x61 -> x62, starting transfers between devices: 64.5 us -> 64 us  [send(): return lax.ppermute(value, AXES, pairs)]
  transfers between devices with their start and end apart: 61 -> 62, of which waited for: 23 -> 25; matrix products, arithmetic and copies ran while one was open for 11% -> 11% of each run, Pallas kernels for 5% -> 4%
where the time goes in v6:
time: 223 us; the launch traced here: 222 us
  waiting for transfers between devices  115 us (52%)
  starting transfers between devices  64 us (29%)
  other arithmetic  13.5 us (6%)
  matrix products  10.4 us (5%)
  Pallas kernels  10 us (4%)
  local copies, waits for them, and re-layouts  6.94 us (3%)
    ppermute x62, waiting for transfers between devices, send(): return lax.ppermute(value, AXES, pairs)  115 us
    ppermute x62, starting transfers between devices, send(): return lax.ppermute(value, AXES, pairs)  64 us
    dot_general x4, matrix products, nt(): lax.dot_general(left, right, (((1,), (1,)), ((), ())), preferred_element_...  4.64 us
  transfers between devices with their start and end apart: 62, of which 25 were waited for; matrix products, arithmetic and copies ran while one was open for 11% of the time, Pallas kernels for 4%

profile of v6, /device:TPU:0, one launch (start us, length us, event | category | flops | bytes accessed | tf_op | source)
XLA Modules:
  0.0 221.9 jit_solution(12021183000099707251)
XLA Ops:
  0.8 1.4 pad_maximum_fusion.2
  3.7 1.1 constant_dynamic-slice_fusion.2
  4.7 3.0 %collective-permute-start = (bf16[2,64,2048]{2,1,0:T(8,128)(2,1)}, bf16[2,64,2048]{2,1,0:T(8,128)(2,1)S(1)}, u32[]{:S(2)}, u32[]{:S(2)}) collective-permute-start(bf16[2,64,2048]{2,1,0:T(8,128)(2,1)} %bitcast.6), channel_id=1, source_target_pairs={{0,2},{1,3},{2,0},{3,1},{4,6},{5,7},{6,4},{7,5},{8,10},{9,11},{10,... | collective-permute-start | bytes 1572872 | tf_op jit(solution)/shard_map/ppermute | solution.py:249
  7.7 1.5 collective-permute-start.1
  9.2 1.6 collective-permute-start.6
  11.9 1.6 collective-permute-start.17
  15.3 17.2 %collective-permute-done.17 = bf16[256,384]{1,0:T(8,128)(2,1)S(1)} collective-permute-done((bf16[256,384]{1,0:T(8,128)(2,1)S(1)}, bf16[256,384]{1,0:T(8,128)(2,1)S(1)}, u32[]{:S(2)}, u32[]{:S(2)}) %collective-permute-start.17) | collective-permute-done | bytes 196640 | tf_op jit(solution)/shard_map/ppermute | solution.py:249
  33.2 2.7 %collective-permute-start.2 = (bf16[2,64,2048]{2,1,0:T(8,128)(2,1)}, bf16[2,64,2048]{2,1,0:T(8,128)(2,1)S(1)}, u32[]{:S(2)}, u32[]{:S(2)}) collective-permute-start(bf16[2,64,2048]{2,1,0:T(8,128)(2,1)} %bitcast.6), channel_id=1, source_target_pairs={{0,18},{1,19},{2,16},{3,17},{4,22},{5,23},{6,20},{7,21},{8,26},{9,... | collective-permute-start | bytes 1572872 | tf_op jit(solution)/shard_map/ppermute | solution.py:249
  36.0 4.4 %collective-permute-start.9 = (bf16[256,768]{1,0:T(8,128)(2,1)S(1)}, bf16[256,768]{1,0:T(8,128)(2,1)S(1)}, u32[]{:S(2)}, u32[]{:S(2)}) collective-permute-start(bf16[256,768]{1,0:T(8,128)(2,1)S(1)} %collective-permute-done.8), channel_id=1, source_target_pairs={{0,4},{1,5},{2,6},{3,7},{4,0},{5,1},{6,2},{7,3},{8,12},{9,13},{10,... | collective-permute-start | bytes 1179656 | tf_op jit(solution)/shard_map/ppermute | solution.py:249
  42.5 1.3 collective-permute-start.11
  44.5 3.0 %collective-permute-done.2 = bf16[2,64,2048]{2,1,0:T(8,128)(2,1)S(1)} collective-permute-done((bf16[2,64,2048]{2,1,0:T(8,128)(2,1)}, bf16[2,64,2048]{2,1,0:T(8,128)(2,1)S(1)}, u32[]{:S(2)}, u32[]{:S(2)}) %collective-permute-start.2) | collective-permute-done | bytes 524320 | tf_op jit(solution)/shard_map/ppermute | solution.py:249
  47.5 1.3 maximum_bitcast_fusion
  49.6 8.5 %collective-permute-done.11 = bf16[256,768]{1,0:T(8,128)(2,1)S(1)} collective-permute-done((bf16[256,768]{1,0:T(8,128)(2,1)S(1)}, bf16[256,768]{1,0:T(8,128)(2,1)S(1)}, u32[]{:S(2)}, u32[]{:S(2)}) %collective-permute-start.11) | collective-permute-done | bytes 393248 | tf_op jit(solution)/shard_map/ppermute | solution.py:249
  58.1 1.3 collective-permute-start.13
  60.2 1.3 collective-permute-start.15
  63.2 8.8 %collective-permute-done.13 = bf16[256,768]{1,0:T(8,128)(2,1)S(1)} collective-permute-done((bf16[256,768]{1,0:T(8,128)(2,1)S(1)}, bf16[256,768]{1,0:T(8,128)(2,1)S(1)}, u32[]{:S(2)}, u32[]{:S(2)}) %collective-permute-start.13) | collective-permute-done | bytes 393248 | tf_op jit(solution)/shard_map/ppermute | solution.py:249
  72.0 3.8 %collective-permute-start.18 = (bf16[512,384]{1,0:T(8,128)(2,1)S(1)}, bf16[512,384]{1,0:T(8,128)(2,1)S(1)}, u32[]{:S(2)}, u32[]{:S(2)}) collective-permute-start(bf16[512,384]{1,0:T(8,128)(2,1)S(1)} %pad_maximum_fusion.10.refs_0_.refs_1_), channel_id=1, source_target_pairs={{0,4},{1,5},{2,6},{3,7},{4,0},{5,1},{6,2},{7,3},{8,12},{9,13},{10,... | collective-permute-start | bytes 1179656 | tf_op jit(solution)/shard_map/ppermute | solution.py:249
  76.6 3.8 %collective-permute-done.15 = bf16[256,768]{1,0:T(8,128)(2,1)S(1)} collective-permute-done((bf16[256,768]{1,0:T(8,128)(2,1)S(1)}, bf16[256,768]{1,0:T(8,128)(2,1)S(1)}, u32[]{:S(2)}, u32[]{:S(2)}) %collective-permute-start.15) | collective-permute-done | bytes 393248 | tf_op jit(solution)/shard_map/ppermute | solution.py:249
  81.2 1.8 fusion.49
  83.0 1.3 collective-permute-start.16
  84.3 1.8 fusion.48
  86.1 10.4 %collective-permute-done.16 = bf16[256,768]{1,0:T(8,128)(2,1)S(1)} collective-permute-done((bf16[256,768]{1,0:T(8,128)(2,1)S(1)}, bf16[256,768]{1,0:T(8,128)(2,1)S(1)}, u32[]{:S(2)}, u32[]{:S(2)}) %collective-permute-start.16) | collective-permute-done | bytes 393248 | tf_op jit(solution)/shard_map/ppermute | solution.py:249
  96.8 1.3 fusion.31
  99.7 1.7 shard_map.124
  101.5 1.3 collective-permute-start.24
  103.8 11.1 %collective-permute-done.24.refs_1_.refs_2_ = bf16[512,384]{1,0:T(8,128)(2,1)S(1)} collective-permute-done((bf16[512,384]{1,0:T(8,128)(2,1)S(1)}, bf16[512,384]{1,0:T(8,128)(2,1)S(1)}, u32[]{:S(2)}, u32[]{:S(2)}) %collective-permute-start.24) | collective-permute-done | bytes 393248 | tf_op jit(solution)/shard_map/ppermute | solution.py:249
  115.4 1.1 fusion.43
  116.5 1.6 collective-permute-start.55
  118.1 1.3 collective-permute-start.30
  119.5 4.4 %collective-permute-done.55 = bf16[2,128,384]{2,1,0:T(8,128)(2,1)S(1)} collective-permute-done((bf16[2,128,384]{2,1,0:T(8,128)(2,1)S(1)}, bf16[2,128,384]{2,1,0:T(8,128)(2,1)S(1)}, u32[]{:S(2)}, u32[]{:S(2)}) %collective-permute-start.55) | collective-permute-done | bytes 196640 | tf_op jit(solution)/shard_map/ppermute | solution.py:249
  124.0 7.9 %collective-permute-done.30.refs_1_.refs_2_ = bf16[512,384]{1,0:T(8,128)(2,1)S(1)} collective-permute-done((bf16[512,384]{1,0:T(8,128)(2,1)S(1)}, bf16[512,384]{1,0:T(8,128)(2,1)S(1)}, u32[]{:S(2)}, u32[]{:S(2)}) %collective-permute-start.30) | collective-permute-done | bytes 393248 | tf_op jit(solution)/shard_map/ppermute | solution.py:249
  133.0 1.6 collective-permute-start.26
  135.1 1.4 collective-permute-start.28
  136.6 2.0 shard_map.125
  138.9 1.5 collective-permute-start.20
  141.5 2.0 collective-permute-done.28
  143.5 1.5 collective-permute-start.22
  147.0 3.1 %collective-permute-done.20 = bf16[128,1024]{1,0:T(8,128)(2,1)S(1)} collective-permute-done((bf16[128,1024]{1,0:T(8,128)(2,1)S(1)}, bf16[128,1024]{1,0:T(8,128)(2,1)S(1)}, u32[]{:S(2)}, u32[]{:S(2)}) %collective-permute-start.20) | collective-permute-done | bytes 262176 | tf_op jit(solution)/shard_map/ppermute | solution.py:249
  150.1 1.5 collective-permute-start.32
  152.1 2.4 %collective-permute-done.22 = bf16[128,1024]{1,0:T(8,128)(2,1)S(1)} collective-permute-done((bf16[128,1024]{1,0:T(8,128)(2,1)S(1)}, bf16[128,1024]{1,0:T(8,128)(2,1)S(1)}, u32[]{:S(2)}, u32[]{:S(2)}) %collective-permute-start.22) | collective-permute-done | bytes 262176 | tf_op jit(solution)/shard_map/ppermute | solution.py:249
  154.6 1.5 collective-permute-start.34
  156.2 1.5 collective-permute-done.32
  157.8 2.7 %collective-permute-done.34 = bf16[128,512]{1,0:T(8,128)(2,1)S(1)} collective-permute-done((bf16[128,512]{1,0:T(8,128)(2,1)S(1)}, bf16[128,512]{1,0:T(8,128)(2,1)S(1)}, u32[]{:S(2)}, u32[]{:S(2)}) %collective-permute-start.34) | collective-permute-done | bytes 131104 | tf_op jit(solution)/shard_map/ppermute | solution.py:249
  161.8 3.0 %collective-permute-start.50 = (bf16[64,512]{1,0:T(8,128)(2,1)S(1)}, bf16[64,512]{1,0:T(8,128)(2,1)S(1)}, u32[]{:S(2)}, u32[]{:S(2)}) collective-permute-start(bf16[64,512]{1,0:T(8,128)(2,1)S(1)} %get-tuple-element.102), channel_id=1, source_target_pairs={{0,8},{1,9},{2,10},{3,11},{4,12},{5,13},{6,14},{7,15},{8,0},{9,1},... | collective-permute-start | bytes 196616 | tf_op jit(solution)/shard_map/ppermute | solution.py:249
  164.8 1.4 collective-permute-start.51
  167.5 1.3 collective-permute-start.58
  168.8 1.3 collective-permute-start.60
  170.1 1.6 collective-permute-start.36
  172.3 1.7 collective-permute-start.42
  174.0 4.9 %collective-permute-done.36 = bf16[64,2048]{1,0:T(8,128)(2,1)S(1)} collective-permute-done((bf16[64,2048]{1,0:T(8,128)(2,1)S(1)}, bf16[64,2048]{1,0:T(8,128)(2,1)S(1)}, u32[]{:S(2)}, u32[]{:S(2)}) %collective-permute-start.36) | collective-permute-done | bytes 262176 | tf_op jit(solution)/shard_map/ppermute | solution.py:249
  178.9 1.9 collective-permute-done.41
  181.6 4.2 %collective-permute-done.42 = bf16[64,2048]{1,0:T(8,128)(2,1)S(1)} collective-permute-done((bf16[64,2048]{1,0:T(8,128)(2,1)S(1)}, bf16[64,2048]{1,0:T(8,128)(2,1)S(1)}, u32[]{:S(2)}, u32[]{:S(2)}) %collective-permute-start.42) | collective-permute-done | bytes 262176 | tf_op jit(solution)/shard_map/ppermute | solution.py:249
  188.4 1.2 convolution_convert_fusion.1
  189.5 1.8 collective-permute-done.52.refs_1_
  192.8 1.2 convolution_convert_fusion
  194.5 1.9 shard_map.131
  196.4 1.6 collective-permute-start.61
  198.4 1.2 add_convert_fusion.1
  199.6 1.2 collective-permute-start.40
  200.8 1.2 add_convert_fusion
  202.6 1.8 collective-permute-start.47
  204.5 4.0 %collective-permute-done.61 = bf16[256,768]{1,0:T(8,128)(2,1)S(1)} collective-permute-done((bf16[256,768]{1,0:T(8,128)(2,1)S(1)}, bf16[256,768]{1,0:T(8,128)(2,1)S(1)}, u32[]{:S(2)}, u32[]{:S(2)}) %collective-permute-start.61) | collective-permute-done | bytes 393248 | tf_op jit(solution)/shard_map/ppermute | solution.py:249
  208.6 10.2 %collective-permute-done.40 = bf16[64,2048]{1,0:T(8,128)(2,1)S(1)} collective-permute-done((bf16[64,2048]{1,0:T(8,128)(2,1)S(1)}, bf16[64,2048]{1,0:T(8,128)(2,1)S(1)}, u32[]{:S(2)}, u32[]{:S(2)}) %collective-permute-start.40) | collective-permute-done | bytes 262176 | tf_op jit(solution)/shard_map/ppermute | solution.py:249
  219.5 1.4 convert_add_fusion
  (205 shorter events, 33.2 us)
Async XLA Ops:
  4.7 37.7 %collective-permute-start = (bf16[2,64,2048]{2,1,0:T(8,128)(2,1)}, bf16[2,64,2048]{2,1,0:T(8,128)(2,1)S(1)}, u32[]{:S(2)}, u32[]{:S(2)}) collective-permute-start(bf16[2,64,2048]{2,1,0:T(8,128)(2,1)} %bitcast.6), channel_id=1, source_target_pairs={{0,2},{1,3},{2,0},{3,1},{4,6},{5,7},{6,4},{7,5},{8,10},{9,11},{10,... | collective-permute-start | bytes 1572872 | tf_op jit(solution)/shard_map/ppermute | solution.py:249
  7.7 36.1 %collective-permute-start.1 = (bf16[2,64,2048]{2,1,0:T(8,128)(2,1)}, bf16[2,64,2048]{2,1,0:T(8,128)(2,1)S(1)}, u32[]{:S(2)}, u32[]{:S(2)}) collective-permute-start(bf16[2,64,2048]{2,1,0:T(8,128)(2,1)} %bitcast.6), channel_id=1, source_target_pairs={{0,16},{1,17},{2,18},{3,19},{4,20},{5,21},{6,22},{7,23},{8,24},{9,... | collective-permute-start | bytes 1572872 | tf_op jit(solution)/shard_map/ppermute | solution.py:249
  9.2 24.0 %collective-permute-start.6 = (bf16[256,768]{1,0:T(8,128)(2,1)S(1)}, bf16[256,768]{1,0:T(8,128)(2,1)}, u32[]{:S(2)}, u32[]{:S(2)}) collective-permute-start(bf16[256,768]{1,0:T(8,128)(2,1)S(1)} %get-tuple-element.61), channel_id=1, source_target_pairs={{0,4},{1,5},{2,6},{3,7},{4,0},{5,1},{6,2},{7,3},{8,12},{9,13},{10,... | collective-permute-start | bytes 1179656 | tf_op jit(solution)/shard_map/ppermute | solution.py:249
  10.8 25.2 %collective-permute-start.8 = (bf16[256,768]{1,0:T(8,128)(2,1)S(1)}, bf16[256,768]{1,0:T(8,128)(2,1)S(1)}, u32[]{:S(2)}, u32[]{:S(2)}) collective-permute-start(bf16[256,768]{1,0:T(8,128)(2,1)S(1)} %get-tuple-element.63), channel_id=1, source_target_pairs={{0,2},{1,3},{2,0},{3,1},{4,6},{5,7},{6,4},{7,5},{8,10},{9,11},{10,... | collective-permute-start | bytes 1179656 | tf_op jit(solution)/shard_map/ppermute | solution.py:249
  11.9 20.6 %collective-permute-start.17 = (bf16[256,384]{1,0:T(8,128)(2,1)S(1)}, bf16[256,384]{1,0:T(8,128)(2,1)S(1)}, u32[]{:S(2)}, u32[]{:S(2)}) collective-permute-start(bf16[256,384]{1,0:T(8,128)(2,1)S(1)} %get-tuple-element.71), channel_id=1, source_target_pairs={{0,2},{1,3},{2,0},{3,1},{4,6},{5,7},{6,4},{7,5},{8,10},{9,11},{10,... | collective-permute-start | bytes 589832 | tf_op jit(solution)/shard_map/ppermute | solution.py:249
  32.5 9.2 %collective-permute-start.7 = (bf16[256,768]{1,0:T(8,128)(2,1)S(1)}, bf16[256,768]{1,0:T(8,128)(2,1)S(1)}, u32[]{:S(2)}, u32[]{:S(2)}) collective-permute-start(bf16[256,768]{1,0:T(8,128)(2,1)S(1)} %get-tuple-element.61), channel_id=1, source_target_pairs={{4,8},{5,9},{6,10},{7,11},{8,4},{9,5},{10,6},{11,7},{20,24},{21,25... | collective-permute-start | bytes 1179656 | tf_op jit(solution)/shard_map/ppermute | solution.py:249
  33.2 14.3 %collective-permute-start.2 = (bf16[2,64,2048]{2,1,0:T(8,128)(2,1)}, bf16[2,64,2048]{2,1,0:T(8,128)(2,1)S(1)}, u32[]{:S(2)}, u32[]{:S(2)}) collective-permute-start(bf16[2,64,2048]{2,1,0:T(8,128)(2,1)} %bitcast.6), channel_id=1, source_target_pairs={{0,18},{1,19},{2,16},{3,17},{4,22},{5,23},{6,20},{7,21},{8,26},{9,... | collective-permute-start | bytes 1572872 | tf_op jit(solution)/shard_map/ppermute | solution.py:249
  36.0 12.8 %collective-permute-start.9 = (bf16[256,768]{1,0:T(8,128)(2,1)S(1)}, bf16[256,768]{1,0:T(8,128)(2,1)S(1)}, u32[]{:S(2)}, u32[]{:S(2)}) collective-permute-start(bf16[256,768]{1,0:T(8,128)(2,1)S(1)} %collective-permute-done.8), channel_id=1, source_target_pairs={{0,4},{1,5},{2,6},{3,7},{4,0},{5,1},{6,2},{7,3},{8,12},{9,13},{10,... | collective-permute-start | bytes 1179656 | tf_op jit(solution)/shard_map/ppermute | solution.py:249
  41.7 7.7 %collective-permute-start.10 = (bf16[256,768]{1,0:T(8,128)(2,1)S(1)}, bf16[256,768]{1,0:T(8,128)(2,1)S(1)}, u32[]{:S(2)}, u32[]{:S(2)}) collective-permute-start(bf16[256,768]{1,0:T(8,128)(2,1)S(1)} %collective-permute-done.8), channel_id=1, source_target_pairs={{4,8},{5,9},{6,10},{7,11},{8,4},{9,5},{10,6},{11,7},{20,24},{21,25... | collective-permute-start | bytes 1179656 | tf_op jit(solution)/shard_map/ppermute | solution.py:249
  42.5 15.6 %collective-permute-start.11 = (bf16[256,768]{1,0:T(8,128)(2,1)S(1)}, bf16[256,768]{1,0:T(8,128)(2,1)S(1)}, u32[]{:S(2)}, u32[]{:S(2)}) collective-permute-start(bf16[256,768]{1,0:T(8,128)(2,1)S(1)} %collective-permute-done.7), channel_id=1, source_target_pairs={{4,0},{5,1},{6,2},{7,3},{8,12},{9,13},{10,14},{11,15},{20,16},{21,... | collective-permute-start | bytes 1179656 | tf_op jit(solution)/shard_map/ppermute | solution.py:249
  43.8 15.7 %collective-permute-start.12 = (bf16[256,768]{1,0:T(8,128)(2,1)}, bf16[256,768]{1,0:T(8,128)(2,1)S(1)}, u32[]{:S(2)}, u32[]{:S(2)}) collective-permute-start(bf16[256,768]{1,0:T(8,128)(2,1)} %collective-permute-done.6), channel_id=1, source_target_pairs={{4,8},{5,9},{6,10},{7,11},{8,4},{9,5},{10,6},{11,7},{20,24},{21,25... | collective-permute-start | bytes 1179656 | tf_op jit(solution)/shard_map/ppermute | solution.py:249
  47.5 12.7 %collective-permute-start.3 = (bf16[2,64,2048]{2,1,0:T(8,128)(2,1)S(1)}, bf16[2,64,2048]{2,1,0:T(8,128)(2,1)S(1)}, u32[]{:S(2)}, u32[]{:S(2)}) collective-permute-start(bf16[2,64,2048]{2,1,0:T(8,128)(2,1)S(1)} %collective-permute-done), channel_id=1, source_target_pairs={{0,1},{1,0},{2,3},{3,2},{4,5},{5,4},{6,7},{7,6},{8,9},{9,8},{10,11... | collective-permute-start | bytes 1572872 | tf_op jit(solution)/shard_map/ppermute | solution.py:249
  48.8 12.7 %collective-permute-start.4 = (bf16[2,64,2048]{2,1,0:T(8,128)(2,1)S(1)}, bf16[2,64,2048]{2,1,0:T(8,128)(2,1)S(1)}, u32[]{:S(2)}, u32[]{:S(2)}) collective-permute-start(bf16[2,64,2048]{2,1,0:T(8,128)(2,1)S(1)} %collective-permute-done.1), channel_id=1, source_target_pairs={{0,1},{1,0},{2,3},{3,2},{4,5},{5,4},{6,7},{7,6},{8,9},{9,8},{10,11... | collective-permute-start | bytes 1572872 | tf_op jit(solution)/shard_map/ppermute | solution.py:249
  49.4 12.1 %collective-permute-start.5 = (bf16[2,64,2048]{2,1,0:T(8,128)(2,1)S(1)}, bf16[2,64,2048]{2,1,0:T(8,128)(2,1)S(1)}, u32[]{:S(2)}, u32[]{:S(2)}) collective-permute-start(bf16[2,64,2048]{2,1,0:T(8,128)(2,1)S(1)} %collective-permute-done.2), channel_id=1, source_target_pairs={{0,1},{1,0},{2,3},{3,2},{4,5},{5,4},{6,7},{7,6},{8,9},{9,8},{10,11... | collective-permute-start | bytes 1572872 | tf_op jit(solution)/shard_map/ppermute | solution.py:249
  58.1 13.9 %collective-permute-start.13 = (bf16[256,768]{1,0:T(8,128)(2,1)S(1)}, bf16[256,768]{1,0:T(8,128)(2,1)S(1)}, u32[]{:S(2)}, u32[]{:S(2)}) collective-permute-start(bf16[256,768]{1,0:T(8,128)(2,1)S(1)} %collective-permute-done.10), channel_id=1, source_target_pairs={{4,0},{5,1},{6,2},{7,3},{8,12},{9,13},{10,14},{11,15},{20,16},{21,... | collective-permute-start | bytes 1179656 | tf_op jit(solution)/shard_map/ppermute | solution.py:249
  59.4 12.5 %collective-permute-start.14 = (bf16[256,768]{1,0:T(8,128)(2,1)S(1)}, bf16[256,768]{1,0:T(8,128)(2,1)S(1)}, u32[]{:S(2)}, u32[]{:S(2)}) collective-permute-start(bf16[256,768]{1,0:T(8,128)(2,1)S(1)} %collective-permute-done.9), channel_id=1, source_target_pairs={{4,8},{5,9},{6,10},{7,11},{8,4},{9,5},{10,6},{11,7},{20,24},{21,25... | collective-permute-start | bytes 1179656 | tf_op jit(solution)/shard_map/ppermute | solution.py:249
  60.2 20.2 %collective-permute-start.15 = (bf16[256,768]{1,0:T(8,128)(2,1)S(1)}, bf16[256,768]{1,0:T(8,128)(2,1)S(1)}, u32[]{:S(2)}, u32[]{:S(2)}) collective-permute-start(bf16[256,768]{1,0:T(8,128)(2,1)S(1)} %collective-permute-done.12), channel_id=1, source_target_pairs={{4,0},{5,1},{6,2},{7,3},{8,12},{9,13},{10,14},{11,15},{20,16},{21,... | collective-permute-start | bytes 1179656 | tf_op jit(solution)/shard_map/ppermute | solution.py:249
  63.2 17.3 %copy-start = (bf16[128,2048]{1,0:T(8,128)(2,1)S(1)}, bf16[128,2048]{1,0:T(8,128)(2,1)}, u32[]{:S(2)}) copy-start(bf16[128,2048]{1,0:T(8,128)(2,1)} %cot_ref) | copy-start | bytes 1572868
  63.2 17.3 %copy-start.4 = (f32[2048]{0:T(1024)S(1)}, f32[2048]{0:T(1024)}, u32[]{:S(2)}) copy-start(f32[2048]{0:T(1024)} %param.14) | copy-start | bytes 24580
  72.0 27.8 %collective-permute-start.18 = (bf16[512,384]{1,0:T(8,128)(2,1)S(1)}, bf16[512,384]{1,0:T(8,128)(2,1)S(1)}, u32[]{:S(2)}, u32[]{:S(2)}) collective-permute-start(bf16[512,384]{1,0:T(8,128)(2,1)S(1)} %pad_maximum_fusion.10.refs_0_.refs_1_), channel_id=1, source_target_pairs={{0,4},{1,5},{2,6},{3,7},{4,0},{5,1},{6,2},{7,3},{8,12},{9,13},{10,... | collective-permute-start | bytes 1179656 | tf_op jit(solution)/shard_map/ppermute | solution.py:249
  75.8 25.7 %collective-permute-start.23 = (bf16[512,384]{1,0:T(8,128)(2,1)S(1)}, bf16[512,384]{1,0:T(8,128)(2,1)S(1)}, u32[]{:S(2)}, u32[]{:S(2)}) collective-permute-start(bf16[512,384]{1,0:T(8,128)(2,1)S(1)} %pad_maximum_fusion.10.refs_0_.refs_1_), channel_id=1, source_target_pairs={{4,8},{5,9},{6,10},{7,11},{8,4},{9,5},{10,6},{11,7},{20,24},{21,25... | collective-permute-start | bytes 1179656 | tf_op jit(solution)/shard_map/ppermute | solution.py:249
  83.0 13.5 %collective-permute-start.16 = (bf16[256,768]{1,0:T(8,128)(2,1)S(1)}, bf16[256,768]{1,0:T(8,128)(2,1)S(1)}, u32[]{:S(2)}, u32[]{:S(2)}) collective-permute-start(bf16[256,768]{1,0:T(8,128)(2,1)S(1)} %collective-permute-done.14), channel_id=1, source_target_pairs={{4,0},{5,1},{6,2},{7,3},{8,12},{9,13},{10,14},{11,15},{20,16},{21,... | collective-permute-start | bytes 1179656 | tf_op jit(solution)/shard_map/ppermute | solution.py:249
  101.5 33.6 %collective-permute-start.19 = (bf16[512,1024]{1,0:T(8,128)(2,1)}, bf16[512,1024]{1,0:T(8,128)(2,1)}, u32[]{:S(2)}, u32[]{:S(2)}) collective-permute-start(bf16[512,1024]{1,0:T(8,128)(2,1)} %shard_map.124), channel_id=1, source_target_pairs={{0,1},{1,0},{2,3},{3,2},{4,5},{5,4},{6,7},{7,6},{8,9},{9,8},{10,11... | collective-permute-start | bytes 3145736 | tf_op jit(solution)/shard_map/ppermute | solution.py:249
  101.5 13.4 %collective-permute-start.24 = (bf16[512,384]{1,0:T(8,128)(2,1)S(1)}, bf16[512,384]{1,0:T(8,128)(2,1)S(1)}, u32[]{:S(2)}, u32[]{:S(2)}) collective-permute-start(bf16[512,384]{1,0:T(8,128)(2,1)S(1)} %collective-permute-done.23.refs_0_.refs_1_), channel_id=1, source_target_pairs={{4,0},{5,1},{6,2},{7,3},{8,12},{9,13},{10,14},{11,15},{20,16},{21,... | collective-permute-start | bytes 1179656 | tf_op jit(solution)/shard_map/ppermute | solution.py:249
  102.9 15.2 %collective-permute-start.29 = (bf16[512,384]{1,0:T(8,128)(2,1)S(1)}, bf16[512,384]{1,0:T(8,128)(2,1)S(1)}, u32[]{:S(2)}, u32[]{:S(2)}) collective-permute-start(bf16[512,384]{1,0:T(8,128)(2,1)S(1)} %collective-permute-done.18.refs_1_.refs_2_), channel_id=1, source_target_pairs={{4,8},{5,9},{6,10},{7,11},{8,4},{9,5},{10,6},{11,7},{20,24},{21,25... | collective-permute-start | bytes 1179656 | tf_op jit(solution)/shard_map/ppermute | solution.py:249
  115.4 17.1 %collective-permute-start.25 = (bf16[512,512]{1,0:T(8,128)(2,1)S(1)}, bf16[512,512]{1,0:T(8,128)(2,1)S(1)}, u32[]{:S(2)}, u32[]{:S(2)}) collective-permute-start(bf16[512,512]{1,0:T(8,128)(2,1)S(1)} %shard_map.126), channel_id=1, source_target_pairs={{0,1},{1,0},{2,3},{3,2},{4,5},{5,4},{6,7},{7,6},{8,9},{9,8},{10,11... | collective-permute-start | bytes 1572872 | tf_op jit(solution)/shard_map/ppermute | solution.py:249
  116.5 7.4 %collective-permute-start.55 = (bf16[2,128,384]{2,1,0:T(8,128)(2,1)S(1)}, bf16[2,128,384]{2,1,0:T(8,128)(2,1)S(1)}, u32[]{:S(2)}, u32[]{:S(2)}) collective-permute-start(bf16[2,128,384]{2,1,0:T(8,128)(2,1)S(1)} %get-tuple-element.151), channel_id=1, source_target_pairs={{0,16},{1,17},{2,18},{3,19},{4,20},{5,21},{6,22},{7,23},{8,24},{9,... | collective-permute-start | bytes 589832 | tf_op jit(solution)/shard_map/ppermute | solution.py:249
  118.1 13.9 %collective-permute-start.30 = (bf16[512,384]{1,0:T(8,128)(2,1)S(1)}, bf16[512,384]{1,0:T(8,128)(2,1)S(1)}, u32[]{:S(2)}, u32[]{:S(2)}) collective-permute-start(bf16[512,384]{1,0:T(8,128)(2,1)S(1)} %collective-permute-done.29.refs_0_.refs_1_), channel_id=1, source_target_pairs={{4,0},{5,1},{6,2},{7,3},{8,12},{9,13},{10,14},{11,15},{20,16},{21,... | collective-permute-start | bytes 1179656 | tf_op jit(solution)/shard_map/ppermute | solution.py:249
  123.9 21.2 %collective-permute-start.56 = (bf16[256,768]{1,0:T(8,128)(2,1)S(1)}, bf16[256,768]{1,0:T(8,128)(2,1)S(1)}, u32[]{:S(2)}, u32[]{:S(2)}) collective-permute-start(bf16[256,768]{1,0:T(8,128)(2,1)S(1)} %pad_maximum_fusion.11.refs_4_), channel_id=1, source_target_pairs={{0,4},{1,5},{2,6},{3,7},{4,0},{5,1},{6,2},{7,3},{8,12},{9,13},{10,... | collective-permute-start | bytes 1179656 | tf_op jit(solution)/shard_map/ppermute | solution.py:249
  132.4 13.4 %collective-permute-start.31 = (bf16[512,512]{1,0:T(8,128)(2,1)S(1)}, bf16[512,512]{1,0:T(8,128)(2,1)S(1)}, u32[]{:S(2)}, u32[]{:S(2)}) collective-permute-start(bf16[512,512]{1,0:T(8,128)(2,1)S(1)} %shard_map.128), channel_id=1, source_target_pairs={{0,1},{1,0},{2,3},{3,2},{4,5},{5,4},{6,7},{7,6},{8,9},{9,8},{10,11... | collective-permute-start | bytes 1572872 | tf_op jit(solution)/shard_map/ppermute | solution.py:249
  133.0 5.9 %collective-permute-start.26 = (bf16[128,512]{1,0:T(8,128)(2,1)S(1)}, bf16[128,512]{1,0:T(8,128)(2,1)S(1)}, u32[]{:S(2)}, u32[]{:S(2)}) collective-permute-start(bf16[128,512]{1,0:T(8,128)(2,1)S(1)} %get-tuple-element.79), channel_id=1, source_target_pairs={{0,2},{1,3},{2,0},{3,1},{4,6},{5,7},{6,4},{7,5},{8,10},{9,11},{10,... | collective-permute-start | bytes 393224 | tf_op jit(solution)/shard_map/ppermute | solution.py:249
  134.6 6.4 %collective-permute-start.27 = (bf16[128,512]{1,0:T(8,128)(2,1)S(1)}, bf16[128,512]{1,0:T(8,128)(2,1)S(1)}, u32[]{:S(2)}, u32[]{:S(2)}) collective-permute-start(bf16[128,512]{1,0:T(8,128)(2,1)S(1)} %get-tuple-element.80), channel_id=1, source_target_pairs={{0,16},{1,17},{2,18},{3,19},{4,20},{5,21},{6,22},{7,23},{8,24},{9,... | collective-permute-start | bytes 393224 | tf_op jit(solution)/shard_map/ppermute | solution.py:249
  135.1 8.4 %collective-permute-start.28 = (bf16[128,512]{1,0:T(8,128)(2,1)S(1)}, bf16[128,512]{1,0:T(8,128)(2,1)S(1)}, u32[]{:S(2)}, u32[]{:S(2)}) collective-permute-start(bf16[128,512]{1,0:T(8,128)(2,1)S(1)} %get-tuple-element.81), channel_id=1, source_target_pairs={{0,18},{1,19},{2,16},{3,17},{4,22},{5,23},{6,20},{7,21},{8,26},{9,... | collective-permute-start | bytes 393224 | tf_op jit(solution)/shard_map/ppermute | solution.py:249
  138.9 11.1 %collective-permute-start.20 = (bf16[128,1024]{1,0:T(8,128)(2,1)S(1)}, bf16[128,1024]{1,0:T(8,128)(2,1)S(1)}, u32[]{:S(2)}, u32[]{:S(2)}) collective-permute-start(bf16[128,1024]{1,0:T(8,128)(2,1)S(1)} %get-tuple-element.75), channel_id=1, source_target_pairs={{0,2},{1,3},{2,0},{3,1},{4,6},{5,7},{6,4},{7,5},{8,10},{9,11},{10,... | collective-permute-start | bytes 786440 | tf_op jit(solution)/shard_map/ppermute | solution.py:249
  140.9 10.6 %collective-permute-start.21 = (bf16[128,1024]{1,0:T(8,128)(2,1)S(1)}, bf16[128,1024]{1,0:T(8,128)(2,1)S(1)}, u32[]{:S(2)}, u32[]{:S(2)}) collective-permute-start(bf16[128,1024]{1,0:T(8,128)(2,1)S(1)} %get-tuple-element.76), channel_id=1, source_target_pairs={{0,16},{1,17},{2,18},{3,19},{4,20},{5,21},{6,22},{7,23},{8,24},{9,... | collective-permute-start | bytes 786440 | tf_op jit(solution)/shard_map/ppermute | solution.py:249
  143.5 11.0 %collective-permute-start.22 = (bf16[128,1024]{1,0:T(8,128)(2,1)S(1)}, bf16[128,1024]{1,0:T(8,128)(2,1)S(1)}, u32[]{:S(2)}, u32[]{:S(2)}) collective-permute-start(bf16[128,1024]{1,0:T(8,128)(2,1)S(1)} %get-tuple-element.77), channel_id=1, source_target_pairs={{0,18},{1,19},{2,16},{3,17},{4,22},{5,23},{6,20},{7,21},{8,26},{9,... | collective-permute-start | bytes 786440 | tf_op jit(solution)/shard_map/ppermute | solution.py:249
  145.1 22.3 %collective-permute-start.57 = (bf16[256,768]{1,0:T(8,128)(2,1)S(1)}, bf16[256,768]{1,0:T(8,128)(2,1)S(1)}, u32[]{:S(2)}, u32[]{:S(2)}) collective-permute-start(bf16[256,768]{1,0:T(8,128)(2,1)S(1)} %pad_maximum_fusion.11.refs_4_), channel_id=1, source_target_pairs={{4,8},{5,9},{6,10},{7,11},{8,4},{9,5},{10,6},{11,7},{20,24},{21,25... | collective-permute-start | bytes 1179656 | tf_op jit(solution)/shard_map/ppermute | solution.py:249
  145.8 21.7 %collective-permute-start.59 = (bf16[256,768]{1,0:T(8,128)(2,1)S(1)}, bf16[256,768]{1,0:T(8,128)(2,1)S(1)}, u32[]{:S(2)}, u32[]{:S(2)}) collective-permute-start(bf16[256,768]{1,0:T(8,128)(2,1)S(1)} %collective-permute-done.56.refs_5_), channel_id=1, source_target_pairs={{4,8},{5,9},{6,10},{7,11},{8,4},{9,5},{10,6},{11,7},{20,24},{21,25... | collective-permute-start | bytes 1179656 | tf_op jit(solution)/shard_map/ppermute | solution.py:249
  150.1 7.6 %collective-permute-start.32 = (bf16[128,512]{1,0:T(8,128)(2,1)S(1)}, bf16[128,512]{1,0:T(8,128)(2,1)S(1)}, u32[]{:S(2)}, u32[]{:S(2)}) collective-permute-start(bf16[128,512]{1,0:T(8,128)(2,1)S(1)} %get-tuple-element.83), channel_id=1, source_target_pairs={{0,2},{1,3},{2,0},{3,1},{4,6},{5,7},{6,4},{7,5},{8,10},{9,11},{10,... | collective-permute-start | bytes 393224 | tf_op jit(solution)/shard_map/ppermute | solution.py:249
  151.6 6.2 %collective-permute-start.33 = (bf16[128,512]{1,0:T(8,128)(2,1)S(1)}, bf16[128,512]{1,0:T(8,128)(2,1)S(1)}, u32[]{:S(2)}, u32[]{:S(2)}) collective-permute-start(bf16[128,512]{1,0:T(8,128)(2,1)S(1)} %get-tuple-element.84), channel_id=1, source_target_pairs={{0,16},{1,17},{2,18},{3,19},{4,20},{5,21},{6,22},{7,23},{8,24},{9,... | collective-permute-start | bytes 393224 | tf_op jit(solution)/shard_map/ppermute | solution.py:249
  154.6 5.9 %collective-permute-start.34 = (bf16[128,512]{1,0:T(8,128)(2,1)S(1)}, bf16[128,512]{1,0:T(8,128)(2,1)S(1)}, u32[]{:S(2)}, u32[]{:S(2)}) collective-permute-start(bf16[128,512]{1,0:T(8,128)(2,1)S(1)} %get-tuple-element.85), channel_id=1, source_target_pairs={{0,18},{1,19},{2,16},{3,17},{4,22},{5,23},{6,20},{7,21},{8,26},{9,... | collective-permute-start | bytes 393224 | tf_op jit(solution)/shard_map/ppermute | solution.py:249
  161.7 7.1 %collective-permute-start.49 = (bf16[64,512]{1,0:T(8,128)(2,1)S(1)}, bf16[64,512]{1,0:T(8,128)(2,1)S(1)}, u32[]{:S(2)}, u32[]{:S(2)}) collective-permute-start(bf16[64,512]{1,0:T(8,128)(2,1)S(1)} %get-tuple-element.101), channel_id=1, source_target_pairs={{0,4},{1,5},{2,6},{3,7},{4,0},{5,1},{6,2},{7,3},{8,12},{9,13},{10,... | collective-permute-start | bytes 196616 | tf_op jit(solution)/shard_map/ppermute | solution.py:249
  161.8 8.3 %collective-permute-start.50 = (bf16[64,512]{1,0:T(8,128)(2,1)S(1)}, bf16[64,512]{1,0:T(8,128)(2,1)S(1)}, u32[]{:S(2)}, u32[]{:S(2)}) collective-permute-start(bf16[64,512]{1,0:T(8,128)(2,1)S(1)} %get-tuple-element.102), channel_id=1, source_target_pairs={{0,8},{1,9},{2,10},{3,11},{4,12},{5,13},{6,14},{7,15},{8,0},{9,1},... | collective-permute-start | bytes 196616 | tf_op jit(solution)/shard_map/ppermute | solution.py:249
  164.8 6.9 %collective-permute-start.51 = (bf16[64,512]{1,0:T(8,128)(2,1)S(1)}, bf16[64,512]{1,0:T(8,128)(2,1)S(1)}, u32[]{:S(2)}, u32[]{:S(2)}) collective-permute-start(bf16[64,512]{1,0:T(8,128)(2,1)S(1)} %get-tuple-element.103), channel_id=1, source_target_pairs={{0,12},{1,13},{2,14},{3,15},{4,8},{5,9},{6,10},{7,11},{8,4},{9,5},... | collective-permute-start | bytes 196616 | tf_op jit(solution)/shard_map/ppermute | solution.py:249
  167.4 4.9 %collective-permute-start.35 = (bf16[64,2048]{1,0:T(8,128)(2,1)S(1)}, bf16[64,2048]{1,0:T(8,128)(2,1)S(1)}, u32[]{:S(2)}, u32[]{:S(2)}) collective-permute-start(bf16[64,2048]{1,0:T(8,128)(2,1)S(1)} %fusion.14), channel_id=1, source_target_pairs={{0,1},{1,0},{2,3},{3,2},{4,5},{5,4},{6,7},{7,6},{8,9},{9,8},{10,11... | collective-permute-start | bytes 786440 | tf_op jit(solution)/shard_map/ppermute | solution.py:249
  167.5 26.4 %collective-permute-start.58 = (bf16[256,768]{1,0:T(8,128)(2,1)S(1)}, bf16[256,768]{1,0:T(8,128)(2,1)S(1)}, u32[]{:S(2)}, u32[]{:S(2)}) collective-permute-start(bf16[256,768]{1,0:T(8,128)(2,1)S(1)} %collective-permute-done.57.refs_6_), channel_id=1, source_target_pairs={{4,0},{5,1},{6,2},{7,3},{8,12},{9,13},{10,14},{11,15},{20,16},{21,... | collective-permute-start | bytes 1179656 | tf_op jit(solution)/shard_map/ppermute | solution.py:249
  168.8 25.7 %collective-permute-start.60 = (bf16[256,768]{1,0:T(8,128)(2,1)S(1)}, bf16[256,768]{1,0:T(8,128)(2,1)S(1)}, u32[]{:S(2)}, u32[]{:S(2)}) collective-permute-start(bf16[256,768]{1,0:T(8,128)(2,1)S(1)} %collective-permute-done.59.refs_8_), channel_id=1, source_target_pairs={{4,0},{5,1},{6,2},{7,3},{8,12},{9,13},{10,14},{11,15},{20,16},{21,... | collective-permute-start | bytes 1179656 | tf_op jit(solution)/shard_map/ppermute | solution.py:249
  170.1 8.8 %collective-permute-start.36 = (bf16[64,2048]{1,0:T(8,128)(2,1)S(1)}, bf16[64,2048]{1,0:T(8,128)(2,1)S(1)}, u32[]{:S(2)}, u32[]{:S(2)}) collective-permute-start(bf16[64,2048]{1,0:T(8,128)(2,1)S(1)} %get-tuple-element.127.refs_0_), channel_id=1, source_target_pairs={{0,2},{1,3},{2,0},{3,1},{4,6},{5,7},{6,4},{7,5},{8,10},{9,11},{10,... | collective-permute-start | bytes 786440 | tf_op jit(solution)/shard_map/ppermute | solution.py:249
  171.7 9.2 %collective-permute-start.41 = (bf16[64,2048]{1,0:T(8,128)(2,1)S(1)}, bf16[64,2048]{1,0:T(8,128)(2,1)S(1)}, u32[]{:S(2)}, u32[]{:S(2)}) collective-permute-start(bf16[64,2048]{1,0:T(8,128)(2,1)S(1)} %get-tuple-element.127.refs_0_), channel_id=1, source_target_pairs={{0,16},{1,17},{2,18},{3,19},{4,20},{5,21},{6,22},{7,23},{8,24},{9,... | collective-permute-start | bytes 786440 | tf_op jit(solution)/shard_map/ppermute | solution.py:249
  172.3 13.5 %collective-permute-start.42 = (bf16[64,2048]{1,0:T(8,128)(2,1)S(1)}, bf16[64,2048]{1,0:T(8,128)(2,1)S(1)}, u32[]{:S(2)}, u32[]{:S(2)}) collective-permute-start(bf16[64,2048]{1,0:T(8,128)(2,1)S(1)} %get-tuple-element.127.refs_0_), channel_id=1, source_target_pairs={{0,18},{1,19},{2,16},{3,17},{4,22},{5,23},{6,20},{7,21},{8,26},{9,... | collective-permute-start | bytes 786440 | tf_op jit(solution)/shard_map/ppermute | solution.py:249
  178.9 7.8 %collective-permute-start.37 = (bf16[64,2048]{1,0:T(8,128)(2,1)S(1)}, bf16[64,2048]{1,0:T(8,128)(2,1)S(1)}, u32[]{:S(2)}, u32[]{:S(2)}) collective-permute-start(bf16[64,2048]{1,0:T(8,128)(2,1)S(1)} %get-tuple-element.127.refs_0_), channel_id=1, source_target_pairs={{0,1},{1,0},{2,3},{3,2},{4,5},{5,4},{6,7},{7,6},{8,9},{9,8},{10,11... | collective-permute-start | bytes 786440 | tf_op jit(solution)/shard_map/ppermute | solution.py:249
  180.9 10.4 %collective-permute-start.52 = (bf16[4,64,512]{2,1,0:T(8,128)(2,1)S(1)}, bf16[4,64,512]{2,1,0:T(8,128)(2,1)S(1)}, u32[]{:S(2)}, u32[]{:S(2)}) collective-permute-start(bf16[4,64,512]{2,1,0:T(8,128)(2,1)S(1)} %pad_maximum_fusion.14.refs_0_), channel_id=1, source_target_pairs={{0,2},{1,3},{2,0},{3,1},{4,6},{5,7},{6,4},{7,5},{8,10},{9,11},{10,... | collective-permute-start | bytes 786440 | tf_op jit(solution)/shard_map/ppermute | solution.py:249
  185.8 1.5 collective-permute-start.38
  186.7 4.6 %collective-permute-start.43 = (bf16[64,2048]{1,0:T(8,128)(2,1)S(1)}, bf16[64,2048]{1,0:T(8,128)(2,1)S(1)}, u32[]{:S(2)}, u32[]{:S(2)}) collective-permute-start(bf16[64,2048]{1,0:T(8,128)(2,1)S(1)} %collective-permute-done.41), channel_id=1, source_target_pairs={{0,1},{1,0},{2,3},{3,2},{4,5},{5,4},{6,7},{7,6},{8,9},{9,8},{10,11... | collective-permute-start | bytes 786440 | tf_op jit(solution)/shard_map/ppermute | solution.py:249
  187.3 4.5 %collective-permute-start.44 = (bf16[64,2048]{1,0:T(8,128)(2,1)S(1)}, bf16[64,2048]{1,0:T(8,128)(2,1)S(1)}, u32[]{:S(2)}, u32[]{:S(2)}) collective-permute-start(bf16[64,2048]{1,0:T(8,128)(2,1)S(1)} %collective-permute-done.42), channel_id=1, source_target_pairs={{0,1},{1,0},{2,3},{3,2},{4,5},{5,4},{6,7},{7,6},{8,9},{9,8},{10,11... | collective-permute-start | bytes 786440 | tf_op jit(solution)/shard_map/ppermute | solution.py:249
  191.3 3.2 %collective-permute-start.53 = (bf16[4,64,512]{2,1,0:T(8,128)(2,1)S(1)}, bf16[4,64,512]{2,1,0:T(8,128)(2,1)S(1)}, u32[]{:S(2)}, u32[]{:S(2)}) collective-permute-start(bf16[4,64,512]{2,1,0:T(8,128)(2,1)S(1)} %pad_maximum_fusion.14.refs_0_), channel_id=1, source_target_pairs={{0,1},{1,0},{2,3},{3,2},{4,5},{5,4},{6,7},{7,6},{8,9},{9,8},{10,11... | collective-permute-start | bytes 786440 | tf_op jit(solution)/shard_map/ppermute | solution.py:249
  191.3 3.1 %collective-permute-start.54 = (bf16[4,64,512]{2,1,0:T(8,128)(2,1)S(1)}, bf16[4,64,512]{2,1,0:T(8,128)(2,1)S(1)}, u32[]{:S(2)}, u32[]{:S(2)}) collective-permute-start(bf16[4,64,512]{2,1,0:T(8,128)(2,1)S(1)} %collective-permute-done.52.refs_1_), channel_id=1, source_target_pairs={{0,1},{1,0},{2,3},{3,2},{4,5},{5,4},{6,7},{7,6},{8,9},{9,8},{10,11... | collective-permute-start | bytes 786440 | tf_op jit(solution)/shard_map/ppermute | solution.py:249
  191.8 6.6 %collective-permute-start.39 = (bf16[128,2048]{1,0:T(8,128)(2,1)S(1)}, bf16[128,2048]{1,0:T(8,128)(2,1)S(1)}, u32[]{:S(2)}, u32[]{:S(2)}) collective-permute-start(bf16[128,2048]{1,0:T(8,128)(2,1)S(1)} %convolution_convert_fusion.1), channel_id=1, source_target_pairs={{0,1},{1,0},{2,3},{3,2},{4,5},{5,4},{6,7},{7,6},{8,9},{9,8},{10,11... | collective-permute-start | bytes 1572872 | tf_op jit(solution)/shard_map/ppermute | solution.py:249
  194.0 6.9 %collective-permute-start.45 = (bf16[128,2048]{1,0:T(8,128)(2,1)S(1)}, bf16[128,2048]{1,0:T(8,128)(2,1)S(1)}, u32[]{:S(2)}, u32[]{:S(2)}) collective-permute-start(bf16[128,2048]{1,0:T(8,128)(2,1)S(1)} %convolution_convert_fusion), channel_id=1, source_target_pairs={{0,1},{1,0},{2,3},{3,2},{4,5},{5,4},{6,7},{7,6},{8,9},{9,8},{10,11... | collective-permute-start | bytes 1572872 | tf_op jit(solution)/shard_map/ppermute | solution.py:249
  196.4 12.1 %collective-permute-start.61 = (bf16[256,768]{1,0:T(8,128)(2,1)S(1)}, bf16[256,768]{1,0:T(8,128)(2,1)S(1)}, u32[]{:S(2)}, u32[]{:S(2)}) collective-permute-start(bf16[256,768]{1,0:T(8,128)(2,1)S(1)} %get-tuple-element.115), channel_id=1, source_target_pairs={{0,2},{1,3},{2,0},{3,1},{4,6},{5,7},{6,4},{7,5},{8,10},{9,11},{10,... | collective-permute-start | bytes 1179656 | tf_op jit(solution)/shard_map/ppermute | solution.py:249
  199.6 19.2 %collective-permute-start.40 = (bf16[64,2048]{1,0:T(8,128)(2,1)S(1)}, bf16[64,2048]{1,0:T(8,128)(2,1)S(1)}, u32[]{:S(2)}, u32[]{:S(2)}) collective-permute-start(bf16[64,2048]{1,0:T(8,128)(2,1)S(1)} %slice.194), channel_id=1, source_target_pairs={{0,2},{1,3},{2,0},{3,1},{4,6},{5,7},{6,4},{7,5},{8,10},{9,11},{10,... | collective-permute-start | bytes 786440 | tf_op jit(solution)/shard_map/ppermute | solution.py:249
  202.0 16.8 %collective-permute-start.46 = (bf16[64,2048]{1,0:T(8,128)(2,1)S(1)}, bf16[64,2048]{1,0:T(8,128)(2,1)S(1)}, u32[]{:S(2)}, u32[]{:S(2)}) collective-permute-start(bf16[64,2048]{1,0:T(8,128)(2,1)S(1)} %get-tuple-element.136), channel_id=1, source_target_pairs={{0,16},{1,17},{2,18},{3,19},{4,20},{5,21},{6,22},{7,23},{8,24},{9,... | collective-permute-start | bytes 786440 | tf_op jit(solution)/shard_map/ppermute | solution.py:249
  202.6 16.2 %collective-permute-start.47 = (bf16[64,2048]{1,0:T(8,128)(2,1)S(1)}, bf16[64,2048]{1,0:T(8,128)(2,1)S(1)}, u32[]{:S(2)}, u32[]{:S(2)}) collective-permute-start(bf16[64,2048]{1,0:T(8,128)(2,1)S(1)} %get-tuple-element.137), channel_id=1, source_target_pairs={{0,18},{1,19},{2,16},{3,17},{4,22},{5,23},{6,20},{7,21},{8,26},{9,... | collective-permute-start | bytes 786440 | tf_op jit(solution)/shard_map/ppermute | solution.py:249
  219.4 1.6 collective-permute-start.48
  (21 other events, 136.2 us)
